TPU v7x, 128 devices: a whole 4x4x4 slice. The times are simulated.
128 devices in a mesh: sp: 16 (over z, y), fs: 4 (over x), tp: 2 (over core).
Axes of the slice: x: 4, y: 4, z: 4, core: 2. Of those that a mesh axis runs over, the one named last changes fastest.
Arguments:
- tokens: bfloat16 [8, 2048, 2048], P('fs', 'sp', 'tp'), may hold values from -8 to 8
- norm_gain: float32 [2048], replicated, may hold values from 0.1 to 1.9
- w_recept: bfloat16 [2048, 768], P(None, 'tp'), may hold values from -0.125 to 0.125
- w_key: bfloat16 [2048, 768], P(None, 'tp'), may hold values from -0.125 to 0.125
- w_value: bfloat16 [2048, 768], P(None, 'tp'), may hold values from -0.125 to 0.125
- w_decay: bfloat16 [2048, 768], P(None, 'tp'), may hold values from -0.125 to 0.125
- w_rate: bfloat16 [2048, 768], P(None, 'tp'), may hold values from -0.125 to 0.125
- w_gate_rec: bfloat16 [2048, 768], P(None, 'tp'), may hold values from -0.125 to 0.125
- w_pool: bfloat16 [2048, 512], P(None, 'tp'), may hold values from -0.125 to 0.125
- w_gate_pool: bfloat16 [2048, 512], P(None, 'tp'), may hold values from -0.125 to 0.125
- decay_base: float32 [768], replicated, may hold values from -12 to -2.5
- rate_base: float32 [768], replicated, may hold values from -7 to 1
- head_gain: float32 [768], replicated, may hold values from 0.1 to 1.9
- pool_mix: bfloat16 [4, 128, 128], replicated, may hold values from -0.5 to 0.5
- pool_scale: float32 [512], replicated, may hold values from 0.3 to 3
- w_out_rec: bfloat16 [768, 2048], P('tp'), may hold values from -0.15625 to 0.15625
- w_out_pool: bfloat16 [512, 2048], P('tp'), may hold values from -0.15625 to 0.15625
- init_state: float32 [8, 12, 64, 64], P('fs', 'tp'), may hold values from -240 to 240
Outputs:
- mixed: bfloat16 [8, 2048, 2048], P('fs', 'sp', 'tp')
All inputs are finite; a program needn't handle non-finite values.
Results may differ from a plain program's by a relative error of at most 0.015.
Values may be sent and summed in bfloat16 or wider, within the bound.
No kernel may reach another device: no remote copies, remote signals or barrier semaphores. Data moves between devices by JAX's collectives and lax.ppermute only.
A program may use at most 128 MiB of HBM per device.

v0:
```python
import functools

import jax
import jax.numpy as jnp
from jax import lax
from jax.experimental import pallas as pl
from jax.experimental.pallas import tpu as pltpu
from jax.sharding import Mesh
from jax.sharding import PartitionSpec as P

D = 2048
HEAD = 64
SPAN = 128
UNITS = 6
SP = ("sp_0", "sp_1")
f32 = jnp.float32
bf16 = jnp.bfloat16
NN = ((1,), (0,))
NT = ((1,), (1,))
TN = ((0,), (0,))
MIB = 2**20


def dot(a, b, dims=NN):
    return lax.dot_general(
        a.astype(bf16), b.astype(bf16), (dims, ((), ())), preferred_element_type=f32
    )


def halves(x):
    high = x.astype(bf16)
    return high, (x - high.astype(f32)).astype(bf16)


def dot_fine_left(a, b, dims=NN):
    high, low = halves(a)
    return dot(high, b, dims) + dot(low, b, dims)


def dot_fine_right(a, b, dims=NN):
    high, low = halves(b)
    return dot(a, high, dims) + dot(a, low, dims)


def iota(rows, cols, dim):
    return lax.broadcasted_iota(jnp.int32, (rows, cols), dim)


def head_masks():
    first = (iota(1, 128, 1) < HEAD).astype(f32)
    return first, 1.0 - first


def both(x, masks):
    return jnp.concatenate([x * masks[0], x * masks[1]], axis=0)


def compose(earlier, later, masks):
    moved = dot_fine_left(earlier, both(later[:HEAD].astype(f32), masks))
    written = later[HEAD:].astype(f32)
    if earlier.shape[0] == HEAD:
        return moved + written
    return jnp.concatenate([moved[:HEAD], moved[HEAD:] + written], axis=0)


def pick(x, size, odd):
    parts = [x[s : s + size] for s in range(size * odd, SPAN, 2 * size)]
    return parts[0] if len(parts) == 1 else jnp.concatenate(parts, axis=0)


def weave(even, odd, size):
    parts = []
    for s in range(0, SPAN // 2, size):
        parts += [even[s : s + size], odd[s : s + size]]
    return jnp.concatenate(parts, axis=0)


def inverses(lowers):
    row, col = iota(SPAN, SPAN, 0), iota(SPAN, SPAN, 1)
    eye = (row == col).astype(f32)
    near = ((row >> 1) == (col >> 1)).astype(f32)
    result = [eye - lower * near for lower in lowers]
    size, level = 2, 1
    while size < SPAN:
        off = (((row >> (level + 1)) == (col >> (level + 1))) & ((row >> level) != (col >> level))).astype(f32)
        if size < 8:
            inner = [dot(lower * off, inv) for lower, inv in zip(lowers, result)]
            result = [inv - dot(inv, part) for inv, part in zip(result, inner)]
        else:
            off = pick(off, size, 1)
            inner = [dot(pick(lower, size, 1) * off, inv) for lower, inv in zip(lowers, result)]
            outer = [
                dot(pick(inv, size, 1), weave(jnp.zeros_like(part), part, size))
                for inv, part in zip(result, inner)
            ]
            result = [
                weave(pick(inv, size, 0), pick(inv, size, 1) - part, size)
                for inv, part in zip(result, outer)
            ]
        size, level = size * 2, level + 1
    return result


def local_kernel(
    own_ref, other_ref, gain_ref, db_ref, rb_ref, wk_ref, wd_ref, wa_ref, wr_ref, wv_ref,
    normed_ref, scale_ref, home_ref, first_ref, second_ref, third_ref,
    wb_ref, wkk_ref, solved_ref, v_ref, rho_ref,
    k_s, d_s, a_s, r_s, v_s, maps, w_bufs, sems,
):
    tp = lax.axis_index("tp")
    y = lax.axis_index("sp_1")
    sources = (wk_ref, wd_ref, wa_ref, wr_ref, wv_ref)
    copies = [pltpu.make_async_copy(src, w_bufs.at[i], sems.at[i]) for i, src in enumerate(sources)]
    for copy in copies:
        copy.start()
    own = own_ref[...].astype(f32)
    other = other_ref[...].astype(f32)
    gain_a, gain_b = gain_ref[:, :1024], gain_ref[:, 1024:]
    is_first = tp == 0
    own_normed = (own * jnp.where(is_first, gain_a, gain_b)).astype(bf16)
    other_normed = (other * jnp.where(is_first, gain_b, gain_a)).astype(bf16)
    squares = jnp.sum(own * own + other * other, axis=1, keepdims=True)
    scale = lax.rsqrt(squares * (1.0 / D) + 0.25)
    normed_ref[:, :1024] = own_normed
    normed_ref[:, 1024:] = other_normed
    scale_ref[...] = jnp.broadcast_to(scale, (256, 128))
    for i, dest in enumerate((k_s, d_s, a_s, r_s, v_s)):
        copies[i].wait()
        total = dot(own_normed, w_bufs[i, pl.ds(tp * 1024, 1024), :])
        total = total + dot(other_normed, w_bufs[i, pl.ds((1 - tp) * 1024, 1024), :])
        rounded = (total * scale).astype(bf16)
        for u in range(UNITS):
            s, h = u // 3, u % 3
            dest[u] = rounded[s * 128 : s * 128 + 128, h * 128 : h * 128 + 128].astype(f32)

    masks = head_masks()
    n = SPAN
    row, col = iota(n, n, 0), iota(n, n, 1)
    strict, inclusive = row > col, row >= col
    triangle = inclusive.astype(f32)
    ones = ((row >> 6) == (col >> 6)).astype(f32)
    wide = (
        jnp.concatenate([masks[0], masks[0]], axis=1),
        jnp.concatenate([masks[1], masks[1]], axis=1),
    )
    slab = iota(HEAD, 128, 0)
    eye = (slab == (iota(HEAD, 128, 1) & 63)).astype(f32)
    units = range(UNITS)
    lowers, alphas, keeps = [], [], []
    for u in units:
        h = u % 3
        lanes = slice(h * 128, h * 128 + 128)
        shifted = slice(384 + h * 128, 384 + h * 128 + 128)
        db = jnp.where(is_first, db_ref[:, lanes], db_ref[:, shifted])
        rb = jnp.where(is_first, rb_ref[:, lanes], rb_ref[:, shifted])
        k = k_s[u]
        log_decay = -0.6065306597126334 * jax.nn.sigmoid(db + d_s[u])
        rate = jax.nn.sigmoid(rb + a_s[u])
        unit_key = k * lax.rsqrt(dot_fine_left(k * k, ones) + 1.0)
        removal = unit_key * rate
        total = dot_fine_right(triangle, log_decay)
        middle, final = total[63:64], total[127:128]
        alpha = jnp.exp(total - log_decay - middle) * unit_key
        fading = jnp.exp(middle - total)
        beta, kappa = removal * fading, k * fading
        rho = r_s[u] * jnp.exp(total - middle)
        ending = jnp.exp(final - total)
        lift = jnp.exp(middle)
        rho_ref[u] = rho * lift
        left = jnp.concatenate([alpha * masks[0], alpha * masks[1], rho * masks[0], rho * masks[1]], axis=0)
        pairs = dot(left, jnp.concatenate([beta, kappa], axis=0), NT)
        lower_kappa = []
        for j in (0, 1):
            lowers.append(jnp.where(strict, pairs[j * n : j * n + n, :n], 0.0))
            lower_kappa.append(jnp.where(strict, pairs[j * n : j * n + n, n:], 0.0).astype(bf16))
            wb_ref[u, :, j * n : j * n + n] = jnp.where(
                inclusive, pairs[(2 + j) * n : (3 + j) * n, :n], 0.0
            ).astype(bf16)
            wkk_ref[u, :, j * n : j * n + n] = jnp.where(
                inclusive, pairs[(2 + j) * n : (3 + j) * n, n:], 0.0
            ).astype(bf16)
        v = v_s[u]
        v_ref[u] = v.astype(bf16)
        carried = dot(jnp.concatenate(lower_kappa, axis=1), both(v, masks))
        keeps.append((alpha * lift, carried, removal * ending, k * ending, jnp.exp(final)))
    inverse = inverses(lowers)
    for u in units:
        alpha, carried, beta_end, kappa_end, gain_end = keeps[u]
        right = jnp.concatenate([alpha, carried], axis=1)
        solved = dot(jnp.concatenate(inverse[2 * u : 2 * u + 2], axis=1), both(right, wide))
        solved_ref[u] = solved.astype(bf16)
        crossed = dot(solved[:, :n], beta_end, TN)
        transit = eye * gain_end - (crossed[:HEAD] * masks[0] + crossed[HEAD:] * masks[1])
        crossed = dot(
            jnp.concatenate([v_s[u], -solved[:, n:]], axis=0),
            jnp.concatenate([kappa_end, beta_end], axis=0),
            TN,
        )
        written = crossed[:HEAD] * masks[0] + crossed[HEAD:] * masks[1]
        maps[u % 3, u // 3, :HEAD] = transit.astype(bf16)
        maps[u % 3, u // 3, HEAD:] = written.astype(bf16)
    maps[3] = jnp.zeros((2, 128, 128), bf16)
    for step, dest in enumerate((home_ref, first_ref, second_ref, third_ref)):
        dest[...] = maps[(y + step) & 3]


def side_kernel(
    normed_ref, scale_ref, wb_ref, wkk_ref, solved_ref, v_ref, rho_ref, wg_ref, wp_ref, wq_ref,
    reads_ref, local_ref, gate_ref, pool_ref, pgate_ref, tail_ref,
    g_buf, p_bufs, sems,
):
    tp = lax.axis_index("tp")
    copies = [
        pltpu.make_async_copy(wp_ref, p_bufs.at[0], sems.at[0]),
        pltpu.make_async_copy(wq_ref, p_bufs.at[1], sems.at[1]),
        pltpu.make_async_copy(wg_ref, g_buf, sems.at[2]),
    ]
    for copy in copies:
        copy.start()
    masks = head_masks()
    wide = (
        jnp.concatenate([masks[0], masks[0]], axis=1),
        jnp.concatenate([masks[1], masks[1]], axis=1),
    )
    for u in range(UNITS):
        removed = dot(wb_ref[u], both(solved_ref[u].astype(f32), wide))
        reads_ref[u] = (rho_ref[u] - removed[:, :128]).astype(bf16)
        local_ref[u] = dot(wkk_ref[u], both(v_ref[u].astype(f32), masks)) - removed[:, 128:]
    scale = scale_ref[:, :1]
    own, other = normed_ref[:, :1024], normed_ref[:, 1024:]

    def project(buf):
        total = dot(own, buf[pl.ds(tp * 1024, 1024), :])
        total = total + dot(other, buf[pl.ds((1 - tp) * 1024, 1024), :])
        return (total * scale).astype(bf16)

    copies[0].wait()
    pool = project(p_bufs.at[0])
    pool_ref[...] = pool
    tail_ref[0] = pool[112:128]
    tail_ref[1] = pool[240:256]
    copies[1].wait()
    pgate_ref[...] = project(p_bufs.at[1])
    copies[2].wait()
    gate_ref[...] = project(g_buf)


def row_kernel(home_ref, first_ref, second_ref, third_ref, prefix_ref, total_ref, maps):
    y = lax.axis_index("sp_1")
    for step, src in enumerate((home_ref, first_ref, second_ref, third_ref)):
        maps[(y + 4 - step) & 3] = src[...]
    masks = head_masks()
    for s in (0, 1):
        so_far = maps[0, s].astype(f32)
        prefix_ref[0, s] = so_far
        for j in (1, 2, 3):
            so_far = compose(so_far, maps[j, s], masks)
            if j < 3:
                prefix_ref[j, s] = so_far
            else:
                total_ref[s] = so_far.astype(bf16)


def column_kernel(
    prefix_ref, first_ref, second_ref, third_ref, init_ref,
    home_ref, one_ref, two_ref, three_ref,
    starts, rows,
):
    y = lax.axis_index("sp_1")
    z = lax.axis_index("sp_0")
    for step, src in enumerate((first_ref, second_ref, third_ref)):
        rows[(z + 3 - step) & 3] = src[...]
    masks = head_masks()
    pair = jnp.minimum(y, 2) * 2
    for s in (0, 1):
        state = jnp.concatenate([init_ref[s, pair], init_ref[s, pair + 1]], axis=1)
        for j in range(3):
            state = jnp.where(j < z, compose(state, rows[j, s], masks), state)
        starts[0, s] = state.astype(bf16)
        for j in range(3):
            starts[j + 1, s] = compose(state, prefix_ref[j, s], masks).astype(bf16)
    for step, dest in enumerate((home_ref, one_ref, two_ref, three_ref)):
        dest[...] = starts[(y + step) & 3]


def pool_kernel(pool_ref, tail_ref, pgate_ref, mix_ref, pscale_ref, out_ref):
    tp = lax.axis_index("tp")
    place = lax.axis_index("sp_0") * 4 + lax.axis_index("sp_1")
    is_first = tp == 0
    factor = jnp.where(is_first, pscale_ref[:, :256], pscale_ref[:, 256:])
    for s in (0, 1):
        current = pool_ref[s * 128 : s * 128 + 128].astype(f32)
        padded = jnp.concatenate([tail_ref[s].astype(f32), current], axis=0)
        sums = {1: padded}
        for by in (1, 2, 4, 8):
            before = sums[by]
            moved = jnp.concatenate([jnp.zeros((by, 256), f32), before[: 144 - by]], axis=0)
            sums[2 * by] = before + moved
        position = (place * 128 + iota(128, 128, 0) + 1).astype(f32)
        for g in (0, 1):
            lanes = slice(g * 128, g * 128 + 128)
            small, large = 2 << g, 8 << g
            trailing = jnp.where(is_first, sums[small][16:, lanes], sums[large][16:, lanes])
            window = jnp.where(is_first, float(small), float(large))
            diffs = trailing / jnp.minimum(position, window) - current[:, lanes]
            mixed = dot(diffs.astype(bf16), mix_ref[tp * 2 + g])
            gate = pgate_ref[s * 128 : s * 128 + 128, lanes].astype(f32)
            out_ref[s * 128 : s * 128 + 128, lanes] = (
                mixed * factor[:, lanes] * (gate * jax.nn.sigmoid(gate))
            ).astype(bf16)


def final_kernel(
    home_ref, one_ref, two_ref, three_ref, reads_ref, local_ref, gate_ref, hgain_ref, pool_ref,
    wr_ref, wp_ref,
    send_ref, keep_ref,
    starts, rec, wr_buf, wp_buf, sems,
):
    tp = lax.axis_index("tp")
    y = lax.axis_index("sp_1")
    copies = [
        pltpu.make_async_copy(wr_ref, wr_buf, sems.at[0]),
        pltpu.make_async_copy(wp_ref, wp_buf, sems.at[1]),
    ]
    for copy in copies:
        copy.start()
    for step, src in enumerate((home_ref, one_ref, two_ref, three_ref)):
        starts[(y + 4 - step) & 3] = src[...]
    masks = head_masks()
    row, col = iota(128, 128, 0), iota(128, 128, 1)
    mean_of = jnp.where((row >> 6) == (col >> 6), 1.0 / HEAD, 0.0).astype(bf16)
    is_first = tp == 0
    for u in range(UNITS):
        s, h = u // 3, u % 3
        lanes = slice(h * 128, h * 128 + 128)
        shifted = slice(384 + h * 128, 384 + h * 128 + 128)
        rows = slice(s * 128, s * 128 + 128)
        out = dot(reads_ref[u], both(starts[h, s].astype(f32), masks), NT) + local_ref[u]
        out = out - dot_fine_left(out, mean_of)
        spread = dot_fine_left(out * out, mean_of)
        gain = jnp.where(is_first, hgain_ref[:, lanes], hgain_ref[:, shifted])
        gate = gate_ref[rows, lanes].astype(f32)
        rec[rows, lanes] = (
            out * lax.rsqrt(spread + 1.0) * gain * (gate * jax.nn.sigmoid(gate))
        ).astype(bf16)
    for copy in copies:
        copy.wait()
    for dest, part in ((send_ref, 1 - tp), (keep_ref, tp)):
        cols = pl.ds(pl.multiple_of(part * 1024, 1024), 1024)
        dest[...] = (dot(rec[...], wr_buf[:, cols]) + dot(pool_ref[...], wp_buf[:, cols])).astype(bf16)


def vmem(count):
    return [pl.BlockSpec(memory_space=pltpu.VMEM)] * count


def hbm(count):
    return [pl.BlockSpec(memory_space=pl.ANY)] * count


def shape(dims, kind=bf16):
    return jax.ShapeDtypeStruct(dims, kind)


def call(body, name, ins, outs, scratch, limit, flops=0):
    return pl.pallas_call(
        body,
        name=name,
        out_shape=outs,
        in_specs=ins,
        out_specs=vmem(len(outs)) if isinstance(outs, (list, tuple)) else vmem(1)[0],
        scratch_shapes=scratch,
        compiler_params=pltpu.CompilerParams(vmem_limit_bytes=limit * MIB),
        cost_estimate=pl.CostEstimate(flops=flops, transcendentals=0, bytes_accessed=0) if flops else None,
    )


def spread_rows(parts, senders, receivers):
    out = []
    for step, part in enumerate(parts, 1):
        pairs = [(i, (i + step) & 3) for i in range(4) if i in senders and ((i + step) & 3) in receivers]
        out.append(lax.ppermute(part, "sp_1", pairs))
    return out


def shards(
    tokens, norm_gain, w_recept, w_key, w_value, w_decay, w_rate, w_gate_rec, w_pool, w_gate_pool,
    decay_base, rate_base, head_gain, pool_mix, pool_scale, w_out_rec, w_out_pool, init_state,
):
    other = lax.ppermute(tokens, "tp", [(0, 1), (1, 0)])
    line = lambda x: x.reshape(1, -1)
    normed, scale, home, m1, m2, m3, wb, wkk, solved, v, rho = call(
        local_kernel,
        "local",
        vmem(5) + hbm(5),
        [
            shape((256, D)), shape((256, 128), f32),
            shape((2, 128, 128)), shape((2, 128, 128)), shape((2, 128, 128)), shape((2, 128, 128)),
            shape((6, 128, 256)), shape((6, 128, 256)), shape((6, 128, 256)),
            shape((6, 128, 128)), shape((6, 128, 128), f32),
        ],
        [pltpu.VMEM((6, 128, 128), f32)] * 5
        + [pltpu.VMEM((4, 2, 128, 128), bf16), pltpu.VMEM((5, D, 384), bf16), pltpu.SemaphoreType.DMA((5,))],
        40,
        4_000_000_000,
    )(
        tokens.reshape(256, 1024), other.reshape(256, 1024), line(norm_gain), line(decay_base), line(rate_base),
        w_key, w_decay, w_rate, w_recept, w_value,
    )
    r1, r2, r3 = spread_rows((m1, m2, m3), (0, 1, 2, 3), (0, 1, 2))
    reads, local, gate, pool, pgate, tail = call(
        side_kernel,
        "side",
        vmem(7) + hbm(3),
        [
            shape((6, 128, 128)), shape((6, 128, 128), f32), shape((256, 384)), shape((256, 256)),
            shape((256, 256)), shape((2, 16, 256)),
        ],
        [pltpu.VMEM((D, 384), bf16), pltpu.VMEM((2, D, 256), bf16), pltpu.SemaphoreType.DMA((3,))],
        24,
        2_000_000_000,
    )(normed, scale, wb, wkk, solved, v, rho, w_gate_rec, w_pool, w_gate_pool)
    halo = lax.ppermute(tail, SP, [(i, i + 1) for i in range(15)])
    prefix, total = call(
        row_kernel,
        "row",
        vmem(4),
        [shape((3, 2, 128, 128), f32), shape((2, 128, 128))],
        [pltpu.VMEM((4, 2, 128, 128), bf16)],
        8,
        100_000_000,
    )(home, r1, r2, r3)
    columns = [
        lax.ppermute(total, "sp_0", [(i, i + step) for i in range(4) if i + step < 4]) for step in (1, 2, 3)
    ]
    s0, s1, s2, s3 = call(
        column_kernel,
        "column",
        vmem(5),
        [shape((2, 64, 128))] * 4,
        [pltpu.VMEM((4, 2, 64, 128), bf16), pltpu.VMEM((4, 2, 128, 128), bf16)],
        8,
        100_000_000,
    )(prefix, *columns, init_state)
    t1, t2, t3 = spread_rows((s1, s2, s3), (0, 1, 2), (0, 1, 2, 3))
    pool_out = call(pool_kernel, "pool", vmem(5), shape((256, 256)), [], 8, 100_000_000)(
        pool, halo, pgate, pool_mix, line(pool_scale)
    )
    send, keep = call(
        final_kernel,
        "final",
        vmem(9) + hbm(2),
        [shape((256, 1024)), shape((256, 1024))],
        [
            pltpu.VMEM((4, 2, 64, 128), bf16), pltpu.VMEM((256, 384), bf16), pltpu.VMEM((384, D), bf16),
            pltpu.VMEM((256, D), bf16), pltpu.SemaphoreType.DMA((2,)),
        ],
        20,
        1_000_000_000,
    )(s0, t1, t2, t3, reads, local, gate, line(head_gain), pool_out, w_out_rec, w_out_pool)
    arrived = lax.ppermute(send, "tp", [(0, 1), (1, 0)])
    mixed = keep.astype(f32) + arrived.astype(f32)
    return mixed.astype(bf16).reshape(2, 128, 1024)


def solution(mesh):
    split = Mesh(
        mesh.devices.reshape(4, 4, mesh.shape["fs"], mesh.shape["tp"]), ("sp_0", "sp_1", "fs", "tp")
    )
    column = P(None, "tp")
    placed = (
        (P("fs", SP, "tp"), P()) + (column,) * 8 + (P(),) * 5
        + (P("tp", None), P("tp", None), P("fs", "tp", None, None))
    )
    return jax.shard_map(
        shards, mesh=split, in_specs=placed, out_specs=P("fs", SP, "tp"), check_vma=False
    )
```

profile of v0, /device:TPU:97, one launch (start us, length us, event | category | flops | bytes accessed | tf_op | source)
XLA Modules:
  0.0 72.1 jit_solution(7670252747580601311)
XLA Ops:
  0.7 0.7 reshape.27.db_ref
  1.4 0.7 reshape.28.rb_ref
  2.4 1.4 %copy-done.3 = bf16[2048,384]{1,0:T(8,128)(2,1)S(1)} copy-done((bf16[2048,384]{1,0:T(8,128)(2,1)S(1)}, bf16[2048,384]{1,0:T(8,128)(2,1)}, u32[]{:S(2)}) %copy-start.3) | copy-done | bytes 1572888
  3.8 1.4 %copy-done.4 = bf16[2048,384]{1,0:T(8,128)(2,1)S(1)} copy-done((bf16[2048,384]{1,0:T(8,128)(2,1)S(1)}, bf16[2048,384]{1,0:T(8,128)(2,1)}, u32[]{:S(2)}) %copy-start.4) | copy-done | bytes 1572888
  5.2 1.4 %copy-done.5 = bf16[2048,384]{1,0:T(8,128)(2,1)S(1)} copy-done((bf16[2048,384]{1,0:T(8,128)(2,1)S(1)}, bf16[2048,384]{1,0:T(8,128)(2,1)}, u32[]{:S(2)}) %copy-start.5) | copy-done | bytes 1572888
  6.7 1.4 %copy-done.6 = bf16[2048,384]{1,0:T(8,128)(2,1)S(1)} copy-done((bf16[2048,384]{1,0:T(8,128)(2,1)S(1)}, bf16[2048,384]{1,0:T(8,128)(2,1)}, u32[]{:S(2)}) %copy-start.6) | copy-done | bytes 1572888
  8.1 1.4 %copy-done.7 = bf16[2048,384]{1,0:T(8,128)(2,1)S(1)} copy-done((bf16[2048,384]{1,0:T(8,128)(2,1)S(1)}, bf16[2048,384]{1,0:T(8,128)(2,1)}, u32[]{:S(2)}) %copy-start.7) | copy-done | bytes 1572888
  9.5 1.0 %copy-done.13 = bf16[2,128,1024]{2,1,0:T(8,128)(2,1)S(1)} copy-done((bf16[2,128,1024]{2,1,0:T(8,128)(2,1)S(1)}, bf16[2,128,1024]{2,1,0:T(8,128)(2,1)}, u32[]{:S(2)}) %copy-start.13) | copy-done | bytes 524312
  10.5 0.7 copy-done.14
  11.2 9.6 %local.1 = (bf16[256,2048]{1,0:T(8,128)(2,1)S(1)}, f32[256,128]{1,0:T(8,128)S(1)}, bf16[2,128,128]{2,1,0:T(8,128)(2,1)S(1)}, bf16[2,128,128]{2,1,0:T(8,128)(2,1)...) custom-call(bf16[256,1024]{1,0:T(8,128)(2,1)S(1)} %bitcast.6, ...), custom_call_target="tpu_custom_call" | custom-call | flops 4000000000 | tf_op jit(solution)/shard_map/local/pallas_call | solution.py:392
  20.8 3.2 %collective-permute-start.1 = (bf16[2,128,128]{2,1,0:T(8,128)(2,1)S(1)}, bf16[2,128,128]{2,1,0:T(8,128)(2,1)S(1)}, u32[]{:S(2)}, u32[]{:S(2)}) collective-permute-start(bf16[2,128,128]{2,1,0:T(8,128)(2,1)S(1)} %get-tuple-element.31), channel_id=1, source_target_pairs={{0,8},{8,16},{24,0},{1,9},{9,17},{25,1},{2,10},{10,18},{26,2},{3,1... | collective-permute-start | bytes 196616 | tf_op jit(solution)/shard_map/ppermute | solution.py:382
  24.0 2.9 %collective-permute-start.2 = (bf16[2,128,128]{2,1,0:T(8,128)(2,1)S(1)}, bf16[2,128,128]{2,1,0:T(8,128)(2,1)S(1)}, u32[]{:S(2)}, u32[]{:S(2)}) collective-permute-start(bf16[2,128,128]{2,1,0:T(8,128)(2,1)S(1)} %get-tuple-element.32), channel_id=1, source_target_pairs={{0,16},{16,0},{24,8},{1,17},{17,1},{25,9},{2,18},{18,2},{26,10},{3... | collective-permute-start | bytes 196616 | tf_op jit(solution)/shard_map/ppermute | solution.py:382
  27.0 1.3 %collective-permute-start.3 = (bf16[2,128,128]{2,1,0:T(8,128)(2,1)S(1)}, bf16[2,128,128]{2,1,0:T(8,128)(2,1)S(1)}, u32[]{:S(2)}, u32[]{:S(2)}) collective-permute-start(bf16[2,128,128]{2,1,0:T(8,128)(2,1)S(1)} %get-tuple-element.33), channel_id=1, source_target_pairs={{8,0},{16,8},{24,16},{9,1},{17,9},{25,17},{10,2},{18,10},{26,18},{... | collective-permute-start | bytes 196616 | tf_op jit(solution)/shard_map/ppermute | solution.py:382
  28.3 2.3 %collective-permute-done.2.second_ref = bf16[2,128,128]{2,1,0:T(8,128)(2,1)S(1)} collective-permute-done((bf16[2,128,128]{2,1,0:T(8,128)(2,1)S(1)}, bf16[2,128,128]{2,1,0:T(8,128)(2,1)S(1)}, u32[]{:S(2)}, u32[]{:S(2)}) %collective-permute-start.2) | collective-permute-done | bytes 65568 | tf_op jit(solution)/shard_map/ppermute | solution.py:382
  30.6 1.4 %collective-permute-done.3.third_ref = bf16[2,128,128]{2,1,0:T(8,128)(2,1)S(1)} collective-permute-done((bf16[2,128,128]{2,1,0:T(8,128)(2,1)S(1)}, bf16[2,128,128]{2,1,0:T(8,128)(2,1)S(1)}, u32[]{:S(2)}, u32[]{:S(2)}) %collective-permute-start.3) | collective-permute-done | bytes 65568 | tf_op jit(solution)/shard_map/ppermute | solution.py:382
  32.6 1.3 %collective-permute-start.4 = (bf16[2,128,128]{2,1,0:T(8,128)(2,1)S(1)}, bf16[2,128,128]{2,1,0:T(8,128)(2,1)S(1)}, u32[]{:S(2)}, u32[]{:S(2)}) collective-permute-start(bf16[2,128,128]{2,1,0:T(8,128)(2,1)S(1)} %get-tuple-element.35), channel_id=1, source_target_pairs={{0,32},{32,64},{64,96},{1,33},{33,65},{65,97},{2,34},{34,66},{66,9... | collective-permute-start | bytes 196616 | tf_op jit(solution)/shard_map/ppermute | solution.py:434
  33.9 1.3 %collective-permute-start.5 = (bf16[2,128,128]{2,1,0:T(8,128)(2,1)S(1)}, bf16[2,128,128]{2,1,0:T(8,128)(2,1)S(1)}, u32[]{:S(2)}, u32[]{:S(2)}) collective-permute-start(bf16[2,128,128]{2,1,0:T(8,128)(2,1)S(1)} %get-tuple-element.35), channel_id=1, source_target_pairs={{0,64},{32,96},{1,65},{33,97},{2,66},{34,98},{3,67},{35,99},{4,68}... | collective-permute-start | bytes 196616 | tf_op jit(solution)/shard_map/ppermute | solution.py:434
  35.2 1.3 %collective-permute-start.6 = (bf16[2,128,128]{2,1,0:T(8,128)(2,1)S(1)}, bf16[2,128,128]{2,1,0:T(8,128)(2,1)S(1)}, u32[]{:S(2)}, u32[]{:S(2)}) collective-permute-start(bf16[2,128,128]{2,1,0:T(8,128)(2,1)S(1)} %get-tuple-element.35), channel_id=1, source_target_pairs={{0,96},{1,97},{2,98},{3,99},{4,100},{5,101},{6,102},{7,103},{8,104... | collective-permute-start | bytes 196616 | tf_op jit(solution)/shard_map/ppermute | solution.py:434
  36.5 1.1 %collective-permute-done.4.first_ref = bf16[2,128,128]{2,1,0:T(8,128)(2,1)S(1)} collective-permute-done((bf16[2,128,128]{2,1,0:T(8,128)(2,1)S(1)}, bf16[2,128,128]{2,1,0:T(8,128)(2,1)S(1)}, u32[]{:S(2)}, u32[]{:S(2)}) %collective-permute-start.4) | collective-permute-done | bytes 65568 | tf_op jit(solution)/shard_map/ppermute | solution.py:434
  37.6 2.8 %collective-permute-done.5.second_ref = bf16[2,128,128]{2,1,0:T(8,128)(2,1)S(1)} collective-permute-done((bf16[2,128,128]{2,1,0:T(8,128)(2,1)S(1)}, bf16[2,128,128]{2,1,0:T(8,128)(2,1)S(1)}, u32[]{:S(2)}, u32[]{:S(2)}) %collective-permute-start.5) | collective-permute-done | bytes 65568 | tf_op jit(solution)/shard_map/ppermute | solution.py:434
  40.4 3.0 %collective-permute-done.6.third_ref = bf16[2,128,128]{2,1,0:T(8,128)(2,1)S(1)} collective-permute-done((bf16[2,128,128]{2,1,0:T(8,128)(2,1)S(1)}, bf16[2,128,128]{2,1,0:T(8,128)(2,1)S(1)}, u32[]{:S(2)}, u32[]{:S(2)}) %collective-permute-start.6) | collective-permute-done | bytes 65568 | tf_op jit(solution)/shard_map/ppermute | solution.py:434
  43.4 1.2 %column.1 = (bf16[2,64,128]{2,1,0:T(8,128)(2,1)S(1)}, bf16[2,64,128]{2,1,0:T(8,128)(2,1)S(1)}, bf16[2,64,128]{2,1,0:T(8,128)(2,1)S(1)}, bf16[2,64,128]{2,1,0:T(8,128)(2,1)S(1)}) custom-call(f32[3,2,128,128]{3,2,1,0:T(8,128)S(1)} %get-tuple-element.34.prefix_ref, bf16[2,128,128]{2,1,0:T(8,128)(2,1)S(1)} %collective-permute-done.4.first_ref, ...), custom_call_target="tpu_custom_call" | custom-call | flops 100000000 | tf_op jit(solution)/shard_map/column/pallas_call | solution.py:436
  44.6 3.6 %collective-permute-start.7 = (bf16[2,64,128]{2,1,0:T(8,128)(2,1)S(1)}, bf16[2,64,128]{2,1,0:T(8,128)(2,1)S(1)}, u32[]{:S(2)}, u32[]{:S(2)}) collective-permute-start(bf16[2,64,128]{2,1,0:T(8,128)(2,1)S(1)} %get-tuple-element.37), channel_id=1, source_target_pairs={{0,8},{8,16},{16,24},{1,9},{9,17},{17,25},{2,10},{10,18},{18,26},{... | collective-permute-start | bytes 98312 | tf_op jit(solution)/shard_map/ppermute | solution.py:382
  48.2 2.5 %collective-permute-start.8 = (bf16[2,64,128]{2,1,0:T(8,128)(2,1)S(1)}, bf16[2,64,128]{2,1,0:T(8,128)(2,1)S(1)}, u32[]{:S(2)}, u32[]{:S(2)}) collective-permute-start(bf16[2,64,128]{2,1,0:T(8,128)(2,1)S(1)} %get-tuple-element.38), channel_id=1, source_target_pairs={{0,16},{8,24},{16,0},{1,17},{9,25},{17,1},{2,18},{10,26},{18,2},{3... | collective-permute-start | bytes 98312 | tf_op jit(solution)/shard_map/ppermute | solution.py:382
  50.7 1.9 %collective-permute-start.9 = (bf16[2,64,128]{2,1,0:T(8,128)(2,1)S(1)}, bf16[2,64,128]{2,1,0:T(8,128)(2,1)S(1)}, u32[]{:S(2)}, u32[]{:S(2)}) collective-permute-start(bf16[2,64,128]{2,1,0:T(8,128)(2,1)S(1)} %get-tuple-element.39), channel_id=1, source_target_pairs={{0,24},{8,0},{16,8},{1,25},{9,1},{17,9},{2,26},{10,2},{18,10},{3,2... | collective-permute-start | bytes 98312 | tf_op jit(solution)/shard_map/ppermute | solution.py:382
  52.7 2.8 %side.1 = (bf16[6,128,128]{2,1,0:T(8,128)(2,1)S(1)}, f32[6,128,128]{2,1,0:T(8,128)S(1)}, bf16[256,384]{1,0:T(8,128)(2,1)S(1)}, bf16[256,256]{1,0:T(8,128)(2,1)S(...) custom-call(bf16[256,2048]{1,0:T(8,128)(2,1)S(1)} %get-tuple-element.40.normed_ref, ...), custom_call_target="tpu_custom_call" | custom-call | flops 2000000000 | tf_op jit(solution)/shard_map/side/pallas_call | solution.py:411
  55.5 3.4 %collective-permute-start.10 = (bf16[2,16,256]{2,1,0:T(8,128)(2,1)S(1)}, bf16[2,16,256]{2,1,0:T(8,128)(2,1)S(1)}, u32[]{:S(2)}, u32[]{:S(2)}) collective-permute-start(bf16[2,16,256]{2,1,0:T(8,128)(2,1)S(1)} %get-tuple-element.51), channel_id=1, source_target_pairs={{0,8},{8,16},{16,24},{24,32},{32,40},{40,48},{48,56},{56,64},{64,7... | collective-permute-start | bytes 49160 | tf_op jit(solution)/shard_map/ppermute | solution.py:423
  58.9 3.2 %collective-permute-done.10.tail_ref = bf16[2,16,256]{2,1,0:T(8,128)(2,1)S(1)} collective-permute-done((bf16[2,16,256]{2,1,0:T(8,128)(2,1)S(1)}, bf16[2,16,256]{2,1,0:T(8,128)(2,1)S(1)}, u32[]{:S(2)}, u32[]{:S(2)}) %collective-permute-start.10) | collective-permute-done | bytes 16416 | tf_op jit(solution)/shard_map/ppermute | solution.py:423
  62.4 2.5 %final.1 = (bf16[256,1024]{1,0:T(8,128)(2,1)S(1)}, bf16[256,1024]{1,0:T(8,128)(2,1)S(1)}) custom-call(bf16[2,64,128]{2,1,0:T(8,128)(2,1)S(1)} %get-tuple-element.36.home_ref, bf16[2,64,128]{2,1,0:T(8,128)(2,1)S(1)} %collective-permute-done.7.one_ref, bf16[2,64,128]{2,1,0:T(8,128)(2,1)S(1)} %collective-permute-done.8.two_ref, ...), custom_call_target="tpu_custom_call" | custom-call | flops 1000000000 | tf_op jit(solution)/shard_map/final/pallas_call | solution.py:449
  65.0 4.6 %collective-permute-start.11 = (bf16[256,1024]{1,0:T(8,128)(2,1)S(1)}, bf16[256,1024]{1,0:T(8,128)(2,1)S(1)}, u32[]{:S(2)}, u32[]{:S(2)}) collective-permute-start(bf16[256,1024]{1,0:T(8,128)(2,1)S(1)} %get-tuple-element.54), channel_id=1, source_target_pairs={{0,1},{1,0},{2,3},{3,2},{4,5},{5,4},{6,7},{7,6},{8,9},{9,8},{10,11... | collective-permute-start | bytes 1572872 | tf_op jit(solution)/shard_map/ppermute | solution.py:461
  69.5 1.5 %collective-permute-done.11 = bf16[256,1024]{1,0:T(8,128)(2,1)S(1)} collective-permute-done((bf16[256,1024]{1,0:T(8,128)(2,1)S(1)}, bf16[256,1024]{1,0:T(8,128)(2,1)S(1)}, u32[]{:S(2)}, u32[]{:S(2)}) %collective-permute-start.11) | collective-permute-done | bytes 524320 | tf_op jit(solution)/shard_map/ppermute | solution.py:461
  71.1 1.0 %add_convert_fusion = bf16[256,1024]{1,0:T(8,128)(2,1)} fusion(bf16[256,1024]{1,0:T(8,128)(2,1)S(1)} %collective-permute-done.11, bf16[256,1024]{1,0:T(8,128)(2,1)S(1)} %get-tuple-element.53), kind=kLoop, calls=%fused_computation | loop fusion | flops 1048576 | bytes 1572864 | tf_op jit(solution)/shard_map/convert_element_type | solution.py:463
  (34 shorter events, 2.0 us)
Async XLA Ops:
  0.0 2.4 %collective-permute-start = (bf16[2,128,1024]{2,1,0:T(8,128)(2,1)}, bf16[2,128,1024]{2,1,0:T(8,128)(2,1)S(1)}, u32[]{:S(2)}, u32[]{:S(2)}) collective-permute-start(bf16[2,128,1024]{2,1,0:T(8,128)(2,1)} %param.18), channel_id=1, source_target_pairs={{0,1},{1,0},{2,3},{3,2},{4,5},{5,4},{6,7},{7,6},{8,9},{9,8},{10,11... | collective-permute-start | bytes 1572872 | tf_op jit(solution)/shard_map/ppermute | solution.py:390
  2.4 1.4 %copy-start.3 = (bf16[2048,384]{1,0:T(8,128)(2,1)S(1)}, bf16[2048,384]{1,0:T(8,128)(2,1)}, u32[]{:S(2)}) copy-start(bf16[2048,384]{1,0:T(8,128)(2,1)} %wk_ref.1) | copy-start | bytes 4718596
  3.8 1.4 %copy-start.4 = (bf16[2048,384]{1,0:T(8,128)(2,1)S(1)}, bf16[2048,384]{1,0:T(8,128)(2,1)}, u32[]{:S(2)}) copy-start(bf16[2048,384]{1,0:T(8,128)(2,1)} %wd_ref.1) | copy-start | bytes 4718596
  5.2 1.4 %copy-start.5 = (bf16[2048,384]{1,0:T(8,128)(2,1)S(1)}, bf16[2048,384]{1,0:T(8,128)(2,1)}, u32[]{:S(2)}) copy-start(bf16[2048,384]{1,0:T(8,128)(2,1)} %wa_ref.1) | copy-start | bytes 4718596
  6.6 1.4 %copy-start.6 = (bf16[2048,384]{1,0:T(8,128)(2,1)S(1)}, bf16[2048,384]{1,0:T(8,128)(2,1)}, u32[]{:S(2)}) copy-start(bf16[2048,384]{1,0:T(8,128)(2,1)} %wr_ref.2) | copy-start | bytes 4718596
  8.1 1.4 %copy-start.7 = (bf16[2048,384]{1,0:T(8,128)(2,1)S(1)}, bf16[2048,384]{1,0:T(8,128)(2,1)}, u32[]{:S(2)}) copy-start(bf16[2048,384]{1,0:T(8,128)(2,1)} %wv_ref.1) | copy-start | bytes 4718596
  9.5 1.0 %copy-start.13 = (bf16[2,128,1024]{2,1,0:T(8,128)(2,1)S(1)}, bf16[2,128,1024]{2,1,0:T(8,128)(2,1)}, u32[]{:S(2)}) copy-start(bf16[2,128,1024]{2,1,0:T(8,128)(2,1)} %param.18) | copy-start | bytes 1572868
  10.5 0.7 copy-start.14
  11.2 32.2 %copy-start = (f32[2,6,64,64]{3,2,1,0:T(8,128)S(1)}, f32[2,6,64,64]{3,2,1,0:T(8,128)}, u32[]{:S(2)}) copy-start(f32[2,6,64,64]{3,2,1,0:T(8,128)} %init_ref.1) | copy-start | bytes 589828
  11.2 41.4 %copy-start.8 = (bf16[2048,384]{1,0:T(8,128)(2,1)S(1)}, bf16[2048,384]{1,0:T(8,128)(2,1)}, u32[]{:S(2)}) copy-start(bf16[2048,384]{1,0:T(8,128)(2,1)} %wg_ref.1) | copy-start | bytes 4718596
  11.2 41.4 %copy-start.10 = (bf16[2048,256]{1,0:T(8,128)(2,1)S(1)}, bf16[2048,256]{1,0:T(8,128)(2,1)}, u32[]{:S(2)}) copy-start(bf16[2048,256]{1,0:T(8,128)(2,1)} %wp_ref.2) | copy-start | bytes 3145732
  11.2 41.4 %copy-start.11 = (bf16[2048,256]{1,0:T(8,128)(2,1)S(1)}, bf16[2048,256]{1,0:T(8,128)(2,1)}, u32[]{:S(2)}) copy-start(bf16[2048,256]{1,0:T(8,128)(2,1)} %wq_ref.1) | copy-start | bytes 3145732
  20.8 7.4 %collective-permute-start.1 = (bf16[2,128,128]{2,1,0:T(8,128)(2,1)S(1)}, bf16[2,128,128]{2,1,0:T(8,128)(2,1)S(1)}, u32[]{:S(2)}, u32[]{:S(2)}) collective-permute-start(bf16[2,128,128]{2,1,0:T(8,128)(2,1)S(1)} %get-tuple-element.31), channel_id=1, source_target_pairs={{0,8},{8,16},{24,0},{1,9},{9,17},{25,1},{2,10},{10,18},{26,2},{3,1... | collective-permute-start | bytes 196616 | tf_op jit(solution)/shard_map/ppermute | solution.py:382
  24.0 6.5 %collective-permute-start.2 = (bf16[2,128,128]{2,1,0:T(8,128)(2,1)S(1)}, bf16[2,128,128]{2,1,0:T(8,128)(2,1)S(1)}, u32[]{:S(2)}, u32[]{:S(2)}) collective-permute-start(bf16[2,128,128]{2,1,0:T(8,128)(2,1)S(1)} %get-tuple-element.32), channel_id=1, source_target_pairs={{0,16},{16,0},{24,8},{1,17},{17,1},{25,9},{2,18},{18,2},{26,10},{3... | collective-permute-start | bytes 196616 | tf_op jit(solution)/shard_map/ppermute | solution.py:382
  27.0 5.0 %collective-permute-start.3 = (bf16[2,128,128]{2,1,0:T(8,128)(2,1)S(1)}, bf16[2,128,128]{2,1,0:T(8,128)(2,1)S(1)}, u32[]{:S(2)}, u32[]{:S(2)}) collective-permute-start(bf16[2,128,128]{2,1,0:T(8,128)(2,1)S(1)} %get-tuple-element.33), channel_id=1, source_target_pairs={{8,0},{16,8},{24,16},{9,1},{17,9},{25,17},{10,2},{18,10},{26,18},{... | collective-permute-start | bytes 196616 | tf_op jit(solution)/shard_map/ppermute | solution.py:382
  32.6 5.0 %collective-permute-start.4 = (bf16[2,128,128]{2,1,0:T(8,128)(2,1)S(1)}, bf16[2,128,128]{2,1,0:T(8,128)(2,1)S(1)}, u32[]{:S(2)}, u32[]{:S(2)}) collective-permute-start(bf16[2,128,128]{2,1,0:T(8,128)(2,1)S(1)} %get-tuple-element.35), channel_id=1, source_target_pairs={{0,32},{32,64},{64,96},{1,33},{33,65},{65,97},{2,34},{34,66},{66,9... | collective-permute-start | bytes 196616 | tf_op jit(solution)/shard_map/ppermute | solution.py:434
  33.9 6.5 %collective-permute-start.5 = (bf16[2,128,128]{2,1,0:T(8,128)(2,1)S(1)}, bf16[2,128,128]{2,1,0:T(8,128)(2,1)S(1)}, u32[]{:S(2)}, u32[]{:S(2)}) collective-permute-start(bf16[2,128,128]{2,1,0:T(8,128)(2,1)S(1)} %get-tuple-element.35), channel_id=1, source_target_pairs={{0,64},{32,96},{1,65},{33,97},{2,66},{34,98},{3,67},{35,99},{4,68}... | collective-permute-start | bytes 196616 | tf_op jit(solution)/shard_map/ppermute | solution.py:434
  35.2 8.2 %collective-permute-start.6 = (bf16[2,128,128]{2,1,0:T(8,128)(2,1)S(1)}, bf16[2,128,128]{2,1,0:T(8,128)(2,1)S(1)}, u32[]{:S(2)}, u32[]{:S(2)}) collective-permute-start(bf16[2,128,128]{2,1,0:T(8,128)(2,1)S(1)} %get-tuple-element.35), channel_id=1, source_target_pairs={{0,96},{1,97},{2,98},{3,99},{4,100},{5,101},{6,102},{7,103},{8,104... | collective-permute-start | bytes 196616 | tf_op jit(solution)/shard_map/ppermute | solution.py:434
  44.6 17.8 %collective-permute-start.7 = (bf16[2,64,128]{2,1,0:T(8,128)(2,1)S(1)}, bf16[2,64,128]{2,1,0:T(8,128)(2,1)S(1)}, u32[]{:S(2)}, u32[]{:S(2)}) collective-permute-start(bf16[2,64,128]{2,1,0:T(8,128)(2,1)S(1)} %get-tuple-element.37), channel_id=1, source_target_pairs={{0,8},{8,16},{16,24},{1,9},{9,17},{17,25},{2,10},{10,18},{18,26},{... | collective-permute-start | bytes 98312 | tf_op jit(solution)/shard_map/ppermute | solution.py:382
  48.2 14.2 %collective-permute-start.8 = (bf16[2,64,128]{2,1,0:T(8,128)(2,1)S(1)}, bf16[2,64,128]{2,1,0:T(8,128)(2,1)S(1)}, u32[]{:S(2)}, u32[]{:S(2)}) collective-permute-start(bf16[2,64,128]{2,1,0:T(8,128)(2,1)S(1)} %get-tuple-element.38), channel_id=1, source_target_pairs={{0,16},{8,24},{16,0},{1,17},{9,25},{17,1},{2,18},{10,26},{18,2},{3... | collective-permute-start | bytes 98312 | tf_op jit(solution)/shard_map/ppermute | solution.py:382
  50.7 11.7 %collective-permute-start.9 = (bf16[2,64,128]{2,1,0:T(8,128)(2,1)S(1)}, bf16[2,64,128]{2,1,0:T(8,128)(2,1)S(1)}, u32[]{:S(2)}, u32[]{:S(2)}) collective-permute-start(bf16[2,64,128]{2,1,0:T(8,128)(2,1)S(1)} %get-tuple-element.39), channel_id=1, source_target_pairs={{0,24},{8,0},{16,8},{1,25},{9,1},{17,9},{2,26},{10,2},{18,10},{3,2... | collective-permute-start | bytes 98312 | tf_op jit(solution)/shard_map/ppermute | solution.py:382
  52.6 6.2 %copy-start.15 = (f32[768]{0:T(1024)S(1)}, f32[768]{0:T(1024)}, u32[]{:S(2)}) copy-start(f32[768]{0:T(1024)} %param.30) | copy-start | bytes 9220
  52.6 9.4 %copy-start.1 = (bf16[4,128,128]{2,1,0:T(8,128)(2,1)S(1)}, bf16[4,128,128]{2,1,0:T(8,128)(2,1)}, u32[]{:S(2)}) copy-start(bf16[4,128,128]{2,1,0:T(8,128)(2,1)} %mix_ref.1) | copy-start | bytes 393220
  52.6 9.4 %copy-start.2 = (f32[512]{0:T(512)S(1)}, f32[512]{0:T(512)}, u32[]{:S(2)}) copy-start(f32[512]{0:T(512)} %param.32) | copy-start | bytes 6148
  52.7 9.7 %copy-start.9 = (bf16[384,2048]{1,0:T(8,128)(2,1)S(1)}, bf16[384,2048]{1,0:T(8,128)(2,1)}, u32[]{:S(2)}) copy-start(bf16[384,2048]{1,0:T(8,128)(2,1)} %wr_ref.3) | copy-start | bytes 4718596
  52.7 9.7 %copy-start.12 = (bf16[256,2048]{1,0:T(8,128)(2,1)S(1)}, bf16[256,2048]{1,0:T(8,128)(2,1)}, u32[]{:S(2)}) copy-start(bf16[256,2048]{1,0:T(8,128)(2,1)} %wp_ref.3) | copy-start | bytes 3145732
  55.5 6.6 %collective-permute-start.10 = (bf16[2,16,256]{2,1,0:T(8,128)(2,1)S(1)}, bf16[2,16,256]{2,1,0:T(8,128)(2,1)S(1)}, u32[]{:S(2)}, u32[]{:S(2)}) collective-permute-start(bf16[2,16,256]{2,1,0:T(8,128)(2,1)S(1)} %get-tuple-element.51), channel_id=1, source_target_pairs={{0,8},{8,16},{16,24},{24,32},{32,40},{40,48},{48,56},{56,64},{64,7... | collective-permute-start | bytes 49160 | tf_op jit(solution)/shard_map/ppermute | solution.py:423
  65.0 6.1 %collective-permute-start.11 = (bf16[256,1024]{1,0:T(8,128)(2,1)S(1)}, bf16[256,1024]{1,0:T(8,128)(2,1)S(1)}, u32[]{:S(2)}, u32[]{:S(2)}) collective-permute-start(bf16[256,1024]{1,0:T(8,128)(2,1)S(1)} %get-tuple-element.54), channel_id=1, source_target_pairs={{0,1},{1,0},{2,3},{3,2},{4,5},{5,4},{6,7},{7,6},{8,9},{9,8},{10,11... | collective-permute-start | bytes 1572872 | tf_op jit(solution)/shard_map/ppermute | solution.py:461
where the time goes:
time: 72.7 us; the launch traced here: 72.1 us
  starting transfers between devices  27.9 us (38%)
  Pallas kernels  17 us (23%)
  waiting for transfers between devices  15.7 us (22%)
  local copies, waits for them, and re-layouts  10.2 us (14%)
  other arithmetic  0.99 us (1%)
    ppermute x6, starting transfers between devices, spread_rows(): out.append(lax.ppermute(part, 'sp_1', pairs))  15.4 us
    pallas_call x1, Pallas kernels, shards(): call(local_kernel, 'local', vmem(5) + hbm(5), [shape((256, D)), shape((25...  9.6 us
    unnamed x32, local copies, waits for them, and re-layouts  8.82 us
    ppermute x3, waiting for transfers between devices, shards(): lax.ppermute(total, 'sp_0', [(i, i + step) for i in range(4) if i + step...  6.87 us
    ppermute x1, starting transfers between devices, shards(): arrived = lax.ppermute(send, 'tp', [(0, 1), (1, 0)])  4.58 us
    ppermute x3, starting transfers between devices, shards(): lax.ppermute(total, 'sp_0', [(i, i + step) for i in range(4) if i + step...  3.88 us
    ppermute x6, waiting for transfers between devices, spread_rows(): out.append(lax.ppermute(part, 'sp_1', pairs))  3.71 us
    ppermute x1, starting transfers between devices, shards(): halo = lax.ppermute(tail, SP, [(i, i + 1) for i in range(15)])  3.36 us
  transfers between devices with their start and end apart: 12, of which 8 were waited for; matrix products, arithmetic and copies ran while one was open for 2% of the time, Pallas kernels for 4%

commit v1 on v0

--- a/solution.py
+++ b/solution.py
@@ -44,6 +44,12 @@
 
 def iota(rows, cols, dim):
     return lax.broadcasted_iota(jnp.int32, (rows, cols), dim)
+
+
+def line_of(ref, lanes):
+    if len(ref.shape) == 1:
+        return ref[lanes].reshape(1, 128)
+    return ref[:, lanes]
 
 
 def head_masks():
@@ -101,34 +107,66 @@
     return result
 
 
-def local_kernel(
-    own_ref, other_ref, gain_ref, db_ref, rb_ref, wk_ref, wd_ref, wa_ref, wr_ref, wv_ref,
-    normed_ref, scale_ref, home_ref, first_ref, second_ref, third_ref,
-    wb_ref, wkk_ref, solved_ref, v_ref, rho_ref,
-    k_s, d_s, a_s, r_s, v_s, maps, w_bufs, sems,
-):
+WIDTHS = (384, 384, 384, 384, 384, 256)
+
+
+def fetch(sources, bufs, first_row, sems):
+    copies = [
+        pltpu.make_async_copy(src.at[pl.ds(pl.multiple_of(first_row, 1024), 1024), :], buf, sems.at[i])
+        for i, (src, buf) in enumerate(zip(sources, bufs))
+    ]
+    for copy in copies:
+        copy.start()
+    return copies
+
+
+def own_kernel(*refs):
+    own_ref, gain_ref = refs[:2]
+    sources, normed_ref, squares_ref, partials = refs[2:8], refs[8], refs[9], refs[10:16]
+    bufs, sems = refs[16:22], refs[22]
+    tp = lax.axis_index("tp")
+    copies = fetch(sources, bufs, tp * 1024, sems)
+    own = own_ref[...].astype(f32)
+    normed = (own * jnp.where(tp == 0, gain_ref[:, :1024], gain_ref[:, 1024:])).astype(bf16)
+    normed_ref[...] = normed
+    squares_ref[...] = jnp.broadcast_to(jnp.sum(own * own, axis=1, keepdims=True), (256, 128))
+    for copy, buf, partial in zip(copies, bufs, partials):
+        copy.wait()
+        partial[...] = dot(normed, buf[...])
+
+
+def local_kernel(*refs):
+    other_ref, gain_ref, squares_ref, db_ref, rb_ref = refs[:5]
+    partials, sources = refs[5:11], refs[11:17]
+    (
+        normed_ref, scale_ref, pool_ref, home_ref, first_ref, second_ref, third_ref,
+        wb_ref, wkk_ref, solved_ref, v_ref, rho_ref,
+    ) = refs[17:29]
+    k_s, d_s, a_s, r_s, v_s, maps = refs[29:35]
+    bufs, sems = refs[35:41], refs[41]
     tp = lax.axis_index("tp")
     y = lax.axis_index("sp_1")
-    sources = (wk_ref, wd_ref, wa_ref, wr_ref, wv_ref)
-    copies = [pltpu.make_async_copy(src, w_bufs.at[i], sems.at[i]) for i, src in enumerate(sources)]
-    for copy in copies:
-        copy.start()
-    own = own_ref[...].astype(f32)
+    copies = fetch(sources, bufs, (1 - tp) * 1024, sems)
+    is_first = tp == 0
     other = other_ref[...].astype(f32)
-    gain_a, gain_b = gain_ref[:, :1024], gain_ref[:, 1024:]
-    is_first = tp == 0
-    own_normed = (own * jnp.where(is_first, gain_a, gain_b)).astype(bf16)
-    other_normed = (other * jnp.where(is_first, gain_b, gain_a)).astype(bf16)
-    squares = jnp.sum(own * own + other * other, axis=1, keepdims=True)
+    normed = (other * jnp.where(is_first, gain_ref[:, 1024:], gain_ref[:, :1024])).astype(bf16)
+    normed_ref[...] = normed
+    squares = squares_ref[:, :1] + jnp.sum(other * other, axis=1, keepdims=True)
     scale = lax.rsqrt(squares * (1.0 / D) + 0.25)
-    normed_ref[:, :1024] = own_normed
-    normed_ref[:, 1024:] = other_normed
     scale_ref[...] = jnp.broadcast_to(scale, (256, 128))
-    for i, dest in enumerate((k_s, d_s, a_s, r_s, v_s)):
+    for i in range(6):
         copies[i].wait()
-        total = dot(own_normed, w_bufs[i, pl.ds(tp * 1024, 1024), :])
-        total = total + dot(other_normed, w_bufs[i, pl.ds((1 - tp) * 1024, 1024), :])
-        rounded = (total * scale).astype(bf16)
+        rounded = ((partials[i][...] + dot(normed, bufs[i][...])) * scale).astype(bf16)
+        if i == 5:
+            pool_ref[...] = rounded
+            for s in (0, 1):
+                for half in (0, 1):
+                    at = 256 + (2 * s + half) * 16
+                    first_ref[at : at + 16] = rounded[
+                        s * 128 + 112 : s * 128 + 128, half * 128 : half * 128 + 128
+                    ]
+            continue
+        dest = (k_s, d_s, a_s, r_s, v_s)[i]
         for u in range(UNITS):
             s, h = u // 3, u % 3
             dest[u] = rounded[s * 128 : s * 128 + 128, h * 128 : h * 128 + 128].astype(f32)
@@ -151,8 +189,8 @@
         h = u % 3
         lanes = slice(h * 128, h * 128 + 128)
         shifted = slice(384 + h * 128, 384 + h * 128 + 128)
-        db = jnp.where(is_first, db_ref[:, lanes], db_ref[:, shifted])
-        rb = jnp.where(is_first, rb_ref[:, lanes], rb_ref[:, shifted])
+        db = jnp.where(is_first, line_of(db_ref, lanes), line_of(db_ref, shifted))
+        rb = jnp.where(is_first, line_of(rb_ref, lanes), line_of(rb_ref, shifted))
         k = k_s[u]
         log_decay = -0.6065306597126334 * jax.nn.sigmoid(db + d_s[u])
         rate = jax.nn.sigmoid(rb + a_s[u])
@@ -197,26 +235,19 @@
             TN,
         )
         written = crossed[:HEAD] * masks[0] + crossed[HEAD:] * masks[1]
-        maps[u % 3, u // 3, :HEAD] = transit.astype(bf16)
-        maps[u % 3, u // 3, HEAD:] = written.astype(bf16)
-    maps[3] = jnp.zeros((2, 128, 128), bf16)
+        at = (u // 3) * 128
+        maps[u % 3, at : at + HEAD] = transit.astype(bf16)
+        maps[u % 3, at + HEAD : at + 128] = written.astype(bf16)
+    maps[3] = jnp.zeros((256, 128), bf16)
     for step, dest in enumerate((home_ref, first_ref, second_ref, third_ref)):
-        dest[...] = maps[(y + step) & 3]
+        dest[:256] = maps[(y + step) & 3]
 
 
 def side_kernel(
-    normed_ref, scale_ref, wb_ref, wkk_ref, solved_ref, v_ref, rho_ref, wg_ref, wp_ref, wq_ref,
-    reads_ref, local_ref, gate_ref, pool_ref, pgate_ref, tail_ref,
-    g_buf, p_bufs, sems,
+    own_ref, other_ref, scale_ref, wb_ref, wkk_ref, solved_ref, v_ref, rho_ref, wg_ref, wq_ref,
+    reads_ref, local_ref, gate_ref, pgate_ref,
 ):
     tp = lax.axis_index("tp")
-    copies = [
-        pltpu.make_async_copy(wp_ref, p_bufs.at[0], sems.at[0]),
-        pltpu.make_async_copy(wq_ref, p_bufs.at[1], sems.at[1]),
-        pltpu.make_async_copy(wg_ref, g_buf, sems.at[2]),
-    ]
-    for copy in copies:
-        copy.start()
     masks = head_masks()
     wide = (
         jnp.concatenate([masks[0], masks[0]], axis=1),
@@ -227,38 +258,30 @@
         reads_ref[u] = (rho_ref[u] - removed[:, :128]).astype(bf16)
         local_ref[u] = dot(wkk_ref[u], both(v_ref[u].astype(f32), masks)) - removed[:, 128:]
     scale = scale_ref[:, :1]
-    own, other = normed_ref[:, :1024], normed_ref[:, 1024:]
-
-    def project(buf):
-        total = dot(own, buf[pl.ds(tp * 1024, 1024), :])
-        total = total + dot(other, buf[pl.ds((1 - tp) * 1024, 1024), :])
-        return (total * scale).astype(bf16)
-
-    copies[0].wait()
-    pool = project(p_bufs.at[0])
-    pool_ref[...] = pool
-    tail_ref[0] = pool[112:128]
-    tail_ref[1] = pool[240:256]
-    copies[1].wait()
-    pgate_ref[...] = project(p_bufs.at[1])
-    copies[2].wait()
-    gate_ref[...] = project(g_buf)
-
-
-def row_kernel(home_ref, first_ref, second_ref, third_ref, prefix_ref, total_ref, maps):
+    mine, theirs = pl.multiple_of(tp * 1024, 1024), pl.multiple_of((1 - tp) * 1024, 1024)
+    for weight, dest in ((wg_ref, gate_ref), (wq_ref, pgate_ref)):
+        total = dot(own_ref[...], weight[pl.ds(mine, 1024), :])
+        total = total + dot(other_ref[...], weight[pl.ds(theirs, 1024), :])
+        dest[...] = (total * scale).astype(bf16)
+
+
+def row_kernel(home_ref, first_ref, second_ref, third_ref, after_ref, prefix_ref, next_ref, total_ref, maps):
     y = lax.axis_index("sp_1")
     for step, src in enumerate((home_ref, first_ref, second_ref, third_ref)):
-        maps[(y + 4 - step) & 3] = src[...]
+        maps[(y + 4 - step) & 3] = src[:256]
+    next_ref[256:] = first_ref[256:]
     masks = head_masks()
     for s in (0, 1):
-        so_far = maps[0, s].astype(f32)
+        rows = slice(s * 128, s * 128 + 128)
+        so_far = maps[0, rows].astype(f32)
         prefix_ref[0, s] = so_far
         for j in (1, 2, 3):
-            so_far = compose(so_far, maps[j, s], masks)
+            so_far = compose(so_far, maps[j, rows], masks)
             if j < 3:
                 prefix_ref[j, s] = so_far
             else:
-                total_ref[s] = so_far.astype(bf16)
+                next_ref[rows] = so_far.astype(bf16)
+                total_ref[rows] = so_far.astype(bf16)
 
 
 def column_kernel(
@@ -269,13 +292,13 @@
     y = lax.axis_index("sp_1")
     z = lax.axis_index("sp_0")
     for step, src in enumerate((first_ref, second_ref, third_ref)):
-        rows[(z + 3 - step) & 3] = src[...]
+        rows[(z + 3 - step) & 3] = src[:256]
     masks = head_masks()
     pair = jnp.minimum(y, 2) * 2
     for s in (0, 1):
         state = jnp.concatenate([init_ref[s, pair], init_ref[s, pair + 1]], axis=1)
         for j in range(3):
-            state = jnp.where(j < z, compose(state, rows[j, s], masks), state)
+            state = jnp.where(j < z, compose(state, rows[j, s * 128 : s * 128 + 128], masks), state)
         starts[0, s] = state.astype(bf16)
         for j in range(3):
             starts[j + 1, s] = compose(state, prefix_ref[j, s], masks).astype(bf16)
@@ -283,14 +306,25 @@
         dest[...] = starts[(y + step) & 3]
 
 
-def pool_kernel(pool_ref, tail_ref, pgate_ref, mix_ref, pscale_ref, out_ref):
+def pool_kernel(pool_ref, beside_ref, above_ref, pgate_ref, mix_ref, pscale_ref, out_ref):
     tp = lax.axis_index("tp")
-    place = lax.axis_index("sp_0") * 4 + lax.axis_index("sp_1")
+    y = lax.axis_index("sp_1")
+    place = lax.axis_index("sp_0") * 4 + y
     is_first = tp == 0
     factor = jnp.where(is_first, pscale_ref[:, :256], pscale_ref[:, 256:])
     for s in (0, 1):
         current = pool_ref[s * 128 : s * 128 + 128].astype(f32)
-        padded = jnp.concatenate([tail_ref[s].astype(f32), current], axis=0)
+        tails = []
+        for half in (0, 1):
+            rows = slice(256 + (2 * s + half) * 16, 272 + (2 * s + half) * 16)
+            tails.append(
+                jnp.where(
+                    place == 0,
+                    0.0,
+                    jnp.where(y > 0, beside_ref[rows].astype(f32), above_ref[rows].astype(f32)),
+                )
+            )
+        padded = jnp.concatenate([jnp.concatenate(tails, axis=1), current], axis=0)
         sums = {1: padded}
         for by in (1, 2, 4, 8):
             before = sums[by]
@@ -314,16 +348,10 @@
     home_ref, one_ref, two_ref, three_ref, reads_ref, local_ref, gate_ref, hgain_ref, pool_ref,
     wr_ref, wp_ref,
     send_ref, keep_ref,
-    starts, rec, wr_buf, wp_buf, sems,
+    starts, rec,
 ):
     tp = lax.axis_index("tp")
     y = lax.axis_index("sp_1")
-    copies = [
-        pltpu.make_async_copy(wr_ref, wr_buf, sems.at[0]),
-        pltpu.make_async_copy(wp_ref, wp_buf, sems.at[1]),
-    ]
-    for copy in copies:
-        copy.start()
     for step, src in enumerate((home_ref, one_ref, two_ref, three_ref)):
         starts[(y + 4 - step) & 3] = src[...]
     masks = head_masks()
@@ -338,16 +366,14 @@
         out = dot(reads_ref[u], both(starts[h, s].astype(f32), masks), NT) + local_ref[u]
         out = out - dot_fine_left(out, mean_of)
         spread = dot_fine_left(out * out, mean_of)
-        gain = jnp.where(is_first, hgain_ref[:, lanes], hgain_ref[:, shifted])
+        gain = jnp.where(is_first, line_of(hgain_ref, lanes), line_of(hgain_ref, shifted))
         gate = gate_ref[rows, lanes].astype(f32)
         rec[rows, lanes] = (
             out * lax.rsqrt(spread + 1.0) * gain * (gate * jax.nn.sigmoid(gate))
         ).astype(bf16)
-    for copy in copies:
-        copy.wait()
     for dest, part in ((send_ref, 1 - tp), (keep_ref, tp)):
         cols = pl.ds(pl.multiple_of(part * 1024, 1024), 1024)
-        dest[...] = (dot(rec[...], wr_buf[:, cols]) + dot(pool_ref[...], wp_buf[:, cols])).astype(bf16)
+        dest[...] = (dot(rec[...], wr_ref[:, cols]) + dot(pool_ref[...], wp_ref[:, cols])).astype(bf16)
 
 
 def vmem(count):
@@ -355,7 +381,7 @@
 
 
 def hbm(count):
-    return [pl.BlockSpec(memory_space=pl.ANY)] * count
+    return [pl.BlockSpec(memory_space=pltpu.HBM)] * count
 
 
 def shape(dims, kind=bf16):
@@ -375,12 +401,10 @@
     )
 
 
-def spread_rows(parts, senders, receivers):
-    out = []
-    for step, part in enumerate(parts, 1):
-        pairs = [(i, (i + step) & 3) for i in range(4) if i in senders and ((i + step) & 3) in receivers]
-        out.append(lax.ppermute(part, "sp_1", pairs))
-    return out
+def around(parts, axis):
+    return [
+        lax.ppermute(part, axis, [(i, (i + step) & 3) for i in range(4)]) for step, part in enumerate(parts, 1)
+    ]
 
 
 def shards(
@@ -389,75 +413,73 @@
 ):
     other = lax.ppermute(tokens, "tp", [(0, 1), (1, 0)])
     line = lambda x: x.reshape(1, -1)
-    normed, scale, home, m1, m2, m3, wb, wkk, solved, v, rho = call(
+    weights = (w_key, w_decay, w_rate, w_recept, w_value, w_pool)
+    bufs = [pltpu.VMEM((1024, width), bf16) for width in WIDTHS] + [pltpu.SemaphoreType.DMA((6,))]
+    own_normed, squares, *partials = call(
+        own_kernel,
+        "own",
+        vmem(2) + hbm(6),
+        [shape((256, 1024)), shape((256, 128), f32)] + [shape((256, width), f32) for width in WIDTHS],
+        bufs,
+        20,
+        1_000_000_000,
+    )(tokens.reshape(256, 1024), line(norm_gain), *weights)
+    normed, scale, pool, home, m1, m2, m3, wb, wkk, solved, v, rho = call(
         local_kernel,
         "local",
-        vmem(5) + hbm(5),
+        vmem(11) + hbm(6),
         [
-            shape((256, D)), shape((256, 128), f32),
-            shape((2, 128, 128)), shape((2, 128, 128)), shape((2, 128, 128)), shape((2, 128, 128)),
+            shape((256, 1024)), shape((256, 128), f32), shape((256, 256)),
+            shape((256, 128)), shape((320, 128)), shape((256, 128)), shape((256, 128)),
             shape((6, 128, 256)), shape((6, 128, 256)), shape((6, 128, 256)),
             shape((6, 128, 128)), shape((6, 128, 128), f32),
         ],
-        [pltpu.VMEM((6, 128, 128), f32)] * 5
-        + [pltpu.VMEM((4, 2, 128, 128), bf16), pltpu.VMEM((5, D, 384), bf16), pltpu.SemaphoreType.DMA((5,))],
-        40,
-        4_000_000_000,
-    )(
-        tokens.reshape(256, 1024), other.reshape(256, 1024), line(norm_gain), line(decay_base), line(rate_base),
-        w_key, w_decay, w_rate, w_recept, w_value,
-    )
-    r1, r2, r3 = spread_rows((m1, m2, m3), (0, 1, 2, 3), (0, 1, 2))
-    reads, local, gate, pool, pgate, tail = call(
+        [pltpu.VMEM((6, 128, 128), f32)] * 5 + [pltpu.VMEM((4, 256, 128), bf16)] + bufs,
+        30,
+        3_000_000_000,
+    )(other.reshape(256, 1024), line(norm_gain), squares, decay_base, rate_base, *partials, *weights)
+    r1, r2, r3 = around((m1, m2, m3), "sp_1")
+    reads, local, gate, pgate = call(
         side_kernel,
         "side",
-        vmem(7) + hbm(3),
-        [
-            shape((6, 128, 128)), shape((6, 128, 128), f32), shape((256, 384)), shape((256, 256)),
-            shape((256, 256)), shape((2, 16, 256)),
-        ],
-        [pltpu.VMEM((D, 384), bf16), pltpu.VMEM((2, D, 256), bf16), pltpu.SemaphoreType.DMA((3,))],
-        24,
-        2_000_000_000,
-    )(normed, scale, wb, wkk, solved, v, rho, w_gate_rec, w_pool, w_gate_pool)
-    halo = lax.ppermute(tail, SP, [(i, i + 1) for i in range(15)])
-    prefix, total = call(
+        vmem(10),
+        [shape((6, 128, 128)), shape((6, 128, 128), f32), shape((256, 384)), shape((256, 256))],
+        [],
+        16,
+        1_000_000_000,
+    )(own_normed, normed, scale, wb, wkk, solved, v, rho, w_gate_rec, w_gate_pool)
+    prefix, onward, total = call(
         row_kernel,
         "row",
-        vmem(4),
-        [shape((3, 2, 128, 128), f32), shape((2, 128, 128))],
-        [pltpu.VMEM((4, 2, 128, 128), bf16)],
+        vmem(4) + [pl.BlockSpec(memory_space=pl.ANY)],
+        [shape((3, 2, 128, 128), f32), shape((320, 128)), shape((256, 128))],
+        [pltpu.VMEM((4, 256, 128), bf16)],
         8,
         100_000_000,
-    )(home, r1, r2, r3)
-    columns = [
-        lax.ppermute(total, "sp_0", [(i, i + step) for i in range(4) if i + step < 4]) for step in (1, 2, 3)
-    ]
+    )(home, r1, r2, r3, pgate)
+    columns = around((onward, total, total), "sp_0")
     s0, s1, s2, s3 = call(
         column_kernel,
         "column",
         vmem(5),
         [shape((2, 64, 128))] * 4,
-        [pltpu.VMEM((4, 2, 64, 128), bf16), pltpu.VMEM((4, 2, 128, 128), bf16)],
+        [pltpu.VMEM((4, 2, 64, 128), bf16), pltpu.VMEM((4, 256, 128), bf16)],
         8,
         100_000_000,
     )(prefix, *columns, init_state)
-    t1, t2, t3 = spread_rows((s1, s2, s3), (0, 1, 2), (0, 1, 2, 3))
-    pool_out = call(pool_kernel, "pool", vmem(5), shape((256, 256)), [], 8, 100_000_000)(
-        pool, halo, pgate, pool_mix, line(pool_scale)
+    t1, t2, t3 = around((s1, s2, s3), "sp_1")
+    pool_out = call(pool_kernel, "pool", vmem(6), shape((256, 256)), [], 8, 100_000_000)(
+        pool, r1, columns[0], pgate, pool_mix, line(pool_scale)
     )
     send, keep = call(
         final_kernel,
         "final",
-        vmem(9) + hbm(2),
+        vmem(11),
         [shape((256, 1024)), shape((256, 1024))],
-        [
-            pltpu.VMEM((4, 2, 64, 128), bf16), pltpu.VMEM((256, 384), bf16), pltpu.VMEM((384, D), bf16),
-            pltpu.VMEM((256, D), bf16), pltpu.SemaphoreType.DMA((2,)),
-        ],
+        [pltpu.VMEM((4, 2, 64, 128), bf16), pltpu.VMEM((256, 384), bf16)],
         20,
         1_000_000_000,
-    )(s0, t1, t2, t3, reads, local, gate, line(head_gain), pool_out, w_out_rec, w_out_pool)
+    )(s0, t1, t2, t3, reads, local, gate, head_gain, pool_out, w_out_rec, w_out_pool)
     arrived = lax.ppermute(send, "tp", [(0, 1), (1, 0)])
     mixed = keep.astype(f32) + arrived.astype(f32)
     return mixed.astype(bf16).reshape(2, 128, 1024)

time: 72.7 us -> 56.8 us (0.78)
  the two profiles are of different devices: /device:TPU:97 before, /device:TPU:1 now
where the time goes in v1:
time: 56.8 us; the launch traced here: 56.4 us
  starting transfers between devices  19 us (33%)
  Pallas kernels  17.1 us (30%)
  local copies, waits for them, and re-layouts  10.3 us (18%)
  waiting for transfers between devices  8.86 us (16%)
  other arithmetic  0.99 us (2%)
    ppermute x9, starting transfers between devices, around(): lax.ppermute(part, axis, [(i, i + step & 3) for i in range(4)])  13.4 us
    unnamed x50, local copies, waits for them, and re-layouts  10.3 us
    pallas_call x1, Pallas kernels, shards(): call(local_kernel, 'local', vmem(11) + hbm(6), [shape((256, 1024)), shape...  8.31 us
    ppermute x9, waiting for transfers between devices, around(): lax.ppermute(part, axis, [(i, i + step & 3) for i in range(4)])  7.32 us
    ppermute x1, starting transfers between devices, shards(): arrived = lax.ppermute(send, 'tp', [(0, 1), (1, 0)])  4.19 us
    pallas_call x1, Pallas kernels, shards(): call(own_kernel, 'own', vmem(2) + hbm(6), [shape((256, 1024)), shape((256...  3.23 us
    pallas_call x1, Pallas kernels, shards(): call(final_kernel, 'final', vmem(11), [shape((256, 1024)), shape((256, 10...  2.21 us
    ppermute x1, waiting for transfers between devices, shards(): arrived = lax.ppermute(send, 'tp', [(0, 1), (1, 0)])  1.54 us
  transfers between devices with their start and end apart: 11, of which 7 were waited for; matrix products, arithmetic and copies ran while one was open for 0% of the time, Pallas kernels for 8%

profile of v1, /device:TPU:1, one launch (start us, length us, event | category | flops | bytes accessed | tf_op | source)
XLA Modules:
  0.0 56.4 jit_solution(17829418284315541904)
XLA Ops:
  0.0 1.4 %collective-permute-start = (bf16[2,128,1024]{2,1,0:T(8,128)(2,1)}, bf16[2,128,1024]{2,1,0:T(8,128)(2,1)S(1)}, u32[]{:S(2)}, u32[]{:S(2)}) collective-permute-start(bf16[2,128,1024]{2,1,0:T(8,128)(2,1)} %param.18), channel_id=1, source_target_pairs={{0,1},{1,0},{2,3},{3,2},{4,5},{5,4},{6,7},{7,6},{8,9},{9,8},{10,11... | collective-permute-start | bytes 1572872 | tf_op jit(solution)/shard_map/ppermute | solution.py:414
  1.4 1.4 %copy-done = bf16[2048,384]{1,0:T(8,128)(2,1)S(1)} copy-done((bf16[2048,384]{1,0:T(8,128)(2,1)S(1)}, bf16[2048,384]{1,0:T(8,128)(2,1)}, u32[]{:S(2)}) %copy-start) | copy-done | bytes 1572888
  2.8 1.4 %copy-done.2 = bf16[2048,384]{1,0:T(8,128)(2,1)S(1)} copy-done((bf16[2048,384]{1,0:T(8,128)(2,1)S(1)}, bf16[2048,384]{1,0:T(8,128)(2,1)}, u32[]{:S(2)}) %copy-start.2) | copy-done | bytes 1572888
  4.2 1.4 %copy-done.4 = bf16[2048,384]{1,0:T(8,128)(2,1)S(1)} copy-done((bf16[2048,384]{1,0:T(8,128)(2,1)S(1)}, bf16[2048,384]{1,0:T(8,128)(2,1)}, u32[]{:S(2)}) %copy-start.4) | copy-done | bytes 1572888
  5.6 1.4 %copy-done.6 = bf16[2048,384]{1,0:T(8,128)(2,1)S(1)} copy-done((bf16[2048,384]{1,0:T(8,128)(2,1)S(1)}, bf16[2048,384]{1,0:T(8,128)(2,1)}, u32[]{:S(2)}) %copy-start.6) | copy-done | bytes 1572888
  7.0 1.4 %copy-done.8 = bf16[2048,384]{1,0:T(8,128)(2,1)S(1)} copy-done((bf16[2048,384]{1,0:T(8,128)(2,1)S(1)}, bf16[2048,384]{1,0:T(8,128)(2,1)}, u32[]{:S(2)}) %copy-start.8) | copy-done | bytes 1572888
  8.4 1.2 %copy-done.10 = bf16[2048,256]{1,0:T(8,128)(2,1)S(1)} copy-done((bf16[2048,256]{1,0:T(8,128)(2,1)S(1)}, bf16[2048,256]{1,0:T(8,128)(2,1)}, u32[]{:S(2)}) %copy-start.10) | copy-done | bytes 1048600
  9.7 1.0 %copy-done.14 = bf16[2,128,1024]{2,1,0:T(8,128)(2,1)S(1)} copy-done((bf16[2,128,1024]{2,1,0:T(8,128)(2,1)S(1)}, bf16[2,128,1024]{2,1,0:T(8,128)(2,1)}, u32[]{:S(2)}) %copy-start.14) | copy-done | bytes 524312
  10.7 0.7 %copy-done.17 = f32[2048]{0:T(1024)S(1)} copy-done((f32[2048]{0:T(1024)S(1)}, f32[2048]{0:T(1024)}, u32[]{:S(2)}) %copy-start.17) | copy-done | bytes 8216
  11.5 3.2 %own.1 = (bf16[256,1024]{1,0:T(8,128)(2,1)S(1)}, f32[256,128]{1,0:T(8,128)S(1)}, f32[256,384]{1,0:T(8,128)S(1)}, f32[256,384]{1,0:T(8,128)S(1)}, f32[256,384]{1,...) custom-call(bf16[256,1024]{1,0:T(8,128)(2,1)S(1)} %bitcast.6, ...), custom_call_target="tpu_custom_call" | custom-call | flops 1000000000 | tf_op jit(solution)/shard_map/own/pallas_call | solution.py:418
  15.0 8.3 %local.1 = (bf16[256,1024]{1,0:T(8,128)(2,1)S(1)}, f32[256,128]{1,0:T(8,128)S(1)}, bf16[256,256]{1,0:T(8,128)(2,1)S(1)}, bf16[256,128]{1,0:T(8,128)(2,1)S(1)}, b...) custom-call(bf16[256,1024]{1,0:T(8,128)(2,1)S(1)} %bitcast.5, ...), custom_call_target="tpu_custom_call" | custom-call | flops 3000000000 | tf_op jit(solution)/shard_map/local/pallas_call | solution.py:427
  23.3 3.1 %collective-permute-start.2 = (bf16[256,128]{1,0:T(8,128)(2,1)S(1)}, bf16[256,128]{1,0:T(8,128)(2,1)S(1)}, u32[]{:S(2)}, u32[]{:S(2)}) collective-permute-start(bf16[256,128]{1,0:T(8,128)(2,1)S(1)} %get-tuple-element.47), channel_id=1, source_target_pairs={{0,16},{8,24},{16,0},{24,8},{1,17},{9,25},{17,1},{25,9},{2,18},{10... | collective-permute-start | bytes 196616 | tf_op jit(solution)/shard_map/ppermute | solution.py:406
  26.4 0.8 %collective-permute-start.3 = (bf16[256,128]{1,0:T(8,128)(2,1)S(1)}, bf16[256,128]{1,0:T(8,128)(2,1)S(1)}, u32[]{:S(2)}, u32[]{:S(2)}) collective-permute-start(bf16[256,128]{1,0:T(8,128)(2,1)S(1)} %get-tuple-element.48), channel_id=1, source_target_pairs={{0,24},{8,0},{16,8},{24,16},{1,25},{9,1},{17,9},{25,17},{2,26},{10... | collective-permute-start | bytes 196616 | tf_op jit(solution)/shard_map/ppermute | solution.py:406
  27.2 0.7 %collective-permute-start.1 = (bf16[320,128]{1,0:T(8,128)(2,1)S(1)}, bf16[320,128]{1,0:T(8,128)(2,1)S(1)}, u32[]{:S(2)}, u32[]{:S(2)}) collective-permute-start(bf16[320,128]{1,0:T(8,128)(2,1)S(1)} %get-tuple-element.46), channel_id=1, source_target_pairs={{0,8},{8,16},{16,24},{24,0},{1,9},{9,17},{17,25},{25,1},{2,10},{10... | collective-permute-start | bytes 245768 | tf_op jit(solution)/shard_map/ppermute | solution.py:406
  27.9 1.2 %side.1 = (bf16[6,128,128]{2,1,0:T(8,128)(2,1)S(1)}, f32[6,128,128]{2,1,0:T(8,128)S(1)}, bf16[256,384]{1,0:T(8,128)(2,1)S(1)}, bf16[256,256]{1,0:T(8,128)(2,1)S(1)}) custom-call(bf16[256,1024]{1,0:T(8,128)(2,1)S(1)} %get-tuple-element.49.own_ref, bf16[256,1024]{1,0:T(8,128)(2,1)S(1)} %get-tuple-element.50.other_ref, ...), custom_call_target="tpu_custom_call" | custom-call | flops 1000000000 | tf_op jit(solution)/shard_map/side/pallas_call | solution.py:442
  29.2 1.2 %collective-permute-done.3.third_ref = bf16[256,128]{1,0:T(8,128)(2,1)S(1)} collective-permute-done((bf16[256,128]{1,0:T(8,128)(2,1)S(1)}, bf16[256,128]{1,0:T(8,128)(2,1)S(1)}, u32[]{:S(2)}, u32[]{:S(2)}) %collective-permute-start.3) | collective-permute-done | bytes 65568 | tf_op jit(solution)/shard_map/ppermute | solution.py:406
  30.4 1.2 %collective-permute-done.1.first_ref.beside_ref = bf16[320,128]{1,0:T(8,128)(2,1)S(1)} collective-permute-done((bf16[320,128]{1,0:T(8,128)(2,1)S(1)}, bf16[320,128]{1,0:T(8,128)(2,1)S(1)}, u32[]{:S(2)}, u32[]{:S(2)}) %collective-permute-start.1) | collective-permute-done | bytes 81952 | tf_op jit(solution)/shard_map/ppermute | solution.py:406
  31.7 0.6 %row.1 = (f32[3,2,128,128]{3,2,1,0:T(8,128)S(1)}, bf16[320,128]{1,0:T(8,128)(2,1)S(1)}, bf16[256,128]{1,0:T(8,128)(2,1)S(1)}) custom-call(bf16[256,128]{1,0:T(8,128)(2,1)S(1)} %get-tuple-element.45.home_ref, bf16[320,128]{1,0:T(8,128)(2,1)S(1)} %collective-permute-done.1.first_ref.beside_ref, bf16[256,128]{1,0:T(8,128)(2,1)S(1)} %collective-permute-done.2.second_ref, ...), custom_call_target="tpu_custom_call" | custom-call | flops 100000000 | tf_op jit(solution)/shard_map/row/pallas_call | solution.py:451
  32.3 1.7 %collective-permute-start.4 = (bf16[320,128]{1,0:T(8,128)(2,1)S(1)}, bf16[320,128]{1,0:T(8,128)(2,1)S(1)}, u32[]{:S(2)}, u32[]{:S(2)}) collective-permute-start(bf16[320,128]{1,0:T(8,128)(2,1)S(1)} %get-tuple-element.59), channel_id=1, source_target_pairs={{0,32},{32,64},{64,96},{96,0},{1,33},{33,65},{65,97},{97,1},{2,34}... | collective-permute-start | bytes 245768 | tf_op jit(solution)/shard_map/ppermute | solution.py:406
  34.0 2.2 %collective-permute-start.6 = (bf16[256,128]{1,0:T(8,128)(2,1)S(1)}, bf16[256,128]{1,0:T(8,128)(2,1)S(1)}, u32[]{:S(2)}, u32[]{:S(2)}) collective-permute-start(bf16[256,128]{1,0:T(8,128)(2,1)S(1)} %get-tuple-element.60), channel_id=1, source_target_pairs={{0,96},{32,0},{64,32},{96,64},{1,97},{33,1},{65,33},{97,65},{2,98}... | collective-permute-start | bytes 196616 | tf_op jit(solution)/shard_map/ppermute | solution.py:406
  36.2 1.2 %collective-permute-start.5 = (bf16[256,128]{1,0:T(8,128)(2,1)S(1)}, bf16[256,128]{1,0:T(8,128)(2,1)S(1)}, u32[]{:S(2)}, u32[]{:S(2)}) collective-permute-start(bf16[256,128]{1,0:T(8,128)(2,1)S(1)} %get-tuple-element.60), channel_id=1, source_target_pairs={{0,64},{32,96},{64,0},{96,32},{1,65},{33,97},{65,1},{97,33},{2,66}... | collective-permute-start | bytes 196616 | tf_op jit(solution)/shard_map/ppermute | solution.py:406
  37.6 3.7 %collective-permute-done.5.second_ref = bf16[256,128]{1,0:T(8,128)(2,1)S(1)} collective-permute-done((bf16[256,128]{1,0:T(8,128)(2,1)S(1)}, bf16[256,128]{1,0:T(8,128)(2,1)S(1)}, u32[]{:S(2)}, u32[]{:S(2)}) %collective-permute-start.5) | collective-permute-done | bytes 65568 | tf_op jit(solution)/shard_map/ppermute | solution.py:406
  41.2 1.2 %column.1 = (bf16[2,64,128]{2,1,0:T(8,128)(2,1)S(1)}, bf16[2,64,128]{2,1,0:T(8,128)(2,1)S(1)}, bf16[2,64,128]{2,1,0:T(8,128)(2,1)S(1)}, bf16[2,64,128]{2,1,0:T(8,128)(2,1)S(1)}) custom-call(f32[3,2,128,128]{3,2,1,0:T(8,128)S(1)} %get-tuple-element.58.prefix_ref, bf16[320,128]{1,0:T(8,128)(2,1)S(1)} %collective-permute-done.4.first_ref.above_ref, ...), custom_call_target="tpu_custom_call" | custom-call | flops 100000000 | tf_op jit(solution)/shard_map/column/pallas_call | solution.py:461
  42.4 0.3 collective-permute-start.7
  42.7 1.9 %collective-permute-start.8 = (bf16[2,64,128]{2,1,0:T(8,128)(2,1)S(1)}, bf16[2,64,128]{2,1,0:T(8,128)(2,1)S(1)}, u32[]{:S(2)}, u32[]{:S(2)}) collective-permute-start(bf16[2,64,128]{2,1,0:T(8,128)(2,1)S(1)} %get-tuple-element.63), channel_id=1, source_target_pairs={{0,16},{8,24},{16,0},{24,8},{1,17},{9,25},{17,1},{25,9},{2,18},{10... | collective-permute-start | bytes 98312 | tf_op jit(solution)/shard_map/ppermute | solution.py:406
  44.7 1.4 %collective-permute-start.9 = (bf16[2,64,128]{2,1,0:T(8,128)(2,1)S(1)}, bf16[2,64,128]{2,1,0:T(8,128)(2,1)S(1)}, u32[]{:S(2)}, u32[]{:S(2)}) collective-permute-start(bf16[2,64,128]{2,1,0:T(8,128)(2,1)S(1)} %get-tuple-element.64), channel_id=1, source_target_pairs={{0,24},{8,0},{16,8},{24,16},{1,25},{9,1},{17,9},{25,17},{2,26},{10... | collective-permute-start | bytes 98312 | tf_op jit(solution)/shard_map/ppermute | solution.py:406
  46.5 0.6 collective-permute-done.8.two_ref
  47.0 0.4 collective-permute-done.9.three_ref
  47.5 2.2 %final.1 = (bf16[256,1024]{1,0:T(8,128)(2,1)S(1)}, bf16[256,1024]{1,0:T(8,128)(2,1)S(1)}) custom-call(bf16[2,64,128]{2,1,0:T(8,128)(2,1)S(1)} %get-tuple-element.61.home_ref, bf16[2,64,128]{2,1,0:T(8,128)(2,1)S(1)} %collective-permute-done.7.one_ref, bf16[2,64,128]{2,1,0:T(8,128)(2,1)S(1)} %collective-permute-done.8.two_ref, ...), custom_call_target="tpu_custom_call" | custom-call | flops 1000000000 | tf_op jit(solution)/shard_map/final/pallas_call | solution.py:474
  49.7 4.2 %collective-permute-start.10 = (bf16[256,1024]{1,0:T(8,128)(2,1)S(1)}, bf16[256,1024]{1,0:T(8,128)(2,1)S(1)}, u32[]{:S(2)}, u32[]{:S(2)}) collective-permute-start(bf16[256,1024]{1,0:T(8,128)(2,1)S(1)} %get-tuple-element.70), channel_id=1, source_target_pairs={{0,1},{1,0},{2,3},{3,2},{4,5},{5,4},{6,7},{7,6},{8,9},{9,8},{10,11... | collective-permute-start | bytes 1572872 | tf_op jit(solution)/shard_map/ppermute | solution.py:483
  53.9 1.5 %collective-permute-done.10 = bf16[256,1024]{1,0:T(8,128)(2,1)S(1)} collective-permute-done((bf16[256,1024]{1,0:T(8,128)(2,1)S(1)}, bf16[256,1024]{1,0:T(8,128)(2,1)S(1)}, u32[]{:S(2)}, u32[]{:S(2)}) %collective-permute-start.10) | collective-permute-done | bytes 524320 | tf_op jit(solution)/shard_map/ppermute | solution.py:483
  55.4 1.0 %add_convert_fusion = bf16[256,1024]{1,0:T(8,128)(2,1)} fusion(bf16[256,1024]{1,0:T(8,128)(2,1)S(1)} %collective-permute-done.10, bf16[256,1024]{1,0:T(8,128)(2,1)S(1)} %get-tuple-element.69), kind=kLoop, calls=%fused_computation | loop fusion | flops 1048576 | bytes 1572864 | tf_op jit(solution)/shard_map/convert_element_type | solution.py:485
  (48 shorter events, 0.7 us)
Async XLA Ops:
  0.0 14.7 %collective-permute-start = (bf16[2,128,1024]{2,1,0:T(8,128)(2,1)}, bf16[2,128,1024]{2,1,0:T(8,128)(2,1)S(1)}, u32[]{:S(2)}, u32[]{:S(2)}) collective-permute-start(bf16[2,128,1024]{2,1,0:T(8,128)(2,1)} %param.18), channel_id=1, source_target_pairs={{0,1},{1,0},{2,3},{3,2},{4,5},{5,4},{6,7},{7,6},{8,9},{9,8},{10,11... | collective-permute-start | bytes 1572872 | tf_op jit(solution)/shard_map/ppermute | solution.py:414
  1.4 1.4 %copy-start = (bf16[2048,384]{1,0:T(8,128)(2,1)S(1)}, bf16[2048,384]{1,0:T(8,128)(2,1)}, u32[]{:S(2)}) copy-start(bf16[2048,384]{1,0:T(8,128)(2,1)} %refs_11_.1) | copy-start | bytes 4718596
  2.8 1.4 %copy-start.2 = (bf16[2048,384]{1,0:T(8,128)(2,1)S(1)}, bf16[2048,384]{1,0:T(8,128)(2,1)}, u32[]{:S(2)}) copy-start(bf16[2048,384]{1,0:T(8,128)(2,1)} %refs_12_.1) | copy-start | bytes 4718596
  4.2 1.4 %copy-start.4 = (bf16[2048,384]{1,0:T(8,128)(2,1)S(1)}, bf16[2048,384]{1,0:T(8,128)(2,1)}, u32[]{:S(2)}) copy-start(bf16[2048,384]{1,0:T(8,128)(2,1)} %refs_13_.1) | copy-start | bytes 4718596
  5.6 1.4 %copy-start.6 = (bf16[2048,384]{1,0:T(8,128)(2,1)S(1)}, bf16[2048,384]{1,0:T(8,128)(2,1)}, u32[]{:S(2)}) copy-start(bf16[2048,384]{1,0:T(8,128)(2,1)} %refs_14_.1) | copy-start | bytes 4718596
  11.4 3.3 %copy-start.1 = (bf16[2048,384]{1,0:T(8,128)(2,1)S(1)}, bf16[2048,384]{1,0:T(8,128)(2,1)}, u32[]{:S(2)}) copy-start(bf16[2048,384]{1,0:T(8,128)(2,1)} %refs_11_.1) | copy-start | bytes 4718596
  11.4 3.3 %copy-start.3 = (bf16[2048,384]{1,0:T(8,128)(2,1)S(1)}, bf16[2048,384]{1,0:T(8,128)(2,1)}, u32[]{:S(2)}) copy-start(bf16[2048,384]{1,0:T(8,128)(2,1)} %refs_12_.1) | copy-start | bytes 4718596
  11.4 3.3 %copy-start.5 = (bf16[2048,384]{1,0:T(8,128)(2,1)S(1)}, bf16[2048,384]{1,0:T(8,128)(2,1)}, u32[]{:S(2)}) copy-start(bf16[2048,384]{1,0:T(8,128)(2,1)} %refs_13_.1) | copy-start | bytes 4718596
  11.4 3.3 %copy-start.7 = (bf16[2048,384]{1,0:T(8,128)(2,1)S(1)}, bf16[2048,384]{1,0:T(8,128)(2,1)}, u32[]{:S(2)}) copy-start(bf16[2048,384]{1,0:T(8,128)(2,1)} %refs_14_.1) | copy-start | bytes 4718596
  11.4 3.3 %copy-start.9 = (bf16[2048,384]{1,0:T(8,128)(2,1)S(1)}, bf16[2048,384]{1,0:T(8,128)(2,1)}, u32[]{:S(2)}) copy-start(bf16[2048,384]{1,0:T(8,128)(2,1)} %refs_15_.1) | copy-start | bytes 4718596
  11.4 3.5 %copy-start.11 = (bf16[2048,256]{1,0:T(8,128)(2,1)S(1)}, bf16[2048,256]{1,0:T(8,128)(2,1)}, u32[]{:S(2)}) copy-start(bf16[2048,256]{1,0:T(8,128)(2,1)} %refs_16_.1) | copy-start | bytes 3145732
  11.4 3.5 %copy-start.18 = (f32[2048]{0:T(1024)S(1)}, f32[2048]{0:T(1024)}, u32[]{:S(2)}) copy-start(f32[2048]{0:T(1024)} %param.19) | copy-start | bytes 24580
  11.4 3.5 %copy-start.19 = (f32[768]{0:T(1024)S(1)}, f32[768]{0:T(1024)}, u32[]{:S(2)}) copy-start(f32[768]{0:T(1024)} %refs_3_.3) | copy-start | bytes 9220
  11.4 3.5 %copy-start.20 = (f32[768]{0:T(1024)S(1)}, f32[768]{0:T(1024)}, u32[]{:S(2)}) copy-start(f32[768]{0:T(1024)} %refs_4_.3) | copy-start | bytes 9220
  14.9 12.9 %copy-start.12 = (bf16[2048,384]{1,0:T(8,128)(2,1)S(1)}, bf16[2048,384]{1,0:T(8,128)(2,1)}, u32[]{:S(2)}) copy-start(bf16[2048,384]{1,0:T(8,128)(2,1)} %wg_ref.1) | copy-start | bytes 4718596
  15.0 12.9 %copy-start.13 = (bf16[2048,256]{1,0:T(8,128)(2,1)S(1)}, bf16[2048,256]{1,0:T(8,128)(2,1)}, u32[]{:S(2)}) copy-start(bf16[2048,256]{1,0:T(8,128)(2,1)} %wq_ref.1) | copy-start | bytes 3145732
  23.3 5.9 %collective-permute-start.2 = (bf16[256,128]{1,0:T(8,128)(2,1)S(1)}, bf16[256,128]{1,0:T(8,128)(2,1)S(1)}, u32[]{:S(2)}, u32[]{:S(2)}) collective-permute-start(bf16[256,128]{1,0:T(8,128)(2,1)S(1)} %get-tuple-element.47), channel_id=1, source_target_pairs={{0,16},{8,24},{16,0},{24,8},{1,17},{9,25},{17,1},{25,9},{2,18},{10... | collective-permute-start | bytes 196616 | tf_op jit(solution)/shard_map/ppermute | solution.py:406
  26.4 4.0 %collective-permute-start.3 = (bf16[256,128]{1,0:T(8,128)(2,1)S(1)}, bf16[256,128]{1,0:T(8,128)(2,1)S(1)}, u32[]{:S(2)}, u32[]{:S(2)}) collective-permute-start(bf16[256,128]{1,0:T(8,128)(2,1)S(1)} %get-tuple-element.48), channel_id=1, source_target_pairs={{0,24},{8,0},{16,8},{24,16},{1,25},{9,1},{17,9},{25,17},{2,26},{10... | collective-permute-start | bytes 196616 | tf_op jit(solution)/shard_map/ppermute | solution.py:406
  27.2 4.5 %collective-permute-start.1 = (bf16[320,128]{1,0:T(8,128)(2,1)S(1)}, bf16[320,128]{1,0:T(8,128)(2,1)S(1)}, u32[]{:S(2)}, u32[]{:S(2)}) collective-permute-start(bf16[320,128]{1,0:T(8,128)(2,1)S(1)} %get-tuple-element.46), channel_id=1, source_target_pairs={{0,8},{8,16},{16,24},{24,0},{1,9},{9,17},{17,25},{25,1},{2,10},{10... | collective-permute-start | bytes 245768 | tf_op jit(solution)/shard_map/ppermute | solution.py:406
  27.9 13.4 %copy-start.15 = (f32[2,6,64,64]{3,2,1,0:T(8,128)S(1)}, f32[2,6,64,64]{3,2,1,0:T(8,128)}, u32[]{:S(2)}) copy-start(f32[2,6,64,64]{3,2,1,0:T(8,128)} %init_ref.1) | copy-start | bytes 589828
  27.9 18.3 %copy-start.16 = (bf16[4,128,128]{2,1,0:T(8,128)(2,1)S(1)}, bf16[4,128,128]{2,1,0:T(8,128)(2,1)}, u32[]{:S(2)}) copy-start(bf16[4,128,128]{2,1,0:T(8,128)(2,1)} %mix_ref.1) | copy-start | bytes 393220
  27.9 18.2 %copy-start.21 = (f32[512]{0:T(512)S(1)}, f32[512]{0:T(512)}, u32[]{:S(2)}) copy-start(f32[512]{0:T(512)} %param.32) | copy-start | bytes 6148
  27.9 19.6 %copy-start.23 = (bf16[256,2048]{1,0:T(8,128)(2,1)S(1)}, bf16[256,2048]{1,0:T(8,128)(2,1)}, u32[]{:S(2)}) copy-start(bf16[256,2048]{1,0:T(8,128)(2,1)} %wp_ref.1) | copy-start | bytes 3145732
  29.2 18.3 %copy-start.22 = (bf16[384,2048]{1,0:T(8,128)(2,1)S(1)}, bf16[384,2048]{1,0:T(8,128)(2,1)}, u32[]{:S(2)}) copy-start(bf16[384,2048]{1,0:T(8,128)(2,1)} %wr_ref.1) | copy-start | bytes 4718596
  29.2 18.3 %copy-start.24 = (f32[768]{0:T(1024)S(1)}, f32[768]{0:T(1024)}, u32[]{:S(2)}) copy-start(f32[768]{0:T(1024)} %hgain_ref.1) | copy-start | bytes 9220
  32.3 8.9 %collective-permute-start.4 = (bf16[320,128]{1,0:T(8,128)(2,1)S(1)}, bf16[320,128]{1,0:T(8,128)(2,1)S(1)}, u32[]{:S(2)}, u32[]{:S(2)}) collective-permute-start(bf16[320,128]{1,0:T(8,128)(2,1)S(1)} %get-tuple-element.59), channel_id=1, source_target_pairs={{0,32},{32,64},{64,96},{96,0},{1,33},{33,65},{65,97},{97,1},{2,34}... | collective-permute-start | bytes 245768 | tf_op jit(solution)/shard_map/ppermute | solution.py:406
  34.0 3.5 %collective-permute-start.6 = (bf16[256,128]{1,0:T(8,128)(2,1)S(1)}, bf16[256,128]{1,0:T(8,128)(2,1)S(1)}, u32[]{:S(2)}, u32[]{:S(2)}) collective-permute-start(bf16[256,128]{1,0:T(8,128)(2,1)S(1)} %get-tuple-element.60), channel_id=1, source_target_pairs={{0,96},{32,0},{64,32},{96,64},{1,97},{33,1},{65,33},{97,65},{2,98}... | collective-permute-start | bytes 196616 | tf_op jit(solution)/shard_map/ppermute | solution.py:406
  36.2 5.0 %collective-permute-start.5 = (bf16[256,128]{1,0:T(8,128)(2,1)S(1)}, bf16[256,128]{1,0:T(8,128)(2,1)S(1)}, u32[]{:S(2)}, u32[]{:S(2)}) collective-permute-start(bf16[256,128]{1,0:T(8,128)(2,1)S(1)} %get-tuple-element.60), channel_id=1, source_target_pairs={{0,64},{32,96},{64,0},{96,32},{1,65},{33,97},{65,1},{97,33},{2,66}... | collective-permute-start | bytes 196616 | tf_op jit(solution)/shard_map/ppermute | solution.py:406
  42.4 4.0 %collective-permute-start.7 = (bf16[2,64,128]{2,1,0:T(8,128)(2,1)S(1)}, bf16[2,64,128]{2,1,0:T(8,128)(2,1)S(1)}, u32[]{:S(2)}, u32[]{:S(2)}) collective-permute-start(bf16[2,64,128]{2,1,0:T(8,128)(2,1)S(1)} %get-tuple-element.62), channel_id=1, source_target_pairs={{0,8},{8,16},{16,24},{24,0},{1,9},{9,17},{17,25},{25,1},{2,10},{10... | collective-permute-start | bytes 98312 | tf_op jit(solution)/shard_map/ppermute | solution.py:406
  42.7 4.3 %collective-permute-start.8 = (bf16[2,64,128]{2,1,0:T(8,128)(2,1)S(1)}, bf16[2,64,128]{2,1,0:T(8,128)(2,1)S(1)}, u32[]{:S(2)}, u32[]{:S(2)}) collective-permute-start(bf16[2,64,128]{2,1,0:T(8,128)(2,1)S(1)} %get-tuple-element.63), channel_id=1, source_target_pairs={{0,16},{8,24},{16,0},{24,8},{1,17},{9,25},{17,1},{25,9},{2,18},{10... | collective-permute-start | bytes 98312 | tf_op jit(solution)/shard_map/ppermute | solution.py:406
  44.7 2.8 %collective-permute-start.9 = (bf16[2,64,128]{2,1,0:T(8,128)(2,1)S(1)}, bf16[2,64,128]{2,1,0:T(8,128)(2,1)S(1)}, u32[]{:S(2)}, u32[]{:S(2)}) collective-permute-start(bf16[2,64,128]{2,1,0:T(8,128)(2,1)S(1)} %get-tuple-element.64), channel_id=1, source_target_pairs={{0,24},{8,0},{16,8},{24,16},{1,25},{9,1},{17,9},{25,17},{2,26},{10... | collective-permute-start | bytes 98312 | tf_op jit(solution)/shard_map/ppermute | solution.py:406
  49.7 5.7 %collective-permute-start.10 = (bf16[256,1024]{1,0:T(8,128)(2,1)S(1)}, bf16[256,1024]{1,0:T(8,128)(2,1)S(1)}, u32[]{:S(2)}, u32[]{:S(2)}) collective-permute-start(bf16[256,1024]{1,0:T(8,128)(2,1)S(1)} %get-tuple-element.70), channel_id=1, source_target_pairs={{0,1},{1,0},{2,3},{3,2},{4,5},{5,4},{6,7},{7,6},{8,9},{9,8},{10,11... | collective-permute-start | bytes 1572872 | tf_op jit(solution)/shard_map/ppermute | solution.py:483
  (4 other events, 4.4 us)

commit v2 on v1

--- a/solution.py
+++ b/solution.py
@@ -121,11 +121,19 @@
 
 
 def own_kernel(*refs):
-    own_ref, gain_ref = refs[:2]
+    token_ref, norm_ref = refs[:2]
     sources, normed_ref, squares_ref, partials = refs[2:8], refs[8], refs[9], refs[10:16]
-    bufs, sems = refs[16:22], refs[22]
+    bufs, sems, own_ref, gain_ref, first_sems = refs[16:22], refs[22], refs[23], refs[24], refs[25]
     tp = lax.axis_index("tp")
+    early = [
+        pltpu.make_async_copy(token_ref, own_ref, first_sems.at[0]),
+        pltpu.make_async_copy(norm_ref, gain_ref, first_sems.at[1]),
+    ]
+    for copy in early:
+        copy.start()
     copies = fetch(sources, bufs, tp * 1024, sems)
+    for copy in early:
+        copy.wait()
     own = own_ref[...].astype(f32)
     normed = (own * jnp.where(tp == 0, gain_ref[:, :1024], gain_ref[:, 1024:])).astype(bf16)
     normed_ref[...] = normed
@@ -413,17 +421,18 @@
 ):
     other = lax.ppermute(tokens, "tp", [(0, 1), (1, 0)])
     line = lambda x: x.reshape(1, -1)
-    weights = (w_key, w_decay, w_rate, w_recept, w_value, w_pool)
+    pinned = lambda x: pltpu.with_memory_space_constraint(x, pltpu.HBM)
+    weights = [pinned(w) for w in (w_key, w_decay, w_rate, w_recept, w_value, w_pool)]
     bufs = [pltpu.VMEM((1024, width), bf16) for width in WIDTHS] + [pltpu.SemaphoreType.DMA((6,))]
     own_normed, squares, *partials = call(
         own_kernel,
         "own",
-        vmem(2) + hbm(6),
+        hbm(8),
         [shape((256, 1024)), shape((256, 128), f32)] + [shape((256, width), f32) for width in WIDTHS],
-        bufs,
+        bufs + [pltpu.VMEM((256, 1024), bf16), pltpu.VMEM((1, D), f32), pltpu.SemaphoreType.DMA((2,))],
         20,
         1_000_000_000,
-    )(tokens.reshape(256, 1024), line(norm_gain), *weights)
+    )(pinned(tokens.reshape(256, 1024)), pinned(line(norm_gain)), *weights)
     normed, scale, pool, home, m1, m2, m3, wb, wkk, solved, v, rho = call(
         local_kernel,
         "local",

time: 56.8 us -> 49 us (0.86)
  local copies, waits for them, and re-layouts: 10.3 us -> 0.06 us
  Pallas kernels: 17.1 us -> 19.7 us
    unnamed x50 -> x22, local copies, waits for them, and re-layouts: 10.3 us -> 0.06 us
    pallas_call x1, Pallas kernels: 3.23 us -> 5.09 us  [shards(): call(own_kernel, 'own', hbm(8), [shape((256, 1024)), shape((256, 128), f3...]
    pallas_call x1, Pallas kernels: 8.31 us -> 9.1 us  [shards(): call(local_kernel, 'local', vmem(11) + hbm(6), [shape((256, 1024)), shape...]
  transfers between devices with their start and end apart: 11 -> 11, of which waited for: 7 -> 8; matrix products, arithmetic and copies ran while one was open for 0% -> 0% of each run, Pallas kernels for 8% -> 13%
where the time goes in v2:
time: 49 us; the launch traced here: 48.9 us
  Pallas kernels  19.7 us (40%)
  starting transfers between devices  19.1 us (39%)
  waiting for transfers between devices  8.95 us (18%)
  other arithmetic  0.99 us (2%)
    ppermute x9, starting transfers between devices, around(): lax.ppermute(part, axis, [(i, i + step & 3) for i in range(4)])  13.6 us
    pallas_call x1, Pallas kernels, shards(): call(local_kernel, 'local', vmem(11) + hbm(6), [shape((256, 1024)), shape...  9.1 us
    ppermute x9, waiting for transfers between devices, around(): lax.ppermute(part, axis, [(i, i + step & 3) for i in range(4)])  7.41 us
    pallas_call x1, Pallas kernels, shards(): call(own_kernel, 'own', hbm(8), [shape((256, 1024)), shape((256, 128), f3...  5.09 us
    ppermute x1, starting transfers between devices, shards(): arrived = lax.ppermute(send, 'tp', [(0, 1), (1, 0)])  4.15 us
    pallas_call x1, Pallas kernels, shards(): call(final_kernel, 'final', vmem(11), [shape((256, 1024)), shape((256, 10...  2.21 us
    ppermute x1, waiting for transfers between devices, shards(): arrived = lax.ppermute(send, 'tp', [(0, 1), (1, 0)])  1.54 us
    ppermute x1, starting transfers between devices, shards(): other = lax.ppermute(tokens, 'tp', [(0, 1), (1, 0)])  1.38 us
  transfers between devices with their start and end apart: 11, of which 8 were waited for; matrix products, arithmetic and copies ran while one was open for 0% of the time, Pallas kernels for 13%

profile of v2, /device:TPU:1, one launch (start us, length us, event | category | flops | bytes accessed | tf_op | source)
XLA Modules:
  0.0 48.9 jit_solution(17492092029335242508)
XLA Ops:
  0.0 1.4 %collective-permute-start = (bf16[2,128,1024]{2,1,0:T(8,128)(2,1)}, bf16[2,128,1024]{2,1,0:T(8,128)(2,1)S(1)}, u32[]{:S(2)}, u32[]{:S(2)}) collective-permute-start(bf16[2,128,1024]{2,1,0:T(8,128)(2,1)} %param.18), channel_id=1, source_target_pairs={{0,1},{1,0},{2,3},{3,2},{4,5},{5,4},{6,7},{7,6},{8,9},{9,8},{10,11... | collective-permute-start | bytes 1572872 | tf_op jit(solution)/shard_map/ppermute | solution.py:422
  1.4 5.1 %own.1 = (bf16[256,1024]{1,0:T(8,128)(2,1)S(1)}, f32[256,128]{1,0:T(8,128)S(1)}, f32[256,384]{1,0:T(8,128)S(1)}, f32[256,384]{1,0:T(8,128)S(1)}, f32[256,384]{1,...) custom-call(bf16[256,1024]{1,0:T(8,128)(2,1)} %bitcast.9, ...), custom_call_target="tpu_custom_call" | custom-call | flops 1000000000 | tf_op jit(solution)/shard_map/own/pallas_call | solution.py:427
  6.5 0.0 copy-start
  6.5 0.0 copy-start.1
  6.5 9.1 %local.1 = (bf16[256,1024]{1,0:T(8,128)(2,1)S(1)}, f32[256,128]{1,0:T(8,128)S(1)}, bf16[256,256]{1,0:T(8,128)(2,1)S(1)}, bf16[256,128]{1,0:T(8,128)(2,1)S(1)}, b...) custom-call(bf16[256,1024]{1,0:T(8,128)(2,1)S(1)} %bitcast.5, ...), custom_call_target="tpu_custom_call" | custom-call | flops 3000000000 | tf_op jit(solution)/shard_map/local/pallas_call | solution.py:436
  15.7 3.1 %collective-permute-start.2 = (bf16[256,128]{1,0:T(8,128)(2,1)S(1)}, bf16[256,128]{1,0:T(8,128)(2,1)S(1)}, u32[]{:S(2)}, u32[]{:S(2)}) collective-permute-start(bf16[256,128]{1,0:T(8,128)(2,1)S(1)} %get-tuple-element.47), channel_id=1, source_target_pairs={{0,16},{8,24},{16,0},{24,8},{1,17},{9,25},{17,1},{25,9},{2,18},{10... | collective-permute-start | bytes 196616 | tf_op jit(solution)/shard_map/ppermute | solution.py:414
  18.8 0.8 %collective-permute-start.3 = (bf16[256,128]{1,0:T(8,128)(2,1)S(1)}, bf16[256,128]{1,0:T(8,128)(2,1)S(1)}, u32[]{:S(2)}, u32[]{:S(2)}) collective-permute-start(bf16[256,128]{1,0:T(8,128)(2,1)S(1)} %get-tuple-element.48), channel_id=1, source_target_pairs={{0,24},{8,0},{16,8},{24,16},{1,25},{9,1},{17,9},{25,17},{2,26},{10... | collective-permute-start | bytes 196616 | tf_op jit(solution)/shard_map/ppermute | solution.py:414
  19.5 0.7 %collective-permute-start.1 = (bf16[320,128]{1,0:T(8,128)(2,1)S(1)}, bf16[320,128]{1,0:T(8,128)(2,1)S(1)}, u32[]{:S(2)}, u32[]{:S(2)}) collective-permute-start(bf16[320,128]{1,0:T(8,128)(2,1)S(1)} %get-tuple-element.46), channel_id=1, source_target_pairs={{0,8},{8,16},{16,24},{24,0},{1,9},{9,17},{17,25},{25,1},{2,10},{10... | collective-permute-start | bytes 245768 | tf_op jit(solution)/shard_map/ppermute | solution.py:414
  20.2 0.0 copy-start.7
  20.3 0.0 copy-start.9
  20.3 1.2 %side.1 = (bf16[6,128,128]{2,1,0:T(8,128)(2,1)S(1)}, f32[6,128,128]{2,1,0:T(8,128)S(1)}, bf16[256,384]{1,0:T(8,128)(2,1)S(1)}, bf16[256,256]{1,0:T(8,128)(2,1)S(1)}) custom-call(bf16[256,1024]{1,0:T(8,128)(2,1)S(1)} %get-tuple-element.49.own_ref, bf16[256,1024]{1,0:T(8,128)(2,1)S(1)} %get-tuple-element.50.other_ref, ...), custom_call_target="tpu_custom_call" | custom-call | flops 1000000000 | tf_op jit(solution)/shard_map/side/pallas_call | solution.py:451
  21.5 0.0 copy-start.10
  21.5 1.3 %collective-permute-done.3.third_ref = bf16[256,128]{1,0:T(8,128)(2,1)S(1)} collective-permute-done((bf16[256,128]{1,0:T(8,128)(2,1)S(1)}, bf16[256,128]{1,0:T(8,128)(2,1)S(1)}, u32[]{:S(2)}, u32[]{:S(2)}) %collective-permute-start.3) | collective-permute-done | bytes 65568 | tf_op jit(solution)/shard_map/ppermute | solution.py:414
  22.8 1.2 %collective-permute-done.1.first_ref.beside_ref = bf16[320,128]{1,0:T(8,128)(2,1)S(1)} collective-permute-done((bf16[320,128]{1,0:T(8,128)(2,1)S(1)}, bf16[320,128]{1,0:T(8,128)(2,1)S(1)}, u32[]{:S(2)}, u32[]{:S(2)}) %collective-permute-start.1) | collective-permute-done | bytes 81952 | tf_op jit(solution)/shard_map/ppermute | solution.py:414
  24.0 0.6 %row.1 = (f32[3,2,128,128]{3,2,1,0:T(8,128)S(1)}, bf16[320,128]{1,0:T(8,128)(2,1)S(1)}, bf16[256,128]{1,0:T(8,128)(2,1)S(1)}) custom-call(bf16[256,128]{1,0:T(8,128)(2,1)S(1)} %get-tuple-element.45.home_ref, bf16[320,128]{1,0:T(8,128)(2,1)S(1)} %collective-permute-done.1.first_ref.beside_ref, bf16[256,128]{1,0:T(8,128)(2,1)S(1)} %collective-permute-done.2.second_ref, ...), custom_call_target="tpu_custom_call" | custom-call | flops 100000000 | tf_op jit(solution)/shard_map/row/pallas_call | solution.py:460
  24.7 1.9 %collective-permute-start.4 = (bf16[320,128]{1,0:T(8,128)(2,1)S(1)}, bf16[320,128]{1,0:T(8,128)(2,1)S(1)}, u32[]{:S(2)}, u32[]{:S(2)}) collective-permute-start(bf16[320,128]{1,0:T(8,128)(2,1)S(1)} %get-tuple-element.59), channel_id=1, source_target_pairs={{0,32},{32,64},{64,96},{96,0},{1,33},{33,65},{65,97},{97,1},{2,34}... | collective-permute-start | bytes 245768 | tf_op jit(solution)/shard_map/ppermute | solution.py:414
  26.6 2.2 %collective-permute-start.6 = (bf16[256,128]{1,0:T(8,128)(2,1)S(1)}, bf16[256,128]{1,0:T(8,128)(2,1)S(1)}, u32[]{:S(2)}, u32[]{:S(2)}) collective-permute-start(bf16[256,128]{1,0:T(8,128)(2,1)S(1)} %get-tuple-element.60), channel_id=1, source_target_pairs={{0,96},{32,0},{64,32},{96,64},{1,97},{33,1},{65,33},{97,65},{2,98}... | collective-permute-start | bytes 196616 | tf_op jit(solution)/shard_map/ppermute | solution.py:414
  28.8 1.2 %collective-permute-start.5 = (bf16[256,128]{1,0:T(8,128)(2,1)S(1)}, bf16[256,128]{1,0:T(8,128)(2,1)S(1)}, u32[]{:S(2)}, u32[]{:S(2)}) collective-permute-start(bf16[256,128]{1,0:T(8,128)(2,1)S(1)} %get-tuple-element.60), channel_id=1, source_target_pairs={{0,64},{32,96},{64,0},{96,32},{1,65},{33,97},{65,1},{97,33},{2,66}... | collective-permute-start | bytes 196616 | tf_op jit(solution)/shard_map/ppermute | solution.py:414
  30.0 0.1 collective-permute-done.6.third_ref
  30.1 3.7 %collective-permute-done.5.second_ref = bf16[256,128]{1,0:T(8,128)(2,1)S(1)} collective-permute-done((bf16[256,128]{1,0:T(8,128)(2,1)S(1)}, bf16[256,128]{1,0:T(8,128)(2,1)S(1)}, u32[]{:S(2)}, u32[]{:S(2)}) %collective-permute-start.5) | collective-permute-done | bytes 65568 | tf_op jit(solution)/shard_map/ppermute | solution.py:414
  33.8 1.2 %column.1 = (bf16[2,64,128]{2,1,0:T(8,128)(2,1)S(1)}, bf16[2,64,128]{2,1,0:T(8,128)(2,1)S(1)}, bf16[2,64,128]{2,1,0:T(8,128)(2,1)S(1)}, bf16[2,64,128]{2,1,0:T(8,128)(2,1)S(1)}) custom-call(f32[3,2,128,128]{3,2,1,0:T(8,128)S(1)} %get-tuple-element.58.prefix_ref, bf16[320,128]{1,0:T(8,128)(2,1)S(1)} %collective-permute-done.4.first_ref.above_ref, ...), custom_call_target="tpu_custom_call" | custom-call | flops 100000000 | tf_op jit(solution)/shard_map/column/pallas_call | solution.py:470
  35.0 0.3 collective-permute-start.7
  35.3 2.0 %collective-permute-start.8 = (bf16[2,64,128]{2,1,0:T(8,128)(2,1)S(1)}, bf16[2,64,128]{2,1,0:T(8,128)(2,1)S(1)}, u32[]{:S(2)}, u32[]{:S(2)}) collective-permute-start(bf16[2,64,128]{2,1,0:T(8,128)(2,1)S(1)} %get-tuple-element.63), channel_id=1, source_target_pairs={{0,16},{8,24},{16,0},{24,8},{1,17},{9,25},{17,1},{25,9},{2,18},{10... | collective-permute-start | bytes 98312 | tf_op jit(solution)/shard_map/ppermute | solution.py:414
  37.3 1.4 %collective-permute-start.9 = (bf16[2,64,128]{2,1,0:T(8,128)(2,1)S(1)}, bf16[2,64,128]{2,1,0:T(8,128)(2,1)S(1)}, u32[]{:S(2)}, u32[]{:S(2)}) collective-permute-start(bf16[2,64,128]{2,1,0:T(8,128)(2,1)S(1)} %get-tuple-element.64), channel_id=1, source_target_pairs={{0,24},{8,0},{16,8},{24,16},{1,25},{9,1},{17,9},{25,17},{2,26},{10... | collective-permute-start | bytes 98312 | tf_op jit(solution)/shard_map/ppermute | solution.py:414
  38.7 0.3 pool.1.pool_ref
  39.0 0.1 collective-permute-done.7.one_ref
  39.0 0.5 %collective-permute-done.8.two_ref = bf16[2,64,128]{2,1,0:T(8,128)(2,1)S(1)} collective-permute-done((bf16[2,64,128]{2,1,0:T(8,128)(2,1)S(1)}, bf16[2,64,128]{2,1,0:T(8,128)(2,1)S(1)}, u32[]{:S(2)}, u32[]{:S(2)}) %collective-permute-start.8) | collective-permute-done | bytes 32800 | tf_op jit(solution)/shard_map/ppermute | solution.py:414
  39.5 0.5 collective-permute-done.9.three_ref
  40.0 2.2 %final.1 = (bf16[256,1024]{1,0:T(8,128)(2,1)S(1)}, bf16[256,1024]{1,0:T(8,128)(2,1)S(1)}) custom-call(bf16[2,64,128]{2,1,0:T(8,128)(2,1)S(1)} %get-tuple-element.61.home_ref, bf16[2,64,128]{2,1,0:T(8,128)(2,1)S(1)} %collective-permute-done.7.one_ref, bf16[2,64,128]{2,1,0:T(8,128)(2,1)S(1)} %collective-permute-done.8.two_ref, ...), custom_call_target="tpu_custom_call" | custom-call | flops 1000000000 | tf_op jit(solution)/shard_map/final/pallas_call | solution.py:483
  42.2 4.1 %collective-permute-start.10 = (bf16[256,1024]{1,0:T(8,128)(2,1)S(1)}, bf16[256,1024]{1,0:T(8,128)(2,1)S(1)}, u32[]{:S(2)}, u32[]{:S(2)}) collective-permute-start(bf16[256,1024]{1,0:T(8,128)(2,1)S(1)} %get-tuple-element.70), channel_id=1, source_target_pairs={{0,1},{1,0},{2,3},{3,2},{4,5},{5,4},{6,7},{7,6},{8,9},{9,8},{10,11... | collective-permute-start | bytes 1572872 | tf_op jit(solution)/shard_map/ppermute | solution.py:492
  46.4 1.5 %collective-permute-done.10 = bf16[256,1024]{1,0:T(8,128)(2,1)S(1)} collective-permute-done((bf16[256,1024]{1,0:T(8,128)(2,1)S(1)}, bf16[256,1024]{1,0:T(8,128)(2,1)S(1)}, u32[]{:S(2)}, u32[]{:S(2)}) %collective-permute-start.10) | collective-permute-done | bytes 524320 | tf_op jit(solution)/shard_map/ppermute | solution.py:492
  47.9 1.0 %add_convert_fusion = bf16[256,1024]{1,0:T(8,128)(2,1)} fusion(bf16[256,1024]{1,0:T(8,128)(2,1)S(1)} %collective-permute-done.10, bf16[256,1024]{1,0:T(8,128)(2,1)S(1)} %get-tuple-element.69), kind=kLoop, calls=%fused_computation | loop fusion | flops 1048576 | bytes 1572864 | tf_op jit(solution)/shard_map/convert_element_type | solution.py:494
  (20 shorter events, 0.0 us)
Async XLA Ops:
  0.0 6.5 %collective-permute-start = (bf16[2,128,1024]{2,1,0:T(8,128)(2,1)}, bf16[2,128,1024]{2,1,0:T(8,128)(2,1)S(1)}, u32[]{:S(2)}, u32[]{:S(2)}) collective-permute-start(bf16[2,128,1024]{2,1,0:T(8,128)(2,1)} %param.18), channel_id=1, source_target_pairs={{0,1},{1,0},{2,3},{3,2},{4,5},{5,4},{6,7},{7,6},{8,9},{9,8},{10,11... | collective-permute-start | bytes 1572872 | tf_op jit(solution)/shard_map/ppermute | solution.py:422
  1.4 5.1 %copy-start.4 = (f32[2048]{0:T(1024)S(1)}, f32[2048]{0:T(1024)}, u32[]{:S(2)}) copy-start(f32[2048]{0:T(1024)} %param.19) | copy-start | bytes 24580
  1.4 5.1 %copy-start.5 = (f32[768]{0:T(1024)S(1)}, f32[768]{0:T(1024)}, u32[]{:S(2)}) copy-start(f32[768]{0:T(1024)} %refs_3_.3) | copy-start | bytes 9220
  1.4 5.1 %copy-start.6 = (f32[768]{0:T(1024)S(1)}, f32[768]{0:T(1024)}, u32[]{:S(2)}) copy-start(f32[768]{0:T(1024)} %refs_4_.3) | copy-start | bytes 9220
  6.5 13.7 %copy-start = (bf16[2048,384]{1,0:T(8,128)(2,1)S(1)}, bf16[2048,384]{1,0:T(8,128)(2,1)}, u32[]{:S(2)}) copy-start(bf16[2048,384]{1,0:T(8,128)(2,1)} %wg_ref.1) | copy-start | bytes 4718596
  6.5 13.7 %copy-start.1 = (bf16[2048,256]{1,0:T(8,128)(2,1)S(1)}, bf16[2048,256]{1,0:T(8,128)(2,1)}, u32[]{:S(2)}) copy-start(bf16[2048,256]{1,0:T(8,128)(2,1)} %wq_ref.1) | copy-start | bytes 3145732
  15.7 5.8 %collective-permute-start.2 = (bf16[256,128]{1,0:T(8,128)(2,1)S(1)}, bf16[256,128]{1,0:T(8,128)(2,1)S(1)}, u32[]{:S(2)}, u32[]{:S(2)}) collective-permute-start(bf16[256,128]{1,0:T(8,128)(2,1)S(1)} %get-tuple-element.47), channel_id=1, source_target_pairs={{0,16},{8,24},{16,0},{24,8},{1,17},{9,25},{17,1},{25,9},{2,18},{10... | collective-permute-start | bytes 196616 | tf_op jit(solution)/shard_map/ppermute | solution.py:414
  18.8 4.1 %collective-permute-start.3 = (bf16[256,128]{1,0:T(8,128)(2,1)S(1)}, bf16[256,128]{1,0:T(8,128)(2,1)S(1)}, u32[]{:S(2)}, u32[]{:S(2)}) collective-permute-start(bf16[256,128]{1,0:T(8,128)(2,1)S(1)} %get-tuple-element.48), channel_id=1, source_target_pairs={{0,24},{8,0},{16,8},{24,16},{1,25},{9,1},{17,9},{25,17},{2,26},{10... | collective-permute-start | bytes 196616 | tf_op jit(solution)/shard_map/ppermute | solution.py:414
  19.5 4.5 %collective-permute-start.1 = (bf16[320,128]{1,0:T(8,128)(2,1)S(1)}, bf16[320,128]{1,0:T(8,128)(2,1)S(1)}, u32[]{:S(2)}, u32[]{:S(2)}) collective-permute-start(bf16[320,128]{1,0:T(8,128)(2,1)S(1)} %get-tuple-element.46), channel_id=1, source_target_pairs={{0,8},{8,16},{16,24},{24,0},{1,9},{9,17},{17,25},{25,1},{2,10},{10... | collective-permute-start | bytes 245768 | tf_op jit(solution)/shard_map/ppermute | solution.py:414
  20.2 13.6 %copy-start.2 = (f32[2,6,64,64]{3,2,1,0:T(8,128)S(1)}, f32[2,6,64,64]{3,2,1,0:T(8,128)}, u32[]{:S(2)}) copy-start(f32[2,6,64,64]{3,2,1,0:T(8,128)} %init_ref.1) | copy-start | bytes 589828
  20.2 18.4 %copy-start.3 = (bf16[4,128,128]{2,1,0:T(8,128)(2,1)S(1)}, bf16[4,128,128]{2,1,0:T(8,128)(2,1)}, u32[]{:S(2)}) copy-start(bf16[4,128,128]{2,1,0:T(8,128)(2,1)} %mix_ref.1) | copy-start | bytes 393220
  20.2 18.4 %copy-start.7 = (f32[512]{0:T(512)S(1)}, f32[512]{0:T(512)}, u32[]{:S(2)}) copy-start(f32[512]{0:T(512)} %param.32) | copy-start | bytes 6148
  20.3 19.8 %copy-start.9 = (bf16[256,2048]{1,0:T(8,128)(2,1)S(1)}, bf16[256,2048]{1,0:T(8,128)(2,1)}, u32[]{:S(2)}) copy-start(bf16[256,2048]{1,0:T(8,128)(2,1)} %wp_ref.1) | copy-start | bytes 3145732
  21.5 18.5 %copy-start.8 = (bf16[384,2048]{1,0:T(8,128)(2,1)S(1)}, bf16[384,2048]{1,0:T(8,128)(2,1)}, u32[]{:S(2)}) copy-start(bf16[384,2048]{1,0:T(8,128)(2,1)} %wr_ref.1) | copy-start | bytes 4718596
  21.5 18.5 %copy-start.10 = (f32[768]{0:T(1024)S(1)}, f32[768]{0:T(1024)}, u32[]{:S(2)}) copy-start(f32[768]{0:T(1024)} %hgain_ref.1) | copy-start | bytes 9220
  24.7 9.1 %collective-permute-start.4 = (bf16[320,128]{1,0:T(8,128)(2,1)S(1)}, bf16[320,128]{1,0:T(8,128)(2,1)S(1)}, u32[]{:S(2)}, u32[]{:S(2)}) collective-permute-start(bf16[320,128]{1,0:T(8,128)(2,1)S(1)} %get-tuple-element.59), channel_id=1, source_target_pairs={{0,32},{32,64},{64,96},{96,0},{1,33},{33,65},{65,97},{97,1},{2,34}... | collective-permute-start | bytes 245768 | tf_op jit(solution)/shard_map/ppermute | solution.py:414
  26.6 3.5 %collective-permute-start.6 = (bf16[256,128]{1,0:T(8,128)(2,1)S(1)}, bf16[256,128]{1,0:T(8,128)(2,1)S(1)}, u32[]{:S(2)}, u32[]{:S(2)}) collective-permute-start(bf16[256,128]{1,0:T(8,128)(2,1)S(1)} %get-tuple-element.60), channel_id=1, source_target_pairs={{0,96},{32,0},{64,32},{96,64},{1,97},{33,1},{65,33},{97,65},{2,98}... | collective-permute-start | bytes 196616 | tf_op jit(solution)/shard_map/ppermute | solution.py:414
  28.8 5.0 %collective-permute-start.5 = (bf16[256,128]{1,0:T(8,128)(2,1)S(1)}, bf16[256,128]{1,0:T(8,128)(2,1)S(1)}, u32[]{:S(2)}, u32[]{:S(2)}) collective-permute-start(bf16[256,128]{1,0:T(8,128)(2,1)S(1)} %get-tuple-element.60), channel_id=1, source_target_pairs={{0,64},{32,96},{64,0},{96,32},{1,65},{33,97},{65,1},{97,33},{2,66}... | collective-permute-start | bytes 196616 | tf_op jit(solution)/shard_map/ppermute | solution.py:414
  35.0 4.0 %collective-permute-start.7 = (bf16[2,64,128]{2,1,0:T(8,128)(2,1)S(1)}, bf16[2,64,128]{2,1,0:T(8,128)(2,1)S(1)}, u32[]{:S(2)}, u32[]{:S(2)}) collective-permute-start(bf16[2,64,128]{2,1,0:T(8,128)(2,1)S(1)} %get-tuple-element.62), channel_id=1, source_target_pairs={{0,8},{8,16},{16,24},{24,0},{1,9},{9,17},{17,25},{25,1},{2,10},{10... | collective-permute-start | bytes 98312 | tf_op jit(solution)/shard_map/ppermute | solution.py:414
  35.3 4.3 %collective-permute-start.8 = (bf16[2,64,128]{2,1,0:T(8,128)(2,1)S(1)}, bf16[2,64,128]{2,1,0:T(8,128)(2,1)S(1)}, u32[]{:S(2)}, u32[]{:S(2)}) collective-permute-start(bf16[2,64,128]{2,1,0:T(8,128)(2,1)S(1)} %get-tuple-element.63), channel_id=1, source_target_pairs={{0,16},{8,24},{16,0},{24,8},{1,17},{9,25},{17,1},{25,9},{2,18},{10... | collective-permute-start | bytes 98312 | tf_op jit(solution)/shard_map/ppermute | solution.py:414
  37.3 2.8 %collective-permute-start.9 = (bf16[2,64,128]{2,1,0:T(8,128)(2,1)S(1)}, bf16[2,64,128]{2,1,0:T(8,128)(2,1)S(1)}, u32[]{:S(2)}, u32[]{:S(2)}) collective-permute-start(bf16[2,64,128]{2,1,0:T(8,128)(2,1)S(1)} %get-tuple-element.64), channel_id=1, source_target_pairs={{0,24},{8,0},{16,8},{24,16},{1,25},{9,1},{17,9},{25,17},{2,26},{10... | collective-permute-start | bytes 98312 | tf_op jit(solution)/shard_map/ppermute | solution.py:414
  42.2 5.7 %collective-permute-start.10 = (bf16[256,1024]{1,0:T(8,128)(2,1)S(1)}, bf16[256,1024]{1,0:T(8,128)(2,1)S(1)}, u32[]{:S(2)}, u32[]{:S(2)}) collective-permute-start(bf16[256,1024]{1,0:T(8,128)(2,1)S(1)} %get-tuple-element.70), channel_id=1, source_target_pairs={{0,1},{1,0},{2,3},{3,2},{4,5},{5,4},{6,7},{7,6},{8,9},{9,8},{10,11... | collective-permute-start | bytes 1572872 | tf_op jit(solution)/shard_map/ppermute | solution.py:492

commit v3 on v2

--- a/solution.py
+++ b/solution.py
@@ -54,15 +54,20 @@
 
 def head_masks():
     first = (iota(1, 128, 1) < HEAD).astype(f32)
-    return first, 1.0 - first
+    return first.astype(bf16), (1.0 - first).astype(bf16)
 
 
 def both(x, masks):
+    x = x.astype(bf16)
     return jnp.concatenate([x * masks[0], x * masks[1]], axis=0)
 
 
+def joined(x):
+    return jnp.where(iota(HEAD, 128, 1) < HEAD, x[:HEAD], x[HEAD:])
+
+
 def compose(earlier, later, masks):
-    moved = dot_fine_left(earlier, both(later[:HEAD].astype(f32), masks))
+    moved = dot_fine_left(earlier, both(later[:HEAD], masks))
     written = later[HEAD:].astype(f32)
     if earlier.shape[0] == HEAD:
         return moved + written
@@ -81,22 +86,33 @@
     return jnp.concatenate(parts, axis=0)
 
 
+def woven(part, size):
+    if size >= 16:
+        part = part.astype(bf16)
+    return weave(jnp.zeros_like(part), part, size)
+
+
 def inverses(lowers):
     row, col = iota(SPAN, SPAN, 0), iota(SPAN, SPAN, 1)
     eye = (row == col).astype(f32)
-    near = ((row >> 1) == (col >> 1)).astype(f32)
-    result = [eye - lower * near for lower in lowers]
+    near = ((row >> 1) == (col >> 1)).astype(bf16)
+    result = [eye - (lower * near).astype(f32) for lower in lowers]
     size, level = 2, 1
     while size < SPAN:
-        off = (((row >> (level + 1)) == (col >> (level + 1))) & ((row >> level) != (col >> level))).astype(f32)
+        off = (((row >> (level + 1)) == (col >> (level + 1))) & ((row >> level) != (col >> level))).astype(bf16)
         if size < 8:
             inner = [dot(lower * off, inv) for lower, inv in zip(lowers, result)]
             result = [inv - dot(inv, part) for inv, part in zip(result, inner)]
         else:
-            off = pick(off, size, 1)
-            inner = [dot(pick(lower, size, 1) * off, inv) for lower, inv in zip(lowers, result)]
+            if size < 16:
+                off = pick(off.astype(f32), size, 1).astype(bf16)
+                odd = [pick(lower.astype(f32), size, 1).astype(bf16) for lower in lowers]
+            else:
+                off = pick(off, size, 1)
+                odd = [pick(lower, size, 1) for lower in lowers]
+            inner = [dot(lower * off, inv) for lower, inv in zip(odd, result)]
             outer = [
-                dot(pick(inv, size, 1), weave(jnp.zeros_like(part), part, size))
+                dot(pick(inv, size, 1), woven(part, size))
                 for inv, part in zip(result, inner)
             ]
             result = [
@@ -110,9 +126,9 @@
 WIDTHS = (384, 384, 384, 384, 384, 256)
 
 
-def fetch(sources, bufs, first_row, sems):
+def fetch(sources, bufs, first_row, sems, base):
     copies = [
-        pltpu.make_async_copy(src.at[pl.ds(pl.multiple_of(first_row, 1024), 1024), :], buf, sems.at[i])
+        pltpu.make_async_copy(src.at[pl.ds(pl.multiple_of(first_row, 1024), 1024), :], buf, sems.at[base + i])
         for i, (src, buf) in enumerate(zip(sources, bufs))
     ]
     for copy in copies:
@@ -122,8 +138,8 @@
 
 def own_kernel(*refs):
     token_ref, norm_ref = refs[:2]
-    sources, normed_ref, squares_ref, partials = refs[2:8], refs[8], refs[9], refs[10:16]
-    bufs, sems, own_ref, gain_ref, first_sems = refs[16:22], refs[22], refs[23], refs[24], refs[25]
+    sources, normed_ref, squares_ref, partials, rest = refs[2:8], refs[8], refs[9], refs[10:16], refs[16:22]
+    bufs, sems, own_ref, gain_ref, first_sems = refs[22:28], refs[28], refs[29], refs[30], refs[31]
     tp = lax.axis_index("tp")
     early = [
         pltpu.make_async_copy(token_ref, own_ref, first_sems.at[0]),
@@ -131,7 +147,8 @@
     ]
     for copy in early:
         copy.start()
-    copies = fetch(sources, bufs, tp * 1024, sems)
+    copies = fetch(sources, bufs, tp * 1024, sems, 0)
+    later = fetch(sources, rest, (1 - tp) * 1024, sems, 6)
     for copy in early:
         copy.wait()
     own = own_ref[...].astype(f32)
@@ -141,20 +158,20 @@
     for copy, buf, partial in zip(copies, bufs, partials):
         copy.wait()
         partial[...] = dot(normed, buf[...])
+    for copy in later:
+        copy.wait()
 
 
 def local_kernel(*refs):
     other_ref, gain_ref, squares_ref, db_ref, rb_ref = refs[:5]
-    partials, sources = refs[5:11], refs[11:17]
+    partials, rest = refs[5:11], refs[11:17]
     (
         normed_ref, scale_ref, pool_ref, home_ref, first_ref, second_ref, third_ref,
-        wb_ref, wkk_ref, solved_ref, v_ref, rho_ref,
+        right_ref, solved_ref, v_ref, rho_ref, lift_ref,
     ) = refs[17:29]
     k_s, d_s, a_s, r_s, v_s, maps = refs[29:35]
-    bufs, sems = refs[35:41], refs[41]
     tp = lax.axis_index("tp")
     y = lax.axis_index("sp_1")
-    copies = fetch(sources, bufs, (1 - tp) * 1024, sems)
     is_first = tp == 0
     other = other_ref[...].astype(f32)
     normed = (other * jnp.where(is_first, gain_ref[:, 1024:], gain_ref[:, :1024])).astype(bf16)
@@ -163,8 +180,7 @@
     scale = lax.rsqrt(squares * (1.0 / D) + 0.25)
     scale_ref[...] = jnp.broadcast_to(scale, (256, 128))
     for i in range(6):
-        copies[i].wait()
-        rounded = ((partials[i][...] + dot(normed, bufs[i][...])) * scale).astype(bf16)
+        rounded = ((partials[i][...] + dot(normed, rest[i][...])) * scale).astype(bf16)
         if i == 5:
             pool_ref[...] = rounded
             for s in (0, 1):
@@ -212,19 +228,15 @@
         rho = r_s[u] * jnp.exp(total - middle)
         ending = jnp.exp(final - total)
         lift = jnp.exp(middle)
-        rho_ref[u] = rho * lift
-        left = jnp.concatenate([alpha * masks[0], alpha * masks[1], rho * masks[0], rho * masks[1]], axis=0)
-        pairs = dot(left, jnp.concatenate([beta, kappa], axis=0), NT)
+        rho_ref[u] = rho
+        lift_ref[u : u + 1] = lift
+        right = jnp.concatenate([beta.astype(bf16), kappa.astype(bf16)], axis=0)
+        right_ref[u] = right
+        pairs = dot(both(alpha, masks), right, NT)
         lower_kappa = []
         for j in (0, 1):
-            lowers.append(jnp.where(strict, pairs[j * n : j * n + n, :n], 0.0))
+            lowers.append(jnp.where(strict, pairs[j * n : j * n + n, :n], 0.0).astype(bf16))
             lower_kappa.append(jnp.where(strict, pairs[j * n : j * n + n, n:], 0.0).astype(bf16))
-            wb_ref[u, :, j * n : j * n + n] = jnp.where(
-                inclusive, pairs[(2 + j) * n : (3 + j) * n, :n], 0.0
-            ).astype(bf16)
-            wkk_ref[u, :, j * n : j * n + n] = jnp.where(
-                inclusive, pairs[(2 + j) * n : (3 + j) * n, n:], 0.0
-            ).astype(bf16)
         v = v_s[u]
         v_ref[u] = v.astype(bf16)
         carried = dot(jnp.concatenate(lower_kappa, axis=1), both(v, masks))
@@ -236,13 +248,13 @@
         solved = dot(jnp.concatenate(inverse[2 * u : 2 * u + 2], axis=1), both(right, wide))
         solved_ref[u] = solved.astype(bf16)
         crossed = dot(solved[:, :n], beta_end, TN)
-        transit = eye * gain_end - (crossed[:HEAD] * masks[0] + crossed[HEAD:] * masks[1])
+        transit = eye * gain_end - joined(crossed)
         crossed = dot(
             jnp.concatenate([v_s[u], -solved[:, n:]], axis=0),
             jnp.concatenate([kappa_end, beta_end], axis=0),
             TN,
         )
-        written = crossed[:HEAD] * masks[0] + crossed[HEAD:] * masks[1]
+        written = joined(crossed)
         at = (u // 3) * 128
         maps[u % 3, at : at + HEAD] = transit.astype(bf16)
         maps[u % 3, at + HEAD : at + 128] = written.astype(bf16)
@@ -252,7 +264,7 @@
 
 
 def side_kernel(
-    own_ref, other_ref, scale_ref, wb_ref, wkk_ref, solved_ref, v_ref, rho_ref, wg_ref, wq_ref,
+    own_ref, other_ref, scale_ref, right_ref, solved_ref, v_ref, rho_ref, lift_ref, wg_ref, wq_ref,
     reads_ref, local_ref, gate_ref, pgate_ref,
 ):
     tp = lax.axis_index("tp")
@@ -261,10 +273,18 @@
         jnp.concatenate([masks[0], masks[0]], axis=1),
         jnp.concatenate([masks[1], masks[1]], axis=1),
     )
+    inclusive = iota(128, 128, 0) >= iota(128, 128, 1)
+    inside = []
     for u in range(UNITS):
-        removed = dot(wb_ref[u], both(solved_ref[u].astype(f32), wide))
-        reads_ref[u] = (rho_ref[u] - removed[:, :128]).astype(bf16)
-        local_ref[u] = dot(wkk_ref[u], both(v_ref[u].astype(f32), masks)) - removed[:, 128:]
+        pairs = dot(both(rho_ref[u], masks), right_ref[u], NT)
+        block = lambda j, c: jnp.where(
+            inclusive, pairs[j * 128 : j * 128 + 128, c * 128 : c * 128 + 128], 0.0
+        ).astype(bf16)
+        inside.append([jnp.concatenate([block(0, c), block(1, c)], axis=1) for c in (0, 1)])
+    for u in range(UNITS):
+        removed = dot(inside[u][0], both(solved_ref[u], wide))
+        reads_ref[u] = (rho_ref[u] * lift_ref[u : u + 1] - removed[:, :128]).astype(bf16)
+        local_ref[u] = dot(inside[u][1], both(v_ref[u], masks)) - removed[:, 128:]
     scale = scale_ref[:, :1]
     mine, theirs = pl.multiple_of(tp * 1024, 1024), pl.multiple_of((1 - tp) * 1024, 1024)
     for weight, dest in ((wg_ref, gate_ref), (wq_ref, pgate_ref)):
@@ -314,7 +334,7 @@
         dest[...] = starts[(y + step) & 3]
 
 
-def pool_kernel(pool_ref, beside_ref, above_ref, pgate_ref, mix_ref, pscale_ref, out_ref):
+def pool_kernel(pool_ref, beside_ref, above_ref, pgate_ref, mix_ref, pscale_ref, wp_ref, part_ref, out_ref):
     tp = lax.axis_index("tp")
     y = lax.axis_index("sp_1")
     place = lax.axis_index("sp_0") * 4 + y
@@ -350,11 +370,12 @@
             out_ref[s * 128 : s * 128 + 128, lanes] = (
                 mixed * factor[:, lanes] * (gate * jax.nn.sigmoid(gate))
             ).astype(bf16)
+    part_ref[...] = dot(out_ref[...], wp_ref[...])
 
 
 def final_kernel(
-    home_ref, one_ref, two_ref, three_ref, reads_ref, local_ref, gate_ref, hgain_ref, pool_ref,
-    wr_ref, wp_ref,
+    home_ref, one_ref, two_ref, three_ref, reads_ref, local_ref, gate_ref, hgain_ref, part_ref,
+    wr_ref,
     send_ref, keep_ref,
     starts, rec,
 ):
@@ -371,7 +392,7 @@
         lanes = slice(h * 128, h * 128 + 128)
         shifted = slice(384 + h * 128, 384 + h * 128 + 128)
         rows = slice(s * 128, s * 128 + 128)
-        out = dot(reads_ref[u], both(starts[h, s].astype(f32), masks), NT) + local_ref[u]
+        out = dot(reads_ref[u], both(starts[h, s], masks), NT) + local_ref[u]
         out = out - dot_fine_left(out, mean_of)
         spread = dot_fine_left(out * out, mean_of)
         gain = jnp.where(is_first, line_of(hgain_ref, lanes), line_of(hgain_ref, shifted))
@@ -381,7 +402,7 @@
         ).astype(bf16)
     for dest, part in ((send_ref, 1 - tp), (keep_ref, tp)):
         cols = pl.ds(pl.multiple_of(part * 1024, 1024), 1024)
-        dest[...] = (dot(rec[...], wr_ref[:, cols]) + dot(pool_ref[...], wp_ref[:, cols])).astype(bf16)
+        dest[...] = (dot(rec[...], wr_ref[:, cols]) + part_ref[:, cols]).astype(bf16)
 
 
 def vmem(count):
@@ -423,30 +444,31 @@
     line = lambda x: x.reshape(1, -1)
     pinned = lambda x: pltpu.with_memory_space_constraint(x, pltpu.HBM)
     weights = [pinned(w) for w in (w_key, w_decay, w_rate, w_recept, w_value, w_pool)]
-    bufs = [pltpu.VMEM((1024, width), bf16) for width in WIDTHS] + [pltpu.SemaphoreType.DMA((6,))]
-    own_normed, squares, *partials = call(
+    bufs = [pltpu.VMEM((1024, width), bf16) for width in WIDTHS] + [pltpu.SemaphoreType.DMA((12,))]
+    own_normed, squares, *halves_of = call(
         own_kernel,
         "own",
         hbm(8),
-        [shape((256, 1024)), shape((256, 128), f32)] + [shape((256, width), f32) for width in WIDTHS],
+        [shape((256, 1024)), shape((256, 128), f32)] + [shape((256, width), f32) for width in WIDTHS]
+        + [shape((1024, width)) for width in WIDTHS],
         bufs + [pltpu.VMEM((256, 1024), bf16), pltpu.VMEM((1, D), f32), pltpu.SemaphoreType.DMA((2,))],
         20,
         1_000_000_000,
     )(pinned(tokens.reshape(256, 1024)), pinned(line(norm_gain)), *weights)
-    normed, scale, pool, home, m1, m2, m3, wb, wkk, solved, v, rho = call(
+    normed, scale, pool, home, m1, m2, m3, right, solved, v, rho, lift = call(
         local_kernel,
         "local",
-        vmem(11) + hbm(6),
+        vmem(17),
         [
             shape((256, 1024)), shape((256, 128), f32), shape((256, 256)),
             shape((256, 128)), shape((320, 128)), shape((256, 128)), shape((256, 128)),
-            shape((6, 128, 256)), shape((6, 128, 256)), shape((6, 128, 256)),
-            shape((6, 128, 128)), shape((6, 128, 128), f32),
+            shape((6, 256, 128)), shape((6, 128, 256)), shape((6, 128, 128)),
+            shape((6, 128, 128), f32), shape((6, 128), f32),
         ],
-        [pltpu.VMEM((6, 128, 128), f32)] * 5 + [pltpu.VMEM((4, 256, 128), bf16)] + bufs,
-        30,
+        [pltpu.VMEM((6, 128, 128), f32)] * 5 + [pltpu.VMEM((4, 256, 128), bf16)],
+        24,
         3_000_000_000,
-    )(other.reshape(256, 1024), line(norm_gain), squares, decay_base, rate_base, *partials, *weights)
+    )(other.reshape(256, 1024), line(norm_gain), squares, decay_base, rate_base, *halves_of)
     r1, r2, r3 = around((m1, m2, m3), "sp_1")
     reads, local, gate, pgate = call(
         side_kernel,
@@ -456,7 +478,7 @@
         [],
         16,
         1_000_000_000,
-    )(own_normed, normed, scale, wb, wkk, solved, v, rho, w_gate_rec, w_gate_pool)
+    )(own_normed, normed, scale, right, solved, v, rho, lift, w_gate_rec, w_gate_pool)
     prefix, onward, total = call(
         row_kernel,
         "row",
@@ -477,18 +499,18 @@
         100_000_000,
     )(prefix, *columns, init_state)
     t1, t2, t3 = around((s1, s2, s3), "sp_1")
-    pool_out = call(pool_kernel, "pool", vmem(6), shape((256, 256)), [], 8, 100_000_000)(
-        pool, r1, columns[0], pgate, pool_mix, line(pool_scale)
-    )
+    pool_part = call(
+        pool_kernel, "pool", vmem(7), shape((256, D), f32), [pltpu.VMEM((256, 256), bf16)], 12, 300_000_000
+    )(pool, r1, columns[0], pgate, pool_mix, line(pool_scale), w_out_pool)
     send, keep = call(
         final_kernel,
         "final",
-        vmem(11),
+        vmem(10),
         [shape((256, 1024)), shape((256, 1024))],
         [pltpu.VMEM((4, 2, 64, 128), bf16), pltpu.VMEM((256, 384), bf16)],
         20,
         1_000_000_000,
-    )(s0, t1, t2, t3, reads, local, gate, head_gain, pool_out, w_out_rec, w_out_pool)
+    )(s0, t1, t2, t3, reads, local, gate, head_gain, pool_part, w_out_rec)
     arrived = lax.ppermute(send, "tp", [(0, 1), (1, 0)])
     mixed = keep.astype(f32) + arrived.astype(f32)
     return mixed.astype(bf16).reshape(2, 128, 1024)

time: 49 us -> 47.4 us (0.967)
  waiting for transfers between devices: 8.95 us -> 7.88 us
  Pallas kernels: 19.7 us -> 19 us
    pallas_call x3, Pallas kernels: 11.6 us -> 9.09 us  [the longest x1 6.49 us: shards(): call(local_kernel, 'local', vmem(17), [shape((256, 1024)), shape((256, 12...]
    pallas_call x1, Pallas kernels: 5.09 us -> 6.35 us  [shards(): call(own_kernel, 'own', hbm(8), [shape((256, 1024)), shape((256, 128), f3...]
    ppermute x9, waiting for transfers between devices: 7.41 us -> 6.34 us  [around(): lax.ppermute(part, axis, [(i, i + step & 3) for i in range(4)])]
    pallas_call x1, Pallas kernels: 1.2 us -> 1.76 us  [shards(): call(side_kernel, 'side', vmem(10), [shape((6, 128, 128)), shape((6, 128,...]
  transfers between devices with their start and end apart: 11 -> 11, of which waited for: 8 -> 7; matrix products, arithmetic and copies ran while one was open for 0% -> 0% of each run, Pallas kernels for 13% -> 19%
where the time goes in v3:
time: 47.4 us; the launch traced here: 47.3 us
  starting transfers between devices  19.1 us (40%)
  Pallas kernels  19 us (40%)
  waiting for transfers between devices  7.88 us (17%)
  other arithmetic  0.99 us (2%)
    ppermute x9, starting transfers between devices, around(): lax.ppermute(part, axis, [(i, i + step & 3) for i in range(4)])  13.5 us
    pallas_call x1, Pallas kernels, shards(): call(local_kernel, 'local', vmem(17), [shape((256, 1024)), shape((256, 12...  6.49 us
    pallas_call x1, Pallas kernels, shards(): call(own_kernel, 'own', hbm(8), [shape((256, 1024)), shape((256, 128), f3...  6.35 us
    ppermute x9, waiting for transfers between devices, around(): lax.ppermute(part, axis, [(i, i + step & 3) for i in range(4)])  6.34 us
    ppermute x1, starting transfers between devices, shards(): arrived = lax.ppermute(send, 'tp', [(0, 1), (1, 0)])  4.23 us
    pallas_call x1, Pallas kernels, shards(): call(final_kernel, 'final', vmem(10), [shape((256, 1024)), shape((256, 10...  1.95 us
    pallas_call x1, Pallas kernels, shards(): call(side_kernel, 'side', vmem(10), [shape((6, 128, 128)), shape((6, 128,...  1.76 us
    ppermute x1, waiting for transfers between devices, shards(): arrived = lax.ppermute(send, 'tp', [(0, 1), (1, 0)])  1.54 us
  transfers between devices with their start and end apart: 11, of which 7 were waited for; matrix products, arithmetic and copies ran while one was open for 0% of the time, Pallas kernels for 19%

profile of v3, /device:TPU:1, one launch (start us, length us, event | category | flops | bytes accessed | tf_op | source)
XLA Modules:
  0.0 47.3 jit_solution(8763267541521468123)
XLA Ops:
  0.0 1.4 %collective-permute-start = (bf16[2,128,1024]{2,1,0:T(8,128)(2,1)}, bf16[2,128,1024]{2,1,0:T(8,128)(2,1)S(1)}, u32[]{:S(2)}, u32[]{:S(2)}) collective-permute-start(bf16[2,128,1024]{2,1,0:T(8,128)(2,1)} %param.18), channel_id=1, source_target_pairs={{0,1},{1,0},{2,3},{3,2},{4,5},{5,4},{6,7},{7,6},{8,9},{9,8},{10,11... | collective-permute-start | bytes 1572872 | tf_op jit(solution)/shard_map/ppermute | solution.py:443
  1.4 6.4 %own.1 = (bf16[256,1024]{1,0:T(8,128)(2,1)S(1)}, f32[256,128]{1,0:T(8,128)S(1)}, f32[256,384]{1,0:T(8,128)S(1)}, f32[256,384]{1,0:T(8,128)S(1)}, f32[256,384]{1,...) custom-call(bf16[256,1024]{1,0:T(8,128)(2,1)} %bitcast.9, ...), custom_call_target="tpu_custom_call" | custom-call | flops 1000000000 | tf_op jit(solution)/shard_map/own/pallas_call | solution.py:448
  7.8 0.0 copy-start
  7.8 0.0 copy-start.3
  7.8 6.5 %local.1 = (bf16[256,1024]{1,0:T(8,128)(2,1)S(1)}, f32[256,128]{1,0:T(8,128)S(1)}, bf16[256,256]{1,0:T(8,128)(2,1)S(1)}, bf16[256,128]{1,0:T(8,128)(2,1)S(1)}, b...) custom-call(bf16[256,1024]{1,0:T(8,128)(2,1)S(1)} %bitcast.8, ...), custom_call_target="tpu_custom_call" | custom-call | flops 3000000000 | tf_op jit(solution)/shard_map/local/pallas_call | solution.py:458
  14.3 3.1 %collective-permute-start.2 = (bf16[256,128]{1,0:T(8,128)(2,1)S(1)}, bf16[256,128]{1,0:T(8,128)(2,1)S(1)}, u32[]{:S(2)}, u32[]{:S(2)}) collective-permute-start(bf16[256,128]{1,0:T(8,128)(2,1)S(1)} %get-tuple-element.59), channel_id=1, source_target_pairs={{0,16},{8,24},{16,0},{24,8},{1,17},{9,25},{17,1},{25,9},{2,18},{10... | collective-permute-start | bytes 196616 | tf_op jit(solution)/shard_map/ppermute | solution.py:435
  17.4 0.8 %collective-permute-start.3 = (bf16[256,128]{1,0:T(8,128)(2,1)S(1)}, bf16[256,128]{1,0:T(8,128)(2,1)S(1)}, u32[]{:S(2)}, u32[]{:S(2)}) collective-permute-start(bf16[256,128]{1,0:T(8,128)(2,1)S(1)} %get-tuple-element.60), channel_id=1, source_target_pairs={{0,24},{8,0},{16,8},{24,16},{1,25},{9,1},{17,9},{25,17},{2,26},{10... | collective-permute-start | bytes 196616 | tf_op jit(solution)/shard_map/ppermute | solution.py:435
  18.2 0.7 %collective-permute-start.1 = (bf16[320,128]{1,0:T(8,128)(2,1)S(1)}, bf16[320,128]{1,0:T(8,128)(2,1)S(1)}, u32[]{:S(2)}, u32[]{:S(2)}) collective-permute-start(bf16[320,128]{1,0:T(8,128)(2,1)S(1)} %get-tuple-element.58), channel_id=1, source_target_pairs={{0,8},{8,16},{16,24},{24,0},{1,9},{9,17},{17,25},{25,1},{2,10},{10... | collective-permute-start | bytes 245768 | tf_op jit(solution)/shard_map/ppermute | solution.py:435
  18.9 0.0 copy-start.8
  18.9 1.8 %side.1 = (bf16[6,128,128]{2,1,0:T(8,128)(2,1)S(1)}, f32[6,128,128]{2,1,0:T(8,128)S(1)}, bf16[256,384]{1,0:T(8,128)(2,1)S(1)}, bf16[256,256]{1,0:T(8,128)(2,1)S(1)}) custom-call(bf16[256,1024]{1,0:T(8,128)(2,1)S(1)} %get-tuple-element.61.own_ref, bf16[256,1024]{1,0:T(8,128)(2,1)S(1)} %get-tuple-element.62.other_ref, ...), custom_call_target="tpu_custom_call" | custom-call | flops 1000000000 | tf_op jit(solution)/shard_map/side/pallas_call | solution.py:473
  20.7 0.0 copy-start.2
  20.7 0.6 %collective-permute-done.3.third_ref = bf16[256,128]{1,0:T(8,128)(2,1)S(1)} collective-permute-done((bf16[256,128]{1,0:T(8,128)(2,1)S(1)}, bf16[256,128]{1,0:T(8,128)(2,1)S(1)}, u32[]{:S(2)}, u32[]{:S(2)}) %collective-permute-start.3) | collective-permute-done | bytes 65568 | tf_op jit(solution)/shard_map/ppermute | solution.py:435
  21.3 1.4 %collective-permute-done.1.first_ref.beside_ref = bf16[320,128]{1,0:T(8,128)(2,1)S(1)} collective-permute-done((bf16[320,128]{1,0:T(8,128)(2,1)S(1)}, bf16[320,128]{1,0:T(8,128)(2,1)S(1)}, u32[]{:S(2)}, u32[]{:S(2)}) %collective-permute-start.1) | collective-permute-done | bytes 81952 | tf_op jit(solution)/shard_map/ppermute | solution.py:435
  22.7 0.6 %row.1 = (f32[3,2,128,128]{3,2,1,0:T(8,128)S(1)}, bf16[320,128]{1,0:T(8,128)(2,1)S(1)}, bf16[256,128]{1,0:T(8,128)(2,1)S(1)}) custom-call(bf16[256,128]{1,0:T(8,128)(2,1)S(1)} %get-tuple-element.57.home_ref, bf16[320,128]{1,0:T(8,128)(2,1)S(1)} %collective-permute-done.1.first_ref.beside_ref, bf16[256,128]{1,0:T(8,128)(2,1)S(1)} %collective-permute-done.2.second_ref, ...), custom_call_target="tpu_custom_call" | custom-call | flops 100000000 | tf_op jit(solution)/shard_map/row/pallas_call | solution.py:482
  23.3 1.7 %collective-permute-start.4 = (bf16[320,128]{1,0:T(8,128)(2,1)S(1)}, bf16[320,128]{1,0:T(8,128)(2,1)S(1)}, u32[]{:S(2)}, u32[]{:S(2)}) collective-permute-start(bf16[320,128]{1,0:T(8,128)(2,1)S(1)} %get-tuple-element.71), channel_id=1, source_target_pairs={{0,32},{32,64},{64,96},{96,0},{1,33},{33,65},{65,97},{97,1},{2,34}... | collective-permute-start | bytes 245768 | tf_op jit(solution)/shard_map/ppermute | solution.py:435
  25.0 2.2 %collective-permute-start.6 = (bf16[256,128]{1,0:T(8,128)(2,1)S(1)}, bf16[256,128]{1,0:T(8,128)(2,1)S(1)}, u32[]{:S(2)}, u32[]{:S(2)}) collective-permute-start(bf16[256,128]{1,0:T(8,128)(2,1)S(1)} %get-tuple-element.72), channel_id=1, source_target_pairs={{0,96},{32,0},{64,32},{96,64},{1,97},{33,1},{65,33},{97,65},{2,98}... | collective-permute-start | bytes 196616 | tf_op jit(solution)/shard_map/ppermute | solution.py:435
  27.2 1.2 %collective-permute-start.5 = (bf16[256,128]{1,0:T(8,128)(2,1)S(1)}, bf16[256,128]{1,0:T(8,128)(2,1)S(1)}, u32[]{:S(2)}, u32[]{:S(2)}) collective-permute-start(bf16[256,128]{1,0:T(8,128)(2,1)S(1)} %get-tuple-element.72), channel_id=1, source_target_pairs={{0,64},{32,96},{64,0},{96,32},{1,65},{33,97},{65,1},{97,33},{2,66}... | collective-permute-start | bytes 196616 | tf_op jit(solution)/shard_map/ppermute | solution.py:435
  28.5 0.1 collective-permute-done.6.third_ref
  28.6 3.6 %collective-permute-done.5.second_ref = bf16[256,128]{1,0:T(8,128)(2,1)S(1)} collective-permute-done((bf16[256,128]{1,0:T(8,128)(2,1)S(1)}, bf16[256,128]{1,0:T(8,128)(2,1)S(1)}, u32[]{:S(2)}, u32[]{:S(2)}) %collective-permute-start.5) | collective-permute-done | bytes 65568 | tf_op jit(solution)/shard_map/ppermute | solution.py:435
  32.2 1.2 %column.1 = (bf16[2,64,128]{2,1,0:T(8,128)(2,1)S(1)}, bf16[2,64,128]{2,1,0:T(8,128)(2,1)S(1)}, bf16[2,64,128]{2,1,0:T(8,128)(2,1)S(1)}, bf16[2,64,128]{2,1,0:T(8,128)(2,1)S(1)}) custom-call(f32[3,2,128,128]{3,2,1,0:T(8,128)S(1)} %get-tuple-element.70.prefix_ref, bf16[320,128]{1,0:T(8,128)(2,1)S(1)} %collective-permute-done.4.first_ref.above_ref, ...), custom_call_target="tpu_custom_call" | custom-call | flops 100000000 | tf_op jit(solution)/shard_map/column/pallas_call | solution.py:492
  33.3 0.3 collective-permute-start.7
  33.6 2.1 %collective-permute-start.8 = (bf16[2,64,128]{2,1,0:T(8,128)(2,1)S(1)}, bf16[2,64,128]{2,1,0:T(8,128)(2,1)S(1)}, u32[]{:S(2)}, u32[]{:S(2)}) collective-permute-start(bf16[2,64,128]{2,1,0:T(8,128)(2,1)S(1)} %get-tuple-element.75), channel_id=1, source_target_pairs={{0,16},{8,24},{16,0},{24,8},{1,17},{9,25},{17,1},{25,9},{2,18},{10... | collective-permute-start | bytes 98312 | tf_op jit(solution)/shard_map/ppermute | solution.py:435
  35.7 1.4 %collective-permute-start.9 = (bf16[2,64,128]{2,1,0:T(8,128)(2,1)S(1)}, bf16[2,64,128]{2,1,0:T(8,128)(2,1)S(1)}, u32[]{:S(2)}, u32[]{:S(2)}) collective-permute-start(bf16[2,64,128]{2,1,0:T(8,128)(2,1)S(1)} %get-tuple-element.76), channel_id=1, source_target_pairs={{0,24},{8,0},{16,8},{24,16},{1,25},{9,1},{17,9},{25,17},{2,26},{10... | collective-permute-start | bytes 98312 | tf_op jit(solution)/shard_map/ppermute | solution.py:435
  37.1 0.0 copy-start.7
  37.2 0.6 %pool.1.part_ref = f32[256,2048]{1,0:T(8,128)S(1)} custom-call(bf16[256,256]{1,0:T(8,128)(2,1)S(1)} %get-tuple-element.80.pool_ref, bf16[320,128]{1,0:T(8,128)(2,1)S(1)} %collective-permute-done.1.first_ref.beside_ref, bf16[320,128]{1,0:T(8,128)(2,1)S(1)} %collective-permute-done.4.first_ref.above_ref, ...), custom_call_target="tpu_custom_call" | custom-call | flops 300000000 | tf_op jit(solution)/shard_map/pool/pallas_call | solution.py:502
  37.8 0.1 collective-permute-done.8.two_ref
  37.9 0.6 %collective-permute-done.9.three_ref = bf16[2,64,128]{2,1,0:T(8,128)(2,1)S(1)} collective-permute-done((bf16[2,64,128]{2,1,0:T(8,128)(2,1)S(1)}, bf16[2,64,128]{2,1,0:T(8,128)(2,1)S(1)}, u32[]{:S(2)}, u32[]{:S(2)}) %collective-permute-start.9) | collective-permute-done | bytes 32800 | tf_op jit(solution)/shard_map/ppermute | solution.py:435
  38.5 0.1 copy-done.1
  38.6 2.0 %final.1 = (bf16[256,1024]{1,0:T(8,128)(2,1)S(1)}, bf16[256,1024]{1,0:T(8,128)(2,1)S(1)}) custom-call(bf16[2,64,128]{2,1,0:T(8,128)(2,1)S(1)} %get-tuple-element.73.home_ref, bf16[2,64,128]{2,1,0:T(8,128)(2,1)S(1)} %collective-permute-done.7.one_ref, bf16[2,64,128]{2,1,0:T(8,128)(2,1)S(1)} %collective-permute-done.8.two_ref, ...), custom_call_target="tpu_custom_call" | custom-call | flops 1000000000 | tf_op jit(solution)/shard_map/final/pallas_call | solution.py:505
  40.5 4.2 %collective-permute-start.10 = (bf16[256,1024]{1,0:T(8,128)(2,1)S(1)}, bf16[256,1024]{1,0:T(8,128)(2,1)S(1)}, u32[]{:S(2)}, u32[]{:S(2)}) collective-permute-start(bf16[256,1024]{1,0:T(8,128)(2,1)S(1)} %get-tuple-element.82), channel_id=1, source_target_pairs={{0,1},{1,0},{2,3},{3,2},{4,5},{5,4},{6,7},{7,6},{8,9},{9,8},{10,11... | collective-permute-start | bytes 1572872 | tf_op jit(solution)/shard_map/ppermute | solution.py:514
  44.7 1.5 %collective-permute-done.10 = bf16[256,1024]{1,0:T(8,128)(2,1)S(1)} collective-permute-done((bf16[256,1024]{1,0:T(8,128)(2,1)S(1)}, bf16[256,1024]{1,0:T(8,128)(2,1)S(1)}, u32[]{:S(2)}, u32[]{:S(2)}) %collective-permute-start.10) | collective-permute-done | bytes 524320 | tf_op jit(solution)/shard_map/ppermute | solution.py:514
  46.3 1.0 %add_convert_fusion = bf16[256,1024]{1,0:T(8,128)(2,1)} fusion(bf16[256,1024]{1,0:T(8,128)(2,1)S(1)} %collective-permute-done.10, bf16[256,1024]{1,0:T(8,128)(2,1)S(1)} %get-tuple-element.81), kind=kLoop, calls=%fused_computation | loop fusion | flops 1048576 | bytes 1572864 | tf_op jit(solution)/shard_map/convert_element_type | solution.py:516
  (20 shorter events, 0.0 us)
Async XLA Ops:
  0.0 7.8 %collective-permute-start = (bf16[2,128,1024]{2,1,0:T(8,128)(2,1)}, bf16[2,128,1024]{2,1,0:T(8,128)(2,1)S(1)}, u32[]{:S(2)}, u32[]{:S(2)}) collective-permute-start(bf16[2,128,1024]{2,1,0:T(8,128)(2,1)} %param.18), channel_id=1, source_target_pairs={{0,1},{1,0},{2,3},{3,2},{4,5},{5,4},{6,7},{7,6},{8,9},{9,8},{10,11... | collective-permute-start | bytes 1572872 | tf_op jit(solution)/shard_map/ppermute | solution.py:443
  1.4 6.4 %copy-start.6 = (f32[2048]{0:T(1024)S(1)}, f32[2048]{0:T(1024)}, u32[]{:S(2)}) copy-start(f32[2048]{0:T(1024)} %param.19) | copy-start | bytes 24580
  1.4 6.4 %copy-start.9 = (f32[768]{0:T(1024)S(1)}, f32[768]{0:T(1024)}, u32[]{:S(2)}) copy-start(f32[768]{0:T(1024)} %refs_3_.3) | copy-start | bytes 9220
  1.4 6.4 %copy-start.10 = (f32[768]{0:T(1024)S(1)}, f32[768]{0:T(1024)}, u32[]{:S(2)}) copy-start(f32[768]{0:T(1024)} %refs_4_.3) | copy-start | bytes 9220
  7.8 11.1 %copy-start = (bf16[2048,384]{1,0:T(8,128)(2,1)S(1)}, bf16[2048,384]{1,0:T(8,128)(2,1)}, u32[]{:S(2)}) copy-start(bf16[2048,384]{1,0:T(8,128)(2,1)} %wg_ref.1) | copy-start | bytes 4718596
  7.8 11.1 %copy-start.3 = (bf16[2048,256]{1,0:T(8,128)(2,1)S(1)}, bf16[2048,256]{1,0:T(8,128)(2,1)}, u32[]{:S(2)}) copy-start(bf16[2048,256]{1,0:T(8,128)(2,1)} %wq_ref.1) | copy-start | bytes 3145732
  14.3 6.4 %collective-permute-start.2 = (bf16[256,128]{1,0:T(8,128)(2,1)S(1)}, bf16[256,128]{1,0:T(8,128)(2,1)S(1)}, u32[]{:S(2)}, u32[]{:S(2)}) collective-permute-start(bf16[256,128]{1,0:T(8,128)(2,1)S(1)} %get-tuple-element.59), channel_id=1, source_target_pairs={{0,16},{8,24},{16,0},{24,8},{1,17},{9,25},{17,1},{25,9},{2,18},{10... | collective-permute-start | bytes 196616 | tf_op jit(solution)/shard_map/ppermute | solution.py:435
  17.4 3.9 %collective-permute-start.3 = (bf16[256,128]{1,0:T(8,128)(2,1)S(1)}, bf16[256,128]{1,0:T(8,128)(2,1)S(1)}, u32[]{:S(2)}, u32[]{:S(2)}) collective-permute-start(bf16[256,128]{1,0:T(8,128)(2,1)S(1)} %get-tuple-element.60), channel_id=1, source_target_pairs={{0,24},{8,0},{16,8},{24,16},{1,25},{9,1},{17,9},{25,17},{2,26},{10... | collective-permute-start | bytes 196616 | tf_op jit(solution)/shard_map/ppermute | solution.py:435
  18.2 4.5 %collective-permute-start.1 = (bf16[320,128]{1,0:T(8,128)(2,1)S(1)}, bf16[320,128]{1,0:T(8,128)(2,1)S(1)}, u32[]{:S(2)}, u32[]{:S(2)}) collective-permute-start(bf16[320,128]{1,0:T(8,128)(2,1)S(1)} %get-tuple-element.58), channel_id=1, source_target_pairs={{0,8},{8,16},{16,24},{24,0},{1,9},{9,17},{17,25},{25,1},{2,10},{10... | collective-permute-start | bytes 245768 | tf_op jit(solution)/shard_map/ppermute | solution.py:435
  18.9 13.3 %copy-start.4 = (f32[2,6,64,64]{3,2,1,0:T(8,128)S(1)}, f32[2,6,64,64]{3,2,1,0:T(8,128)}, u32[]{:S(2)}) copy-start(f32[2,6,64,64]{3,2,1,0:T(8,128)} %init_ref.1) | copy-start | bytes 589828
  18.9 18.2 %copy-start.5 = (bf16[4,128,128]{2,1,0:T(8,128)(2,1)S(1)}, bf16[4,128,128]{2,1,0:T(8,128)(2,1)}, u32[]{:S(2)}) copy-start(bf16[4,128,128]{2,1,0:T(8,128)(2,1)} %mix_ref.1) | copy-start | bytes 393220
  18.9 18.2 %copy-start.8 = (f32[512]{0:T(512)S(1)}, f32[512]{0:T(512)}, u32[]{:S(2)}) copy-start(f32[512]{0:T(512)} %param.32) | copy-start | bytes 6148
  20.7 16.5 %copy-start.2 = (bf16[256,2048]{1,0:T(8,128)(2,1)S(1)}, bf16[256,2048]{1,0:T(8,128)(2,1)}, u32[]{:S(2)}) copy-start(bf16[256,2048]{1,0:T(8,128)(2,1)} %wp_ref.1) | copy-start | bytes 3145732
  23.3 8.8 %collective-permute-start.4 = (bf16[320,128]{1,0:T(8,128)(2,1)S(1)}, bf16[320,128]{1,0:T(8,128)(2,1)S(1)}, u32[]{:S(2)}, u32[]{:S(2)}) collective-permute-start(bf16[320,128]{1,0:T(8,128)(2,1)S(1)} %get-tuple-element.71), channel_id=1, source_target_pairs={{0,32},{32,64},{64,96},{96,0},{1,33},{33,65},{65,97},{97,1},{2,34}... | collective-permute-start | bytes 245768 | tf_op jit(solution)/shard_map/ppermute | solution.py:435
  25.0 3.5 %collective-permute-start.6 = (bf16[256,128]{1,0:T(8,128)(2,1)S(1)}, bf16[256,128]{1,0:T(8,128)(2,1)S(1)}, u32[]{:S(2)}, u32[]{:S(2)}) collective-permute-start(bf16[256,128]{1,0:T(8,128)(2,1)S(1)} %get-tuple-element.72), channel_id=1, source_target_pairs={{0,96},{32,0},{64,32},{96,64},{1,97},{33,1},{65,33},{97,65},{2,98}... | collective-permute-start | bytes 196616 | tf_op jit(solution)/shard_map/ppermute | solution.py:435
  27.2 4.9 %collective-permute-start.5 = (bf16[256,128]{1,0:T(8,128)(2,1)S(1)}, bf16[256,128]{1,0:T(8,128)(2,1)S(1)}, u32[]{:S(2)}, u32[]{:S(2)}) collective-permute-start(bf16[256,128]{1,0:T(8,128)(2,1)S(1)} %get-tuple-element.72), channel_id=1, source_target_pairs={{0,64},{32,96},{64,0},{96,32},{1,65},{33,97},{65,1},{97,33},{2,66}... | collective-permute-start | bytes 196616 | tf_op jit(solution)/shard_map/ppermute | solution.py:435
  33.3 4.5 %collective-permute-start.7 = (bf16[2,64,128]{2,1,0:T(8,128)(2,1)S(1)}, bf16[2,64,128]{2,1,0:T(8,128)(2,1)S(1)}, u32[]{:S(2)}, u32[]{:S(2)}) collective-permute-start(bf16[2,64,128]{2,1,0:T(8,128)(2,1)S(1)} %get-tuple-element.74), channel_id=1, source_target_pairs={{0,8},{8,16},{16,24},{24,0},{1,9},{9,17},{17,25},{25,1},{2,10},{10... | collective-permute-start | bytes 98312 | tf_op jit(solution)/shard_map/ppermute | solution.py:435
  33.6 4.3 %collective-permute-start.8 = (bf16[2,64,128]{2,1,0:T(8,128)(2,1)S(1)}, bf16[2,64,128]{2,1,0:T(8,128)(2,1)S(1)}, u32[]{:S(2)}, u32[]{:S(2)}) collective-permute-start(bf16[2,64,128]{2,1,0:T(8,128)(2,1)S(1)} %get-tuple-element.75), channel_id=1, source_target_pairs={{0,16},{8,24},{16,0},{24,8},{1,17},{9,25},{17,1},{25,9},{2,18},{10... | collective-permute-start | bytes 98312 | tf_op jit(solution)/shard_map/ppermute | solution.py:435
  35.7 2.8 %collective-permute-start.9 = (bf16[2,64,128]{2,1,0:T(8,128)(2,1)S(1)}, bf16[2,64,128]{2,1,0:T(8,128)(2,1)S(1)}, u32[]{:S(2)}, u32[]{:S(2)}) collective-permute-start(bf16[2,64,128]{2,1,0:T(8,128)(2,1)S(1)} %get-tuple-element.76), channel_id=1, source_target_pairs={{0,24},{8,0},{16,8},{24,16},{1,25},{9,1},{17,9},{25,17},{2,26},{10... | collective-permute-start | bytes 98312 | tf_op jit(solution)/shard_map/ppermute | solution.py:435
  37.1 1.4 %copy-start.1 = (bf16[384,2048]{1,0:T(8,128)(2,1)S(1)}, bf16[384,2048]{1,0:T(8,128)(2,1)}, u32[]{:S(2)}) copy-start(bf16[384,2048]{1,0:T(8,128)(2,1)} %wr_ref.1) | copy-start | bytes 4718596
  37.1 1.4 %copy-start.7 = (f32[768]{0:T(1024)S(1)}, f32[768]{0:T(1024)}, u32[]{:S(2)}) copy-start(f32[768]{0:T(1024)} %hgain_ref.1) | copy-start | bytes 9220
  40.5 5.8 %collective-permute-start.10 = (bf16[256,1024]{1,0:T(8,128)(2,1)S(1)}, bf16[256,1024]{1,0:T(8,128)(2,1)S(1)}, u32[]{:S(2)}, u32[]{:S(2)}) collective-permute-start(bf16[256,1024]{1,0:T(8,128)(2,1)S(1)} %get-tuple-element.82), channel_id=1, source_target_pairs={{0,1},{1,0},{2,3},{3,2},{4,5},{5,4},{6,7},{7,6},{8,9},{9,8},{10,11... | collective-permute-start | bytes 1572872 | tf_op jit(solution)/shard_map/ppermute | solution.py:514

commit v4 on v3

--- a/solution.py
+++ b/solution.py
@@ -92,8 +92,16 @@
     return weave(jnp.zeros_like(part), part, size)
 
 
-def inverses(lowers):
-    row, col = iota(SPAN, SPAN, 0), iota(SPAN, SPAN, 1)
+def blocks(x):
+    x = x.astype(bf16)
+    zero = jnp.zeros((SPAN, 128), bf16)
+    return jnp.concatenate(
+        [jnp.concatenate([x[:, :128], zero], axis=1), jnp.concatenate([zero, x[:, 128:]], axis=1)], axis=0
+    )
+
+
+def inverses(lowers, fill):
+    row, col = iota(SPAN, 256, 0), iota(SPAN, 256, 1) & 127
     eye = (row == col).astype(f32)
     near = ((row >> 1) == (col >> 1)).astype(bf16)
     result = [eye - (lower * near).astype(f32) for lower in lowers]
@@ -101,8 +109,9 @@
     while size < SPAN:
         off = (((row >> (level + 1)) == (col >> (level + 1))) & ((row >> level) != (col >> level))).astype(bf16)
         if size < 8:
-            inner = [dot(lower * off, inv) for lower, inv in zip(lowers, result)]
-            result = [inv - dot(inv, part) for inv, part in zip(result, inner)]
+            inner = [dot(lower * off, blocks(inv)) for lower, inv in zip(lowers, result)]
+            fill(level)
+            result = [inv - dot(inv, blocks(part)) for inv, part in zip(result, inner)]
         else:
             if size < 16:
                 off = pick(off.astype(f32), size, 1).astype(bf16)
@@ -110,10 +119,10 @@
             else:
                 off = pick(off, size, 1)
                 odd = [pick(lower, size, 1) for lower in lowers]
-            inner = [dot(lower * off, inv) for lower, inv in zip(odd, result)]
+            inner = [dot(lower * off, blocks(inv)) for lower, inv in zip(odd, result)]
+            fill(level)
             outer = [
-                dot(pick(inv, size, 1), woven(part, size))
-                for inv, part in zip(result, inner)
+                dot(pick(inv, size, 1), blocks(woven(part, size))) for inv, part in zip(result, inner)
             ]
             result = [
                 weave(pick(inv, size, 0), pick(inv, size, 1) - part, size)
@@ -126,52 +135,65 @@
 WIDTHS = (384, 384, 384, 384, 384, 256)
 
 
-def fetch(sources, bufs, first_row, sems, base):
-    copies = [
-        pltpu.make_async_copy(src.at[pl.ds(pl.multiple_of(first_row, 1024), 1024), :], buf, sems.at[base + i])
-        for i, (src, buf) in enumerate(zip(sources, bufs))
-    ]
-    for copy in copies:
-        copy.start()
-    return copies
+def fetch(src, buf, first_row, sem):
+    return pltpu.make_async_copy(src.at[pl.ds(pl.multiple_of(first_row, 1024), 1024), :], buf, sem)
+
+
+EARLY = 3
 
 
 def own_kernel(*refs):
     token_ref, norm_ref = refs[:2]
-    sources, normed_ref, squares_ref, partials, rest = refs[2:8], refs[8], refs[9], refs[10:16], refs[16:22]
-    bufs, sems, own_ref, gain_ref, first_sems = refs[22:28], refs[28], refs[29], refs[30], refs[31]
+    sources, normed_ref, squares_ref, partials, rest = refs[2:8], refs[8], refs[9], refs[10:16], refs[16:19]
+    bufs, sems, own_ref, gain_ref, first_sems = refs[19:25], refs[25], refs[26], refs[27], refs[28]
     tp = lax.axis_index("tp")
     early = [
-        pltpu.make_async_copy(token_ref, own_ref, first_sems.at[0]),
-        pltpu.make_async_copy(norm_ref, gain_ref, first_sems.at[1]),
+        pltpu.make_async_copy(norm_ref, gain_ref, first_sems.at[0]),
+        pltpu.make_async_copy(token_ref, own_ref, first_sems.at[1]),
     ]
-    for copy in early:
+    mine = [fetch(src, buf, tp * 1024, sems.at[i]) for i, (src, buf) in enumerate(zip(sources, bufs))]
+    others = [
+        fetch(src, buf, (1 - tp) * 1024, sems.at[6 + i]) for i, (src, buf) in enumerate(zip(sources, rest))
+    ]
+    queue = mine + others
+    for copy in early + queue[:2]:
         copy.start()
-    copies = fetch(sources, bufs, tp * 1024, sems, 0)
-    later = fetch(sources, rest, (1 - tp) * 1024, sems, 6)
     for copy in early:
         copy.wait()
+    for copy in queue[2:4]:
+        copy.start()
     own = own_ref[...].astype(f32)
     normed = (own * jnp.where(tp == 0, gain_ref[:, :1024], gain_ref[:, 1024:])).astype(bf16)
     normed_ref[...] = normed
     squares_ref[...] = jnp.broadcast_to(jnp.sum(own * own, axis=1, keepdims=True), (256, 128))
-    for copy, buf, partial in zip(copies, bufs, partials):
+    started = 4
+    for i, (copy, buf, partial) in enumerate(zip(mine, bufs, partials)):
         copy.wait()
+        for extra in queue[started : started + (1 if i else 2)]:
+            extra.start()
+        started += 1 if i else 2
         partial[...] = dot(normed, buf[...])
-    for copy in later:
+    for extra in queue[started:]:
+        extra.start()
+    for copy in others:
         copy.wait()
 
 
 def local_kernel(*refs):
     other_ref, gain_ref, squares_ref, db_ref, rb_ref = refs[:5]
-    partials, rest = refs[5:11], refs[11:17]
+    partials, ready, sources = refs[5:11], refs[11:14], refs[14:17]
     (
         normed_ref, scale_ref, pool_ref, home_ref, first_ref, second_ref, third_ref,
-        right_ref, solved_ref, v_ref, rho_ref, lift_ref,
-    ) = refs[17:29]
-    k_s, d_s, a_s, r_s, v_s, maps = refs[29:35]
+        right_ref, solved_ref, v_ref, r_ref, grow_ref, lift_ref,
+    ) = refs[17:30]
+    k_s, d_s, a_s, maps = refs[30:34]
+    bufs, sems = refs[34:37], refs[37]
     tp = lax.axis_index("tp")
     y = lax.axis_index("sp_1")
+    copies = [fetch(src, buf, (1 - tp) * 1024, sems.at[i]) for i, (src, buf) in enumerate(zip(sources, bufs))]
+    for copy in copies:
+        copy.start()
+    rest = tuple(ready) + tuple(bufs)
     is_first = tp == 0
     other = other_ref[...].astype(f32)
     normed = (other * jnp.where(is_first, gain_ref[:, 1024:], gain_ref[:, :1024])).astype(bf16)
@@ -179,21 +201,34 @@
     squares = squares_ref[:, :1] + jnp.sum(other * other, axis=1, keepdims=True)
     scale = lax.rsqrt(squares * (1.0 / D) + 0.25)
     scale_ref[...] = jnp.broadcast_to(scale, (256, 128))
-    for i in range(6):
-        rounded = ((partials[i][...] + dot(normed, rest[i][...])) * scale).astype(bf16)
-        if i == 5:
-            pool_ref[...] = rounded
+    def project(i, rows):
+        total = partials[i][rows] + dot(normed_ref[rows], rest[i][...])
+        return (total * scale_ref[rows, :1]).astype(bf16)
+
+    for i, dest in enumerate((k_s, d_s, a_s)):
+        rounded = project(i, slice(0, 256))
+        for u in range(UNITS):
+            s, h = u // 3, u % 3
+            dest[u] = rounded[s * 128 : s * 128 + 128, h * 128 : h * 128 + 128].astype(f32)
+    for copy in copies:
+        copy.wait()
+
+    def fill(level):
+        if level > 3:
+            return
+        if level == 3:
+            pool = project(5, slice(0, 256))
+            pool_ref[...] = pool
             for s in (0, 1):
                 for half in (0, 1):
                     at = 256 + (2 * s + half) * 16
-                    first_ref[at : at + 16] = rounded[
-                        s * 128 + 112 : s * 128 + 128, half * 128 : half * 128 + 128
-                    ]
-            continue
-        dest = (k_s, d_s, a_s, r_s, v_s)[i]
+                    first_ref[at : at + 16] = pool[s * 128 + 112 : s * 128 + 128, half * 128 : half * 128 + 128]
+            return
+        dest = (v_ref, r_ref)[level - 1]
+        rounded = project(2 + level, slice(0, 256))
         for u in range(UNITS):
             s, h = u // 3, u % 3
-            dest[u] = rounded[s * 128 : s * 128 + 128, h * 128 : h * 128 + 128].astype(f32)
+            dest[u] = rounded[s * 128 : s * 128 + 128, h * 128 : h * 128 + 128]
 
     masks = head_masks()
     n = SPAN
@@ -208,7 +243,7 @@
     slab = iota(HEAD, 128, 0)
     eye = (slab == (iota(HEAD, 128, 1) & 63)).astype(f32)
     units = range(UNITS)
-    lowers, alphas, keeps = [], [], []
+    first_stage = []
     for u in units:
         h = u % 3
         lanes = slice(h * 128, h * 128 + 128)
@@ -217,44 +252,54 @@
         rb = jnp.where(is_first, line_of(rb_ref, lanes), line_of(rb_ref, shifted))
         k = k_s[u]
         log_decay = -0.6065306597126334 * jax.nn.sigmoid(db + d_s[u])
-        rate = jax.nn.sigmoid(rb + a_s[u])
-        unit_key = k * lax.rsqrt(dot_fine_left(k * k, ones) + 1.0)
-        removal = unit_key * rate
-        total = dot_fine_right(triangle, log_decay)
-        middle, final = total[63:64], total[127:128]
-        alpha = jnp.exp(total - log_decay - middle) * unit_key
-        fading = jnp.exp(middle - total)
-        beta, kappa = removal * fading, k * fading
-        rho = r_s[u] * jnp.exp(total - middle)
-        ending = jnp.exp(final - total)
+        first_stage.append(
+            (log_decay, jax.nn.sigmoid(rb + a_s[u]), dot(k * k, ones), dot_fine_right(triangle, log_decay))
+        )
+    second_stage = []
+    for u in units:
+        log_decay, rate, squared, total = first_stage[u]
+        k = k_s[u]
+        middle = total[63:64]
+        unit_key = k * lax.rsqrt(squared + 1.0)
+        centred = total - middle
+        alpha = jnp.exp(centred - log_decay) * unit_key
+        fading = jnp.exp(-centred)
+        grow_ref[u] = jnp.exp(centred)
         lift = jnp.exp(middle)
-        rho_ref[u] = rho
         lift_ref[u : u + 1] = lift
-        right = jnp.concatenate([beta.astype(bf16), kappa.astype(bf16)], axis=0)
+        right = jnp.concatenate(
+            [(unit_key * rate * fading).astype(bf16), (k * fading).astype(bf16)], axis=0
+        )
         right_ref[u] = right
-        pairs = dot(both(alpha, masks), right, NT)
-        lower_kappa = []
-        for j in (0, 1):
-            lowers.append(jnp.where(strict, pairs[j * n : j * n + n, :n], 0.0).astype(bf16))
-            lower_kappa.append(jnp.where(strict, pairs[j * n : j * n + n, n:], 0.0).astype(bf16))
-        v = v_s[u]
-        v_ref[u] = v.astype(bf16)
-        carried = dot(jnp.concatenate(lower_kappa, axis=1), both(v, masks))
-        keeps.append((alpha * lift, carried, removal * ending, k * ending, jnp.exp(final)))
-    inverse = inverses(lowers)
+        ends = (jnp.exp(total[127:128]), jnp.exp(centred[127:128]))
+        second_stage.append((right, alpha * lift, ends, dot(both(alpha, masks), right, NT)))
+    lowers, carries = [], []
     for u in units:
-        alpha, carried, beta_end, kappa_end, gain_end = keeps[u]
-        right = jnp.concatenate([alpha, carried], axis=1)
-        solved = dot(jnp.concatenate(inverse[2 * u : 2 * u + 2], axis=1), both(right, wide))
-        solved_ref[u] = solved.astype(bf16)
-        crossed = dot(solved[:, :n], beta_end, TN)
-        transit = eye * gain_end - joined(crossed)
-        crossed = dot(
-            jnp.concatenate([v_s[u], -solved[:, n:]], axis=0),
-            jnp.concatenate([kappa_end, beta_end], axis=0),
-            TN,
-        )
-        written = joined(crossed)
+        pairs = second_stage[u][3]
+        block = lambda j, c: jnp.where(
+            strict, pairs[j * n : j * n + n, c * n : c * n + n], 0.0
+        ).astype(bf16)
+        lowers.append(jnp.concatenate([block(0, 0), block(1, 0)], axis=1))
+        carries.append(jnp.concatenate([block(0, 1), block(1, 1)], axis=1))
+    inverse = inverses(lowers, fill)
+    carries = [dot(carries[u], both(v_ref[u], masks)) for u in units]
+    solutions = []
+    for u in units:
+        wanted = jnp.concatenate([second_stage[u][1].astype(bf16), carries[u].astype(bf16)], axis=1)
+        solved = dot(inverse[u], both(wanted, wide)).astype(bf16)
+        solved_ref[u] = solved
+        solutions.append(solved)
+    for u in units:
+        right, _, ends, _ = second_stage[u]
+        solved = solutions[u]
+        transit = eye * ends[0] - joined(dot(solved[:, :n], right[:n], TN)) * ends[1]
+        written = joined(
+            dot(
+                jnp.concatenate([-solved[:, n:], v_ref[u]], axis=0),
+                right,
+                TN,
+            )
+        ) * ends[1]
         at = (u // 3) * 128
         maps[u % 3, at : at + HEAD] = transit.astype(bf16)
         maps[u % 3, at + HEAD : at + 128] = written.astype(bf16)
@@ -264,7 +309,7 @@
 
 
 def side_kernel(
-    own_ref, other_ref, scale_ref, right_ref, solved_ref, v_ref, rho_ref, lift_ref, wg_ref, wq_ref,
+    own_ref, other_ref, scale_ref, right_ref, solved_ref, v_ref, r_ref, grow_ref, lift_ref, wg_ref, wq_ref,
     reads_ref, local_ref, gate_ref, pgate_ref,
 ):
     tp = lax.axis_index("tp")
@@ -274,16 +319,18 @@
         jnp.concatenate([masks[1], masks[1]], axis=1),
     )
     inclusive = iota(128, 128, 0) >= iota(128, 128, 1)
-    inside = []
+    inside, rhos = [], []
     for u in range(UNITS):
-        pairs = dot(both(rho_ref[u], masks), right_ref[u], NT)
+        rho = r_ref[u].astype(f32) * grow_ref[u]
+        rhos.append(rho * lift_ref[u : u + 1])
+        pairs = dot(both(rho, masks), right_ref[u], NT)
         block = lambda j, c: jnp.where(
             inclusive, pairs[j * 128 : j * 128 + 128, c * 128 : c * 128 + 128], 0.0
         ).astype(bf16)
         inside.append([jnp.concatenate([block(0, c), block(1, c)], axis=1) for c in (0, 1)])
     for u in range(UNITS):
         removed = dot(inside[u][0], both(solved_ref[u], wide))
-        reads_ref[u] = (rho_ref[u] * lift_ref[u : u + 1] - removed[:, :128]).astype(bf16)
+        reads_ref[u] = (rhos[u] - removed[:, :128]).astype(bf16)
         local_ref[u] = dot(inside[u][1], both(v_ref[u], masks)) - removed[:, 128:]
     scale = scale_ref[:, :1]
     mine, theirs = pl.multiple_of(tp * 1024, 1024), pl.multiple_of((1 - tp) * 1024, 1024)
@@ -443,42 +490,44 @@
     other = lax.ppermute(tokens, "tp", [(0, 1), (1, 0)])
     line = lambda x: x.reshape(1, -1)
     pinned = lambda x: pltpu.with_memory_space_constraint(x, pltpu.HBM)
-    weights = [pinned(w) for w in (w_key, w_decay, w_rate, w_recept, w_value, w_pool)]
-    bufs = [pltpu.VMEM((1024, width), bf16) for width in WIDTHS] + [pltpu.SemaphoreType.DMA((12,))]
+    weights = [pinned(w) for w in (w_key, w_decay, w_rate, w_value, w_recept, w_pool)]
+    bufs = [pltpu.VMEM((1024, width), bf16) for width in WIDTHS] + [pltpu.SemaphoreType.DMA((9,))]
     own_normed, squares, *halves_of = call(
         own_kernel,
         "own",
         hbm(8),
         [shape((256, 1024)), shape((256, 128), f32)] + [shape((256, width), f32) for width in WIDTHS]
-        + [shape((1024, width)) for width in WIDTHS],
+        + [shape((1024, width)) for width in WIDTHS[:EARLY]],
         bufs + [pltpu.VMEM((256, 1024), bf16), pltpu.VMEM((1, D), f32), pltpu.SemaphoreType.DMA((2,))],
         20,
         1_000_000_000,
     )(pinned(tokens.reshape(256, 1024)), pinned(line(norm_gain)), *weights)
-    normed, scale, pool, home, m1, m2, m3, right, solved, v, rho, lift = call(
+    normed, scale, pool, home, m1, m2, m3, right, solved, v, r, grow, lift = call(
         local_kernel,
         "local",
-        vmem(17),
+        vmem(14) + hbm(3),
         [
             shape((256, 1024)), shape((256, 128), f32), shape((256, 256)),
             shape((256, 128)), shape((320, 128)), shape((256, 128)), shape((256, 128)),
             shape((6, 256, 128)), shape((6, 128, 256)), shape((6, 128, 128)),
-            shape((6, 128, 128), f32), shape((6, 128), f32),
+            shape((6, 128, 128)), shape((6, 128, 128), f32), shape((6, 128), f32),
         ],
-        [pltpu.VMEM((6, 128, 128), f32)] * 5 + [pltpu.VMEM((4, 256, 128), bf16)],
+        [pltpu.VMEM((6, 128, 128), f32)] * 3 + [pltpu.VMEM((4, 256, 128), bf16)]
+        + [pltpu.VMEM((1024, width), bf16) for width in WIDTHS[EARLY:]]
+        + [pltpu.SemaphoreType.DMA((3,))],
         24,
         3_000_000_000,
-    )(other.reshape(256, 1024), line(norm_gain), squares, decay_base, rate_base, *halves_of)
+    )(other.reshape(256, 1024), line(norm_gain), squares, decay_base, rate_base, *halves_of, *weights[EARLY:])
     r1, r2, r3 = around((m1, m2, m3), "sp_1")
     reads, local, gate, pgate = call(
         side_kernel,
         "side",
-        vmem(10),
+        vmem(11),
         [shape((6, 128, 128)), shape((6, 128, 128), f32), shape((256, 384)), shape((256, 256))],
         [],
         16,
         1_000_000_000,
-    )(own_normed, normed, scale, right, solved, v, rho, lift, w_gate_rec, w_gate_pool)
+    )(own_normed, normed, scale, right, solved, v, r, grow, lift, w_gate_rec, w_gate_pool)
     prefix, onward, total = call(
         row_kernel,
         "row",

time: 47.4 us -> 45.3 us (0.956)
  Pallas kernels: 19 us -> 16.8 us
    pallas_call x1, Pallas kernels: 6.35 us -> 4.18 us  [shards(): call(own_kernel, 'own', hbm(8), [shape((256, 1024)), shape((256, 128), f3...]
  transfers between devices with their start and end apart: 11 -> 11, of which waited for: 7 -> 7; matrix products, arithmetic and copies ran while one was open for 0% -> 0% of each run, Pallas kernels for 19% -> 15%
where the time goes in v4:
time: 45.3 us; the launch traced here: 45.2 us
  starting transfers between devices  19.1 us (42%)
  Pallas kernels  16.8 us (37%)
  waiting for transfers between devices  7.98 us (18%)
  other arithmetic  0.99 us (2%)
    ppermute x9, starting transfers between devices, around(): lax.ppermute(part, axis, [(i, i + step & 3) for i in range(4)])  13.6 us
    pallas_call x1, Pallas kernels, shards(): call(local_kernel, 'local', vmem(14) + hbm(3), [shape((256, 1024)), shape...  6.48 us
    ppermute x9, waiting for transfers between devices, around(): lax.ppermute(part, axis, [(i, i + step & 3) for i in range(4)])  6.44 us
    pallas_call x1, Pallas kernels, shards(): call(own_kernel, 'own', hbm(8), [shape((256, 1024)), shape((256, 128), f3...  4.18 us
    ppermute x1, starting transfers between devices, shards(): arrived = lax.ppermute(send, 'tp', [(0, 1), (1, 0)])  4.12 us
    pallas_call x1, Pallas kernels, shards(): call(final_kernel, 'final', vmem(10), [shape((256, 1024)), shape((256, 10...  1.95 us
    pallas_call x1, Pallas kernels, shards(): call(side_kernel, 'side', vmem(11), [shape((6, 128, 128)), shape((6, 128,...  1.76 us
    ppermute x1, waiting for transfers between devices, shards(): arrived = lax.ppermute(send, 'tp', [(0, 1), (1, 0)])  1.54 us
  transfers between devices with their start and end apart: 11, of which 7 were waited for; matrix products, arithmetic and copies ran while one was open for 0% of the time, Pallas kernels for 15%

profile of v4, /device:TPU:1, one launch (start us, length us, event | category | flops | bytes accessed | tf_op | source)
XLA Modules:
  0.0 45.2 jit_solution(15984536421727071960)
XLA Ops:
  0.0 1.4 %collective-permute-start = (bf16[2,128,1024]{2,1,0:T(8,128)(2,1)}, bf16[2,128,1024]{2,1,0:T(8,128)(2,1)S(1)}, u32[]{:S(2)}, u32[]{:S(2)}) collective-permute-start(bf16[2,128,1024]{2,1,0:T(8,128)(2,1)} %param.18), channel_id=1, source_target_pairs={{0,1},{1,0},{2,3},{3,2},{4,5},{5,4},{6,7},{7,6},{8,9},{9,8},{10,11... | collective-permute-start | bytes 1572872 | tf_op jit(solution)/shard_map/ppermute | solution.py:490
  1.4 4.2 %own.1 = (bf16[256,1024]{1,0:T(8,128)(2,1)S(1)}, f32[256,128]{1,0:T(8,128)S(1)}, f32[256,384]{1,0:T(8,128)S(1)}, f32[256,384]{1,0:T(8,128)S(1)}, f32[256,384]{1,...) custom-call(bf16[256,1024]{1,0:T(8,128)(2,1)} %bitcast.9, ...), custom_call_target="tpu_custom_call" | custom-call | flops 1000000000 | tf_op jit(solution)/shard_map/own/pallas_call | solution.py:495
  5.6 0.0 copy-start
  5.6 0.0 copy-start.3
  5.6 6.5 %local.1 = (bf16[256,1024]{1,0:T(8,128)(2,1)S(1)}, f32[256,128]{1,0:T(8,128)S(1)}, bf16[256,256]{1,0:T(8,128)(2,1)S(1)}, bf16[256,128]{1,0:T(8,128)(2,1)S(1)}, b...) custom-call(bf16[256,1024]{1,0:T(8,128)(2,1)S(1)} %bitcast.8, ...), custom_call_target="tpu_custom_call" | custom-call | flops 3000000000 | tf_op jit(solution)/shard_map/local/pallas_call | solution.py:505
  12.1 3.1 %collective-permute-start.2 = (bf16[256,128]{1,0:T(8,128)(2,1)S(1)}, bf16[256,128]{1,0:T(8,128)(2,1)S(1)}, u32[]{:S(2)}, u32[]{:S(2)}) collective-permute-start(bf16[256,128]{1,0:T(8,128)(2,1)S(1)} %get-tuple-element.54), channel_id=1, source_target_pairs={{0,16},{8,24},{16,0},{24,8},{1,17},{9,25},{17,1},{25,9},{2,18},{10... | collective-permute-start | bytes 196616 | tf_op jit(solution)/shard_map/ppermute | solution.py:482
  15.2 0.8 %collective-permute-start.3 = (bf16[256,128]{1,0:T(8,128)(2,1)S(1)}, bf16[256,128]{1,0:T(8,128)(2,1)S(1)}, u32[]{:S(2)}, u32[]{:S(2)}) collective-permute-start(bf16[256,128]{1,0:T(8,128)(2,1)S(1)} %get-tuple-element.55), channel_id=1, source_target_pairs={{0,24},{8,0},{16,8},{24,16},{1,25},{9,1},{17,9},{25,17},{2,26},{10... | collective-permute-start | bytes 196616 | tf_op jit(solution)/shard_map/ppermute | solution.py:482
  16.0 0.7 %collective-permute-start.1 = (bf16[320,128]{1,0:T(8,128)(2,1)S(1)}, bf16[320,128]{1,0:T(8,128)(2,1)S(1)}, u32[]{:S(2)}, u32[]{:S(2)}) collective-permute-start(bf16[320,128]{1,0:T(8,128)(2,1)S(1)} %get-tuple-element.53), channel_id=1, source_target_pairs={{0,8},{8,16},{16,24},{24,0},{1,9},{9,17},{17,25},{25,1},{2,10},{10... | collective-permute-start | bytes 245768 | tf_op jit(solution)/shard_map/ppermute | solution.py:482
  16.7 0.0 copy-start.8
  16.7 1.8 %side.1 = (bf16[6,128,128]{2,1,0:T(8,128)(2,1)S(1)}, f32[6,128,128]{2,1,0:T(8,128)S(1)}, bf16[256,384]{1,0:T(8,128)(2,1)S(1)}, bf16[256,256]{1,0:T(8,128)(2,1)S(1)}) custom-call(bf16[256,1024]{1,0:T(8,128)(2,1)S(1)} %get-tuple-element.56.own_ref, bf16[256,1024]{1,0:T(8,128)(2,1)S(1)} %get-tuple-element.57.other_ref, ...), custom_call_target="tpu_custom_call" | custom-call | flops 1000000000 | tf_op jit(solution)/shard_map/side/pallas_call | solution.py:522
  18.5 0.0 copy-start.2
  18.5 0.7 %collective-permute-done.3.third_ref = bf16[256,128]{1,0:T(8,128)(2,1)S(1)} collective-permute-done((bf16[256,128]{1,0:T(8,128)(2,1)S(1)}, bf16[256,128]{1,0:T(8,128)(2,1)S(1)}, u32[]{:S(2)}, u32[]{:S(2)}) %collective-permute-start.3) | collective-permute-done | bytes 65568 | tf_op jit(solution)/shard_map/ppermute | solution.py:482
  19.3 1.2 %collective-permute-done.1.first_ref.beside_ref = bf16[320,128]{1,0:T(8,128)(2,1)S(1)} collective-permute-done((bf16[320,128]{1,0:T(8,128)(2,1)S(1)}, bf16[320,128]{1,0:T(8,128)(2,1)S(1)}, u32[]{:S(2)}, u32[]{:S(2)}) %collective-permute-start.1) | collective-permute-done | bytes 81952 | tf_op jit(solution)/shard_map/ppermute | solution.py:482
  20.5 0.6 %row.1 = (f32[3,2,128,128]{3,2,1,0:T(8,128)S(1)}, bf16[320,128]{1,0:T(8,128)(2,1)S(1)}, bf16[256,128]{1,0:T(8,128)(2,1)S(1)}) custom-call(bf16[256,128]{1,0:T(8,128)(2,1)S(1)} %get-tuple-element.52.home_ref, bf16[320,128]{1,0:T(8,128)(2,1)S(1)} %collective-permute-done.1.first_ref.beside_ref, bf16[256,128]{1,0:T(8,128)(2,1)S(1)} %collective-permute-done.2.second_ref, ...), custom_call_target="tpu_custom_call" | custom-call | flops 100000000 | tf_op jit(solution)/shard_map/row/pallas_call | solution.py:531
  21.2 1.7 %collective-permute-start.4 = (bf16[320,128]{1,0:T(8,128)(2,1)S(1)}, bf16[320,128]{1,0:T(8,128)(2,1)S(1)}, u32[]{:S(2)}, u32[]{:S(2)}) collective-permute-start(bf16[320,128]{1,0:T(8,128)(2,1)S(1)} %get-tuple-element.67), channel_id=1, source_target_pairs={{0,32},{32,64},{64,96},{96,0},{1,33},{33,65},{65,97},{97,1},{2,34}... | collective-permute-start | bytes 245768 | tf_op jit(solution)/shard_map/ppermute | solution.py:482
  22.9 2.2 %collective-permute-start.6 = (bf16[256,128]{1,0:T(8,128)(2,1)S(1)}, bf16[256,128]{1,0:T(8,128)(2,1)S(1)}, u32[]{:S(2)}, u32[]{:S(2)}) collective-permute-start(bf16[256,128]{1,0:T(8,128)(2,1)S(1)} %get-tuple-element.68), channel_id=1, source_target_pairs={{0,96},{32,0},{64,32},{96,64},{1,97},{33,1},{65,33},{97,65},{2,98}... | collective-permute-start | bytes 196616 | tf_op jit(solution)/shard_map/ppermute | solution.py:482
  25.1 1.2 %collective-permute-start.5 = (bf16[256,128]{1,0:T(8,128)(2,1)S(1)}, bf16[256,128]{1,0:T(8,128)(2,1)S(1)}, u32[]{:S(2)}, u32[]{:S(2)}) collective-permute-start(bf16[256,128]{1,0:T(8,128)(2,1)S(1)} %get-tuple-element.68), channel_id=1, source_target_pairs={{0,64},{32,96},{64,0},{96,32},{1,65},{33,97},{65,1},{97,33},{2,66}... | collective-permute-start | bytes 196616 | tf_op jit(solution)/shard_map/ppermute | solution.py:482
  26.3 0.1 collective-permute-done.6.third_ref
  26.4 3.7 %collective-permute-done.5.second_ref = bf16[256,128]{1,0:T(8,128)(2,1)S(1)} collective-permute-done((bf16[256,128]{1,0:T(8,128)(2,1)S(1)}, bf16[256,128]{1,0:T(8,128)(2,1)S(1)}, u32[]{:S(2)}, u32[]{:S(2)}) %collective-permute-start.5) | collective-permute-done | bytes 65568 | tf_op jit(solution)/shard_map/ppermute | solution.py:482
  30.1 1.2 %column.1 = (bf16[2,64,128]{2,1,0:T(8,128)(2,1)S(1)}, bf16[2,64,128]{2,1,0:T(8,128)(2,1)S(1)}, bf16[2,64,128]{2,1,0:T(8,128)(2,1)S(1)}, bf16[2,64,128]{2,1,0:T(8,128)(2,1)S(1)}) custom-call(f32[3,2,128,128]{3,2,1,0:T(8,128)S(1)} %get-tuple-element.66.prefix_ref, bf16[320,128]{1,0:T(8,128)(2,1)S(1)} %collective-permute-done.4.first_ref.above_ref, ...), custom_call_target="tpu_custom_call" | custom-call | flops 100000000 | tf_op jit(solution)/shard_map/column/pallas_call | solution.py:541
  31.3 0.5 %collective-permute-start.7 = (bf16[2,64,128]{2,1,0:T(8,128)(2,1)S(1)}, bf16[2,64,128]{2,1,0:T(8,128)(2,1)S(1)}, u32[]{:S(2)}, u32[]{:S(2)}) collective-permute-start(bf16[2,64,128]{2,1,0:T(8,128)(2,1)S(1)} %get-tuple-element.70), channel_id=1, source_target_pairs={{0,8},{8,16},{16,24},{24,0},{1,9},{9,17},{17,25},{25,1},{2,10},{10... | collective-permute-start | bytes 98312 | tf_op jit(solution)/shard_map/ppermute | solution.py:482
  31.8 2.0 %collective-permute-start.8 = (bf16[2,64,128]{2,1,0:T(8,128)(2,1)S(1)}, bf16[2,64,128]{2,1,0:T(8,128)(2,1)S(1)}, u32[]{:S(2)}, u32[]{:S(2)}) collective-permute-start(bf16[2,64,128]{2,1,0:T(8,128)(2,1)S(1)} %get-tuple-element.71), channel_id=1, source_target_pairs={{0,16},{8,24},{16,0},{24,8},{1,17},{9,25},{17,1},{25,9},{2,18},{10... | collective-permute-start | bytes 98312 | tf_op jit(solution)/shard_map/ppermute | solution.py:482
  33.7 1.4 %collective-permute-start.9 = (bf16[2,64,128]{2,1,0:T(8,128)(2,1)S(1)}, bf16[2,64,128]{2,1,0:T(8,128)(2,1)S(1)}, u32[]{:S(2)}, u32[]{:S(2)}) collective-permute-start(bf16[2,64,128]{2,1,0:T(8,128)(2,1)S(1)} %get-tuple-element.72), channel_id=1, source_target_pairs={{0,24},{8,0},{16,8},{24,16},{1,25},{9,1},{17,9},{25,17},{2,26},{10... | collective-permute-start | bytes 98312 | tf_op jit(solution)/shard_map/ppermute | solution.py:482
  35.2 0.0 copy-start.7
  35.2 0.6 %pool.1.part_ref = f32[256,2048]{1,0:T(8,128)S(1)} custom-call(bf16[256,256]{1,0:T(8,128)(2,1)S(1)} %get-tuple-element.76.pool_ref, bf16[320,128]{1,0:T(8,128)(2,1)S(1)} %collective-permute-done.1.first_ref.beside_ref, bf16[320,128]{1,0:T(8,128)(2,1)S(1)} %collective-permute-done.4.first_ref.above_ref, ...), custom_call_target="tpu_custom_call" | custom-call | flops 300000000 | tf_op jit(solution)/shard_map/pool/pallas_call | solution.py:551
  35.8 0.2 collective-permute-done.8.two_ref
  36.0 0.5 collective-permute-done.9.three_ref
  36.5 0.1 copy-done.1
  36.6 2.0 %final.1 = (bf16[256,1024]{1,0:T(8,128)(2,1)S(1)}, bf16[256,1024]{1,0:T(8,128)(2,1)S(1)}) custom-call(bf16[2,64,128]{2,1,0:T(8,128)(2,1)S(1)} %get-tuple-element.69.home_ref, bf16[2,64,128]{2,1,0:T(8,128)(2,1)S(1)} %collective-permute-done.7.one_ref, bf16[2,64,128]{2,1,0:T(8,128)(2,1)S(1)} %collective-permute-done.8.two_ref, ...), custom_call_target="tpu_custom_call" | custom-call | flops 1000000000 | tf_op jit(solution)/shard_map/final/pallas_call | solution.py:554
  38.5 4.1 %collective-permute-start.10 = (bf16[256,1024]{1,0:T(8,128)(2,1)S(1)}, bf16[256,1024]{1,0:T(8,128)(2,1)S(1)}, u32[]{:S(2)}, u32[]{:S(2)}) collective-permute-start(bf16[256,1024]{1,0:T(8,128)(2,1)S(1)} %get-tuple-element.78), channel_id=1, source_target_pairs={{0,1},{1,0},{2,3},{3,2},{4,5},{5,4},{6,7},{7,6},{8,9},{9,8},{10,11... | collective-permute-start | bytes 1572872 | tf_op jit(solution)/shard_map/ppermute | solution.py:563
  42.6 1.5 %collective-permute-done.10 = bf16[256,1024]{1,0:T(8,128)(2,1)S(1)} collective-permute-done((bf16[256,1024]{1,0:T(8,128)(2,1)S(1)}, bf16[256,1024]{1,0:T(8,128)(2,1)S(1)}, u32[]{:S(2)}, u32[]{:S(2)}) %collective-permute-start.10) | collective-permute-done | bytes 524320 | tf_op jit(solution)/shard_map/ppermute | solution.py:563
  44.2 1.0 %add_convert_fusion = bf16[256,1024]{1,0:T(8,128)(2,1)} fusion(bf16[256,1024]{1,0:T(8,128)(2,1)S(1)} %collective-permute-done.10, bf16[256,1024]{1,0:T(8,128)(2,1)S(1)} %get-tuple-element.77), kind=kLoop, calls=%fused_computation | loop fusion | flops 1048576 | bytes 1572864 | tf_op jit(solution)/shard_map/convert_element_type | solution.py:565
  (20 shorter events, 0.0 us)
Async XLA Ops:
  0.0 5.6 %collective-permute-start = (bf16[2,128,1024]{2,1,0:T(8,128)(2,1)}, bf16[2,128,1024]{2,1,0:T(8,128)(2,1)S(1)}, u32[]{:S(2)}, u32[]{:S(2)}) collective-permute-start(bf16[2,128,1024]{2,1,0:T(8,128)(2,1)} %param.18), channel_id=1, source_target_pairs={{0,1},{1,0},{2,3},{3,2},{4,5},{5,4},{6,7},{7,6},{8,9},{9,8},{10,11... | collective-permute-start | bytes 1572872 | tf_op jit(solution)/shard_map/ppermute | solution.py:490
  1.4 4.2 %copy-start.6 = (f32[2048]{0:T(1024)S(1)}, f32[2048]{0:T(1024)}, u32[]{:S(2)}) copy-start(f32[2048]{0:T(1024)} %param.19) | copy-start | bytes 24580
  1.4 4.2 %copy-start.9 = (f32[768]{0:T(1024)S(1)}, f32[768]{0:T(1024)}, u32[]{:S(2)}) copy-start(f32[768]{0:T(1024)} %refs_3_.3) | copy-start | bytes 9220
  1.4 4.2 %copy-start.10 = (f32[768]{0:T(1024)S(1)}, f32[768]{0:T(1024)}, u32[]{:S(2)}) copy-start(f32[768]{0:T(1024)} %refs_4_.3) | copy-start | bytes 9220
  5.6 11.1 %copy-start = (bf16[2048,384]{1,0:T(8,128)(2,1)S(1)}, bf16[2048,384]{1,0:T(8,128)(2,1)}, u32[]{:S(2)}) copy-start(bf16[2048,384]{1,0:T(8,128)(2,1)} %wg_ref.1) | copy-start | bytes 4718596
  5.6 11.1 %copy-start.3 = (bf16[2048,256]{1,0:T(8,128)(2,1)S(1)}, bf16[2048,256]{1,0:T(8,128)(2,1)}, u32[]{:S(2)}) copy-start(bf16[2048,256]{1,0:T(8,128)(2,1)} %wq_ref.1) | copy-start | bytes 3145732
  12.1 6.4 %collective-permute-start.2 = (bf16[256,128]{1,0:T(8,128)(2,1)S(1)}, bf16[256,128]{1,0:T(8,128)(2,1)S(1)}, u32[]{:S(2)}, u32[]{:S(2)}) collective-permute-start(bf16[256,128]{1,0:T(8,128)(2,1)S(1)} %get-tuple-element.54), channel_id=1, source_target_pairs={{0,16},{8,24},{16,0},{24,8},{1,17},{9,25},{17,1},{25,9},{2,18},{10... | collective-permute-start | bytes 196616 | tf_op jit(solution)/shard_map/ppermute | solution.py:482
  15.2 4.0 %collective-permute-start.3 = (bf16[256,128]{1,0:T(8,128)(2,1)S(1)}, bf16[256,128]{1,0:T(8,128)(2,1)S(1)}, u32[]{:S(2)}, u32[]{:S(2)}) collective-permute-start(bf16[256,128]{1,0:T(8,128)(2,1)S(1)} %get-tuple-element.55), channel_id=1, source_target_pairs={{0,24},{8,0},{16,8},{24,16},{1,25},{9,1},{17,9},{25,17},{2,26},{10... | collective-permute-start | bytes 196616 | tf_op jit(solution)/shard_map/ppermute | solution.py:482
  16.0 4.5 %collective-permute-start.1 = (bf16[320,128]{1,0:T(8,128)(2,1)S(1)}, bf16[320,128]{1,0:T(8,128)(2,1)S(1)}, u32[]{:S(2)}, u32[]{:S(2)}) collective-permute-start(bf16[320,128]{1,0:T(8,128)(2,1)S(1)} %get-tuple-element.53), channel_id=1, source_target_pairs={{0,8},{8,16},{16,24},{24,0},{1,9},{9,17},{17,25},{25,1},{2,10},{10... | collective-permute-start | bytes 245768 | tf_op jit(solution)/shard_map/ppermute | solution.py:482
  16.7 13.4 %copy-start.4 = (f32[2,6,64,64]{3,2,1,0:T(8,128)S(1)}, f32[2,6,64,64]{3,2,1,0:T(8,128)}, u32[]{:S(2)}) copy-start(f32[2,6,64,64]{3,2,1,0:T(8,128)} %init_ref.1) | copy-start | bytes 589828
  16.7 18.4 %copy-start.5 = (bf16[4,128,128]{2,1,0:T(8,128)(2,1)S(1)}, bf16[4,128,128]{2,1,0:T(8,128)(2,1)}, u32[]{:S(2)}) copy-start(bf16[4,128,128]{2,1,0:T(8,128)(2,1)} %mix_ref.1) | copy-start | bytes 393220
  16.7 18.4 %copy-start.8 = (f32[512]{0:T(512)S(1)}, f32[512]{0:T(512)}, u32[]{:S(2)}) copy-start(f32[512]{0:T(512)} %param.32) | copy-start | bytes 6148
  18.5 16.6 %copy-start.2 = (bf16[256,2048]{1,0:T(8,128)(2,1)S(1)}, bf16[256,2048]{1,0:T(8,128)(2,1)}, u32[]{:S(2)}) copy-start(bf16[256,2048]{1,0:T(8,128)(2,1)} %wp_ref.1) | copy-start | bytes 3145732
  21.2 8.9 %collective-permute-start.4 = (bf16[320,128]{1,0:T(8,128)(2,1)S(1)}, bf16[320,128]{1,0:T(8,128)(2,1)S(1)}, u32[]{:S(2)}, u32[]{:S(2)}) collective-permute-start(bf16[320,128]{1,0:T(8,128)(2,1)S(1)} %get-tuple-element.67), channel_id=1, source_target_pairs={{0,32},{32,64},{64,96},{96,0},{1,33},{33,65},{65,97},{97,1},{2,34}... | collective-permute-start | bytes 245768 | tf_op jit(solution)/shard_map/ppermute | solution.py:482
  22.9 3.5 %collective-permute-start.6 = (bf16[256,128]{1,0:T(8,128)(2,1)S(1)}, bf16[256,128]{1,0:T(8,128)(2,1)S(1)}, u32[]{:S(2)}, u32[]{:S(2)}) collective-permute-start(bf16[256,128]{1,0:T(8,128)(2,1)S(1)} %get-tuple-element.68), channel_id=1, source_target_pairs={{0,96},{32,0},{64,32},{96,64},{1,97},{33,1},{65,33},{97,65},{2,98}... | collective-permute-start | bytes 196616 | tf_op jit(solution)/shard_map/ppermute | solution.py:482
  25.1 5.0 %collective-permute-start.5 = (bf16[256,128]{1,0:T(8,128)(2,1)S(1)}, bf16[256,128]{1,0:T(8,128)(2,1)S(1)}, u32[]{:S(2)}, u32[]{:S(2)}) collective-permute-start(bf16[256,128]{1,0:T(8,128)(2,1)S(1)} %get-tuple-element.68), channel_id=1, source_target_pairs={{0,64},{32,96},{64,0},{96,32},{1,65},{33,97},{65,1},{97,33},{2,66}... | collective-permute-start | bytes 196616 | tf_op jit(solution)/shard_map/ppermute | solution.py:482
  31.3 4.6 %collective-permute-start.7 = (bf16[2,64,128]{2,1,0:T(8,128)(2,1)S(1)}, bf16[2,64,128]{2,1,0:T(8,128)(2,1)S(1)}, u32[]{:S(2)}, u32[]{:S(2)}) collective-permute-start(bf16[2,64,128]{2,1,0:T(8,128)(2,1)S(1)} %get-tuple-element.70), channel_id=1, source_target_pairs={{0,8},{8,16},{16,24},{24,0},{1,9},{9,17},{17,25},{25,1},{2,10},{10... | collective-permute-start | bytes 98312 | tf_op jit(solution)/shard_map/ppermute | solution.py:482
  31.8 4.3 %collective-permute-start.8 = (bf16[2,64,128]{2,1,0:T(8,128)(2,1)S(1)}, bf16[2,64,128]{2,1,0:T(8,128)(2,1)S(1)}, u32[]{:S(2)}, u32[]{:S(2)}) collective-permute-start(bf16[2,64,128]{2,1,0:T(8,128)(2,1)S(1)} %get-tuple-element.71), channel_id=1, source_target_pairs={{0,16},{8,24},{16,0},{24,8},{1,17},{9,25},{17,1},{25,9},{2,18},{10... | collective-permute-start | bytes 98312 | tf_op jit(solution)/shard_map/ppermute | solution.py:482
  33.7 2.8 %collective-permute-start.9 = (bf16[2,64,128]{2,1,0:T(8,128)(2,1)S(1)}, bf16[2,64,128]{2,1,0:T(8,128)(2,1)S(1)}, u32[]{:S(2)}, u32[]{:S(2)}) collective-permute-start(bf16[2,64,128]{2,1,0:T(8,128)(2,1)S(1)} %get-tuple-element.72), channel_id=1, source_target_pairs={{0,24},{8,0},{16,8},{24,16},{1,25},{9,1},{17,9},{25,17},{2,26},{10... | collective-permute-start | bytes 98312 | tf_op jit(solution)/shard_map/ppermute | solution.py:482
  35.1 1.4 %copy-start.1 = (bf16[384,2048]{1,0:T(8,128)(2,1)S(1)}, bf16[384,2048]{1,0:T(8,128)(2,1)}, u32[]{:S(2)}) copy-start(bf16[384,2048]{1,0:T(8,128)(2,1)} %wr_ref.1) | copy-start | bytes 4718596
  35.2 1.4 %copy-start.7 = (f32[768]{0:T(1024)S(1)}, f32[768]{0:T(1024)}, u32[]{:S(2)}) copy-start(f32[768]{0:T(1024)} %hgain_ref.1) | copy-start | bytes 9220
  38.5 5.7 %collective-permute-start.10 = (bf16[256,1024]{1,0:T(8,128)(2,1)S(1)}, bf16[256,1024]{1,0:T(8,128)(2,1)S(1)}, u32[]{:S(2)}, u32[]{:S(2)}) collective-permute-start(bf16[256,1024]{1,0:T(8,128)(2,1)S(1)} %get-tuple-element.78), channel_id=1, source_target_pairs={{0,1},{1,0},{2,3},{3,2},{4,5},{5,4},{6,7},{7,6},{8,9},{9,8},{10,11... | collective-permute-start | bytes 1572872 | tf_op jit(solution)/shard_map/ppermute | solution.py:563

commit v5 on v4

--- a/solution.py
+++ b/solution.py
@@ -132,68 +132,81 @@
     return result
 
 
-WIDTHS = (384, 384, 384, 384, 384, 256)
-
-
-def fetch(src, buf, first_row, sem):
-    return pltpu.make_async_copy(src.at[pl.ds(pl.multiple_of(first_row, 1024), 1024), :], buf, sem)
-
-
-EARLY = 3
+GROUPS = ((384, 384), (384, 384), (384, 256))
+WIDE = tuple(sum(group) for group in GROUPS)
+
+
+def fetch(sources, buf, first_row, sems, base):
+    copies, at = [], 0
+    for i, src in enumerate(sources):
+        width = src.shape[1]
+        copies.append(
+            pltpu.make_async_copy(
+                src.at[pl.ds(pl.multiple_of(first_row, 1024), 1024), :],
+                buf.at[:, at : at + width],
+                sems.at[base + i],
+            )
+        )
+        at += width
+    return copies
+
+
+def begin(copies):
+    for copy in copies:
+        copy.start()
+
+
+def finish(copies):
+    for copy in copies:
+        copy.wait()
 
 
 def own_kernel(*refs):
     token_ref, norm_ref = refs[:2]
-    sources, normed_ref, squares_ref, partials, rest = refs[2:8], refs[8], refs[9], refs[10:16], refs[16:19]
-    bufs, sems, own_ref, gain_ref, first_sems = refs[19:25], refs[25], refs[26], refs[27], refs[28]
+    sources, normed_ref, squares_ref, partials, rest = refs[2:8], refs[8], refs[9], refs[10:13], refs[13]
+    bufs, sems, own_ref, gain_ref, first_sems = refs[14:17], refs[17], refs[18], refs[19], refs[20]
     tp = lax.axis_index("tp")
     early = [
         pltpu.make_async_copy(norm_ref, gain_ref, first_sems.at[0]),
         pltpu.make_async_copy(token_ref, own_ref, first_sems.at[1]),
     ]
-    mine = [fetch(src, buf, tp * 1024, sems.at[i]) for i, (src, buf) in enumerate(zip(sources, bufs))]
-    others = [
-        fetch(src, buf, (1 - tp) * 1024, sems.at[6 + i]) for i, (src, buf) in enumerate(zip(sources, rest))
-    ]
-    queue = mine + others
-    for copy in early + queue[:2]:
-        copy.start()
-    for copy in early:
-        copy.wait()
-    for copy in queue[2:4]:
-        copy.start()
+    mine = [fetch(sources[2 * i : 2 * i + 2], bufs[i], tp * 1024, sems, 2 * i) for i in range(3)]
+    others = fetch(sources[:2], rest, (1 - tp) * 1024, sems, 6)
+    begin(early)
+    begin(mine[0])
+    finish(early)
+    begin(mine[1])
     own = own_ref[...].astype(f32)
     normed = (own * jnp.where(tp == 0, gain_ref[:, :1024], gain_ref[:, 1024:])).astype(bf16)
     normed_ref[...] = normed
     squares_ref[...] = jnp.broadcast_to(jnp.sum(own * own, axis=1, keepdims=True), (256, 128))
-    started = 4
-    for i, (copy, buf, partial) in enumerate(zip(mine, bufs, partials)):
-        copy.wait()
-        for extra in queue[started : started + (1 if i else 2)]:
-            extra.start()
-        started += 1 if i else 2
-        partial[...] = dot(normed, buf[...])
-    for extra in queue[started:]:
-        extra.start()
-    for copy in others:
-        copy.wait()
+    for i in range(3):
+        finish(mine[i])
+        if i == 0:
+            begin(mine[2])
+        if i == 1:
+            begin(others)
+        partials[i][...] = dot(normed, bufs[i][...])
+    finish(others)
 
 
 def local_kernel(*refs):
     other_ref, gain_ref, squares_ref, db_ref, rb_ref = refs[:5]
-    partials, ready, sources = refs[5:11], refs[11:14], refs[14:17]
+    partials, ready, sources = refs[5:8], refs[8], refs[9:13]
     (
         normed_ref, scale_ref, pool_ref, home_ref, first_ref, second_ref, third_ref,
         right_ref, solved_ref, v_ref, r_ref, grow_ref, lift_ref,
-    ) = refs[17:30]
-    k_s, d_s, a_s, maps = refs[30:34]
-    bufs, sems = refs[34:37], refs[37]
+    ) = refs[13:26]
+    k_s, d_s, a_s, maps = refs[26:30]
+    bufs, sems = refs[30:32], refs[32]
     tp = lax.axis_index("tp")
     y = lax.axis_index("sp_1")
-    copies = [fetch(src, buf, (1 - tp) * 1024, sems.at[i]) for i, (src, buf) in enumerate(zip(sources, bufs))]
-    for copy in copies:
-        copy.start()
-    rest = tuple(ready) + tuple(bufs)
+    copies = [
+        fetch(sources[2 * i : 2 * i + 2], bufs[i], (1 - tp) * 1024, sems, 2 * i) for i in range(2)
+    ]
+    begin(copies[0])
+    begin(copies[1])
+    rest = (ready,) + tuple(bufs)
     is_first = tp == 0
     other = other_ref[...].astype(f32)
     normed = (other * jnp.where(is_first, gain_ref[:, 1024:], gain_ref[:, :1024])).astype(bf16)
@@ -201,34 +214,31 @@
     squares = squares_ref[:, :1] + jnp.sum(other * other, axis=1, keepdims=True)
     scale = lax.rsqrt(squares * (1.0 / D) + 0.25)
     scale_ref[...] = jnp.broadcast_to(scale, (256, 128))
-    def project(i, rows):
-        total = partials[i][rows] + dot(normed_ref[rows], rest[i][...])
-        return (total * scale_ref[rows, :1]).astype(bf16)
-
-    for i, dest in enumerate((k_s, d_s, a_s)):
-        rounded = project(i, slice(0, 256))
+
+    def project(i):
+        total = partials[i][...] + dot(normed_ref[...], rest[i][...])
+        return (total * scale_ref[:, :1]).astype(bf16)
+
+    def place(dest, rounded, at, kind):
         for u in range(UNITS):
             s, h = u // 3, u % 3
-            dest[u] = rounded[s * 128 : s * 128 + 128, h * 128 : h * 128 + 128].astype(f32)
-    for copy in copies:
-        copy.wait()
+            dest[u] = rounded[s * 128 : s * 128 + 128, at + h * 128 : at + h * 128 + 128].astype(kind)
+
+    rounded = project(0)
+    place(k_s, rounded, 0, f32)
+    place(d_s, rounded, 384, f32)
 
     def fill(level):
-        if level > 3:
+        if level != 1:
             return
-        if level == 3:
-            pool = project(5, slice(0, 256))
-            pool_ref[...] = pool
-            for s in (0, 1):
-                for half in (0, 1):
-                    at = 256 + (2 * s + half) * 16
-                    first_ref[at : at + 16] = pool[s * 128 + 112 : s * 128 + 128, half * 128 : half * 128 + 128]
-            return
-        dest = (v_ref, r_ref)[level - 1]
-        rounded = project(2 + level, slice(0, 256))
-        for u in range(UNITS):
-            s, h = u // 3, u % 3
-            dest[u] = rounded[s * 128 : s * 128 + 128, h * 128 : h * 128 + 128]
+        rounded = project(2)
+        place(r_ref, rounded, 0, bf16)
+        pool = rounded[:, 384:]
+        pool_ref[...] = pool
+        for s in (0, 1):
+            for half in (0, 1):
+                at = 256 + (2 * s + half) * 16
+                first_ref[at : at + 16] = pool[s * 128 + 112 : s * 128 + 128, half * 128 : half * 128 + 128]
 
     masks = head_masks()
     n = SPAN
@@ -249,15 +259,21 @@
         lanes = slice(h * 128, h * 128 + 128)
         shifted = slice(384 + h * 128, 384 + h * 128 + 128)
         db = jnp.where(is_first, line_of(db_ref, lanes), line_of(db_ref, shifted))
-        rb = jnp.where(is_first, line_of(rb_ref, lanes), line_of(rb_ref, shifted))
         k = k_s[u]
         log_decay = -0.6065306597126334 * jax.nn.sigmoid(db + d_s[u])
-        first_stage.append(
-            (log_decay, jax.nn.sigmoid(rb + a_s[u]), dot(k * k, ones), dot_fine_right(triangle, log_decay))
-        )
+        first_stage.append((log_decay, dot(k * k, ones), dot_fine_right(triangle, log_decay)))
+    finish(copies[0])
+    rounded = project(1)
+    place(a_s, rounded, 0, f32)
+    place(v_ref, rounded, 384, bf16)
     second_stage = []
     for u in units:
-        log_decay, rate, squared, total = first_stage[u]
+        h = u % 3
+        lanes = slice(h * 128, h * 128 + 128)
+        shifted = slice(384 + h * 128, 384 + h * 128 + 128)
+        rb = jnp.where(is_first, line_of(rb_ref, lanes), line_of(rb_ref, shifted))
+        rate = jax.nn.sigmoid(rb + a_s[u])
+        log_decay, squared, total = first_stage[u]
         k = k_s[u]
         middle = total[63:64]
         unit_key = k * lax.rsqrt(squared + 1.0)
@@ -273,6 +289,7 @@
         right_ref[u] = right
         ends = (jnp.exp(total[127:128]), jnp.exp(centred[127:128]))
         second_stage.append((right, alpha * lift, ends, dot(both(alpha, masks), right, NT)))
+    finish(copies[1])
     lowers, carries = [], []
     for u in units:
         pairs = second_stage[u][3]
@@ -311,8 +328,14 @@
 def side_kernel(
     own_ref, other_ref, scale_ref, right_ref, solved_ref, v_ref, r_ref, grow_ref, lift_ref, wg_ref, wq_ref,
     reads_ref, local_ref, gate_ref, pgate_ref,
+    buf, sems,
 ):
     tp = lax.axis_index("tp")
+    copies = [
+        pltpu.make_async_copy(wg_ref, buf.at[:, :384], sems.at[0]),
+        pltpu.make_async_copy(wq_ref, buf.at[:, 384:], sems.at[1]),
+    ]
+    begin(copies)
     masks = head_masks()
     wide = (
         jnp.concatenate([masks[0], masks[0]], axis=1),
@@ -334,10 +357,11 @@
         local_ref[u] = dot(inside[u][1], both(v_ref[u], masks)) - removed[:, 128:]
     scale = scale_ref[:, :1]
     mine, theirs = pl.multiple_of(tp * 1024, 1024), pl.multiple_of((1 - tp) * 1024, 1024)
-    for weight, dest in ((wg_ref, gate_ref), (wq_ref, pgate_ref)):
-        total = dot(own_ref[...], weight[pl.ds(mine, 1024), :])
-        total = total + dot(other_ref[...], weight[pl.ds(theirs, 1024), :])
-        dest[...] = (total * scale).astype(bf16)
+    finish(copies)
+    total = dot(own_ref[...], buf[pl.ds(mine, 1024), :]) + dot(other_ref[...], buf[pl.ds(theirs, 1024), :])
+    rounded = (total * scale).astype(bf16)
+    gate_ref[...] = rounded[:, :384]
+    pgate_ref[...] = rounded[:, 384:]
 
 
 def row_kernel(home_ref, first_ref, second_ref, third_ref, after_ref, prefix_ref, next_ref, total_ref, maps):
@@ -423,8 +447,8 @@
 def final_kernel(
     home_ref, one_ref, two_ref, three_ref, reads_ref, local_ref, gate_ref, hgain_ref, part_ref,
     wr_ref,
-    send_ref, keep_ref,
-    starts, rec,
+    send_ref, rec,
+    starts,
 ):
     tp = lax.axis_index("tp")
     y = lax.axis_index("sp_1")
@@ -447,9 +471,13 @@
         rec[rows, lanes] = (
             out * lax.rsqrt(spread + 1.0) * gain * (gate * jax.nn.sigmoid(gate))
         ).astype(bf16)
-    for dest, part in ((send_ref, 1 - tp), (keep_ref, tp)):
-        cols = pl.ds(pl.multiple_of(part * 1024, 1024), 1024)
-        dest[...] = (dot(rec[...], wr_ref[:, cols]) + part_ref[:, cols]).astype(bf16)
+    cols = pl.ds(pl.multiple_of((1 - tp) * 1024, 1024), 1024)
+    send_ref[...] = (dot(rec[...], wr_ref[:, cols]) + part_ref[:, cols]).astype(bf16)
+
+
+def keep_kernel(rec_ref, part_ref, wr_ref, keep_ref):
+    cols = pl.ds(pl.multiple_of(lax.axis_index("tp") * 1024, 1024), 1024)
+    keep_ref[...] = (dot(rec_ref[...], wr_ref[:, cols]) + part_ref[:, cols]).astype(bf16)
 
 
 def vmem(count):
@@ -491,43 +519,50 @@
     line = lambda x: x.reshape(1, -1)
     pinned = lambda x: pltpu.with_memory_space_constraint(x, pltpu.HBM)
     weights = [pinned(w) for w in (w_key, w_decay, w_rate, w_value, w_recept, w_pool)]
-    bufs = [pltpu.VMEM((1024, width), bf16) for width in WIDTHS] + [pltpu.SemaphoreType.DMA((9,))]
-    own_normed, squares, *halves_of = call(
+    own_normed, squares, *prepared = call(
         own_kernel,
         "own",
         hbm(8),
-        [shape((256, 1024)), shape((256, 128), f32)] + [shape((256, width), f32) for width in WIDTHS]
-        + [shape((1024, width)) for width in WIDTHS[:EARLY]],
-        bufs + [pltpu.VMEM((256, 1024), bf16), pltpu.VMEM((1, D), f32), pltpu.SemaphoreType.DMA((2,))],
+        [shape((256, 1024)), shape((256, 128), f32)]
+        + [shape((256, width), f32) for width in WIDE]
+        + [shape((1024, WIDE[0]))],
+        [pltpu.VMEM((1024, width), bf16) for width in WIDE]
+        + [
+            pltpu.SemaphoreType.DMA((8,)), pltpu.VMEM((256, 1024), bf16), pltpu.VMEM((1, D), f32),
+            pltpu.SemaphoreType.DMA((2,)),
+        ],
         20,
         1_000_000_000,
     )(pinned(tokens.reshape(256, 1024)), pinned(line(norm_gain)), *weights)
     normed, scale, pool, home, m1, m2, m3, right, solved, v, r, grow, lift = call(
         local_kernel,
         "local",
-        vmem(14) + hbm(3),
+        vmem(9) + hbm(4),
         [
             shape((256, 1024)), shape((256, 128), f32), shape((256, 256)),
             shape((256, 128)), shape((320, 128)), shape((256, 128)), shape((256, 128)),
             shape((6, 256, 128)), shape((6, 128, 256)), shape((6, 128, 128)),
             shape((6, 128, 128)), shape((6, 128, 128), f32), shape((6, 128), f32),
         ],
-        [pltpu.VMEM((6, 128, 128), f32)] * 3 + [pltpu.VMEM((4, 256, 128), bf16)]
-        + [pltpu.VMEM((1024, width), bf16) for width in WIDTHS[EARLY:]]
-        + [pltpu.SemaphoreType.DMA((3,))],
+        [pltpu.VMEM((6, 128, 128), f32)] * 3
+        + [pltpu.VMEM((4, 256, 128), bf16)]
+        + [pltpu.VMEM((1024, width), bf16) for width in WIDE[1:]]
+        + [pltpu.SemaphoreType.DMA((4,))],
         24,
         3_000_000_000,
-    )(other.reshape(256, 1024), line(norm_gain), squares, decay_base, rate_base, *halves_of, *weights[EARLY:])
+    )(
+        other.reshape(256, 1024), line(norm_gain), squares, decay_base, rate_base, *prepared, *weights[2:]
+    )
     r1, r2, r3 = around((m1, m2, m3), "sp_1")
     reads, local, gate, pgate = call(
         side_kernel,
         "side",
-        vmem(11),
+        vmem(9) + hbm(2),
         [shape((6, 128, 128)), shape((6, 128, 128), f32), shape((256, 384)), shape((256, 256))],
-        [],
+        [pltpu.VMEM((D, 640), bf16), pltpu.SemaphoreType.DMA((2,))],
         16,
         1_000_000_000,
-    )(own_normed, normed, scale, right, solved, v, r, grow, lift, w_gate_rec, w_gate_pool)
+    )(own_normed, normed, scale, right, solved, v, r, grow, lift, pinned(w_gate_rec), pinned(w_gate_pool))
     prefix, onward, total = call(
         row_kernel,
         "row",
@@ -551,16 +586,17 @@
     pool_part = call(
         pool_kernel, "pool", vmem(7), shape((256, D), f32), [pltpu.VMEM((256, 256), bf16)], 12, 300_000_000
     )(pool, r1, columns[0], pgate, pool_mix, line(pool_scale), w_out_pool)
-    send, keep = call(
+    send, rec = call(
         final_kernel,
         "final",
         vmem(10),
-        [shape((256, 1024)), shape((256, 1024))],
-        [pltpu.VMEM((4, 2, 64, 128), bf16), pltpu.VMEM((256, 384), bf16)],
+        [shape((256, 1024)), shape((256, 384))],
+        [pltpu.VMEM((4, 2, 64, 128), bf16)],
         20,
         1_000_000_000,
     )(s0, t1, t2, t3, reads, local, gate, head_gain, pool_part, w_out_rec)
     arrived = lax.ppermute(send, "tp", [(0, 1), (1, 0)])
+    keep = call(keep_kernel, "keep", vmem(3), shape((256, 1024)), [], 8, 300_000_000)(rec, pool_part, w_out_rec)
     mixed = keep.astype(f32) + arrived.astype(f32)
     return mixed.astype(bf16).reshape(2, 128, 1024)
 

time: 45.3 us -> 45.2 us (level)
  Pallas kernels: 16.8 us -> 18.6 us
  waiting for transfers between devices: 7.98 us -> 6.44 us
    pallas_call x3 -> x4, Pallas kernels: 10.2 us -> 12.1 us  [the longest x1 6.84 us: shards(): call(local_kernel, 'local', vmem(9) + hbm(4), [shape((256, 1024)), shape(...]
    ppermute x9, waiting for transfers between devices: 6.44 us -> 5.34 us  [around(): lax.ppermute(part, axis, [(i, i + step & 3) for i in range(4)])]
  transfers between devices with their start and end apart: 11 -> 11, of which waited for: 7 -> 6; matrix products, arithmetic and copies ran while one was open for 0% -> 0% of each run, Pallas kernels for 15% -> 19%
where the time goes in v5:
time: 45.2 us; the launch traced here: 45 us
  starting transfers between devices  18.7 us (41%)
  Pallas kernels  18.6 us (41%)
  waiting for transfers between devices  6.44 us (14%)
  other arithmetic  0.99 us (2%)
    ppermute x9, starting transfers between devices, around(): lax.ppermute(part, axis, [(i, i + step & 3) for i in range(4)])  13.4 us
    pallas_call x1, Pallas kernels, shards(): call(local_kernel, 'local', vmem(9) + hbm(4), [shape((256, 1024)), shape(...  6.84 us
    ppermute x9, waiting for transfers between devices, around(): lax.ppermute(part, axis, [(i, i + step & 3) for i in range(4)])  5.34 us
    pallas_call x1, Pallas kernels, shards(): call(own_kernel, 'own', hbm(8), [shape((256, 1024)), shape((256, 128), f3...  4.12 us
    ppermute x1, starting transfers between devices, shards(): arrived = lax.ppermute(send, 'tp', [(0, 1), (1, 0)])  3.93 us
    pallas_call x1, Pallas kernels, shards(): call(side_kernel, 'side', vmem(9) + hbm(2), [shape((6, 128, 128)), shape(...  3.12 us
    pallas_call x1, Pallas kernels, shards(): call(final_kernel, 'final', vmem(10), [shape((256, 1024)), shape((256, 38...  1.66 us
    ppermute x1, starting transfers between devices, shards(): other = lax.ppermute(tokens, 'tp', [(0, 1), (1, 0)])  1.38 us
  transfers between devices with their start and end apart: 11, of which 6 were waited for; matrix products, arithmetic and copies ran while one was open for 0% of the time, Pallas kernels for 19%

profile of v5, /device:TPU:1, one launch (start us, length us, event | category | flops | bytes accessed | tf_op | source)
XLA Modules:
  0.0 45.0 jit_solution(11037472958396883877)
XLA Ops:
  0.0 1.4 %collective-permute-start = (bf16[2,128,1024]{2,1,0:T(8,128)(2,1)}, bf16[2,128,1024]{2,1,0:T(8,128)(2,1)S(1)}, u32[]{:S(2)}, u32[]{:S(2)}) collective-permute-start(bf16[2,128,1024]{2,1,0:T(8,128)(2,1)} %param.18), channel_id=1, source_target_pairs={{0,1},{1,0},{2,3},{3,2},{4,5},{5,4},{6,7},{7,6},{8,9},{9,8},{10,11... | collective-permute-start | bytes 1572872 | tf_op jit(solution)/shard_map/ppermute | solution.py:518
  1.4 4.1 %own.1 = (bf16[256,1024]{1,0:T(8,128)(2,1)S(1)}, f32[256,128]{1,0:T(8,128)S(1)}, f32[256,768]{1,0:T(8,128)S(1)}, f32[256,768]{1,0:T(8,128)S(1)}, f32[256,640]{1,0:T(8,128)S(1)}, /*index=5*/bf16[1024,768]{1,0:T(8,128)(2,1)S(1)}) custom-call(bf16[256,1024]{1,0:T(8,128)(2,1)} %bitcast.9, f32[1,2048]{1,0:T(1,128)} %bitcast.5, bf16[2048,384]{1,0:T(8,128)(2,1)} %refs_2_.1, ...), custom_call_target="tpu_custom_call" | custom-call | flops 1000000000 | tf_op jit(solution)/shard_map/own/pallas_call | solution.py:522
  5.5 0.0 collective-permute-done
  5.6 6.8 %local.1 = (bf16[256,1024]{1,0:T(8,128)(2,1)S(1)}, f32[256,128]{1,0:T(8,128)S(1)}, bf16[256,256]{1,0:T(8,128)(2,1)S(1)}, bf16[256,128]{1,0:T(8,128)(2,1)S(1)}, b...) custom-call(bf16[256,1024]{1,0:T(8,128)(2,1)S(1)} %bitcast.8, ...), custom_call_target="tpu_custom_call" | custom-call | flops 3000000000 | tf_op jit(solution)/shard_map/local/pallas_call | solution.py:537
  12.4 3.1 %collective-permute-start.2 = (bf16[256,128]{1,0:T(8,128)(2,1)S(1)}, bf16[256,128]{1,0:T(8,128)(2,1)S(1)}, u32[]{:S(2)}, u32[]{:S(2)}) collective-permute-start(bf16[256,128]{1,0:T(8,128)(2,1)S(1)} %get-tuple-element.44), channel_id=1, source_target_pairs={{0,16},{8,24},{16,0},{24,8},{1,17},{9,25},{17,1},{25,9},{2,18},{10... | collective-permute-start | bytes 196616 | tf_op jit(solution)/shard_map/ppermute | solution.py:510
  15.5 0.8 %collective-permute-start.3 = (bf16[256,128]{1,0:T(8,128)(2,1)S(1)}, bf16[256,128]{1,0:T(8,128)(2,1)S(1)}, u32[]{:S(2)}, u32[]{:S(2)}) collective-permute-start(bf16[256,128]{1,0:T(8,128)(2,1)S(1)} %get-tuple-element.45), channel_id=1, source_target_pairs={{0,24},{8,0},{16,8},{24,16},{1,25},{9,1},{17,9},{25,17},{2,26},{10... | collective-permute-start | bytes 196616 | tf_op jit(solution)/shard_map/ppermute | solution.py:510
  16.3 0.7 %collective-permute-start.1 = (bf16[320,128]{1,0:T(8,128)(2,1)S(1)}, bf16[320,128]{1,0:T(8,128)(2,1)S(1)}, u32[]{:S(2)}, u32[]{:S(2)}) collective-permute-start(bf16[320,128]{1,0:T(8,128)(2,1)S(1)} %get-tuple-element.43), channel_id=1, source_target_pairs={{0,8},{8,16},{16,24},{24,0},{1,9},{9,17},{17,25},{25,1},{2,10},{10... | collective-permute-start | bytes 245768 | tf_op jit(solution)/shard_map/ppermute | solution.py:510
  17.0 3.1 %side.1 = (bf16[6,128,128]{2,1,0:T(8,128)(2,1)S(1)}, f32[6,128,128]{2,1,0:T(8,128)S(1)}, bf16[256,384]{1,0:T(8,128)(2,1)S(1)}, bf16[256,256]{1,0:T(8,128)(2,1)S(1)}) custom-call(bf16[256,1024]{1,0:T(8,128)(2,1)S(1)} %get-tuple-element.46.own_ref, bf16[256,1024]{1,0:T(8,128)(2,1)S(1)} %get-tuple-element.47.other_ref, ...), custom_call_target="tpu_custom_call" | custom-call | flops 1000000000 | tf_op jit(solution)/shard_map/side/pallas_call | solution.py:557
  20.1 0.0 copy-start.1
  20.1 0.0 collective-permute-done.2.second_ref
  20.1 0.0 collective-permute-done.3.third_ref
  20.1 0.6 %collective-permute-done.1.first_ref.beside_ref = bf16[320,128]{1,0:T(8,128)(2,1)S(1)} collective-permute-done((bf16[320,128]{1,0:T(8,128)(2,1)S(1)}, bf16[320,128]{1,0:T(8,128)(2,1)S(1)}, u32[]{:S(2)}, u32[]{:S(2)}) %collective-permute-start.1) | collective-permute-done | bytes 81952 | tf_op jit(solution)/shard_map/ppermute | solution.py:510
  20.8 0.6 %row.1 = (f32[3,2,128,128]{3,2,1,0:T(8,128)S(1)}, bf16[320,128]{1,0:T(8,128)(2,1)S(1)}, bf16[256,128]{1,0:T(8,128)(2,1)S(1)}) custom-call(bf16[256,128]{1,0:T(8,128)(2,1)S(1)} %get-tuple-element.42.home_ref, bf16[320,128]{1,0:T(8,128)(2,1)S(1)} %collective-permute-done.1.first_ref.beside_ref, bf16[256,128]{1,0:T(8,128)(2,1)S(1)} %collective-permute-done.2.second_ref, ...), custom_call_target="tpu_custom_call" | custom-call | flops 100000000 | tf_op jit(solution)/shard_map/row/pallas_call | solution.py:566
  21.4 1.7 %collective-permute-start.4 = (bf16[320,128]{1,0:T(8,128)(2,1)S(1)}, bf16[320,128]{1,0:T(8,128)(2,1)S(1)}, u32[]{:S(2)}, u32[]{:S(2)}) collective-permute-start(bf16[320,128]{1,0:T(8,128)(2,1)S(1)} %get-tuple-element.57), channel_id=1, source_target_pairs={{0,32},{32,64},{64,96},{96,0},{1,33},{33,65},{65,97},{97,1},{2,34}... | collective-permute-start | bytes 245768 | tf_op jit(solution)/shard_map/ppermute | solution.py:510
  23.1 2.2 %collective-permute-start.6 = (bf16[256,128]{1,0:T(8,128)(2,1)S(1)}, bf16[256,128]{1,0:T(8,128)(2,1)S(1)}, u32[]{:S(2)}, u32[]{:S(2)}) collective-permute-start(bf16[256,128]{1,0:T(8,128)(2,1)S(1)} %get-tuple-element.58), channel_id=1, source_target_pairs={{0,96},{32,0},{64,32},{96,64},{1,97},{33,1},{65,33},{97,65},{2,98}... | collective-permute-start | bytes 196616 | tf_op jit(solution)/shard_map/ppermute | solution.py:510
  25.3 1.2 %collective-permute-start.5 = (bf16[256,128]{1,0:T(8,128)(2,1)S(1)}, bf16[256,128]{1,0:T(8,128)(2,1)S(1)}, u32[]{:S(2)}, u32[]{:S(2)}) collective-permute-start(bf16[256,128]{1,0:T(8,128)(2,1)S(1)} %get-tuple-element.58), channel_id=1, source_target_pairs={{0,64},{32,96},{64,0},{96,32},{1,65},{33,97},{65,1},{97,33},{2,66}... | collective-permute-start | bytes 196616 | tf_op jit(solution)/shard_map/ppermute | solution.py:510
  26.6 0.1 collective-permute-done.6.third_ref
  26.7 3.7 %collective-permute-done.5.second_ref = bf16[256,128]{1,0:T(8,128)(2,1)S(1)} collective-permute-done((bf16[256,128]{1,0:T(8,128)(2,1)S(1)}, bf16[256,128]{1,0:T(8,128)(2,1)S(1)}, u32[]{:S(2)}, u32[]{:S(2)}) %collective-permute-start.5) | collective-permute-done | bytes 65568 | tf_op jit(solution)/shard_map/ppermute | solution.py:510
  30.4 0.0 collective-permute-done.4.first_ref.above_ref
  30.4 1.2 %column.1 = (bf16[2,64,128]{2,1,0:T(8,128)(2,1)S(1)}, bf16[2,64,128]{2,1,0:T(8,128)(2,1)S(1)}, bf16[2,64,128]{2,1,0:T(8,128)(2,1)S(1)}, bf16[2,64,128]{2,1,0:T(8,128)(2,1)S(1)}) custom-call(f32[3,2,128,128]{3,2,1,0:T(8,128)S(1)} %get-tuple-element.56.prefix_ref, bf16[320,128]{1,0:T(8,128)(2,1)S(1)} %collective-permute-done.4.first_ref.above_ref, ...), custom_call_target="tpu_custom_call" | custom-call | flops 100000000 | tf_op jit(solution)/shard_map/column/pallas_call | solution.py:576
  31.5 0.3 collective-permute-start.7
  31.9 2.2 %collective-permute-start.8 = (bf16[2,64,128]{2,1,0:T(8,128)(2,1)S(1)}, bf16[2,64,128]{2,1,0:T(8,128)(2,1)S(1)}, u32[]{:S(2)}, u32[]{:S(2)}) collective-permute-start(bf16[2,64,128]{2,1,0:T(8,128)(2,1)S(1)} %get-tuple-element.61), channel_id=1, source_target_pairs={{0,16},{8,24},{16,0},{24,8},{1,17},{9,25},{17,1},{25,9},{2,18},{10... | collective-permute-start | bytes 98312 | tf_op jit(solution)/shard_map/ppermute | solution.py:510
  34.1 1.2 %collective-permute-start.9 = (bf16[2,64,128]{2,1,0:T(8,128)(2,1)S(1)}, bf16[2,64,128]{2,1,0:T(8,128)(2,1)S(1)}, u32[]{:S(2)}, u32[]{:S(2)}) collective-permute-start(bf16[2,64,128]{2,1,0:T(8,128)(2,1)S(1)} %get-tuple-element.62), channel_id=1, source_target_pairs={{0,24},{8,0},{16,8},{24,16},{1,25},{9,1},{17,9},{25,17},{2,26},{10... | collective-permute-start | bytes 98312 | tf_op jit(solution)/shard_map/ppermute | solution.py:510
  35.3 0.0 copy-start.5
  35.3 0.7 %pool.1.part_ref = f32[256,2048]{1,0:T(8,128)S(1)} custom-call(bf16[256,256]{1,0:T(8,128)(2,1)S(1)} %get-tuple-element.66.pool_ref, bf16[320,128]{1,0:T(8,128)(2,1)S(1)} %collective-permute-done.1.first_ref.beside_ref, bf16[320,128]{1,0:T(8,128)(2,1)S(1)} %collective-permute-done.4.first_ref.above_ref, ...), custom_call_target="tpu_custom_call" | custom-call | flops 300000000 | tf_op jit(solution)/shard_map/pool/pallas_call | solution.py:586
  35.9 0.2 collective-permute-done.8.two_ref
  36.1 0.7 %collective-permute-done.9.three_ref = bf16[2,64,128]{2,1,0:T(8,128)(2,1)S(1)} collective-permute-done((bf16[2,64,128]{2,1,0:T(8,128)(2,1)S(1)}, bf16[2,64,128]{2,1,0:T(8,128)(2,1)S(1)}, u32[]{:S(2)}, u32[]{:S(2)}) %collective-permute-start.9) | collective-permute-done | bytes 32800 | tf_op jit(solution)/shard_map/ppermute | solution.py:510
  36.8 1.7 %final.1 = (bf16[256,1024]{1,0:T(8,128)(2,1)S(1)}, bf16[256,384]{1,0:T(8,128)(2,1)S(1)}) custom-call(bf16[2,64,128]{2,1,0:T(8,128)(2,1)S(1)} %get-tuple-element.59.home_ref, bf16[2,64,128]{2,1,0:T(8,128)(2,1)S(1)} %collective-permute-done.7.one_ref, bf16[2,64,128]{2,1,0:T(8,128)(2,1)S(1)} %collective-permute-done.8.two_ref, ...), custom_call_target="tpu_custom_call" | custom-call | flops 1000000000 | tf_op jit(solution)/shard_map/final/pallas_call | solution.py:589
  38.5 3.9 %collective-permute-start.10 = (bf16[256,1024]{1,0:T(8,128)(2,1)S(1)}, bf16[256,1024]{1,0:T(8,128)(2,1)S(1)}, u32[]{:S(2)}, u32[]{:S(2)}) collective-permute-start(bf16[256,1024]{1,0:T(8,128)(2,1)S(1)} %get-tuple-element.68), channel_id=1, source_target_pairs={{0,1},{1,0},{2,3},{3,2},{4,5},{5,4},{6,7},{7,6},{8,9},{9,8},{10,11... | collective-permute-start | bytes 1572872 | tf_op jit(solution)/shard_map/ppermute | solution.py:598
  42.4 0.4 keep.1
  42.9 1.1 %collective-permute-done.10 = bf16[256,1024]{1,0:T(8,128)(2,1)S(1)} collective-permute-done((bf16[256,1024]{1,0:T(8,128)(2,1)S(1)}, bf16[256,1024]{1,0:T(8,128)(2,1)S(1)}, u32[]{:S(2)}, u32[]{:S(2)}) %collective-permute-start.10) | collective-permute-done | bytes 524320 | tf_op jit(solution)/shard_map/ppermute | solution.py:598
  44.0 1.0 %add_convert_fusion = bf16[256,1024]{1,0:T(8,128)(2,1)} fusion(bf16[256,1024]{1,0:T(8,128)(2,1)S(1)} %collective-permute-done.10, bf16[256,1024]{1,0:T(8,128)(2,1)S(1)} %keep.1), kind=kLoop, calls=%fused_computation | loop fusion | flops 1048576 | bytes 1572864 | tf_op jit(solution)/shard_map/convert_element_type | solution.py:601
  (17 shorter events, 0.0 us)
Async XLA Ops:
  0.0 5.5 %collective-permute-start = (bf16[2,128,1024]{2,1,0:T(8,128)(2,1)}, bf16[2,128,1024]{2,1,0:T(8,128)(2,1)S(1)}, u32[]{:S(2)}, u32[]{:S(2)}) collective-permute-start(bf16[2,128,1024]{2,1,0:T(8,128)(2,1)} %param.18), channel_id=1, source_target_pairs={{0,1},{1,0},{2,3},{3,2},{4,5},{5,4},{6,7},{7,6},{8,9},{9,8},{10,11... | collective-permute-start | bytes 1572872 | tf_op jit(solution)/shard_map/ppermute | solution.py:518
  1.4 4.1 %copy-start.4 = (f32[2048]{0:T(1024)S(1)}, f32[2048]{0:T(1024)}, u32[]{:S(2)}) copy-start(f32[2048]{0:T(1024)} %param.19) | copy-start | bytes 24580
  1.4 4.2 %copy-start.7 = (f32[768]{0:T(1024)S(1)}, f32[768]{0:T(1024)}, u32[]{:S(2)}) copy-start(f32[768]{0:T(1024)} %refs_3_.3) | copy-start | bytes 9220
  1.4 4.2 %copy-start.8 = (f32[768]{0:T(1024)S(1)}, f32[768]{0:T(1024)}, u32[]{:S(2)}) copy-start(f32[768]{0:T(1024)} %refs_4_.3) | copy-start | bytes 9220
  12.4 7.7 %collective-permute-start.2 = (bf16[256,128]{1,0:T(8,128)(2,1)S(1)}, bf16[256,128]{1,0:T(8,128)(2,1)S(1)}, u32[]{:S(2)}, u32[]{:S(2)}) collective-permute-start(bf16[256,128]{1,0:T(8,128)(2,1)S(1)} %get-tuple-element.44), channel_id=1, source_target_pairs={{0,16},{8,24},{16,0},{24,8},{1,17},{9,25},{17,1},{25,9},{2,18},{10... | collective-permute-start | bytes 196616 | tf_op jit(solution)/shard_map/ppermute | solution.py:510
  15.5 4.6 %collective-permute-start.3 = (bf16[256,128]{1,0:T(8,128)(2,1)S(1)}, bf16[256,128]{1,0:T(8,128)(2,1)S(1)}, u32[]{:S(2)}, u32[]{:S(2)}) collective-permute-start(bf16[256,128]{1,0:T(8,128)(2,1)S(1)} %get-tuple-element.45), channel_id=1, source_target_pairs={{0,24},{8,0},{16,8},{24,16},{1,25},{9,1},{17,9},{25,17},{2,26},{10... | collective-permute-start | bytes 196616 | tf_op jit(solution)/shard_map/ppermute | solution.py:510
  16.3 4.5 %collective-permute-start.1 = (bf16[320,128]{1,0:T(8,128)(2,1)S(1)}, bf16[320,128]{1,0:T(8,128)(2,1)S(1)}, u32[]{:S(2)}, u32[]{:S(2)}) collective-permute-start(bf16[320,128]{1,0:T(8,128)(2,1)S(1)} %get-tuple-element.43), channel_id=1, source_target_pairs={{0,8},{8,16},{16,24},{24,0},{1,9},{9,17},{17,25},{25,1},{2,10},{10... | collective-permute-start | bytes 245768 | tf_op jit(solution)/shard_map/ppermute | solution.py:510
  17.0 13.4 %copy-start.2 = (f32[2,6,64,64]{3,2,1,0:T(8,128)S(1)}, f32[2,6,64,64]{3,2,1,0:T(8,128)}, u32[]{:S(2)}) copy-start(f32[2,6,64,64]{3,2,1,0:T(8,128)} %init_ref.1) | copy-start | bytes 589828
  17.0 18.3 %copy-start.3 = (bf16[4,128,128]{2,1,0:T(8,128)(2,1)S(1)}, bf16[4,128,128]{2,1,0:T(8,128)(2,1)}, u32[]{:S(2)}) copy-start(bf16[4,128,128]{2,1,0:T(8,128)(2,1)} %mix_ref.1) | copy-start | bytes 393220
  17.0 18.3 %copy-start.6 = (f32[512]{0:T(512)S(1)}, f32[512]{0:T(512)}, u32[]{:S(2)}) copy-start(f32[512]{0:T(512)} %param.32) | copy-start | bytes 6148
  20.1 15.1 %copy-start.1 = (bf16[256,2048]{1,0:T(8,128)(2,1)S(1)}, bf16[256,2048]{1,0:T(8,128)(2,1)}, u32[]{:S(2)}) copy-start(bf16[256,2048]{1,0:T(8,128)(2,1)} %wp_ref.1) | copy-start | bytes 3145732
  21.4 8.9 %collective-permute-start.4 = (bf16[320,128]{1,0:T(8,128)(2,1)S(1)}, bf16[320,128]{1,0:T(8,128)(2,1)S(1)}, u32[]{:S(2)}, u32[]{:S(2)}) collective-permute-start(bf16[320,128]{1,0:T(8,128)(2,1)S(1)} %get-tuple-element.57), channel_id=1, source_target_pairs={{0,32},{32,64},{64,96},{96,0},{1,33},{33,65},{65,97},{97,1},{2,34}... | collective-permute-start | bytes 245768 | tf_op jit(solution)/shard_map/ppermute | solution.py:510
  23.1 3.5 %collective-permute-start.6 = (bf16[256,128]{1,0:T(8,128)(2,1)S(1)}, bf16[256,128]{1,0:T(8,128)(2,1)S(1)}, u32[]{:S(2)}, u32[]{:S(2)}) collective-permute-start(bf16[256,128]{1,0:T(8,128)(2,1)S(1)} %get-tuple-element.58), channel_id=1, source_target_pairs={{0,96},{32,0},{64,32},{96,64},{1,97},{33,1},{65,33},{97,65},{2,98}... | collective-permute-start | bytes 196616 | tf_op jit(solution)/shard_map/ppermute | solution.py:510
  25.3 5.0 %collective-permute-start.5 = (bf16[256,128]{1,0:T(8,128)(2,1)S(1)}, bf16[256,128]{1,0:T(8,128)(2,1)S(1)}, u32[]{:S(2)}, u32[]{:S(2)}) collective-permute-start(bf16[256,128]{1,0:T(8,128)(2,1)S(1)} %get-tuple-element.58), channel_id=1, source_target_pairs={{0,64},{32,96},{64,0},{96,32},{1,65},{33,97},{65,1},{97,33},{2,66}... | collective-permute-start | bytes 196616 | tf_op jit(solution)/shard_map/ppermute | solution.py:510
  31.5 4.4 %collective-permute-start.7 = (bf16[2,64,128]{2,1,0:T(8,128)(2,1)S(1)}, bf16[2,64,128]{2,1,0:T(8,128)(2,1)S(1)}, u32[]{:S(2)}, u32[]{:S(2)}) collective-permute-start(bf16[2,64,128]{2,1,0:T(8,128)(2,1)S(1)} %get-tuple-element.60), channel_id=1, source_target_pairs={{0,8},{8,16},{16,24},{24,0},{1,9},{9,17},{17,25},{25,1},{2,10},{10... | collective-permute-start | bytes 98312 | tf_op jit(solution)/shard_map/ppermute | solution.py:510
  31.9 4.3 %collective-permute-start.8 = (bf16[2,64,128]{2,1,0:T(8,128)(2,1)S(1)}, bf16[2,64,128]{2,1,0:T(8,128)(2,1)S(1)}, u32[]{:S(2)}, u32[]{:S(2)}) collective-permute-start(bf16[2,64,128]{2,1,0:T(8,128)(2,1)S(1)} %get-tuple-element.61), channel_id=1, source_target_pairs={{0,16},{8,24},{16,0},{24,8},{1,17},{9,25},{17,1},{25,9},{2,18},{10... | collective-permute-start | bytes 98312 | tf_op jit(solution)/shard_map/ppermute | solution.py:510
  34.1 2.8 %collective-permute-start.9 = (bf16[2,64,128]{2,1,0:T(8,128)(2,1)S(1)}, bf16[2,64,128]{2,1,0:T(8,128)(2,1)S(1)}, u32[]{:S(2)}, u32[]{:S(2)}) collective-permute-start(bf16[2,64,128]{2,1,0:T(8,128)(2,1)S(1)} %get-tuple-element.62), channel_id=1, source_target_pairs={{0,24},{8,0},{16,8},{24,16},{1,25},{9,1},{17,9},{25,17},{2,26},{10... | collective-permute-start | bytes 98312 | tf_op jit(solution)/shard_map/ppermute | solution.py:510
  35.2 1.6 %copy-start = (bf16[384,2048]{1,0:T(8,128)(2,1)S(1)}, bf16[384,2048]{1,0:T(8,128)(2,1)}, u32[]{:S(2)}) copy-start(bf16[384,2048]{1,0:T(8,128)(2,1)} %wr_ref.3) | copy-start | bytes 4718596
  35.3 1.6 %copy-start.5 = (f32[768]{0:T(1024)S(1)}, f32[768]{0:T(1024)}, u32[]{:S(2)}) copy-start(f32[768]{0:T(1024)} %hgain_ref.1) | copy-start | bytes 9220
  38.5 5.5 %collective-permute-start.10 = (bf16[256,1024]{1,0:T(8,128)(2,1)S(1)}, bf16[256,1024]{1,0:T(8,128)(2,1)S(1)}, u32[]{:S(2)}, u32[]{:S(2)}) collective-permute-start(bf16[256,1024]{1,0:T(8,128)(2,1)S(1)} %get-tuple-element.68), channel_id=1, source_target_pairs={{0,1},{1,0},{2,3},{3,2},{4,5},{5,4},{6,7},{7,6},{8,9},{9,8},{10,11... | collective-permute-start | bytes 1572872 | tf_op jit(solution)/shard_map/ppermute | solution.py:598

commit v6 on v5

--- a/solution.py
+++ b/solution.py
@@ -132,10 +132,6 @@
     return result
 
 
-GROUPS = ((384, 384), (384, 384), (384, 256))
-WIDE = tuple(sum(group) for group in GROUPS)
-
-
 def fetch(sources, buf, first_row, sems, base):
     copies, at = [], 0
     for i, src in enumerate(sources):
@@ -163,50 +159,48 @@
 
 def own_kernel(*refs):
     token_ref, norm_ref = refs[:2]
-    sources, normed_ref, squares_ref, partials, rest = refs[2:8], refs[8], refs[9], refs[10:13], refs[13]
-    bufs, sems, own_ref, gain_ref, first_sems = refs[14:17], refs[17], refs[18], refs[19], refs[20]
+    sources, normed_ref, squares_ref, partials, rest = refs[2:6], refs[6], refs[7], refs[8:10], refs[10:12]
+    bufs, sems, own_ref, gain_ref, first_sems = refs[12:14], refs[14], refs[15], refs[16], refs[17]
     tp = lax.axis_index("tp")
     early = [
         pltpu.make_async_copy(norm_ref, gain_ref, first_sems.at[0]),
         pltpu.make_async_copy(token_ref, own_ref, first_sems.at[1]),
     ]
-    mine = [fetch(sources[2 * i : 2 * i + 2], bufs[i], tp * 1024, sems, 2 * i) for i in range(3)]
-    others = fetch(sources[:2], rest, (1 - tp) * 1024, sems, 6)
+    mine = [fetch(sources[2 * i : 2 * i + 2], bufs[i], tp * 1024, sems, 2 * i) for i in range(2)]
+    others = [
+        fetch(sources[2 * i : 2 * i + 2], rest[i], (1 - tp) * 1024, sems, 4 + 2 * i) for i in range(2)
+    ]
     begin(early)
     begin(mine[0])
+    pl.delay(400)
+    begin(mine[1])
+    pl.delay(400)
+    begin(others[0])
     finish(early)
-    begin(mine[1])
     own = own_ref[...].astype(f32)
     normed = (own * jnp.where(tp == 0, gain_ref[:, :1024], gain_ref[:, 1024:])).astype(bf16)
     normed_ref[...] = normed
     squares_ref[...] = jnp.broadcast_to(jnp.sum(own * own, axis=1, keepdims=True), (256, 128))
-    for i in range(3):
+    begin(others[1])
+    for i in range(2):
         finish(mine[i])
-        if i == 0:
-            begin(mine[2])
-        if i == 1:
-            begin(others)
-        partials[i][...] = dot(normed, bufs[i][...])
-    finish(others)
+        partials[i][...] = dot(normed_ref[...], bufs[i][...])
+    finish(others[0])
+    finish(others[1])
 
 
 def local_kernel(*refs):
-    other_ref, gain_ref, squares_ref, db_ref, rb_ref = refs[:5]
-    partials, ready, sources = refs[5:8], refs[8], refs[9:13]
+    other_ref, own_ref, gain_ref, squares_ref, db_ref, rb_ref = refs[:6]
+    partials, rest, pool_weight = refs[6:8], refs[8:10], refs[10]
     (
         normed_ref, scale_ref, pool_ref, home_ref, first_ref, second_ref, third_ref,
-        right_ref, solved_ref, v_ref, r_ref, grow_ref, lift_ref,
-    ) = refs[13:26]
-    k_s, d_s, a_s, maps = refs[26:30]
-    bufs, sems = refs[30:32], refs[32]
+        right_ref, solved_ref, v_ref, grow_ref, lift_ref,
+    ) = refs[11:23]
+    k_s, d_s, a_s, maps, pool_buf, sems = refs[23:29]
     tp = lax.axis_index("tp")
     y = lax.axis_index("sp_1")
-    copies = [
-        fetch(sources[2 * i : 2 * i + 2], bufs[i], (1 - tp) * 1024, sems, 2 * i) for i in range(2)
-    ]
-    begin(copies[0])
-    begin(copies[1])
-    rest = (ready,) + tuple(bufs)
+    copy = pltpu.make_async_copy(pool_weight, pool_buf, sems.at[0])
+    copy.start()
     is_first = tp == 0
     other = other_ref[...].astype(f32)
     normed = (other * jnp.where(is_first, gain_ref[:, 1024:], gain_ref[:, :1024])).astype(bf16)
@@ -227,13 +221,16 @@
     rounded = project(0)
     place(k_s, rounded, 0, f32)
     place(d_s, rounded, 384, f32)
+    rounded = project(1)
+    place(a_s, rounded, 0, f32)
+    place(v_ref, rounded, 384, bf16)
 
     def fill(level):
         if level != 1:
             return
-        rounded = project(2)
-        place(r_ref, rounded, 0, bf16)
-        pool = rounded[:, 384:]
+        total = dot(own_ref[...], pool_buf[pl.ds(pl.multiple_of(tp * 1024, 1024), 1024), :])
+        total = total + dot(normed_ref[...], pool_buf[pl.ds(pl.multiple_of((1 - tp) * 1024, 1024), 1024), :])
+        pool = (total * scale_ref[:, :1]).astype(bf16)
         pool_ref[...] = pool
         for s in (0, 1):
             for half in (0, 1):
@@ -262,10 +259,6 @@
         k = k_s[u]
         log_decay = -0.6065306597126334 * jax.nn.sigmoid(db + d_s[u])
         first_stage.append((log_decay, dot(k * k, ones), dot_fine_right(triangle, log_decay)))
-    finish(copies[0])
-    rounded = project(1)
-    place(a_s, rounded, 0, f32)
-    place(v_ref, rounded, 384, bf16)
     second_stage = []
     for u in units:
         h = u % 3
@@ -289,7 +282,7 @@
         right_ref[u] = right
         ends = (jnp.exp(total[127:128]), jnp.exp(centred[127:128]))
         second_stage.append((right, alpha * lift, ends, dot(both(alpha, masks), right, NT)))
-    finish(copies[1])
+    copy.wait()
     lowers, carries = [], []
     for u in units:
         pairs = second_stage[u][3]
@@ -326,16 +319,19 @@
 
 
 def side_kernel(
-    own_ref, other_ref, scale_ref, right_ref, solved_ref, v_ref, r_ref, grow_ref, lift_ref, wg_ref, wq_ref,
+    own_ref, other_ref, scale_ref, right_ref, solved_ref, v_ref, grow_ref, lift_ref, wr_ref, wg_ref, wq_ref,
     reads_ref, local_ref, gate_ref, pgate_ref,
-    buf, sems,
 ):
     tp = lax.axis_index("tp")
-    copies = [
-        pltpu.make_async_copy(wg_ref, buf.at[:, :384], sems.at[0]),
-        pltpu.make_async_copy(wq_ref, buf.at[:, 384:], sems.at[1]),
-    ]
-    begin(copies)
+    scale = scale_ref[:, :1]
+    mine, theirs = pl.multiple_of(tp * 1024, 1024), pl.multiple_of((1 - tp) * 1024, 1024)
+
+    def project(weight):
+        total = dot(own_ref[...], weight[pl.ds(mine, 1024), :])
+        total = total + dot(other_ref[...], weight[pl.ds(theirs, 1024), :])
+        return (total * scale).astype(bf16)
+
+    receptance = project(wr_ref)
     masks = head_masks()
     wide = (
         jnp.concatenate([masks[0], masks[0]], axis=1),
@@ -344,7 +340,8 @@
     inclusive = iota(128, 128, 0) >= iota(128, 128, 1)
     inside, rhos = [], []
     for u in range(UNITS):
-        rho = r_ref[u].astype(f32) * grow_ref[u]
+        s, h = u // 3, u % 3
+        rho = receptance[s * 128 : s * 128 + 128, h * 128 : h * 128 + 128].astype(f32) * grow_ref[u]
         rhos.append(rho * lift_ref[u : u + 1])
         pairs = dot(both(rho, masks), right_ref[u], NT)
         block = lambda j, c: jnp.where(
@@ -355,13 +352,8 @@
         removed = dot(inside[u][0], both(solved_ref[u], wide))
         reads_ref[u] = (rhos[u] - removed[:, :128]).astype(bf16)
         local_ref[u] = dot(inside[u][1], both(v_ref[u], masks)) - removed[:, 128:]
-    scale = scale_ref[:, :1]
-    mine, theirs = pl.multiple_of(tp * 1024, 1024), pl.multiple_of((1 - tp) * 1024, 1024)
-    finish(copies)
-    total = dot(own_ref[...], buf[pl.ds(mine, 1024), :]) + dot(other_ref[...], buf[pl.ds(theirs, 1024), :])
-    rounded = (total * scale).astype(bf16)
-    gate_ref[...] = rounded[:, :384]
-    pgate_ref[...] = rounded[:, 384:]
+    gate_ref[...] = project(wg_ref)
+    pgate_ref[...] = project(wq_ref)
 
 
 def row_kernel(home_ref, first_ref, second_ref, third_ref, after_ref, prefix_ref, next_ref, total_ref, maps):
@@ -518,15 +510,15 @@
     other = lax.ppermute(tokens, "tp", [(0, 1), (1, 0)])
     line = lambda x: x.reshape(1, -1)
     pinned = lambda x: pltpu.with_memory_space_constraint(x, pltpu.HBM)
-    weights = [pinned(w) for w in (w_key, w_decay, w_rate, w_value, w_recept, w_pool)]
+    weights = [pinned(w) for w in (w_key, w_decay, w_rate, w_value)]
     own_normed, squares, *prepared = call(
         own_kernel,
         "own",
-        hbm(8),
+        hbm(6),
         [shape((256, 1024)), shape((256, 128), f32)]
-        + [shape((256, width), f32) for width in WIDE]
-        + [shape((1024, WIDE[0]))],
-        [pltpu.VMEM((1024, width), bf16) for width in WIDE]
+        + [shape((256, 768), f32)] * 2
+        + [shape((1024, 768))] * 2,
+        [pltpu.VMEM((1024, 768), bf16)] * 2
         + [
             pltpu.SemaphoreType.DMA((8,)), pltpu.VMEM((256, 1024), bf16), pltpu.VMEM((1, D), f32),
             pltpu.SemaphoreType.DMA((2,)),
@@ -534,35 +526,35 @@
         20,
         1_000_000_000,
     )(pinned(tokens.reshape(256, 1024)), pinned(line(norm_gain)), *weights)
-    normed, scale, pool, home, m1, m2, m3, right, solved, v, r, grow, lift = call(
+    normed, scale, pool, home, m1, m2, m3, right, solved, v, grow, lift = call(
         local_kernel,
         "local",
-        vmem(9) + hbm(4),
+        vmem(10) + hbm(1),
         [
             shape((256, 1024)), shape((256, 128), f32), shape((256, 256)),
             shape((256, 128)), shape((320, 128)), shape((256, 128)), shape((256, 128)),
             shape((6, 256, 128)), shape((6, 128, 256)), shape((6, 128, 128)),
-            shape((6, 128, 128)), shape((6, 128, 128), f32), shape((6, 128), f32),
+            shape((6, 128, 128), f32), shape((6, 128), f32),
         ],
         [pltpu.VMEM((6, 128, 128), f32)] * 3
         + [pltpu.VMEM((4, 256, 128), bf16)]
-        + [pltpu.VMEM((1024, width), bf16) for width in WIDE[1:]]
-        + [pltpu.SemaphoreType.DMA((4,))],
+        + [pltpu.VMEM((D, 256), bf16), pltpu.SemaphoreType.DMA((1,))],
         24,
         3_000_000_000,
     )(
-        other.reshape(256, 1024), line(norm_gain), squares, decay_base, rate_base, *prepared, *weights[2:]
+        other.reshape(256, 1024), own_normed, line(norm_gain), squares, decay_base, rate_base, *prepared,
+        pinned(w_pool),
     )
     r1, r2, r3 = around((m1, m2, m3), "sp_1")
     reads, local, gate, pgate = call(
         side_kernel,
         "side",
-        vmem(9) + hbm(2),
+        vmem(11),
         [shape((6, 128, 128)), shape((6, 128, 128), f32), shape((256, 384)), shape((256, 256))],
-        [pltpu.VMEM((D, 640), bf16), pltpu.SemaphoreType.DMA((2,))],
+        [],
         16,
         1_000_000_000,
-    )(own_normed, normed, scale, right, solved, v, r, grow, lift, pinned(w_gate_rec), pinned(w_gate_pool))
+    )(own_normed, normed, scale, right, solved, v, grow, lift, w_recept, w_gate_rec, w_gate_pool)
     prefix, onward, total = call(
         row_kernel,
         "row",

time: 45.2 us -> 43.5 us (0.962)
  Pallas kernels: 18.6 us -> 16.3 us
    pallas_call x3, Pallas kernels: 14.1 us -> 11.8 us  [the longest x1 6.03 us: shards(): call(local_kernel, 'local', vmem(10) + hbm(1), [shape((256, 1024)), shape...]
  transfers between devices with their start and end apart: 11 -> 11, of which waited for: 6 -> 6; matrix products, arithmetic and copies ran while one was open for 0% -> 0% of each run, Pallas kernels for 19% -> 16%
where the time goes in v6:
time: 43.5 us; the launch traced here: 43.4 us
  starting transfers between devices  18.9 us (43%)
  Pallas kernels  16.3 us (37%)
  waiting for transfers between devices  6.84 us (16%)
  other arithmetic  0.99 us (2%)
    ppermute x9, starting transfers between devices, around(): lax.ppermute(part, axis, [(i, i + step & 3) for i in range(4)])  13.4 us
    pallas_call x1, Pallas kernels, shards(): call(local_kernel, 'local', vmem(10) + hbm(1), [shape((256, 1024)), shape...  6.03 us
    ppermute x9, waiting for transfers between devices, around(): lax.ppermute(part, axis, [(i, i + step & 3) for i in range(4)])  5.74 us
    ppermute x1, starting transfers between devices, shards(): arrived = lax.ppermute(send, 'tp', [(0, 1), (1, 0)])  4.12 us
    pallas_call x1, Pallas kernels, shards(): call(own_kernel, 'own', hbm(6), [shape((256, 1024)), shape((256, 128), f3...  3.28 us
    pallas_call x1, Pallas kernels, shards(): call(side_kernel, 'side', vmem(11), [shape((6, 128, 128)), shape((6, 128,...  2.47 us
    pallas_call x1, Pallas kernels, shards(): call(final_kernel, 'final', vmem(10), [shape((256, 1024)), shape((256, 38...  1.66 us
    ppermute x1, starting transfers between devices, shards(): other = lax.ppermute(tokens, 'tp', [(0, 1), (1, 0)])  1.38 us
  transfers between devices with their start and end apart: 11, of which 6 were waited for; matrix products, arithmetic and copies ran while one was open for 0% of the time, Pallas kernels for 16%

profile of v6, /device:TPU:1, one launch (start us, length us, event | category | flops | bytes accessed | tf_op | source)
XLA Modules:
  0.0 43.4 jit_solution(3571369087238609233)
XLA Ops:
  0.0 1.4 %collective-permute-start = (bf16[2,128,1024]{2,1,0:T(8,128)(2,1)}, bf16[2,128,1024]{2,1,0:T(8,128)(2,1)S(1)}, u32[]{:S(2)}, u32[]{:S(2)}) collective-permute-start(bf16[2,128,1024]{2,1,0:T(8,128)(2,1)} %param.18), channel_id=1, source_target_pairs={{0,1},{1,0},{2,3},{3,2},{4,5},{5,4},{6,7},{7,6},{8,9},{9,8},{10,11... | collective-permute-start | bytes 1572872 | tf_op jit(solution)/shard_map/ppermute | solution.py:510
  1.4 3.3 %own.1 = (bf16[256,1024]{1,0:T(8,128)(2,1)S(1)}, f32[256,128]{1,0:T(8,128)S(1)}, f32[256,768]{1,0:T(8,128)S(1)}, f32[256,768]{1,0:T(8,128)S(1)}, bf16[1024,768]{...) custom-call(bf16[256,1024]{1,0:T(8,128)(2,1)} %bitcast.9, f32[1,2048]{1,0:T(1,128)} %bitcast.5, bf16[2048,384]{1,0:T(8,128)(2,1)} %refs_2_.1, ...), custom_call_target="tpu_custom_call" | custom-call | flops 1000000000 | tf_op jit(solution)/shard_map/own/pallas_call | solution.py:514
  4.7 0.0 copy-start.1
  4.8 6.0 %local.1 = (bf16[256,1024]{1,0:T(8,128)(2,1)S(1)}, f32[256,128]{1,0:T(8,128)S(1)}, bf16[256,256]{1,0:T(8,128)(2,1)S(1)}, bf16[256,128]{1,0:T(8,128)(2,1)S(1)}, b...) custom-call(bf16[256,1024]{1,0:T(8,128)(2,1)S(1)} %bitcast.8, ...), custom_call_target="tpu_custom_call" | custom-call | flops 3000000000 | tf_op jit(solution)/shard_map/local/pallas_call | solution.py:529
  10.8 3.1 %collective-permute-start.2 = (bf16[256,128]{1,0:T(8,128)(2,1)S(1)}, bf16[256,128]{1,0:T(8,128)(2,1)S(1)}, u32[]{:S(2)}, u32[]{:S(2)}) collective-permute-start(bf16[256,128]{1,0:T(8,128)(2,1)S(1)} %get-tuple-element.44), channel_id=1, source_target_pairs={{0,16},{8,24},{16,0},{24,8},{1,17},{9,25},{17,1},{25,9},{2,18},{10... | collective-permute-start | bytes 196616 | tf_op jit(solution)/shard_map/ppermute | solution.py:502
  13.9 0.8 %collective-permute-start.3 = (bf16[256,128]{1,0:T(8,128)(2,1)S(1)}, bf16[256,128]{1,0:T(8,128)(2,1)S(1)}, u32[]{:S(2)}, u32[]{:S(2)}) collective-permute-start(bf16[256,128]{1,0:T(8,128)(2,1)S(1)} %get-tuple-element.45), channel_id=1, source_target_pairs={{0,24},{8,0},{16,8},{24,16},{1,25},{9,1},{17,9},{25,17},{2,26},{10... | collective-permute-start | bytes 196616 | tf_op jit(solution)/shard_map/ppermute | solution.py:502
  14.7 0.7 %collective-permute-start.1 = (bf16[320,128]{1,0:T(8,128)(2,1)S(1)}, bf16[320,128]{1,0:T(8,128)(2,1)S(1)}, u32[]{:S(2)}, u32[]{:S(2)}) collective-permute-start(bf16[320,128]{1,0:T(8,128)(2,1)S(1)} %get-tuple-element.43), channel_id=1, source_target_pairs={{0,8},{8,16},{16,24},{24,0},{1,9},{9,17},{17,25},{25,1},{2,10},{10... | collective-permute-start | bytes 245768 | tf_op jit(solution)/shard_map/ppermute | solution.py:502
  15.4 0.0 copy-start.6
  15.4 0.0 copy-start.9
  15.4 2.5 %side.1 = (bf16[6,128,128]{2,1,0:T(8,128)(2,1)S(1)}, f32[6,128,128]{2,1,0:T(8,128)S(1)}, bf16[256,384]{1,0:T(8,128)(2,1)S(1)}, bf16[256,256]{1,0:T(8,128)(2,1)S(1)}) custom-call(bf16[256,1024]{1,0:T(8,128)(2,1)S(1)} %get-tuple-element.36.refs_1_.own_ref, bf16[256,1024]{1,0:T(8,128)(2,1)S(1)} %get-tuple-element.46.other_ref, ...), custom_call_target="tpu_custom_call" | custom-call | flops 1000000000 | tf_op jit(solution)/shard_map/side/pallas_call | solution.py:549
  17.9 0.0 collective-permute-done.3.third_ref
  17.9 1.2 %collective-permute-done.1.first_ref.beside_ref = bf16[320,128]{1,0:T(8,128)(2,1)S(1)} collective-permute-done((bf16[320,128]{1,0:T(8,128)(2,1)S(1)}, bf16[320,128]{1,0:T(8,128)(2,1)S(1)}, u32[]{:S(2)}, u32[]{:S(2)}) %collective-permute-start.1) | collective-permute-done | bytes 81952 | tf_op jit(solution)/shard_map/ppermute | solution.py:502
  19.2 0.6 %row.1 = (f32[3,2,128,128]{3,2,1,0:T(8,128)S(1)}, bf16[320,128]{1,0:T(8,128)(2,1)S(1)}, bf16[256,128]{1,0:T(8,128)(2,1)S(1)}) custom-call(bf16[256,128]{1,0:T(8,128)(2,1)S(1)} %get-tuple-element.42.home_ref, bf16[320,128]{1,0:T(8,128)(2,1)S(1)} %collective-permute-done.1.first_ref.beside_ref, bf16[256,128]{1,0:T(8,128)(2,1)S(1)} %collective-permute-done.2.second_ref, ...), custom_call_target="tpu_custom_call" | custom-call | flops 100000000 | tf_op jit(solution)/shard_map/row/pallas_call | solution.py:558
  19.8 1.7 %collective-permute-start.4 = (bf16[320,128]{1,0:T(8,128)(2,1)S(1)}, bf16[320,128]{1,0:T(8,128)(2,1)S(1)}, u32[]{:S(2)}, u32[]{:S(2)}) collective-permute-start(bf16[320,128]{1,0:T(8,128)(2,1)S(1)} %get-tuple-element.55), channel_id=1, source_target_pairs={{0,32},{32,64},{64,96},{96,0},{1,33},{33,65},{65,97},{97,1},{2,34}... | collective-permute-start | bytes 245768 | tf_op jit(solution)/shard_map/ppermute | solution.py:502
  21.5 2.2 %collective-permute-start.6 = (bf16[256,128]{1,0:T(8,128)(2,1)S(1)}, bf16[256,128]{1,0:T(8,128)(2,1)S(1)}, u32[]{:S(2)}, u32[]{:S(2)}) collective-permute-start(bf16[256,128]{1,0:T(8,128)(2,1)S(1)} %get-tuple-element.56), channel_id=1, source_target_pairs={{0,96},{32,0},{64,32},{96,64},{1,97},{33,1},{65,33},{97,65},{2,98}... | collective-permute-start | bytes 196616 | tf_op jit(solution)/shard_map/ppermute | solution.py:502
  23.7 1.2 %collective-permute-start.5 = (bf16[256,128]{1,0:T(8,128)(2,1)S(1)}, bf16[256,128]{1,0:T(8,128)(2,1)S(1)}, u32[]{:S(2)}, u32[]{:S(2)}) collective-permute-start(bf16[256,128]{1,0:T(8,128)(2,1)S(1)} %get-tuple-element.56), channel_id=1, source_target_pairs={{0,64},{32,96},{64,0},{96,32},{1,65},{33,97},{65,1},{97,33},{2,66}... | collective-permute-start | bytes 196616 | tf_op jit(solution)/shard_map/ppermute | solution.py:502
  25.0 0.1 collective-permute-done.6.third_ref
  25.1 3.7 %collective-permute-done.5.second_ref = bf16[256,128]{1,0:T(8,128)(2,1)S(1)} collective-permute-done((bf16[256,128]{1,0:T(8,128)(2,1)S(1)}, bf16[256,128]{1,0:T(8,128)(2,1)S(1)}, u32[]{:S(2)}, u32[]{:S(2)}) %collective-permute-start.5) | collective-permute-done | bytes 65568 | tf_op jit(solution)/shard_map/ppermute | solution.py:502
  28.8 1.2 %column.1 = (bf16[2,64,128]{2,1,0:T(8,128)(2,1)S(1)}, bf16[2,64,128]{2,1,0:T(8,128)(2,1)S(1)}, bf16[2,64,128]{2,1,0:T(8,128)(2,1)S(1)}, bf16[2,64,128]{2,1,0:T(8,128)(2,1)S(1)}) custom-call(f32[3,2,128,128]{3,2,1,0:T(8,128)S(1)} %get-tuple-element.54.prefix_ref, bf16[320,128]{1,0:T(8,128)(2,1)S(1)} %collective-permute-done.4.first_ref.above_ref, ...), custom_call_target="tpu_custom_call" | custom-call | flops 100000000 | tf_op jit(solution)/shard_map/column/pallas_call | solution.py:568
  29.9 0.3 collective-permute-start.7
  30.3 1.9 %collective-permute-start.8 = (bf16[2,64,128]{2,1,0:T(8,128)(2,1)S(1)}, bf16[2,64,128]{2,1,0:T(8,128)(2,1)S(1)}, u32[]{:S(2)}, u32[]{:S(2)}) collective-permute-start(bf16[2,64,128]{2,1,0:T(8,128)(2,1)S(1)} %get-tuple-element.59), channel_id=1, source_target_pairs={{0,16},{8,24},{16,0},{24,8},{1,17},{9,25},{17,1},{25,9},{2,18},{10... | collective-permute-start | bytes 98312 | tf_op jit(solution)/shard_map/ppermute | solution.py:502
  32.2 1.4 %collective-permute-start.9 = (bf16[2,64,128]{2,1,0:T(8,128)(2,1)S(1)}, bf16[2,64,128]{2,1,0:T(8,128)(2,1)S(1)}, u32[]{:S(2)}, u32[]{:S(2)}) collective-permute-start(bf16[2,64,128]{2,1,0:T(8,128)(2,1)S(1)} %get-tuple-element.60), channel_id=1, source_target_pairs={{0,24},{8,0},{16,8},{24,16},{1,25},{9,1},{17,9},{25,17},{2,26},{10... | collective-permute-start | bytes 98312 | tf_op jit(solution)/shard_map/ppermute | solution.py:502
  33.6 0.0 copy-start.8
  33.7 0.6 %pool.1.part_ref = f32[256,2048]{1,0:T(8,128)S(1)} custom-call(bf16[256,256]{1,0:T(8,128)(2,1)S(1)} %get-tuple-element.64.pool_ref, bf16[320,128]{1,0:T(8,128)(2,1)S(1)} %collective-permute-done.1.first_ref.beside_ref, bf16[320,128]{1,0:T(8,128)(2,1)S(1)} %collective-permute-done.4.first_ref.above_ref, ...), custom_call_target="tpu_custom_call" | custom-call | flops 300000000 | tf_op jit(solution)/shard_map/pool/pallas_call | solution.py:578
  34.3 0.2 collective-permute-done.8.two_ref
  34.5 0.4 %collective-permute-done.9.three_ref = bf16[2,64,128]{2,1,0:T(8,128)(2,1)S(1)} collective-permute-done((bf16[2,64,128]{2,1,0:T(8,128)(2,1)S(1)}, bf16[2,64,128]{2,1,0:T(8,128)(2,1)S(1)}, u32[]{:S(2)}, u32[]{:S(2)}) %collective-permute-start.9) | collective-permute-done | bytes 32800 | tf_op jit(solution)/shard_map/ppermute | solution.py:502
  35.0 0.1 copy-done
  35.0 1.7 %final.1 = (bf16[256,1024]{1,0:T(8,128)(2,1)S(1)}, bf16[256,384]{1,0:T(8,128)(2,1)S(1)}) custom-call(bf16[2,64,128]{2,1,0:T(8,128)(2,1)S(1)} %get-tuple-element.57.home_ref, bf16[2,64,128]{2,1,0:T(8,128)(2,1)S(1)} %collective-permute-done.7.one_ref, bf16[2,64,128]{2,1,0:T(8,128)(2,1)S(1)} %collective-permute-done.8.two_ref, ...), custom_call_target="tpu_custom_call" | custom-call | flops 1000000000 | tf_op jit(solution)/shard_map/final/pallas_call | solution.py:581
  36.7 4.1 %collective-permute-start.10 = (bf16[256,1024]{1,0:T(8,128)(2,1)S(1)}, bf16[256,1024]{1,0:T(8,128)(2,1)S(1)}, u32[]{:S(2)}, u32[]{:S(2)}) collective-permute-start(bf16[256,1024]{1,0:T(8,128)(2,1)S(1)} %get-tuple-element.66), channel_id=1, source_target_pairs={{0,1},{1,0},{2,3},{3,2},{4,5},{5,4},{6,7},{7,6},{8,9},{9,8},{10,11... | collective-permute-start | bytes 1572872 | tf_op jit(solution)/shard_map/ppermute | solution.py:590
  40.8 0.4 %keep.1 = bf16[256,1024]{1,0:T(8,128)(2,1)S(1)} custom-call(bf16[256,384]{1,0:T(8,128)(2,1)S(1)} %get-tuple-element.65.rec_ref, f32[256,2048]{1,0:T(8,128)S(1)} %pool.1.part_ref, bf16[384,2048]{1,0:T(8,128)(2,1)S(1)} %copy-done), custom_call_target="tpu_custom_call" | custom-call | flops 300000000 | tf_op jit(solution)/shard_map/keep/pallas_call | solution.py:591
  41.3 1.1 %collective-permute-done.10 = bf16[256,1024]{1,0:T(8,128)(2,1)S(1)} collective-permute-done((bf16[256,1024]{1,0:T(8,128)(2,1)S(1)}, bf16[256,1024]{1,0:T(8,128)(2,1)S(1)}, u32[]{:S(2)}, u32[]{:S(2)}) %collective-permute-start.10) | collective-permute-done | bytes 524320 | tf_op jit(solution)/shard_map/ppermute | solution.py:590
  42.4 1.0 %add_convert_fusion = bf16[256,1024]{1,0:T(8,128)(2,1)} fusion(bf16[256,1024]{1,0:T(8,128)(2,1)S(1)} %collective-permute-done.10, bf16[256,1024]{1,0:T(8,128)(2,1)S(1)} %keep.1), kind=kLoop, calls=%fused_computation | loop fusion | flops 1048576 | bytes 1572864 | tf_op jit(solution)/shard_map/convert_element_type | solution.py:593
  (23 shorter events, 0.1 us)
Async XLA Ops:
  0.0 4.7 %collective-permute-start = (bf16[2,128,1024]{2,1,0:T(8,128)(2,1)}, bf16[2,128,1024]{2,1,0:T(8,128)(2,1)S(1)}, u32[]{:S(2)}, u32[]{:S(2)}) collective-permute-start(bf16[2,128,1024]{2,1,0:T(8,128)(2,1)} %param.18), channel_id=1, source_target_pairs={{0,1},{1,0},{2,3},{3,2},{4,5},{5,4},{6,7},{7,6},{8,9},{9,8},{10,11... | collective-permute-start | bytes 1572872 | tf_op jit(solution)/shard_map/ppermute | solution.py:510
  1.4 3.3 %copy-start.7 = (f32[2048]{0:T(1024)S(1)}, f32[2048]{0:T(1024)}, u32[]{:S(2)}) copy-start(f32[2048]{0:T(1024)} %param.19) | copy-start | bytes 24580
  1.4 3.3 %copy-start.10 = (f32[768]{0:T(1024)S(1)}, f32[768]{0:T(1024)}, u32[]{:S(2)}) copy-start(f32[768]{0:T(1024)} %refs_4_.3) | copy-start | bytes 9220
  1.4 3.3 %copy-start.11 = (f32[768]{0:T(1024)S(1)}, f32[768]{0:T(1024)}, u32[]{:S(2)}) copy-start(f32[768]{0:T(1024)} %refs_5_.3) | copy-start | bytes 9220
  4.7 10.7 %copy-start.1 = (bf16[2048,384]{1,0:T(8,128)(2,1)S(1)}, bf16[2048,384]{1,0:T(8,128)(2,1)}, u32[]{:S(2)}) copy-start(bf16[2048,384]{1,0:T(8,128)(2,1)} %wr_ref.3) | copy-start | bytes 4718596
  4.7 10.6 %copy-start.2 = (bf16[2048,384]{1,0:T(8,128)(2,1)S(1)}, bf16[2048,384]{1,0:T(8,128)(2,1)}, u32[]{:S(2)}) copy-start(bf16[2048,384]{1,0:T(8,128)(2,1)} %wg_ref.1) | copy-start | bytes 4718596
  4.7 10.6 %copy-start.4 = (bf16[2048,256]{1,0:T(8,128)(2,1)S(1)}, bf16[2048,256]{1,0:T(8,128)(2,1)}, u32[]{:S(2)}) copy-start(bf16[2048,256]{1,0:T(8,128)(2,1)} %wq_ref.1) | copy-start | bytes 3145732
  10.8 7.1 %collective-permute-start.2 = (bf16[256,128]{1,0:T(8,128)(2,1)S(1)}, bf16[256,128]{1,0:T(8,128)(2,1)S(1)}, u32[]{:S(2)}, u32[]{:S(2)}) collective-permute-start(bf16[256,128]{1,0:T(8,128)(2,1)S(1)} %get-tuple-element.44), channel_id=1, source_target_pairs={{0,16},{8,24},{16,0},{24,8},{1,17},{9,25},{17,1},{25,9},{2,18},{10... | collective-permute-start | bytes 196616 | tf_op jit(solution)/shard_map/ppermute | solution.py:502
  13.9 4.0 %collective-permute-start.3 = (bf16[256,128]{1,0:T(8,128)(2,1)S(1)}, bf16[256,128]{1,0:T(8,128)(2,1)S(1)}, u32[]{:S(2)}, u32[]{:S(2)}) collective-permute-start(bf16[256,128]{1,0:T(8,128)(2,1)S(1)} %get-tuple-element.45), channel_id=1, source_target_pairs={{0,24},{8,0},{16,8},{24,16},{1,25},{9,1},{17,9},{25,17},{2,26},{10... | collective-permute-start | bytes 196616 | tf_op jit(solution)/shard_map/ppermute | solution.py:502
  14.7 4.5 %collective-permute-start.1 = (bf16[320,128]{1,0:T(8,128)(2,1)S(1)}, bf16[320,128]{1,0:T(8,128)(2,1)S(1)}, u32[]{:S(2)}, u32[]{:S(2)}) collective-permute-start(bf16[320,128]{1,0:T(8,128)(2,1)S(1)} %get-tuple-element.43), channel_id=1, source_target_pairs={{0,8},{8,16},{16,24},{24,0},{1,9},{9,17},{17,25},{25,1},{2,10},{10... | collective-permute-start | bytes 245768 | tf_op jit(solution)/shard_map/ppermute | solution.py:502
  15.4 13.4 %copy-start.5 = (f32[2,6,64,64]{3,2,1,0:T(8,128)S(1)}, f32[2,6,64,64]{3,2,1,0:T(8,128)}, u32[]{:S(2)}) copy-start(f32[2,6,64,64]{3,2,1,0:T(8,128)} %init_ref.1) | copy-start | bytes 589828
  15.4 18.2 %copy-start.6 = (bf16[4,128,128]{2,1,0:T(8,128)(2,1)S(1)}, bf16[4,128,128]{2,1,0:T(8,128)(2,1)}, u32[]{:S(2)}) copy-start(bf16[4,128,128]{2,1,0:T(8,128)(2,1)} %mix_ref.1) | copy-start | bytes 393220
  15.4 18.2 %copy-start.9 = (f32[512]{0:T(512)S(1)}, f32[512]{0:T(512)}, u32[]{:S(2)}) copy-start(f32[512]{0:T(512)} %param.32) | copy-start | bytes 6148
  17.9 15.7 %copy-start.3 = (bf16[256,2048]{1,0:T(8,128)(2,1)S(1)}, bf16[256,2048]{1,0:T(8,128)(2,1)}, u32[]{:S(2)}) copy-start(bf16[256,2048]{1,0:T(8,128)(2,1)} %wp_ref.1) | copy-start | bytes 3145732
  19.8 8.9 %collective-permute-start.4 = (bf16[320,128]{1,0:T(8,128)(2,1)S(1)}, bf16[320,128]{1,0:T(8,128)(2,1)S(1)}, u32[]{:S(2)}, u32[]{:S(2)}) collective-permute-start(bf16[320,128]{1,0:T(8,128)(2,1)S(1)} %get-tuple-element.55), channel_id=1, source_target_pairs={{0,32},{32,64},{64,96},{96,0},{1,33},{33,65},{65,97},{97,1},{2,34}... | collective-permute-start | bytes 245768 | tf_op jit(solution)/shard_map/ppermute | solution.py:502
  21.5 3.5 %collective-permute-start.6 = (bf16[256,128]{1,0:T(8,128)(2,1)S(1)}, bf16[256,128]{1,0:T(8,128)(2,1)S(1)}, u32[]{:S(2)}, u32[]{:S(2)}) collective-permute-start(bf16[256,128]{1,0:T(8,128)(2,1)S(1)} %get-tuple-element.56), channel_id=1, source_target_pairs={{0,96},{32,0},{64,32},{96,64},{1,97},{33,1},{65,33},{97,65},{2,98}... | collective-permute-start | bytes 196616 | tf_op jit(solution)/shard_map/ppermute | solution.py:502
  23.7 5.0 %collective-permute-start.5 = (bf16[256,128]{1,0:T(8,128)(2,1)S(1)}, bf16[256,128]{1,0:T(8,128)(2,1)S(1)}, u32[]{:S(2)}, u32[]{:S(2)}) collective-permute-start(bf16[256,128]{1,0:T(8,128)(2,1)S(1)} %get-tuple-element.56), channel_id=1, source_target_pairs={{0,64},{32,96},{64,0},{96,32},{1,65},{33,97},{65,1},{97,33},{2,66}... | collective-permute-start | bytes 196616 | tf_op jit(solution)/shard_map/ppermute | solution.py:502
  29.9 4.4 %collective-permute-start.7 = (bf16[2,64,128]{2,1,0:T(8,128)(2,1)S(1)}, bf16[2,64,128]{2,1,0:T(8,128)(2,1)S(1)}, u32[]{:S(2)}, u32[]{:S(2)}) collective-permute-start(bf16[2,64,128]{2,1,0:T(8,128)(2,1)S(1)} %get-tuple-element.58), channel_id=1, source_target_pairs={{0,8},{8,16},{16,24},{24,0},{1,9},{9,17},{17,25},{25,1},{2,10},{10... | collective-permute-start | bytes 98312 | tf_op jit(solution)/shard_map/ppermute | solution.py:502
  30.3 4.3 %collective-permute-start.8 = (bf16[2,64,128]{2,1,0:T(8,128)(2,1)S(1)}, bf16[2,64,128]{2,1,0:T(8,128)(2,1)S(1)}, u32[]{:S(2)}, u32[]{:S(2)}) collective-permute-start(bf16[2,64,128]{2,1,0:T(8,128)(2,1)S(1)} %get-tuple-element.59), channel_id=1, source_target_pairs={{0,16},{8,24},{16,0},{24,8},{1,17},{9,25},{17,1},{25,9},{2,18},{10... | collective-permute-start | bytes 98312 | tf_op jit(solution)/shard_map/ppermute | solution.py:502
  32.2 2.8 %collective-permute-start.9 = (bf16[2,64,128]{2,1,0:T(8,128)(2,1)S(1)}, bf16[2,64,128]{2,1,0:T(8,128)(2,1)S(1)}, u32[]{:S(2)}, u32[]{:S(2)}) collective-permute-start(bf16[2,64,128]{2,1,0:T(8,128)(2,1)S(1)} %get-tuple-element.60), channel_id=1, source_target_pairs={{0,24},{8,0},{16,8},{24,16},{1,25},{9,1},{17,9},{25,17},{2,26},{10... | collective-permute-start | bytes 98312 | tf_op jit(solution)/shard_map/ppermute | solution.py:502
  33.6 1.4 %copy-start = (bf16[384,2048]{1,0:T(8,128)(2,1)S(1)}, bf16[384,2048]{1,0:T(8,128)(2,1)}, u32[]{:S(2)}) copy-start(bf16[384,2048]{1,0:T(8,128)(2,1)} %wr_ref.5) | copy-start | bytes 4718596
  33.6 1.4 %copy-start.8 = (f32[768]{0:T(1024)S(1)}, f32[768]{0:T(1024)}, u32[]{:S(2)}) copy-start(f32[768]{0:T(1024)} %hgain_ref.1) | copy-start | bytes 9220
  36.7 5.7 %collective-permute-start.10 = (bf16[256,1024]{1,0:T(8,128)(2,1)S(1)}, bf16[256,1024]{1,0:T(8,128)(2,1)S(1)}, u32[]{:S(2)}, u32[]{:S(2)}) collective-permute-start(bf16[256,1024]{1,0:T(8,128)(2,1)S(1)} %get-tuple-element.66), channel_id=1, source_target_pairs={{0,1},{1,0},{2,3},{3,2},{4,5},{5,4},{6,7},{7,6},{8,9},{9,8},{10,11... | collective-permute-start | bytes 1572872 | tf_op jit(solution)/shard_map/ppermute | solution.py:590

commit v7 on v6

--- a/solution.py
+++ b/solution.py
@@ -159,17 +159,17 @@
 
 def own_kernel(*refs):
     token_ref, norm_ref = refs[:2]
-    sources, normed_ref, squares_ref, partials, rest = refs[2:6], refs[6], refs[7], refs[8:10], refs[10:12]
-    bufs, sems, own_ref, gain_ref, first_sems = refs[12:14], refs[14], refs[15], refs[16], refs[17]
+    sources, normed_ref, squares_ref, partial_ref, rest_ref = refs[2:6], *refs[6:10]
+    buf, sems, own_ref, gain_ref, first_sems = refs[10:15]
     tp = lax.axis_index("tp")
     early = [
         pltpu.make_async_copy(norm_ref, gain_ref, first_sems.at[0]),
         pltpu.make_async_copy(token_ref, own_ref, first_sems.at[1]),
     ]
-    mine = [fetch(sources[2 * i : 2 * i + 2], bufs[i], tp * 1024, sems, 2 * i) for i in range(2)]
-    others = [
-        fetch(sources[2 * i : 2 * i + 2], rest[i], (1 - tp) * 1024, sems, 4 + 2 * i) for i in range(2)
-    ]
+    mine = fetch(sources, buf, tp * 1024, sems, 0)
+    others = fetch(sources, rest_ref, (1 - tp) * 1024, sems, 4)
+    mine = (mine[:2], mine[2:])
+    others = (others[:2], others[2:])
     begin(early)
     begin(mine[0])
     pl.delay(400)
@@ -184,23 +184,23 @@
     begin(others[1])
     for i in range(2):
         finish(mine[i])
-        partials[i][...] = dot(normed_ref[...], bufs[i][...])
+        cols = slice(768 * i, 768 * i + 768)
+        partial_ref[:, cols] = dot(normed_ref[...], buf[:, cols])
     finish(others[0])
     finish(others[1])
 
 
 def local_kernel(*refs):
     other_ref, own_ref, gain_ref, squares_ref, db_ref, rb_ref = refs[:6]
-    partials, rest, pool_weight = refs[6:8], refs[8:10], refs[10]
+    partial_ref, rest_ref, pool_weight = refs[6:9]
     (
         normed_ref, scale_ref, pool_ref, home_ref, first_ref, second_ref, third_ref,
         right_ref, solved_ref, v_ref, grow_ref, lift_ref,
-    ) = refs[11:23]
-    k_s, d_s, a_s, maps, pool_buf, sems = refs[23:29]
+    ) = refs[9:21]
+    k_s, d_s, a_s, maps, pool_buf, sems = refs[21:27]
     tp = lax.axis_index("tp")
     y = lax.axis_index("sp_1")
-    copy = pltpu.make_async_copy(pool_weight, pool_buf, sems.at[0])
-    copy.start()
+    pool_buf = pool_weight
     is_first = tp == 0
     other = other_ref[...].astype(f32)
     normed = (other * jnp.where(is_first, gain_ref[:, 1024:], gain_ref[:, :1024])).astype(bf16)
@@ -209,33 +209,34 @@
     scale = lax.rsqrt(squares * (1.0 / D) + 0.25)
     scale_ref[...] = jnp.broadcast_to(scale, (256, 128))
 
-    def project(i):
-        total = partials[i][...] + dot(normed_ref[...], rest[i][...])
-        return (total * scale_ref[:, :1]).astype(bf16)
-
-    def place(dest, rounded, at, kind):
-        for u in range(UNITS):
-            s, h = u // 3, u % 3
-            dest[u] = rounded[s * 128 : s * 128 + 128, at + h * 128 : at + h * 128 + 128].astype(kind)
-
-    rounded = project(0)
-    place(k_s, rounded, 0, f32)
-    place(d_s, rounded, 384, f32)
-    rounded = project(1)
-    place(a_s, rounded, 0, f32)
-    place(v_ref, rounded, 384, bf16)
+    def project(rows, cols):
+        total = partial_ref[rows, cols] + dot(normed_ref[rows], rest_ref[:, cols])
+        return (total * scale_ref[rows, :1]).astype(bf16)
+
+    rounded = project(slice(0, 256), slice(0, 1152))
+    for u in range(UNITS):
+        s, h = u // 3, u % 3
+        for i, dest in enumerate((k_s, d_s, a_s)):
+            at = 384 * i + h * 128
+            dest[u] = rounded[s * 128 : s * 128 + 128, at : at + 128].astype(f32)
 
     def fill(level):
-        if level != 1:
+        if level > 4:
             return
-        total = dot(own_ref[...], pool_buf[pl.ds(pl.multiple_of(tp * 1024, 1024), 1024), :])
-        total = total + dot(normed_ref[...], pool_buf[pl.ds(pl.multiple_of((1 - tp) * 1024, 1024), 1024), :])
-        pool = (total * scale_ref[:, :1]).astype(bf16)
-        pool_ref[...] = pool
-        for s in (0, 1):
-            for half in (0, 1):
-                at = 256 + (2 * s + half) * 16
-                first_ref[at : at + 16] = pool[s * 128 + 112 : s * 128 + 128, half * 128 : half * 128 + 128]
+        s = (level - 1) & 1
+        rows = slice(s * 128, s * 128 + 128)
+        if level <= 2:
+            value = project(rows, slice(1152, 1536))
+            for h in range(3):
+                v_ref[3 * s + h] = value[:, h * 128 : h * 128 + 128]
+            return
+        total = dot(own_ref[rows], pool_buf[pl.ds(pl.multiple_of(tp * 1024, 1024), 1024), :])
+        total = total + dot(normed_ref[rows], pool_buf[pl.ds(pl.multiple_of((1 - tp) * 1024, 1024), 1024), :])
+        pool = (total * scale_ref[rows, :1]).astype(bf16)
+        pool_ref[rows] = pool
+        for half in (0, 1):
+            at = 256 + (2 * s + half) * 16
+            first_ref[at : at + 16] = pool[112:128, half * 128 : half * 128 + 128]
 
     masks = head_masks()
     n = SPAN
@@ -282,7 +283,6 @@
         right_ref[u] = right
         ends = (jnp.exp(total[127:128]), jnp.exp(centred[127:128]))
         second_stage.append((right, alpha * lift, ends, dot(both(alpha, masks), right, NT)))
-    copy.wait()
     lowers, carries = [], []
     for u in units:
         pairs = second_stage[u][3]
@@ -516,9 +516,8 @@
         "own",
         hbm(6),
         [shape((256, 1024)), shape((256, 128), f32)]
-        + [shape((256, 768), f32)] * 2
-        + [shape((1024, 768))] * 2,
-        [pltpu.VMEM((1024, 768), bf16)] * 2
+        + [shape((256, 1536), f32), shape((1024, 1536))],
+        [pltpu.VMEM((1024, 1536), bf16)]
         + [
             pltpu.SemaphoreType.DMA((8,)), pltpu.VMEM((256, 1024), bf16), pltpu.VMEM((1, D), f32),
             pltpu.SemaphoreType.DMA((2,)),
@@ -529,7 +528,7 @@
     normed, scale, pool, home, m1, m2, m3, right, solved, v, grow, lift = call(
         local_kernel,
         "local",
-        vmem(10) + hbm(1),
+        vmem(9),
         [
             shape((256, 1024)), shape((256, 128), f32), shape((256, 256)),
             shape((256, 128)), shape((320, 128)), shape((256, 128)), shape((256, 128)),
@@ -543,7 +542,7 @@
         3_000_000_000,
     )(
         other.reshape(256, 1024), own_normed, line(norm_gain), squares, decay_base, rate_base, *prepared,
-        pinned(w_pool),
+        w_pool,
     )
     r1, r2, r3 = around((m1, m2, m3), "sp_1")
     reads, local, gate, pgate = call(

time: 43.5 us -> 42.4 us (0.975)
  Pallas kernels: 16.3 us -> 15.3 us
    pallas_call x1, Pallas kernels: 6.03 us -> 4.86 us  [shards(): call(local_kernel, 'local', vmem(9), [shape((256, 1024)), shape((256, 128...]
where the time goes in v7:
time: 42.4 us; the launch traced here: 42.3 us
  starting transfers between devices  18.9 us (45%)
  Pallas kernels  15.3 us (36%)
  waiting for transfers between devices  6.8 us (16%)
  other arithmetic  0.99 us (2%)
    ppermute x9, starting transfers between devices, around(): lax.ppermute(part, axis, [(i, i + step & 3) for i in range(4)])  13.4 us
    ppermute x9, waiting for transfers between devices, around(): lax.ppermute(part, axis, [(i, i + step & 3) for i in range(4)])  5.7 us
    pallas_call x1, Pallas kernels, shards(): call(local_kernel, 'local', vmem(9), [shape((256, 1024)), shape((256, 128...  4.86 us
    ppermute x1, starting transfers between devices, shards(): arrived = lax.ppermute(send, 'tp', [(0, 1), (1, 0)])  4.14 us
    pallas_call x1, Pallas kernels, shards(): call(own_kernel, 'own', hbm(6), [shape((256, 1024)), shape((256, 128), f3...  3.39 us
    pallas_call x1, Pallas kernels, shards(): call(side_kernel, 'side', vmem(11), [shape((6, 128, 128)), shape((6, 128,...  2.47 us
    pallas_call x1, Pallas kernels, shards(): call(final_kernel, 'final', vmem(10), [shape((256, 1024)), shape((256, 38...  1.66 us
    ppermute x1, starting transfers between devices, shards(): other = lax.ppermute(tokens, 'tp', [(0, 1), (1, 0)])  1.38 us
  transfers between devices with their start and end apart: 11, of which 6 were waited for; matrix products, arithmetic and copies ran while one was open for 0% of the time, Pallas kernels for 16%

profile of v7, /device:TPU:1, one launch (start us, length us, event | category | flops | bytes accessed | tf_op | source)
XLA Modules:
  0.0 42.3 jit_solution(15540492084260493151)
XLA Ops:
  0.0 1.4 %collective-permute-start = (bf16[2,128,1024]{2,1,0:T(8,128)(2,1)}, bf16[2,128,1024]{2,1,0:T(8,128)(2,1)S(1)}, u32[]{:S(2)}, u32[]{:S(2)}) collective-permute-start(bf16[2,128,1024]{2,1,0:T(8,128)(2,1)} %param.18), channel_id=1, source_target_pairs={{0,1},{1,0},{2,3},{3,2},{4,5},{5,4},{6,7},{7,6},{8,9},{9,8},{10,11... | collective-permute-start | bytes 1572872 | tf_op jit(solution)/shard_map/ppermute | solution.py:510
  1.4 3.4 %own.1 = (bf16[256,1024]{1,0:T(8,128)(2,1)S(1)}, f32[256,128]{1,0:T(8,128)S(1)}, f32[256,1536]{1,0:T(8,128)S(1)}, bf16[1024,1536]{1,0:T(8,128)(2,1)S(1)}) custom-call(bf16[256,1024]{1,0:T(8,128)(2,1)} %bitcast.9, f32[1,2048]{1,0:T(1,128)} %bitcast.5, bf16[2048,384]{1,0:T(8,128)(2,1)} %refs_2_.1, bf16[2048,384]{1,0:T(8,128)(2,1)} %refs_3_.1, ...), custom_call_target="tpu_custom_call" | custom-call | flops 1000000000 | tf_op jit(solution)/shard_map/own/pallas_call | solution.py:514
  4.9 0.0 copy-start.4
  4.9 4.9 %local.1 = (bf16[256,1024]{1,0:T(8,128)(2,1)S(1)}, f32[256,128]{1,0:T(8,128)S(1)}, bf16[256,256]{1,0:T(8,128)(2,1)S(1)}, bf16[256,128]{1,0:T(8,128)(2,1)S(1)}, b...) custom-call(bf16[256,1024]{1,0:T(8,128)(2,1)S(1)} %bitcast.8, ...), custom_call_target="tpu_custom_call" | custom-call | flops 3000000000 | tf_op jit(solution)/shard_map/local/pallas_call | solution.py:528
  9.7 3.1 %collective-permute-start.2 = (bf16[256,128]{1,0:T(8,128)(2,1)S(1)}, bf16[256,128]{1,0:T(8,128)(2,1)S(1)}, u32[]{:S(2)}, u32[]{:S(2)}) collective-permute-start(bf16[256,128]{1,0:T(8,128)(2,1)S(1)} %get-tuple-element.40), channel_id=1, source_target_pairs={{0,16},{8,24},{16,0},{24,8},{1,17},{9,25},{17,1},{25,9},{2,18},{10... | collective-permute-start | bytes 196616 | tf_op jit(solution)/shard_map/ppermute | solution.py:502
  12.8 0.8 %collective-permute-start.3 = (bf16[256,128]{1,0:T(8,128)(2,1)S(1)}, bf16[256,128]{1,0:T(8,128)(2,1)S(1)}, u32[]{:S(2)}, u32[]{:S(2)}) collective-permute-start(bf16[256,128]{1,0:T(8,128)(2,1)S(1)} %get-tuple-element.41), channel_id=1, source_target_pairs={{0,24},{8,0},{16,8},{24,16},{1,25},{9,1},{17,9},{25,17},{2,26},{10... | collective-permute-start | bytes 196616 | tf_op jit(solution)/shard_map/ppermute | solution.py:502
  13.6 0.7 %collective-permute-start.1 = (bf16[320,128]{1,0:T(8,128)(2,1)S(1)}, bf16[320,128]{1,0:T(8,128)(2,1)S(1)}, u32[]{:S(2)}, u32[]{:S(2)}) collective-permute-start(bf16[320,128]{1,0:T(8,128)(2,1)S(1)} %get-tuple-element.39), channel_id=1, source_target_pairs={{0,8},{8,16},{16,24},{24,0},{1,9},{9,17},{17,25},{25,1},{2,10},{10... | collective-permute-start | bytes 245768 | tf_op jit(solution)/shard_map/ppermute | solution.py:502
  14.3 0.0 copy-start.6
  14.3 0.0 copy-start.9
  14.4 2.5 %side.1 = (bf16[6,128,128]{2,1,0:T(8,128)(2,1)S(1)}, f32[6,128,128]{2,1,0:T(8,128)S(1)}, bf16[256,384]{1,0:T(8,128)(2,1)S(1)}, bf16[256,256]{1,0:T(8,128)(2,1)S(1)}) custom-call(bf16[256,1024]{1,0:T(8,128)(2,1)S(1)} %get-tuple-element.34.refs_1_.own_ref, bf16[256,1024]{1,0:T(8,128)(2,1)S(1)} %get-tuple-element.42.other_ref, ...), custom_call_target="tpu_custom_call" | custom-call | flops 1000000000 | tf_op jit(solution)/shard_map/side/pallas_call | solution.py:548
  16.9 0.0 collective-permute-done.3.third_ref
  16.9 1.3 %collective-permute-done.1.first_ref.beside_ref = bf16[320,128]{1,0:T(8,128)(2,1)S(1)} collective-permute-done((bf16[320,128]{1,0:T(8,128)(2,1)S(1)}, bf16[320,128]{1,0:T(8,128)(2,1)S(1)}, u32[]{:S(2)}, u32[]{:S(2)}) %collective-permute-start.1) | collective-permute-done | bytes 81952 | tf_op jit(solution)/shard_map/ppermute | solution.py:502
  18.1 0.6 %row.1 = (f32[3,2,128,128]{3,2,1,0:T(8,128)S(1)}, bf16[320,128]{1,0:T(8,128)(2,1)S(1)}, bf16[256,128]{1,0:T(8,128)(2,1)S(1)}) custom-call(bf16[256,128]{1,0:T(8,128)(2,1)S(1)} %get-tuple-element.38.home_ref, bf16[320,128]{1,0:T(8,128)(2,1)S(1)} %collective-permute-done.1.first_ref.beside_ref, bf16[256,128]{1,0:T(8,128)(2,1)S(1)} %collective-permute-done.2.second_ref, ...), custom_call_target="tpu_custom_call" | custom-call | flops 100000000 | tf_op jit(solution)/shard_map/row/pallas_call | solution.py:557
  18.8 1.7 %collective-permute-start.4 = (bf16[320,128]{1,0:T(8,128)(2,1)S(1)}, bf16[320,128]{1,0:T(8,128)(2,1)S(1)}, u32[]{:S(2)}, u32[]{:S(2)}) collective-permute-start(bf16[320,128]{1,0:T(8,128)(2,1)S(1)} %get-tuple-element.51), channel_id=1, source_target_pairs={{0,32},{32,64},{64,96},{96,0},{1,33},{33,65},{65,97},{97,1},{2,34}... | collective-permute-start | bytes 245768 | tf_op jit(solution)/shard_map/ppermute | solution.py:502
  20.5 2.2 %collective-permute-start.6 = (bf16[256,128]{1,0:T(8,128)(2,1)S(1)}, bf16[256,128]{1,0:T(8,128)(2,1)S(1)}, u32[]{:S(2)}, u32[]{:S(2)}) collective-permute-start(bf16[256,128]{1,0:T(8,128)(2,1)S(1)} %get-tuple-element.52), channel_id=1, source_target_pairs={{0,96},{32,0},{64,32},{96,64},{1,97},{33,1},{65,33},{97,65},{2,98}... | collective-permute-start | bytes 196616 | tf_op jit(solution)/shard_map/ppermute | solution.py:502
  22.7 1.2 %collective-permute-start.5 = (bf16[256,128]{1,0:T(8,128)(2,1)S(1)}, bf16[256,128]{1,0:T(8,128)(2,1)S(1)}, u32[]{:S(2)}, u32[]{:S(2)}) collective-permute-start(bf16[256,128]{1,0:T(8,128)(2,1)S(1)} %get-tuple-element.52), channel_id=1, source_target_pairs={{0,64},{32,96},{64,0},{96,32},{1,65},{33,97},{65,1},{97,33},{2,66}... | collective-permute-start | bytes 196616 | tf_op jit(solution)/shard_map/ppermute | solution.py:502
  23.9 0.1 collective-permute-done.6.third_ref
  24.0 3.7 %collective-permute-done.5.second_ref = bf16[256,128]{1,0:T(8,128)(2,1)S(1)} collective-permute-done((bf16[256,128]{1,0:T(8,128)(2,1)S(1)}, bf16[256,128]{1,0:T(8,128)(2,1)S(1)}, u32[]{:S(2)}, u32[]{:S(2)}) %collective-permute-start.5) | collective-permute-done | bytes 65568 | tf_op jit(solution)/shard_map/ppermute | solution.py:502
  27.7 1.2 %column.1 = (bf16[2,64,128]{2,1,0:T(8,128)(2,1)S(1)}, bf16[2,64,128]{2,1,0:T(8,128)(2,1)S(1)}, bf16[2,64,128]{2,1,0:T(8,128)(2,1)S(1)}, bf16[2,64,128]{2,1,0:T(8,128)(2,1)S(1)}) custom-call(f32[3,2,128,128]{3,2,1,0:T(8,128)S(1)} %get-tuple-element.50.prefix_ref, bf16[320,128]{1,0:T(8,128)(2,1)S(1)} %collective-permute-done.4.first_ref.above_ref, ...), custom_call_target="tpu_custom_call" | custom-call | flops 100000000 | tf_op jit(solution)/shard_map/column/pallas_call | solution.py:567
  28.8 0.3 collective-permute-start.7
  29.2 2.0 %collective-permute-start.8 = (bf16[2,64,128]{2,1,0:T(8,128)(2,1)S(1)}, bf16[2,64,128]{2,1,0:T(8,128)(2,1)S(1)}, u32[]{:S(2)}, u32[]{:S(2)}) collective-permute-start(bf16[2,64,128]{2,1,0:T(8,128)(2,1)S(1)} %get-tuple-element.55), channel_id=1, source_target_pairs={{0,16},{8,24},{16,0},{24,8},{1,17},{9,25},{17,1},{25,9},{2,18},{10... | collective-permute-start | bytes 98312 | tf_op jit(solution)/shard_map/ppermute | solution.py:502
  31.1 1.4 %collective-permute-start.9 = (bf16[2,64,128]{2,1,0:T(8,128)(2,1)S(1)}, bf16[2,64,128]{2,1,0:T(8,128)(2,1)S(1)}, u32[]{:S(2)}, u32[]{:S(2)}) collective-permute-start(bf16[2,64,128]{2,1,0:T(8,128)(2,1)S(1)} %get-tuple-element.56), channel_id=1, source_target_pairs={{0,24},{8,0},{16,8},{24,16},{1,25},{9,1},{17,9},{25,17},{2,26},{10... | collective-permute-start | bytes 98312 | tf_op jit(solution)/shard_map/ppermute | solution.py:502
  32.6 0.0 copy-start.8
  32.6 0.6 %pool.1.part_ref = f32[256,2048]{1,0:T(8,128)S(1)} custom-call(bf16[256,256]{1,0:T(8,128)(2,1)S(1)} %get-tuple-element.60.pool_ref, bf16[320,128]{1,0:T(8,128)(2,1)S(1)} %collective-permute-done.1.first_ref.beside_ref, bf16[320,128]{1,0:T(8,128)(2,1)S(1)} %collective-permute-done.4.first_ref.above_ref, ...), custom_call_target="tpu_custom_call" | custom-call | flops 300000000 | tf_op jit(solution)/shard_map/pool/pallas_call | solution.py:577
  33.3 0.2 collective-permute-done.8.two_ref
  33.5 0.5 %collective-permute-done.9.three_ref = bf16[2,64,128]{2,1,0:T(8,128)(2,1)S(1)} collective-permute-done((bf16[2,64,128]{2,1,0:T(8,128)(2,1)S(1)}, bf16[2,64,128]{2,1,0:T(8,128)(2,1)S(1)}, u32[]{:S(2)}, u32[]{:S(2)}) %collective-permute-start.9) | collective-permute-done | bytes 32800 | tf_op jit(solution)/shard_map/ppermute | solution.py:502
  33.9 0.1 copy-done
  34.0 1.7 %final.1 = (bf16[256,1024]{1,0:T(8,128)(2,1)S(1)}, bf16[256,384]{1,0:T(8,128)(2,1)S(1)}) custom-call(bf16[2,64,128]{2,1,0:T(8,128)(2,1)S(1)} %get-tuple-element.53.home_ref, bf16[2,64,128]{2,1,0:T(8,128)(2,1)S(1)} %collective-permute-done.7.one_ref, bf16[2,64,128]{2,1,0:T(8,128)(2,1)S(1)} %collective-permute-done.8.two_ref, ...), custom_call_target="tpu_custom_call" | custom-call | flops 1000000000 | tf_op jit(solution)/shard_map/final/pallas_call | solution.py:580
  35.7 4.1 %collective-permute-start.10 = (bf16[256,1024]{1,0:T(8,128)(2,1)S(1)}, bf16[256,1024]{1,0:T(8,128)(2,1)S(1)}, u32[]{:S(2)}, u32[]{:S(2)}) collective-permute-start(bf16[256,1024]{1,0:T(8,128)(2,1)S(1)} %get-tuple-element.62), channel_id=1, source_target_pairs={{0,1},{1,0},{2,3},{3,2},{4,5},{5,4},{6,7},{7,6},{8,9},{9,8},{10,11... | collective-permute-start | bytes 1572872 | tf_op jit(solution)/shard_map/ppermute | solution.py:589
  39.8 0.4 %keep.1 = bf16[256,1024]{1,0:T(8,128)(2,1)S(1)} custom-call(bf16[256,384]{1,0:T(8,128)(2,1)S(1)} %get-tuple-element.61.rec_ref, f32[256,2048]{1,0:T(8,128)S(1)} %pool.1.part_ref, bf16[384,2048]{1,0:T(8,128)(2,1)S(1)} %copy-done), custom_call_target="tpu_custom_call" | custom-call | flops 300000000 | tf_op jit(solution)/shard_map/keep/pallas_call | solution.py:590
  40.2 1.1 %collective-permute-done.10 = bf16[256,1024]{1,0:T(8,128)(2,1)S(1)} collective-permute-done((bf16[256,1024]{1,0:T(8,128)(2,1)S(1)}, bf16[256,1024]{1,0:T(8,128)(2,1)S(1)}, u32[]{:S(2)}, u32[]{:S(2)}) %collective-permute-start.10) | collective-permute-done | bytes 524320 | tf_op jit(solution)/shard_map/ppermute | solution.py:589
  41.3 1.0 %add_convert_fusion = bf16[256,1024]{1,0:T(8,128)(2,1)} fusion(bf16[256,1024]{1,0:T(8,128)(2,1)S(1)} %collective-permute-done.10, bf16[256,1024]{1,0:T(8,128)(2,1)S(1)} %keep.1), kind=kLoop, calls=%fused_computation | loop fusion | flops 1048576 | bytes 1572864 | tf_op jit(solution)/shard_map/convert_element_type | solution.py:592
  (25 shorter events, 0.1 us)
Async XLA Ops:
  0.0 4.8 %collective-permute-start = (bf16[2,128,1024]{2,1,0:T(8,128)(2,1)}, bf16[2,128,1024]{2,1,0:T(8,128)(2,1)S(1)}, u32[]{:S(2)}, u32[]{:S(2)}) collective-permute-start(bf16[2,128,1024]{2,1,0:T(8,128)(2,1)} %param.18), channel_id=1, source_target_pairs={{0,1},{1,0},{2,3},{3,2},{4,5},{5,4},{6,7},{7,6},{8,9},{9,8},{10,11... | collective-permute-start | bytes 1572872 | tf_op jit(solution)/shard_map/ppermute | solution.py:510
  1.4 3.4 %copy-start.7 = (f32[2048]{0:T(1024)S(1)}, f32[2048]{0:T(1024)}, u32[]{:S(2)}) copy-start(f32[2048]{0:T(1024)} %param.19) | copy-start | bytes 24580
  1.4 3.4 %copy-start.10 = (bf16[2048,256]{1,0:T(8,128)(2,1)S(1)}, bf16[2048,256]{1,0:T(8,128)(2,1)}, u32[]{:S(2)}) copy-start(bf16[2048,256]{1,0:T(8,128)(2,1)} %refs_8_.1) | copy-start | bytes 3145732
  1.4 3.4 %copy-start.11 = (f32[768]{0:T(1024)S(1)}, f32[768]{0:T(1024)}, u32[]{:S(2)}) copy-start(f32[768]{0:T(1024)} %refs_4_.3) | copy-start | bytes 9220
  1.4 3.4 %copy-start.12 = (f32[768]{0:T(1024)S(1)}, f32[768]{0:T(1024)}, u32[]{:S(2)}) copy-start(f32[768]{0:T(1024)} %refs_5_.3) | copy-start | bytes 9220
  4.8 9.5 %copy-start.1 = (bf16[2048,384]{1,0:T(8,128)(2,1)S(1)}, bf16[2048,384]{1,0:T(8,128)(2,1)}, u32[]{:S(2)}) copy-start(bf16[2048,384]{1,0:T(8,128)(2,1)} %wr_ref.3) | copy-start | bytes 4718596
  4.9 9.5 %copy-start.2 = (bf16[2048,384]{1,0:T(8,128)(2,1)S(1)}, bf16[2048,384]{1,0:T(8,128)(2,1)}, u32[]{:S(2)}) copy-start(bf16[2048,384]{1,0:T(8,128)(2,1)} %wg_ref.1) | copy-start | bytes 4718596
  4.9 9.5 %copy-start.4 = (bf16[2048,256]{1,0:T(8,128)(2,1)S(1)}, bf16[2048,256]{1,0:T(8,128)(2,1)}, u32[]{:S(2)}) copy-start(bf16[2048,256]{1,0:T(8,128)(2,1)} %wq_ref.1) | copy-start | bytes 3145732
  9.7 7.1 %collective-permute-start.2 = (bf16[256,128]{1,0:T(8,128)(2,1)S(1)}, bf16[256,128]{1,0:T(8,128)(2,1)S(1)}, u32[]{:S(2)}, u32[]{:S(2)}) collective-permute-start(bf16[256,128]{1,0:T(8,128)(2,1)S(1)} %get-tuple-element.40), channel_id=1, source_target_pairs={{0,16},{8,24},{16,0},{24,8},{1,17},{9,25},{17,1},{25,9},{2,18},{10... | collective-permute-start | bytes 196616 | tf_op jit(solution)/shard_map/ppermute | solution.py:502
  12.8 4.0 %collective-permute-start.3 = (bf16[256,128]{1,0:T(8,128)(2,1)S(1)}, bf16[256,128]{1,0:T(8,128)(2,1)S(1)}, u32[]{:S(2)}, u32[]{:S(2)}) collective-permute-start(bf16[256,128]{1,0:T(8,128)(2,1)S(1)} %get-tuple-element.41), channel_id=1, source_target_pairs={{0,24},{8,0},{16,8},{24,16},{1,25},{9,1},{17,9},{25,17},{2,26},{10... | collective-permute-start | bytes 196616 | tf_op jit(solution)/shard_map/ppermute | solution.py:502
  13.6 4.5 %collective-permute-start.1 = (bf16[320,128]{1,0:T(8,128)(2,1)S(1)}, bf16[320,128]{1,0:T(8,128)(2,1)S(1)}, u32[]{:S(2)}, u32[]{:S(2)}) collective-permute-start(bf16[320,128]{1,0:T(8,128)(2,1)S(1)} %get-tuple-element.39), channel_id=1, source_target_pairs={{0,8},{8,16},{16,24},{24,0},{1,9},{9,17},{17,25},{25,1},{2,10},{10... | collective-permute-start | bytes 245768 | tf_op jit(solution)/shard_map/ppermute | solution.py:502
  14.3 13.4 %copy-start.5 = (f32[2,6,64,64]{3,2,1,0:T(8,128)S(1)}, f32[2,6,64,64]{3,2,1,0:T(8,128)}, u32[]{:S(2)}) copy-start(f32[2,6,64,64]{3,2,1,0:T(8,128)} %init_ref.1) | copy-start | bytes 589828
  14.3 18.2 %copy-start.6 = (bf16[4,128,128]{2,1,0:T(8,128)(2,1)S(1)}, bf16[4,128,128]{2,1,0:T(8,128)(2,1)}, u32[]{:S(2)}) copy-start(bf16[4,128,128]{2,1,0:T(8,128)(2,1)} %mix_ref.1) | copy-start | bytes 393220
  14.3 18.2 %copy-start.9 = (f32[512]{0:T(512)S(1)}, f32[512]{0:T(512)}, u32[]{:S(2)}) copy-start(f32[512]{0:T(512)} %param.32) | copy-start | bytes 6148
  16.8 15.7 %copy-start.3 = (bf16[256,2048]{1,0:T(8,128)(2,1)S(1)}, bf16[256,2048]{1,0:T(8,128)(2,1)}, u32[]{:S(2)}) copy-start(bf16[256,2048]{1,0:T(8,128)(2,1)} %wp_ref.1) | copy-start | bytes 3145732
  18.8 8.9 %collective-permute-start.4 = (bf16[320,128]{1,0:T(8,128)(2,1)S(1)}, bf16[320,128]{1,0:T(8,128)(2,1)S(1)}, u32[]{:S(2)}, u32[]{:S(2)}) collective-permute-start(bf16[320,128]{1,0:T(8,128)(2,1)S(1)} %get-tuple-element.51), channel_id=1, source_target_pairs={{0,32},{32,64},{64,96},{96,0},{1,33},{33,65},{65,97},{97,1},{2,34}... | collective-permute-start | bytes 245768 | tf_op jit(solution)/shard_map/ppermute | solution.py:502
  20.5 3.5 %collective-permute-start.6 = (bf16[256,128]{1,0:T(8,128)(2,1)S(1)}, bf16[256,128]{1,0:T(8,128)(2,1)S(1)}, u32[]{:S(2)}, u32[]{:S(2)}) collective-permute-start(bf16[256,128]{1,0:T(8,128)(2,1)S(1)} %get-tuple-element.52), channel_id=1, source_target_pairs={{0,96},{32,0},{64,32},{96,64},{1,97},{33,1},{65,33},{97,65},{2,98}... | collective-permute-start | bytes 196616 | tf_op jit(solution)/shard_map/ppermute | solution.py:502
  22.7 5.0 %collective-permute-start.5 = (bf16[256,128]{1,0:T(8,128)(2,1)S(1)}, bf16[256,128]{1,0:T(8,128)(2,1)S(1)}, u32[]{:S(2)}, u32[]{:S(2)}) collective-permute-start(bf16[256,128]{1,0:T(8,128)(2,1)S(1)} %get-tuple-element.52), channel_id=1, source_target_pairs={{0,64},{32,96},{64,0},{96,32},{1,65},{33,97},{65,1},{97,33},{2,66}... | collective-permute-start | bytes 196616 | tf_op jit(solution)/shard_map/ppermute | solution.py:502
  28.8 4.4 %collective-permute-start.7 = (bf16[2,64,128]{2,1,0:T(8,128)(2,1)S(1)}, bf16[2,64,128]{2,1,0:T(8,128)(2,1)S(1)}, u32[]{:S(2)}, u32[]{:S(2)}) collective-permute-start(bf16[2,64,128]{2,1,0:T(8,128)(2,1)S(1)} %get-tuple-element.54), channel_id=1, source_target_pairs={{0,8},{8,16},{16,24},{24,0},{1,9},{9,17},{17,25},{25,1},{2,10},{10... | collective-permute-start | bytes 98312 | tf_op jit(solution)/shard_map/ppermute | solution.py:502
  29.2 4.3 %collective-permute-start.8 = (bf16[2,64,128]{2,1,0:T(8,128)(2,1)S(1)}, bf16[2,64,128]{2,1,0:T(8,128)(2,1)S(1)}, u32[]{:S(2)}, u32[]{:S(2)}) collective-permute-start(bf16[2,64,128]{2,1,0:T(8,128)(2,1)S(1)} %get-tuple-element.55), channel_id=1, source_target_pairs={{0,16},{8,24},{16,0},{24,8},{1,17},{9,25},{17,1},{25,9},{2,18},{10... | collective-permute-start | bytes 98312 | tf_op jit(solution)/shard_map/ppermute | solution.py:502
  31.1 2.8 %collective-permute-start.9 = (bf16[2,64,128]{2,1,0:T(8,128)(2,1)S(1)}, bf16[2,64,128]{2,1,0:T(8,128)(2,1)S(1)}, u32[]{:S(2)}, u32[]{:S(2)}) collective-permute-start(bf16[2,64,128]{2,1,0:T(8,128)(2,1)S(1)} %get-tuple-element.56), channel_id=1, source_target_pairs={{0,24},{8,0},{16,8},{24,16},{1,25},{9,1},{17,9},{25,17},{2,26},{10... | collective-permute-start | bytes 98312 | tf_op jit(solution)/shard_map/ppermute | solution.py:502
  32.6 1.4 %copy-start = (bf16[384,2048]{1,0:T(8,128)(2,1)S(1)}, bf16[384,2048]{1,0:T(8,128)(2,1)}, u32[]{:S(2)}) copy-start(bf16[384,2048]{1,0:T(8,128)(2,1)} %wr_ref.5) | copy-start | bytes 4718596
  32.6 1.4 %copy-start.8 = (f32[768]{0:T(1024)S(1)}, f32[768]{0:T(1024)}, u32[]{:S(2)}) copy-start(f32[768]{0:T(1024)} %hgain_ref.1) | copy-start | bytes 9220
  35.7 5.7 %collective-permute-start.10 = (bf16[256,1024]{1,0:T(8,128)(2,1)S(1)}, bf16[256,1024]{1,0:T(8,128)(2,1)S(1)}, u32[]{:S(2)}, u32[]{:S(2)}) collective-permute-start(bf16[256,1024]{1,0:T(8,128)(2,1)S(1)} %get-tuple-element.62), channel_id=1, source_target_pairs={{0,1},{1,0},{2,3},{3,2},{4,5},{5,4},{6,7},{7,6},{8,9},{9,8},{10,11... | collective-permute-start | bytes 1572872 | tf_op jit(solution)/shard_map/ppermute | solution.py:589

commit v8 on v7

--- a/solution.py
+++ b/solution.py
@@ -67,7 +67,16 @@
 
 
 def compose(earlier, later, masks):
-    moved = dot_fine_left(earlier, both(later[:HEAD], masks))
+    high, low = halves(earlier) if earlier.dtype == f32 else (earlier, None)
+    upper, lower = halves(later[:HEAD]) if later.dtype == f32 else (later[:HEAD], None)
+    left, right = [high], [both(upper, masks)]
+    if low is not None:
+        left.append(low)
+        right.append(right[0])
+    if lower is not None:
+        left.append(high)
+        right.append(both(lower, masks))
+    moved = dot(jnp.concatenate(left, axis=1), jnp.concatenate(right, axis=0))
     written = later[HEAD:].astype(f32)
     if earlier.shape[0] == HEAD:
         return moved + written
@@ -364,15 +373,15 @@
     masks = head_masks()
     for s in (0, 1):
         rows = slice(s * 128, s * 128 + 128)
-        so_far = maps[0, rows].astype(f32)
-        prefix_ref[0, s] = so_far
-        for j in (1, 2, 3):
-            so_far = compose(so_far, maps[j, rows], masks)
-            if j < 3:
-                prefix_ref[j, s] = so_far
-            else:
-                next_ref[rows] = so_far.astype(bf16)
-                total_ref[rows] = so_far.astype(bf16)
+        own = [maps[j, rows] for j in range(4)]
+        front = compose(own[0], own[1], masks)
+        back = compose(own[2], own[3], masks)
+        whole = compose(front, back, masks).astype(bf16)
+        next_ref[rows] = whole
+        total_ref[rows] = whole
+        prefix_ref[0, s] = own[0].astype(f32)
+        prefix_ref[1, s] = front
+        prefix_ref[2, s] = compose(front, own[2], masks)
 
 
 def column_kernel(
@@ -388,8 +397,11 @@
     pair = jnp.minimum(y, 2) * 2
     for s in (0, 1):
         state = jnp.concatenate([init_ref[s, pair], init_ref[s, pair + 1]], axis=1)
-        for j in range(3):
-            state = jnp.where(j < z, compose(state, rows[j, s * 128 : s * 128 + 128], masks), state)
+        later = [rows[j, s * 128 : s * 128 + 128] for j in range(3)]
+        first = compose(state, later[0], masks)
+        second = compose(first, later[1], masks)
+        third = compose(first, compose(later[1], later[2], masks), masks)
+        state = jnp.where(z == 0, state, jnp.where(z == 1, first, jnp.where(z == 2, second, third)))
         starts[0, s] = state.astype(bf16)
         for j in range(3):
             starts[j + 1, s] = compose(state, prefix_ref[j, s], masks).astype(bf16)
@@ -457,7 +469,7 @@
         rows = slice(s * 128, s * 128 + 128)
         out = dot(reads_ref[u], both(starts[h, s], masks), NT) + local_ref[u]
         out = out - dot_fine_left(out, mean_of)
-        spread = dot_fine_left(out * out, mean_of)
+        spread = dot(out * out, mean_of)
         gain = jnp.where(is_first, line_of(hgain_ref, lanes), line_of(hgain_ref, shifted))
         gate = gate_ref[rows, lanes].astype(f32)
         rec[rows, lanes] = (
@@ -470,6 +482,16 @@
 def keep_kernel(rec_ref, part_ref, wr_ref, keep_ref):
     cols = pl.ds(pl.multiple_of(lax.axis_index("tp") * 1024, 1024), 1024)
     keep_ref[...] = (dot(rec_ref[...], wr_ref[:, cols]) + part_ref[:, cols]).astype(bf16)
+
+
+def sum_kernel(keep_ref, arrived_ref, out_ref, buf, sems):
+    copies = []
+    for i in range(4):
+        rows = slice(i * 64, i * 64 + 64)
+        buf[rows] = (keep_ref[rows].astype(f32) + arrived_ref[rows].astype(f32)).astype(bf16)
+        copies.append(pltpu.make_async_copy(buf.at[rows], out_ref.at[rows], sems.at[i]))
+        copies[-1].start()
+    finish(copies)
 
 
 def vmem(count):
@@ -588,8 +610,16 @@
     )(s0, t1, t2, t3, reads, local, gate, head_gain, pool_part, w_out_rec)
     arrived = lax.ppermute(send, "tp", [(0, 1), (1, 0)])
     keep = call(keep_kernel, "keep", vmem(3), shape((256, 1024)), [], 8, 300_000_000)(rec, pool_part, w_out_rec)
-    mixed = keep.astype(f32) + arrived.astype(f32)
-    return mixed.astype(bf16).reshape(2, 128, 1024)
+    mixed = pl.pallas_call(
+        sum_kernel,
+        name="sum",
+        out_shape=shape((256, 1024)),
+        in_specs=vmem(2),
+        out_specs=hbm(1)[0],
+        scratch_shapes=[pltpu.VMEM((256, 1024), bf16), pltpu.SemaphoreType.DMA((4,))],
+        compiler_params=pltpu.CompilerParams(vmem_limit_bytes=4 * MIB),
+    )(keep, arrived)
+    return mixed.reshape(2, 128, 1024)
 
 
 def solution(mesh):

time: 42.4 us -> 41.9 us (0.988)
  other arithmetic: 0.99 us -> 0 us
  Pallas kernels: 15.3 us -> 15.8 us
    convert_element_type x1 -> x0, other arithmetic: 0.99 us -> none  [shards(): return mixed.astype(bf16).reshape(2, 128, 1024)]
    pallas_call x0 -> x1, Pallas kernels: none -> 0.85 us  [shards(): pl.pallas_call(sum_kernel, name='sum', out_shape=shape((256, 1024)), in_s...]
  transfers between devices with their start and end apart: 11 -> 11, of which waited for: 6 -> 6; matrix products, arithmetic and copies ran while one was open for 0% -> 0% of each run, Pallas kernels for 16% -> 17%
where the time goes in v8:
time: 41.9 us; the launch traced here: 41.8 us
  starting transfers between devices  18.9 us (45%)
  Pallas kernels  15.8 us (38%)
  waiting for transfers between devices  6.81 us (16%)
    ppermute x9, starting transfers between devices, around(): lax.ppermute(part, axis, [(i, i + step & 3) for i in range(4)])  13.4 us
    ppermute x9, waiting for transfers between devices, around(): lax.ppermute(part, axis, [(i, i + step & 3) for i in range(4)])  5.71 us
    pallas_call x1, Pallas kernels, shards(): call(local_kernel, 'local', vmem(9), [shape((256, 1024)), shape((256, 128...  4.86 us
    ppermute x1, starting transfers between devices, shards(): arrived = lax.ppermute(send, 'tp', [(0, 1), (1, 0)])  4.15 us
    pallas_call x1, Pallas kernels, shards(): call(own_kernel, 'own', hbm(6), [shape((256, 1024)), shape((256, 128), f3...  3.39 us
    pallas_call x1, Pallas kernels, shards(): call(side_kernel, 'side', vmem(11), [shape((6, 128, 128)), shape((6, 128,...  2.47 us
    pallas_call x1, Pallas kernels, shards(): call(final_kernel, 'final', vmem(10), [shape((256, 1024)), shape((256, 38...  1.64 us
    ppermute x1, starting transfers between devices, shards(): other = lax.ppermute(tokens, 'tp', [(0, 1), (1, 0)])  1.38 us
  transfers between devices with their start and end apart: 11, of which 6 were waited for; matrix products, arithmetic and copies ran while one was open for 0% of the time, Pallas kernels for 17%

profile of v8, /device:TPU:1, one launch (start us, length us, event | category | flops | bytes accessed | tf_op | source)
XLA Modules:
  0.0 41.8 jit_solution(6845370483675910008)
XLA Ops:
  0.0 1.4 %collective-permute-start = (bf16[2,128,1024]{2,1,0:T(8,128)(2,1)}, bf16[2,128,1024]{2,1,0:T(8,128)(2,1)S(1)}, u32[]{:S(2)}, u32[]{:S(2)}) collective-permute-start(bf16[2,128,1024]{2,1,0:T(8,128)(2,1)} %param.18), channel_id=1, source_target_pairs={{0,1},{1,0},{2,3},{3,2},{4,5},{5,4},{6,7},{7,6},{8,9},{9,8},{10,11... | collective-permute-start | bytes 1572872 | tf_op jit(solution)/shard_map/ppermute | solution.py:532
  1.4 3.4 %own.1 = (bf16[256,1024]{1,0:T(8,128)(2,1)S(1)}, f32[256,128]{1,0:T(8,128)S(1)}, f32[256,1536]{1,0:T(8,128)S(1)}, bf16[1024,1536]{1,0:T(8,128)(2,1)S(1)}) custom-call(bf16[256,1024]{1,0:T(8,128)(2,1)} %bitcast.9, f32[1,2048]{1,0:T(1,128)} %bitcast.5, bf16[2048,384]{1,0:T(8,128)(2,1)} %refs_2_.1, bf16[2048,384]{1,0:T(8,128)(2,1)} %refs_3_.1, ...), custom_call_target="tpu_custom_call" | custom-call | flops 1000000000 | tf_op jit(solution)/shard_map/own/pallas_call | solution.py:536
  4.8 0.0 copy-start.1
  4.9 0.0 copy-start.2
  4.9 0.0 copy-start.4
  4.9 4.9 %local.1 = (bf16[256,1024]{1,0:T(8,128)(2,1)S(1)}, f32[256,128]{1,0:T(8,128)S(1)}, bf16[256,256]{1,0:T(8,128)(2,1)S(1)}, bf16[256,128]{1,0:T(8,128)(2,1)S(1)}, b...) custom-call(bf16[256,1024]{1,0:T(8,128)(2,1)S(1)} %bitcast.8, ...), custom_call_target="tpu_custom_call" | custom-call | flops 3000000000 | tf_op jit(solution)/shard_map/local/pallas_call | solution.py:550
  9.7 3.1 %collective-permute-start.2 = (bf16[256,128]{1,0:T(8,128)(2,1)S(1)}, bf16[256,128]{1,0:T(8,128)(2,1)S(1)}, u32[]{:S(2)}, u32[]{:S(2)}) collective-permute-start(bf16[256,128]{1,0:T(8,128)(2,1)S(1)} %get-tuple-element.40), channel_id=1, source_target_pairs={{0,16},{8,24},{16,0},{24,8},{1,17},{9,25},{17,1},{25,9},{2,18},{10... | collective-permute-start | bytes 196616 | tf_op jit(solution)/shard_map/ppermute | solution.py:524
  12.8 0.8 %collective-permute-start.3 = (bf16[256,128]{1,0:T(8,128)(2,1)S(1)}, bf16[256,128]{1,0:T(8,128)(2,1)S(1)}, u32[]{:S(2)}, u32[]{:S(2)}) collective-permute-start(bf16[256,128]{1,0:T(8,128)(2,1)S(1)} %get-tuple-element.41), channel_id=1, source_target_pairs={{0,24},{8,0},{16,8},{24,16},{1,25},{9,1},{17,9},{25,17},{2,26},{10... | collective-permute-start | bytes 196616 | tf_op jit(solution)/shard_map/ppermute | solution.py:524
  13.6 0.7 %collective-permute-start.1 = (bf16[320,128]{1,0:T(8,128)(2,1)S(1)}, bf16[320,128]{1,0:T(8,128)(2,1)S(1)}, u32[]{:S(2)}, u32[]{:S(2)}) collective-permute-start(bf16[320,128]{1,0:T(8,128)(2,1)S(1)} %get-tuple-element.39), channel_id=1, source_target_pairs={{0,8},{8,16},{16,24},{24,0},{1,9},{9,17},{17,25},{25,1},{2,10},{10... | collective-permute-start | bytes 245768 | tf_op jit(solution)/shard_map/ppermute | solution.py:524
  14.3 0.0 copy-start.6
  14.4 2.5 %side.1 = (bf16[6,128,128]{2,1,0:T(8,128)(2,1)S(1)}, f32[6,128,128]{2,1,0:T(8,128)S(1)}, bf16[256,384]{1,0:T(8,128)(2,1)S(1)}, bf16[256,256]{1,0:T(8,128)(2,1)S(1)}) custom-call(bf16[256,1024]{1,0:T(8,128)(2,1)S(1)} %get-tuple-element.34.refs_1_.own_ref, bf16[256,1024]{1,0:T(8,128)(2,1)S(1)} %get-tuple-element.42.other_ref, ...), custom_call_target="tpu_custom_call" | custom-call | flops 1000000000 | tf_op jit(solution)/shard_map/side/pallas_call | solution.py:570
  16.9 0.0 collective-permute-done.3.third_ref
  16.9 1.3 %collective-permute-done.1.first_ref.beside_ref = bf16[320,128]{1,0:T(8,128)(2,1)S(1)} collective-permute-done((bf16[320,128]{1,0:T(8,128)(2,1)S(1)}, bf16[320,128]{1,0:T(8,128)(2,1)S(1)}, u32[]{:S(2)}, u32[]{:S(2)}) %collective-permute-start.1) | collective-permute-done | bytes 81952 | tf_op jit(solution)/shard_map/ppermute | solution.py:524
  18.1 0.6 %row.1 = (f32[3,2,128,128]{3,2,1,0:T(8,128)S(1)}, bf16[320,128]{1,0:T(8,128)(2,1)S(1)}, bf16[256,128]{1,0:T(8,128)(2,1)S(1)}) custom-call(bf16[256,128]{1,0:T(8,128)(2,1)S(1)} %get-tuple-element.38.home_ref, bf16[320,128]{1,0:T(8,128)(2,1)S(1)} %collective-permute-done.1.first_ref.beside_ref, bf16[256,128]{1,0:T(8,128)(2,1)S(1)} %collective-permute-done.2.second_ref, ...), custom_call_target="tpu_custom_call" | custom-call | flops 100000000 | tf_op jit(solution)/shard_map/row/pallas_call | solution.py:579
  18.7 1.7 %collective-permute-start.4 = (bf16[320,128]{1,0:T(8,128)(2,1)S(1)}, bf16[320,128]{1,0:T(8,128)(2,1)S(1)}, u32[]{:S(2)}, u32[]{:S(2)}) collective-permute-start(bf16[320,128]{1,0:T(8,128)(2,1)S(1)} %get-tuple-element.51), channel_id=1, source_target_pairs={{0,32},{32,64},{64,96},{96,0},{1,33},{33,65},{65,97},{97,1},{2,34}... | collective-permute-start | bytes 245768 | tf_op jit(solution)/shard_map/ppermute | solution.py:524
  20.4 2.2 %collective-permute-start.6 = (bf16[256,128]{1,0:T(8,128)(2,1)S(1)}, bf16[256,128]{1,0:T(8,128)(2,1)S(1)}, u32[]{:S(2)}, u32[]{:S(2)}) collective-permute-start(bf16[256,128]{1,0:T(8,128)(2,1)S(1)} %get-tuple-element.52), channel_id=1, source_target_pairs={{0,96},{32,0},{64,32},{96,64},{1,97},{33,1},{65,33},{97,65},{2,98}... | collective-permute-start | bytes 196616 | tf_op jit(solution)/shard_map/ppermute | solution.py:524
  22.6 1.2 %collective-permute-start.5 = (bf16[256,128]{1,0:T(8,128)(2,1)S(1)}, bf16[256,128]{1,0:T(8,128)(2,1)S(1)}, u32[]{:S(2)}, u32[]{:S(2)}) collective-permute-start(bf16[256,128]{1,0:T(8,128)(2,1)S(1)} %get-tuple-element.52), channel_id=1, source_target_pairs={{0,64},{32,96},{64,0},{96,32},{1,65},{33,97},{65,1},{97,33},{2,66}... | collective-permute-start | bytes 196616 | tf_op jit(solution)/shard_map/ppermute | solution.py:524
  23.8 0.1 collective-permute-done.6.third_ref
  23.9 3.7 %collective-permute-done.5.second_ref = bf16[256,128]{1,0:T(8,128)(2,1)S(1)} collective-permute-done((bf16[256,128]{1,0:T(8,128)(2,1)S(1)}, bf16[256,128]{1,0:T(8,128)(2,1)S(1)}, u32[]{:S(2)}, u32[]{:S(2)}) %collective-permute-start.5) | collective-permute-done | bytes 65568 | tf_op jit(solution)/shard_map/ppermute | solution.py:524
  27.6 0.9 %column.1 = (bf16[2,64,128]{2,1,0:T(8,128)(2,1)S(1)}, bf16[2,64,128]{2,1,0:T(8,128)(2,1)S(1)}, bf16[2,64,128]{2,1,0:T(8,128)(2,1)S(1)}, bf16[2,64,128]{2,1,0:T(8,128)(2,1)S(1)}) custom-call(f32[3,2,128,128]{3,2,1,0:T(8,128)S(1)} %get-tuple-element.50.prefix_ref, bf16[320,128]{1,0:T(8,128)(2,1)S(1)} %collective-permute-done.4.first_ref.above_ref, ...), custom_call_target="tpu_custom_call" | custom-call | flops 100000000 | tf_op jit(solution)/shard_map/column/pallas_call | solution.py:589
  28.5 0.3 collective-permute-start.7
  28.8 2.0 %collective-permute-start.8 = (bf16[2,64,128]{2,1,0:T(8,128)(2,1)S(1)}, bf16[2,64,128]{2,1,0:T(8,128)(2,1)S(1)}, u32[]{:S(2)}, u32[]{:S(2)}) collective-permute-start(bf16[2,64,128]{2,1,0:T(8,128)(2,1)S(1)} %get-tuple-element.55), channel_id=1, source_target_pairs={{0,16},{8,24},{16,0},{24,8},{1,17},{9,25},{17,1},{25,9},{2,18},{10... | collective-permute-start | bytes 98312 | tf_op jit(solution)/shard_map/ppermute | solution.py:524
  30.8 1.4 %collective-permute-start.9 = (bf16[2,64,128]{2,1,0:T(8,128)(2,1)S(1)}, bf16[2,64,128]{2,1,0:T(8,128)(2,1)S(1)}, u32[]{:S(2)}, u32[]{:S(2)}) collective-permute-start(bf16[2,64,128]{2,1,0:T(8,128)(2,1)S(1)} %get-tuple-element.56), channel_id=1, source_target_pairs={{0,24},{8,0},{16,8},{24,16},{1,25},{9,1},{17,9},{25,17},{2,26},{10... | collective-permute-start | bytes 98312 | tf_op jit(solution)/shard_map/ppermute | solution.py:524
  32.3 0.6 %pool.1.part_ref = f32[256,2048]{1,0:T(8,128)S(1)} custom-call(bf16[256,256]{1,0:T(8,128)(2,1)S(1)} %get-tuple-element.60.pool_ref, bf16[320,128]{1,0:T(8,128)(2,1)S(1)} %collective-permute-done.1.first_ref.beside_ref, bf16[320,128]{1,0:T(8,128)(2,1)S(1)} %collective-permute-done.4.first_ref.above_ref, ...), custom_call_target="tpu_custom_call" | custom-call | flops 300000000 | tf_op jit(solution)/shard_map/pool/pallas_call | solution.py:599
  32.9 0.2 collective-permute-done.8.two_ref
  33.1 0.5 %collective-permute-done.9.three_ref = bf16[2,64,128]{2,1,0:T(8,128)(2,1)S(1)} collective-permute-done((bf16[2,64,128]{2,1,0:T(8,128)(2,1)S(1)}, bf16[2,64,128]{2,1,0:T(8,128)(2,1)S(1)}, u32[]{:S(2)}, u32[]{:S(2)}) %collective-permute-start.9) | collective-permute-done | bytes 32800 | tf_op jit(solution)/shard_map/ppermute | solution.py:524
  33.6 0.1 copy-done
  33.6 1.6 %final.1 = (bf16[256,1024]{1,0:T(8,128)(2,1)S(1)}, bf16[256,384]{1,0:T(8,128)(2,1)S(1)}) custom-call(bf16[2,64,128]{2,1,0:T(8,128)(2,1)S(1)} %get-tuple-element.53.home_ref, bf16[2,64,128]{2,1,0:T(8,128)(2,1)S(1)} %collective-permute-done.7.one_ref, bf16[2,64,128]{2,1,0:T(8,128)(2,1)S(1)} %collective-permute-done.8.two_ref, ...), custom_call_target="tpu_custom_call" | custom-call | flops 1000000000 | tf_op jit(solution)/shard_map/final/pallas_call | solution.py:602
  35.3 4.1 %collective-permute-start.10 = (bf16[256,1024]{1,0:T(8,128)(2,1)S(1)}, bf16[256,1024]{1,0:T(8,128)(2,1)S(1)}, u32[]{:S(2)}, u32[]{:S(2)}) collective-permute-start(bf16[256,1024]{1,0:T(8,128)(2,1)S(1)} %get-tuple-element.62), channel_id=1, source_target_pairs={{0,1},{1,0},{2,3},{3,2},{4,5},{5,4},{6,7},{7,6},{8,9},{9,8},{10,11... | collective-permute-start | bytes 1572872 | tf_op jit(solution)/shard_map/ppermute | solution.py:611
  39.4 0.4 %keep.1.keep_ref = bf16[256,1024]{1,0:T(8,128)(2,1)S(1)} custom-call(bf16[256,384]{1,0:T(8,128)(2,1)S(1)} %get-tuple-element.61.rec_ref, f32[256,2048]{1,0:T(8,128)S(1)} %pool.1.part_ref, bf16[384,2048]{1,0:T(8,128)(2,1)S(1)} %copy-done), custom_call_target="tpu_custom_call" | custom-call | flops 300000000 | tf_op jit(solution)/shard_map/keep/pallas_call | solution.py:612
  39.9 1.1 %collective-permute-done.10.arrived_ref = bf16[256,1024]{1,0:T(8,128)(2,1)S(1)} collective-permute-done((bf16[256,1024]{1,0:T(8,128)(2,1)S(1)}, bf16[256,1024]{1,0:T(8,128)(2,1)S(1)}, u32[]{:S(2)}, u32[]{:S(2)}) %collective-permute-start.10) | collective-permute-done | bytes 524320 | tf_op jit(solution)/shard_map/ppermute | solution.py:611
  41.0 0.8 %sum.1 = bf16[256,1024]{1,0:T(8,128)(2,1)} custom-call(bf16[256,1024]{1,0:T(8,128)(2,1)S(1)} %keep.1.keep_ref, bf16[256,1024]{1,0:T(8,128)(2,1)S(1)} %collective-permute-done.10.arrived_ref), custom_call_target="tpu_custom_call" | custom-call | tf_op jit(solution)/shard_map/sum/pallas_call | solution.py:613
  (25 shorter events, 0.1 us)
Async XLA Ops:
  0.0 4.8 %collective-permute-start = (bf16[2,128,1024]{2,1,0:T(8,128)(2,1)}, bf16[2,128,1024]{2,1,0:T(8,128)(2,1)S(1)}, u32[]{:S(2)}, u32[]{:S(2)}) collective-permute-start(bf16[2,128,1024]{2,1,0:T(8,128)(2,1)} %param.18), channel_id=1, source_target_pairs={{0,1},{1,0},{2,3},{3,2},{4,5},{5,4},{6,7},{7,6},{8,9},{9,8},{10,11... | collective-permute-start | bytes 1572872 | tf_op jit(solution)/shard_map/ppermute | solution.py:532
  1.4 3.4 %copy-start.7 = (f32[2048]{0:T(1024)S(1)}, f32[2048]{0:T(1024)}, u32[]{:S(2)}) copy-start(f32[2048]{0:T(1024)} %param.19) | copy-start | bytes 24580
  1.4 3.4 %copy-start.10 = (bf16[2048,256]{1,0:T(8,128)(2,1)S(1)}, bf16[2048,256]{1,0:T(8,128)(2,1)}, u32[]{:S(2)}) copy-start(bf16[2048,256]{1,0:T(8,128)(2,1)} %refs_8_.1) | copy-start | bytes 3145732
  1.4 3.4 %copy-start.11 = (f32[768]{0:T(1024)S(1)}, f32[768]{0:T(1024)}, u32[]{:S(2)}) copy-start(f32[768]{0:T(1024)} %refs_4_.3) | copy-start | bytes 9220
  1.4 3.4 %copy-start.12 = (f32[768]{0:T(1024)S(1)}, f32[768]{0:T(1024)}, u32[]{:S(2)}) copy-start(f32[768]{0:T(1024)} %refs_5_.3) | copy-start | bytes 9220
  4.8 9.5 %copy-start.1 = (bf16[2048,384]{1,0:T(8,128)(2,1)S(1)}, bf16[2048,384]{1,0:T(8,128)(2,1)}, u32[]{:S(2)}) copy-start(bf16[2048,384]{1,0:T(8,128)(2,1)} %wr_ref.3) | copy-start | bytes 4718596
  4.9 9.5 %copy-start.2 = (bf16[2048,384]{1,0:T(8,128)(2,1)S(1)}, bf16[2048,384]{1,0:T(8,128)(2,1)}, u32[]{:S(2)}) copy-start(bf16[2048,384]{1,0:T(8,128)(2,1)} %wg_ref.1) | copy-start | bytes 4718596
  4.9 9.5 %copy-start.4 = (bf16[2048,256]{1,0:T(8,128)(2,1)S(1)}, bf16[2048,256]{1,0:T(8,128)(2,1)}, u32[]{:S(2)}) copy-start(bf16[2048,256]{1,0:T(8,128)(2,1)} %wq_ref.1) | copy-start | bytes 3145732
  9.7 7.1 %collective-permute-start.2 = (bf16[256,128]{1,0:T(8,128)(2,1)S(1)}, bf16[256,128]{1,0:T(8,128)(2,1)S(1)}, u32[]{:S(2)}, u32[]{:S(2)}) collective-permute-start(bf16[256,128]{1,0:T(8,128)(2,1)S(1)} %get-tuple-element.40), channel_id=1, source_target_pairs={{0,16},{8,24},{16,0},{24,8},{1,17},{9,25},{17,1},{25,9},{2,18},{10... | collective-permute-start | bytes 196616 | tf_op jit(solution)/shard_map/ppermute | solution.py:524
  12.8 4.0 %collective-permute-start.3 = (bf16[256,128]{1,0:T(8,128)(2,1)S(1)}, bf16[256,128]{1,0:T(8,128)(2,1)S(1)}, u32[]{:S(2)}, u32[]{:S(2)}) collective-permute-start(bf16[256,128]{1,0:T(8,128)(2,1)S(1)} %get-tuple-element.41), channel_id=1, source_target_pairs={{0,24},{8,0},{16,8},{24,16},{1,25},{9,1},{17,9},{25,17},{2,26},{10... | collective-permute-start | bytes 196616 | tf_op jit(solution)/shard_map/ppermute | solution.py:524
  13.6 4.5 %collective-permute-start.1 = (bf16[320,128]{1,0:T(8,128)(2,1)S(1)}, bf16[320,128]{1,0:T(8,128)(2,1)S(1)}, u32[]{:S(2)}, u32[]{:S(2)}) collective-permute-start(bf16[320,128]{1,0:T(8,128)(2,1)S(1)} %get-tuple-element.39), channel_id=1, source_target_pairs={{0,8},{8,16},{16,24},{24,0},{1,9},{9,17},{17,25},{25,1},{2,10},{10... | collective-permute-start | bytes 245768 | tf_op jit(solution)/shard_map/ppermute | solution.py:524
  14.3 13.3 %copy-start.5 = (f32[2,6,64,64]{3,2,1,0:T(8,128)S(1)}, f32[2,6,64,64]{3,2,1,0:T(8,128)}, u32[]{:S(2)}) copy-start(f32[2,6,64,64]{3,2,1,0:T(8,128)} %init_ref.1) | copy-start | bytes 589828
  14.3 17.9 %copy-start.6 = (bf16[4,128,128]{2,1,0:T(8,128)(2,1)S(1)}, bf16[4,128,128]{2,1,0:T(8,128)(2,1)}, u32[]{:S(2)}) copy-start(bf16[4,128,128]{2,1,0:T(8,128)(2,1)} %mix_ref.1) | copy-start | bytes 393220
  14.3 17.9 %copy-start.9 = (f32[512]{0:T(512)S(1)}, f32[512]{0:T(512)}, u32[]{:S(2)}) copy-start(f32[512]{0:T(512)} %param.32) | copy-start | bytes 6148
  16.8 15.4 %copy-start.3 = (bf16[256,2048]{1,0:T(8,128)(2,1)S(1)}, bf16[256,2048]{1,0:T(8,128)(2,1)}, u32[]{:S(2)}) copy-start(bf16[256,2048]{1,0:T(8,128)(2,1)} %wp_ref.1) | copy-start | bytes 3145732
  18.7 8.9 %collective-permute-start.4 = (bf16[320,128]{1,0:T(8,128)(2,1)S(1)}, bf16[320,128]{1,0:T(8,128)(2,1)S(1)}, u32[]{:S(2)}, u32[]{:S(2)}) collective-permute-start(bf16[320,128]{1,0:T(8,128)(2,1)S(1)} %get-tuple-element.51), channel_id=1, source_target_pairs={{0,32},{32,64},{64,96},{96,0},{1,33},{33,65},{65,97},{97,1},{2,34}... | collective-permute-start | bytes 245768 | tf_op jit(solution)/shard_map/ppermute | solution.py:524
  20.4 3.5 %collective-permute-start.6 = (bf16[256,128]{1,0:T(8,128)(2,1)S(1)}, bf16[256,128]{1,0:T(8,128)(2,1)S(1)}, u32[]{:S(2)}, u32[]{:S(2)}) collective-permute-start(bf16[256,128]{1,0:T(8,128)(2,1)S(1)} %get-tuple-element.52), channel_id=1, source_target_pairs={{0,96},{32,0},{64,32},{96,64},{1,97},{33,1},{65,33},{97,65},{2,98}... | collective-permute-start | bytes 196616 | tf_op jit(solution)/shard_map/ppermute | solution.py:524
  22.6 5.0 %collective-permute-start.5 = (bf16[256,128]{1,0:T(8,128)(2,1)S(1)}, bf16[256,128]{1,0:T(8,128)(2,1)S(1)}, u32[]{:S(2)}, u32[]{:S(2)}) collective-permute-start(bf16[256,128]{1,0:T(8,128)(2,1)S(1)} %get-tuple-element.52), channel_id=1, source_target_pairs={{0,64},{32,96},{64,0},{96,32},{1,65},{33,97},{65,1},{97,33},{2,66}... | collective-permute-start | bytes 196616 | tf_op jit(solution)/shard_map/ppermute | solution.py:524
  28.5 4.4 %collective-permute-start.7 = (bf16[2,64,128]{2,1,0:T(8,128)(2,1)S(1)}, bf16[2,64,128]{2,1,0:T(8,128)(2,1)S(1)}, u32[]{:S(2)}, u32[]{:S(2)}) collective-permute-start(bf16[2,64,128]{2,1,0:T(8,128)(2,1)S(1)} %get-tuple-element.54), channel_id=1, source_target_pairs={{0,8},{8,16},{16,24},{24,0},{1,9},{9,17},{17,25},{25,1},{2,10},{10... | collective-permute-start | bytes 98312 | tf_op jit(solution)/shard_map/ppermute | solution.py:524
  28.8 4.3 %collective-permute-start.8 = (bf16[2,64,128]{2,1,0:T(8,128)(2,1)S(1)}, bf16[2,64,128]{2,1,0:T(8,128)(2,1)S(1)}, u32[]{:S(2)}, u32[]{:S(2)}) collective-permute-start(bf16[2,64,128]{2,1,0:T(8,128)(2,1)S(1)} %get-tuple-element.55), channel_id=1, source_target_pairs={{0,16},{8,24},{16,0},{24,8},{1,17},{9,25},{17,1},{25,9},{2,18},{10... | collective-permute-start | bytes 98312 | tf_op jit(solution)/shard_map/ppermute | solution.py:524
  30.8 2.8 %collective-permute-start.9 = (bf16[2,64,128]{2,1,0:T(8,128)(2,1)S(1)}, bf16[2,64,128]{2,1,0:T(8,128)(2,1)S(1)}, u32[]{:S(2)}, u32[]{:S(2)}) collective-permute-start(bf16[2,64,128]{2,1,0:T(8,128)(2,1)S(1)} %get-tuple-element.56), channel_id=1, source_target_pairs={{0,24},{8,0},{16,8},{24,16},{1,25},{9,1},{17,9},{25,17},{2,26},{10... | collective-permute-start | bytes 98312 | tf_op jit(solution)/shard_map/ppermute | solution.py:524
  32.2 1.4 %copy-start = (bf16[384,2048]{1,0:T(8,128)(2,1)S(1)}, bf16[384,2048]{1,0:T(8,128)(2,1)}, u32[]{:S(2)}) copy-start(bf16[384,2048]{1,0:T(8,128)(2,1)} %wr_ref.5) | copy-start | bytes 4718596
  32.2 1.4 %copy-start.8 = (f32[768]{0:T(1024)S(1)}, f32[768]{0:T(1024)}, u32[]{:S(2)}) copy-start(f32[768]{0:T(1024)} %hgain_ref.1) | copy-start | bytes 9220
  35.3 5.7 %collective-permute-start.10 = (bf16[256,1024]{1,0:T(8,128)(2,1)S(1)}, bf16[256,1024]{1,0:T(8,128)(2,1)S(1)}, u32[]{:S(2)}, u32[]{:S(2)}) collective-permute-start(bf16[256,1024]{1,0:T(8,128)(2,1)S(1)} %get-tuple-element.62), channel_id=1, source_target_pairs={{0,1},{1,0},{2,3},{3,2},{4,5},{5,4},{6,7},{7,6},{8,9},{9,8},{10,11... | collective-permute-start | bytes 1572872 | tf_op jit(solution)/shard_map/ppermute | solution.py:611

commit v9 on v8

--- a/solution.py
+++ b/solution.py
@@ -33,13 +33,13 @@
 
 
 def dot_fine_left(a, b, dims=NN):
-    high, low = halves(a)
-    return dot(high, b, dims) + dot(low, b, dims)
+    b = b.astype(bf16)
+    return dot(jnp.concatenate(halves(a), axis=1), jnp.concatenate([b, b], axis=0), dims)
 
 
 def dot_fine_right(a, b, dims=NN):
-    high, low = halves(b)
-    return dot(a, high, dims) + dot(a, low, dims)
+    a = a.astype(bf16)
+    return dot(jnp.concatenate([a, a], axis=1), jnp.concatenate(halves(b), axis=0), dims)
 
 
 def iota(rows, cols, dim):
@@ -304,10 +304,19 @@
     carries = [dot(carries[u], both(v_ref[u], masks)) for u in units]
     solutions = []
     for u in units:
-        wanted = jnp.concatenate([second_stage[u][1].astype(bf16), carries[u].astype(bf16)], axis=1)
-        solved = dot(inverse[u], both(wanted, wide)).astype(bf16)
+        wanted = jnp.concatenate([second_stage[u][1], carries[u]], axis=1)
+        solutions.append((wanted, dot(inverse[u], both(wanted, wide))))
+    missing = []
+    for u in units:
+        wanted, solved = solutions[u]
+        high, low = halves(solved)
+        left = jnp.concatenate([lowers[u], lowers[u]], axis=1)
+        applied = dot(left, jnp.concatenate([both(high, wide), both(low, wide)], axis=0))
+        missing.append(wanted - solved - applied)
+    for u in units:
+        solved = (solutions[u][1] + dot(inverse[u], both(missing[u], wide))).astype(bf16)
         solved_ref[u] = solved
-        solutions.append(solved)
+        solutions[u] = solved
     for u in units:
         right, _, ends, _ = second_stage[u]
         solved = solutions[u]

time: 41.9 us -> 42.2 us (level)
    pallas_call x1, Pallas kernels: 4.86 us -> 5.29 us  [shards(): call(local_kernel, 'local', vmem(9), [shape((256, 1024)), shape((256, 128...]
where the time goes in v9:
time: 42.2 us; the launch traced here: 42.1 us
  starting transfers between devices  19 us (45%)
  Pallas kernels  16.1 us (38%)
  waiting for transfers between devices  6.79 us (16%)
    ppermute x9, starting transfers between devices, around(): lax.ppermute(part, axis, [(i, i + step & 3) for i in range(4)])  13.4 us
    ppermute x9, waiting for transfers between devices, around(): lax.ppermute(part, axis, [(i, i + step & 3) for i in range(4)])  5.69 us
    pallas_call x1, Pallas kernels, shards(): call(local_kernel, 'local', vmem(9), [shape((256, 1024)), shape((256, 128...  5.29 us
    ppermute x1, starting transfers between devices, shards(): arrived = lax.ppermute(send, 'tp', [(0, 1), (1, 0)])  4.14 us
    pallas_call x1, Pallas kernels, shards(): call(own_kernel, 'own', hbm(6), [shape((256, 1024)), shape((256, 128), f3...  3.39 us
    pallas_call x1, Pallas kernels, shards(): call(side_kernel, 'side', vmem(11), [shape((6, 128, 128)), shape((6, 128,...  2.47 us
    pallas_call x1, Pallas kernels, shards(): call(final_kernel, 'final', vmem(10), [shape((256, 1024)), shape((256, 38...  1.51 us
    ppermute x1, starting transfers between devices, shards(): other = lax.ppermute(tokens, 'tp', [(0, 1), (1, 0)])  1.38 us
  transfers between devices with their start and end apart: 11, of which 6 were waited for; matrix products, arithmetic and copies ran while one was open for 0% of the time, Pallas kernels for 17%

profile of v9, /device:TPU:1, one launch (start us, length us, event | category | flops | bytes accessed | tf_op | source)
XLA Modules:
  0.0 42.1 jit_solution(8572372735779161206)
XLA Ops:
  0.0 1.4 %collective-permute-start = (bf16[2,128,1024]{2,1,0:T(8,128)(2,1)}, bf16[2,128,1024]{2,1,0:T(8,128)(2,1)S(1)}, u32[]{:S(2)}, u32[]{:S(2)}) collective-permute-start(bf16[2,128,1024]{2,1,0:T(8,128)(2,1)} %param.18), channel_id=1, source_target_pairs={{0,1},{1,0},{2,3},{3,2},{4,5},{5,4},{6,7},{7,6},{8,9},{9,8},{10,11... | collective-permute-start | bytes 1572872 | tf_op jit(solution)/shard_map/ppermute | solution.py:541
  1.4 3.4 %own.1 = (bf16[256,1024]{1,0:T(8,128)(2,1)S(1)}, f32[256,128]{1,0:T(8,128)S(1)}, f32[256,1536]{1,0:T(8,128)S(1)}, bf16[1024,1536]{1,0:T(8,128)(2,1)S(1)}) custom-call(bf16[256,1024]{1,0:T(8,128)(2,1)} %bitcast.9, f32[1,2048]{1,0:T(1,128)} %bitcast.5, bf16[2048,384]{1,0:T(8,128)(2,1)} %refs_2_.1, bf16[2048,384]{1,0:T(8,128)(2,1)} %refs_3_.1, ...), custom_call_target="tpu_custom_call" | custom-call | flops 1000000000 | tf_op jit(solution)/shard_map/own/pallas_call | solution.py:545
  4.8 0.0 copy-start.1
  4.9 0.0 copy-start.4
  4.9 5.3 %local.1 = (bf16[256,1024]{1,0:T(8,128)(2,1)S(1)}, f32[256,128]{1,0:T(8,128)S(1)}, bf16[256,256]{1,0:T(8,128)(2,1)S(1)}, bf16[256,128]{1,0:T(8,128)(2,1)S(1)}, b...) custom-call(bf16[256,1024]{1,0:T(8,128)(2,1)S(1)} %bitcast.8, ...), custom_call_target="tpu_custom_call" | custom-call | flops 3000000000 | tf_op jit(solution)/shard_map/local/pallas_call | solution.py:559
  10.2 3.1 %collective-permute-start.2 = (bf16[256,128]{1,0:T(8,128)(2,1)S(1)}, bf16[256,128]{1,0:T(8,128)(2,1)S(1)}, u32[]{:S(2)}, u32[]{:S(2)}) collective-permute-start(bf16[256,128]{1,0:T(8,128)(2,1)S(1)} %get-tuple-element.40), channel_id=1, source_target_pairs={{0,16},{8,24},{16,0},{24,8},{1,17},{9,25},{17,1},{25,9},{2,18},{10... | collective-permute-start | bytes 196616 | tf_op jit(solution)/shard_map/ppermute | solution.py:533
  13.3 0.8 %collective-permute-start.3 = (bf16[256,128]{1,0:T(8,128)(2,1)S(1)}, bf16[256,128]{1,0:T(8,128)(2,1)S(1)}, u32[]{:S(2)}, u32[]{:S(2)}) collective-permute-start(bf16[256,128]{1,0:T(8,128)(2,1)S(1)} %get-tuple-element.41), channel_id=1, source_target_pairs={{0,24},{8,0},{16,8},{24,16},{1,25},{9,1},{17,9},{25,17},{2,26},{10... | collective-permute-start | bytes 196616 | tf_op jit(solution)/shard_map/ppermute | solution.py:533
  14.1 0.7 %collective-permute-start.1 = (bf16[320,128]{1,0:T(8,128)(2,1)S(1)}, bf16[320,128]{1,0:T(8,128)(2,1)S(1)}, u32[]{:S(2)}, u32[]{:S(2)}) collective-permute-start(bf16[320,128]{1,0:T(8,128)(2,1)S(1)} %get-tuple-element.39), channel_id=1, source_target_pairs={{0,8},{8,16},{16,24},{24,0},{1,9},{9,17},{17,25},{25,1},{2,10},{10... | collective-permute-start | bytes 245768 | tf_op jit(solution)/shard_map/ppermute | solution.py:533
  14.8 0.0 copy-start.6
  14.8 0.0 copy-start.9
  14.8 2.5 %side.1 = (bf16[6,128,128]{2,1,0:T(8,128)(2,1)S(1)}, f32[6,128,128]{2,1,0:T(8,128)S(1)}, bf16[256,384]{1,0:T(8,128)(2,1)S(1)}, bf16[256,256]{1,0:T(8,128)(2,1)S(1)}) custom-call(bf16[256,1024]{1,0:T(8,128)(2,1)S(1)} %get-tuple-element.34.refs_1_.own_ref, bf16[256,1024]{1,0:T(8,128)(2,1)S(1)} %get-tuple-element.42.other_ref, ...), custom_call_target="tpu_custom_call" | custom-call | flops 1000000000 | tf_op jit(solution)/shard_map/side/pallas_call | solution.py:579
  17.3 1.3 %collective-permute-done.1.first_ref.beside_ref = bf16[320,128]{1,0:T(8,128)(2,1)S(1)} collective-permute-done((bf16[320,128]{1,0:T(8,128)(2,1)S(1)}, bf16[320,128]{1,0:T(8,128)(2,1)S(1)}, u32[]{:S(2)}, u32[]{:S(2)}) %collective-permute-start.1) | collective-permute-done | bytes 81952 | tf_op jit(solution)/shard_map/ppermute | solution.py:533
  18.6 0.6 %row.1 = (f32[3,2,128,128]{3,2,1,0:T(8,128)S(1)}, bf16[320,128]{1,0:T(8,128)(2,1)S(1)}, bf16[256,128]{1,0:T(8,128)(2,1)S(1)}) custom-call(bf16[256,128]{1,0:T(8,128)(2,1)S(1)} %get-tuple-element.38.home_ref, bf16[320,128]{1,0:T(8,128)(2,1)S(1)} %collective-permute-done.1.first_ref.beside_ref, bf16[256,128]{1,0:T(8,128)(2,1)S(1)} %collective-permute-done.2.second_ref, ...), custom_call_target="tpu_custom_call" | custom-call | flops 100000000 | tf_op jit(solution)/shard_map/row/pallas_call | solution.py:588
  19.1 1.7 %collective-permute-start.4 = (bf16[320,128]{1,0:T(8,128)(2,1)S(1)}, bf16[320,128]{1,0:T(8,128)(2,1)S(1)}, u32[]{:S(2)}, u32[]{:S(2)}) collective-permute-start(bf16[320,128]{1,0:T(8,128)(2,1)S(1)} %get-tuple-element.51), channel_id=1, source_target_pairs={{0,32},{32,64},{64,96},{96,0},{1,33},{33,65},{65,97},{97,1},{2,34}... | collective-permute-start | bytes 245768 | tf_op jit(solution)/shard_map/ppermute | solution.py:533
  20.8 2.2 %collective-permute-start.6 = (bf16[256,128]{1,0:T(8,128)(2,1)S(1)}, bf16[256,128]{1,0:T(8,128)(2,1)S(1)}, u32[]{:S(2)}, u32[]{:S(2)}) collective-permute-start(bf16[256,128]{1,0:T(8,128)(2,1)S(1)} %get-tuple-element.52), channel_id=1, source_target_pairs={{0,96},{32,0},{64,32},{96,64},{1,97},{33,1},{65,33},{97,65},{2,98}... | collective-permute-start | bytes 196616 | tf_op jit(solution)/shard_map/ppermute | solution.py:533
  23.1 1.2 %collective-permute-start.5 = (bf16[256,128]{1,0:T(8,128)(2,1)S(1)}, bf16[256,128]{1,0:T(8,128)(2,1)S(1)}, u32[]{:S(2)}, u32[]{:S(2)}) collective-permute-start(bf16[256,128]{1,0:T(8,128)(2,1)S(1)} %get-tuple-element.52), channel_id=1, source_target_pairs={{0,64},{32,96},{64,0},{96,32},{1,65},{33,97},{65,1},{97,33},{2,66}... | collective-permute-start | bytes 196616 | tf_op jit(solution)/shard_map/ppermute | solution.py:533
  24.3 0.1 collective-permute-done.6.third_ref
  24.4 3.7 %collective-permute-done.5.second_ref = bf16[256,128]{1,0:T(8,128)(2,1)S(1)} collective-permute-done((bf16[256,128]{1,0:T(8,128)(2,1)S(1)}, bf16[256,128]{1,0:T(8,128)(2,1)S(1)}, u32[]{:S(2)}, u32[]{:S(2)}) %collective-permute-start.5) | collective-permute-done | bytes 65568 | tf_op jit(solution)/shard_map/ppermute | solution.py:533
  28.1 0.9 %column.1 = (bf16[2,64,128]{2,1,0:T(8,128)(2,1)S(1)}, bf16[2,64,128]{2,1,0:T(8,128)(2,1)S(1)}, bf16[2,64,128]{2,1,0:T(8,128)(2,1)S(1)}, bf16[2,64,128]{2,1,0:T(8,128)(2,1)S(1)}) custom-call(f32[3,2,128,128]{3,2,1,0:T(8,128)S(1)} %get-tuple-element.50.prefix_ref, bf16[320,128]{1,0:T(8,128)(2,1)S(1)} %collective-permute-done.4.first_ref.above_ref, ...), custom_call_target="tpu_custom_call" | custom-call | flops 100000000 | tf_op jit(solution)/shard_map/column/pallas_call | solution.py:598
  28.9 0.3 collective-permute-start.7
  29.3 2.0 %collective-permute-start.8 = (bf16[2,64,128]{2,1,0:T(8,128)(2,1)S(1)}, bf16[2,64,128]{2,1,0:T(8,128)(2,1)S(1)}, u32[]{:S(2)}, u32[]{:S(2)}) collective-permute-start(bf16[2,64,128]{2,1,0:T(8,128)(2,1)S(1)} %get-tuple-element.55), channel_id=1, source_target_pairs={{0,16},{8,24},{16,0},{24,8},{1,17},{9,25},{17,1},{25,9},{2,18},{10... | collective-permute-start | bytes 98312 | tf_op jit(solution)/shard_map/ppermute | solution.py:533
  31.3 1.4 %collective-permute-start.9 = (bf16[2,64,128]{2,1,0:T(8,128)(2,1)S(1)}, bf16[2,64,128]{2,1,0:T(8,128)(2,1)S(1)}, u32[]{:S(2)}, u32[]{:S(2)}) collective-permute-start(bf16[2,64,128]{2,1,0:T(8,128)(2,1)S(1)} %get-tuple-element.56), channel_id=1, source_target_pairs={{0,24},{8,0},{16,8},{24,16},{1,25},{9,1},{17,9},{25,17},{2,26},{10... | collective-permute-start | bytes 98312 | tf_op jit(solution)/shard_map/ppermute | solution.py:533
  32.7 0.0 copy-start.8
  32.7 0.6 %pool.1.part_ref = f32[256,2048]{1,0:T(8,128)S(1)} custom-call(bf16[256,256]{1,0:T(8,128)(2,1)S(1)} %get-tuple-element.60.pool_ref, bf16[320,128]{1,0:T(8,128)(2,1)S(1)} %collective-permute-done.1.first_ref.beside_ref, bf16[320,128]{1,0:T(8,128)(2,1)S(1)} %collective-permute-done.4.first_ref.above_ref, ...), custom_call_target="tpu_custom_call" | custom-call | flops 300000000 | tf_op jit(solution)/shard_map/pool/pallas_call | solution.py:608
  33.4 0.2 collective-permute-done.8.two_ref
  33.6 0.5 %collective-permute-done.9.three_ref = bf16[2,64,128]{2,1,0:T(8,128)(2,1)S(1)} collective-permute-done((bf16[2,64,128]{2,1,0:T(8,128)(2,1)S(1)}, bf16[2,64,128]{2,1,0:T(8,128)(2,1)S(1)}, u32[]{:S(2)}, u32[]{:S(2)}) %collective-permute-start.9) | collective-permute-done | bytes 32800 | tf_op jit(solution)/shard_map/ppermute | solution.py:533
  34.0 0.1 copy-done
  34.1 1.5 %final.1 = (bf16[256,1024]{1,0:T(8,128)(2,1)S(1)}, bf16[256,384]{1,0:T(8,128)(2,1)S(1)}) custom-call(bf16[2,64,128]{2,1,0:T(8,128)(2,1)S(1)} %get-tuple-element.53.home_ref, bf16[2,64,128]{2,1,0:T(8,128)(2,1)S(1)} %collective-permute-done.7.one_ref, bf16[2,64,128]{2,1,0:T(8,128)(2,1)S(1)} %collective-permute-done.8.two_ref, ...), custom_call_target="tpu_custom_call" | custom-call | flops 1000000000 | tf_op jit(solution)/shard_map/final/pallas_call | solution.py:611
  35.6 4.1 %collective-permute-start.10 = (bf16[256,1024]{1,0:T(8,128)(2,1)S(1)}, bf16[256,1024]{1,0:T(8,128)(2,1)S(1)}, u32[]{:S(2)}, u32[]{:S(2)}) collective-permute-start(bf16[256,1024]{1,0:T(8,128)(2,1)S(1)} %get-tuple-element.62), channel_id=1, source_target_pairs={{0,1},{1,0},{2,3},{3,2},{4,5},{5,4},{6,7},{7,6},{8,9},{9,8},{10,11... | collective-permute-start | bytes 1572872 | tf_op jit(solution)/shard_map/ppermute | solution.py:620
  39.7 0.4 %keep.1.keep_ref = bf16[256,1024]{1,0:T(8,128)(2,1)S(1)} custom-call(bf16[256,384]{1,0:T(8,128)(2,1)S(1)} %get-tuple-element.61.rec_ref, f32[256,2048]{1,0:T(8,128)S(1)} %pool.1.part_ref, bf16[384,2048]{1,0:T(8,128)(2,1)S(1)} %copy-done), custom_call_target="tpu_custom_call" | custom-call | flops 300000000 | tf_op jit(solution)/shard_map/keep/pallas_call | solution.py:621
  40.2 1.1 %collective-permute-done.10.arrived_ref = bf16[256,1024]{1,0:T(8,128)(2,1)S(1)} collective-permute-done((bf16[256,1024]{1,0:T(8,128)(2,1)S(1)}, bf16[256,1024]{1,0:T(8,128)(2,1)S(1)}, u32[]{:S(2)}, u32[]{:S(2)}) %collective-permute-start.10) | collective-permute-done | bytes 524320 | tf_op jit(solution)/shard_map/ppermute | solution.py:620
  41.3 0.8 %sum.1 = bf16[256,1024]{1,0:T(8,128)(2,1)} custom-call(bf16[256,1024]{1,0:T(8,128)(2,1)S(1)} %keep.1.keep_ref, bf16[256,1024]{1,0:T(8,128)(2,1)S(1)} %collective-permute-done.10.arrived_ref), custom_call_target="tpu_custom_call" | custom-call | tf_op jit(solution)/shard_map/sum/pallas_call | solution.py:622
  (25 shorter events, 0.1 us)
Async XLA Ops:
  0.0 4.8 %collective-permute-start = (bf16[2,128,1024]{2,1,0:T(8,128)(2,1)}, bf16[2,128,1024]{2,1,0:T(8,128)(2,1)S(1)}, u32[]{:S(2)}, u32[]{:S(2)}) collective-permute-start(bf16[2,128,1024]{2,1,0:T(8,128)(2,1)} %param.18), channel_id=1, source_target_pairs={{0,1},{1,0},{2,3},{3,2},{4,5},{5,4},{6,7},{7,6},{8,9},{9,8},{10,11... | collective-permute-start | bytes 1572872 | tf_op jit(solution)/shard_map/ppermute | solution.py:541
  1.4 3.4 %copy-start.7 = (f32[2048]{0:T(1024)S(1)}, f32[2048]{0:T(1024)}, u32[]{:S(2)}) copy-start(f32[2048]{0:T(1024)} %param.19) | copy-start | bytes 24580
  1.4 3.4 %copy-start.10 = (bf16[2048,256]{1,0:T(8,128)(2,1)S(1)}, bf16[2048,256]{1,0:T(8,128)(2,1)}, u32[]{:S(2)}) copy-start(bf16[2048,256]{1,0:T(8,128)(2,1)} %refs_8_.1) | copy-start | bytes 3145732
  1.4 3.4 %copy-start.11 = (f32[768]{0:T(1024)S(1)}, f32[768]{0:T(1024)}, u32[]{:S(2)}) copy-start(f32[768]{0:T(1024)} %refs_4_.3) | copy-start | bytes 9220
  1.4 3.4 %copy-start.12 = (f32[768]{0:T(1024)S(1)}, f32[768]{0:T(1024)}, u32[]{:S(2)}) copy-start(f32[768]{0:T(1024)} %refs_5_.3) | copy-start | bytes 9220
  4.8 9.9 %copy-start.1 = (bf16[2048,384]{1,0:T(8,128)(2,1)S(1)}, bf16[2048,384]{1,0:T(8,128)(2,1)}, u32[]{:S(2)}) copy-start(bf16[2048,384]{1,0:T(8,128)(2,1)} %wr_ref.3) | copy-start | bytes 4718596
  4.9 9.9 %copy-start.2 = (bf16[2048,384]{1,0:T(8,128)(2,1)S(1)}, bf16[2048,384]{1,0:T(8,128)(2,1)}, u32[]{:S(2)}) copy-start(bf16[2048,384]{1,0:T(8,128)(2,1)} %wg_ref.1) | copy-start | bytes 4718596
  4.9 9.9 %copy-start.4 = (bf16[2048,256]{1,0:T(8,128)(2,1)S(1)}, bf16[2048,256]{1,0:T(8,128)(2,1)}, u32[]{:S(2)}) copy-start(bf16[2048,256]{1,0:T(8,128)(2,1)} %wq_ref.1) | copy-start | bytes 3145732
  10.2 7.1 %collective-permute-start.2 = (bf16[256,128]{1,0:T(8,128)(2,1)S(1)}, bf16[256,128]{1,0:T(8,128)(2,1)S(1)}, u32[]{:S(2)}, u32[]{:S(2)}) collective-permute-start(bf16[256,128]{1,0:T(8,128)(2,1)S(1)} %get-tuple-element.40), channel_id=1, source_target_pairs={{0,16},{8,24},{16,0},{24,8},{1,17},{9,25},{17,1},{25,9},{2,18},{10... | collective-permute-start | bytes 196616 | tf_op jit(solution)/shard_map/ppermute | solution.py:533
  13.3 4.0 %collective-permute-start.3 = (bf16[256,128]{1,0:T(8,128)(2,1)S(1)}, bf16[256,128]{1,0:T(8,128)(2,1)S(1)}, u32[]{:S(2)}, u32[]{:S(2)}) collective-permute-start(bf16[256,128]{1,0:T(8,128)(2,1)S(1)} %get-tuple-element.41), channel_id=1, source_target_pairs={{0,24},{8,0},{16,8},{24,16},{1,25},{9,1},{17,9},{25,17},{2,26},{10... | collective-permute-start | bytes 196616 | tf_op jit(solution)/shard_map/ppermute | solution.py:533
  14.1 4.5 %collective-permute-start.1 = (bf16[320,128]{1,0:T(8,128)(2,1)S(1)}, bf16[320,128]{1,0:T(8,128)(2,1)S(1)}, u32[]{:S(2)}, u32[]{:S(2)}) collective-permute-start(bf16[320,128]{1,0:T(8,128)(2,1)S(1)} %get-tuple-element.39), channel_id=1, source_target_pairs={{0,8},{8,16},{16,24},{24,0},{1,9},{9,17},{17,25},{25,1},{2,10},{10... | collective-permute-start | bytes 245768 | tf_op jit(solution)/shard_map/ppermute | solution.py:533
  14.8 13.3 %copy-start.5 = (f32[2,6,64,64]{3,2,1,0:T(8,128)S(1)}, f32[2,6,64,64]{3,2,1,0:T(8,128)}, u32[]{:S(2)}) copy-start(f32[2,6,64,64]{3,2,1,0:T(8,128)} %init_ref.1) | copy-start | bytes 589828
  14.8 17.9 %copy-start.6 = (bf16[4,128,128]{2,1,0:T(8,128)(2,1)S(1)}, bf16[4,128,128]{2,1,0:T(8,128)(2,1)}, u32[]{:S(2)}) copy-start(bf16[4,128,128]{2,1,0:T(8,128)(2,1)} %mix_ref.1) | copy-start | bytes 393220
  14.8 17.9 %copy-start.9 = (f32[512]{0:T(512)S(1)}, f32[512]{0:T(512)}, u32[]{:S(2)}) copy-start(f32[512]{0:T(512)} %param.32) | copy-start | bytes 6148
  17.3 15.4 %copy-start.3 = (bf16[256,2048]{1,0:T(8,128)(2,1)S(1)}, bf16[256,2048]{1,0:T(8,128)(2,1)}, u32[]{:S(2)}) copy-start(bf16[256,2048]{1,0:T(8,128)(2,1)} %wp_ref.1) | copy-start | bytes 3145732
  19.1 8.9 %collective-permute-start.4 = (bf16[320,128]{1,0:T(8,128)(2,1)S(1)}, bf16[320,128]{1,0:T(8,128)(2,1)S(1)}, u32[]{:S(2)}, u32[]{:S(2)}) collective-permute-start(bf16[320,128]{1,0:T(8,128)(2,1)S(1)} %get-tuple-element.51), channel_id=1, source_target_pairs={{0,32},{32,64},{64,96},{96,0},{1,33},{33,65},{65,97},{97,1},{2,34}... | collective-permute-start | bytes 245768 | tf_op jit(solution)/shard_map/ppermute | solution.py:533
  20.8 3.5 %collective-permute-start.6 = (bf16[256,128]{1,0:T(8,128)(2,1)S(1)}, bf16[256,128]{1,0:T(8,128)(2,1)S(1)}, u32[]{:S(2)}, u32[]{:S(2)}) collective-permute-start(bf16[256,128]{1,0:T(8,128)(2,1)S(1)} %get-tuple-element.52), channel_id=1, source_target_pairs={{0,96},{32,0},{64,32},{96,64},{1,97},{33,1},{65,33},{97,65},{2,98}... | collective-permute-start | bytes 196616 | tf_op jit(solution)/shard_map/ppermute | solution.py:533
  23.1 5.0 %collective-permute-start.5 = (bf16[256,128]{1,0:T(8,128)(2,1)S(1)}, bf16[256,128]{1,0:T(8,128)(2,1)S(1)}, u32[]{:S(2)}, u32[]{:S(2)}) collective-permute-start(bf16[256,128]{1,0:T(8,128)(2,1)S(1)} %get-tuple-element.52), channel_id=1, source_target_pairs={{0,64},{32,96},{64,0},{96,32},{1,65},{33,97},{65,1},{97,33},{2,66}... | collective-permute-start | bytes 196616 | tf_op jit(solution)/shard_map/ppermute | solution.py:533
  28.9 4.4 %collective-permute-start.7 = (bf16[2,64,128]{2,1,0:T(8,128)(2,1)S(1)}, bf16[2,64,128]{2,1,0:T(8,128)(2,1)S(1)}, u32[]{:S(2)}, u32[]{:S(2)}) collective-permute-start(bf16[2,64,128]{2,1,0:T(8,128)(2,1)S(1)} %get-tuple-element.54), channel_id=1, source_target_pairs={{0,8},{8,16},{16,24},{24,0},{1,9},{9,17},{17,25},{25,1},{2,10},{10... | collective-permute-start | bytes 98312 | tf_op jit(solution)/shard_map/ppermute | solution.py:533
  29.3 4.3 %collective-permute-start.8 = (bf16[2,64,128]{2,1,0:T(8,128)(2,1)S(1)}, bf16[2,64,128]{2,1,0:T(8,128)(2,1)S(1)}, u32[]{:S(2)}, u32[]{:S(2)}) collective-permute-start(bf16[2,64,128]{2,1,0:T(8,128)(2,1)S(1)} %get-tuple-element.55), channel_id=1, source_target_pairs={{0,16},{8,24},{16,0},{24,8},{1,17},{9,25},{17,1},{25,9},{2,18},{10... | collective-permute-start | bytes 98312 | tf_op jit(solution)/shard_map/ppermute | solution.py:533
  31.3 2.8 %collective-permute-start.9 = (bf16[2,64,128]{2,1,0:T(8,128)(2,1)S(1)}, bf16[2,64,128]{2,1,0:T(8,128)(2,1)S(1)}, u32[]{:S(2)}, u32[]{:S(2)}) collective-permute-start(bf16[2,64,128]{2,1,0:T(8,128)(2,1)S(1)} %get-tuple-element.56), channel_id=1, source_target_pairs={{0,24},{8,0},{16,8},{24,16},{1,25},{9,1},{17,9},{25,17},{2,26},{10... | collective-permute-start | bytes 98312 | tf_op jit(solution)/shard_map/ppermute | solution.py:533
  32.7 1.4 %copy-start = (bf16[384,2048]{1,0:T(8,128)(2,1)S(1)}, bf16[384,2048]{1,0:T(8,128)(2,1)}, u32[]{:S(2)}) copy-start(bf16[384,2048]{1,0:T(8,128)(2,1)} %wr_ref.5) | copy-start | bytes 4718596
  32.7 1.4 %copy-start.8 = (f32[768]{0:T(1024)S(1)}, f32[768]{0:T(1024)}, u32[]{:S(2)}) copy-start(f32[768]{0:T(1024)} %hgain_ref.1) | copy-start | bytes 9220
  35.6 5.7 %collective-permute-start.10 = (bf16[256,1024]{1,0:T(8,128)(2,1)S(1)}, bf16[256,1024]{1,0:T(8,128)(2,1)S(1)}, u32[]{:S(2)}, u32[]{:S(2)}) collective-permute-start(bf16[256,1024]{1,0:T(8,128)(2,1)S(1)} %get-tuple-element.62), channel_id=1, source_target_pairs={{0,1},{1,0},{2,3},{3,2},{4,5},{5,4},{6,7},{7,6},{8,9},{9,8},{10,11... | collective-permute-start | bytes 1572872 | tf_op jit(solution)/shard_map/ppermute | solution.py:620

commit v10 on v9

--- a/solution.py
+++ b/solution.py
@@ -115,29 +115,20 @@
     near = ((row >> 1) == (col >> 1)).astype(bf16)
     result = [eye - (lower * near).astype(f32) for lower in lowers]
     size, level = 2, 1
-    while size < SPAN:
+    while size < 8:
         off = (((row >> (level + 1)) == (col >> (level + 1))) & ((row >> level) != (col >> level))).astype(bf16)
-        if size < 8:
-            inner = [dot(lower * off, blocks(inv)) for lower, inv in zip(lowers, result)]
-            fill(level)
-            result = [inv - dot(inv, blocks(part)) for inv, part in zip(result, inner)]
-        else:
-            if size < 16:
-                off = pick(off.astype(f32), size, 1).astype(bf16)
-                odd = [pick(lower.astype(f32), size, 1).astype(bf16) for lower in lowers]
-            else:
-                off = pick(off, size, 1)
-                odd = [pick(lower, size, 1) for lower in lowers]
-            inner = [dot(lower * off, blocks(inv)) for lower, inv in zip(odd, result)]
-            fill(level)
-            outer = [
-                dot(pick(inv, size, 1), blocks(woven(part, size))) for inv, part in zip(result, inner)
-            ]
-            result = [
-                weave(pick(inv, size, 0), pick(inv, size, 1) - part, size)
-                for inv, part in zip(result, outer)
-            ]
+        inner = [dot(lower * off, blocks(inv)) for lower, inv in zip(lowers, result)]
+        fill(level)
+        result = [inv - dot(inv, blocks(part)) for inv, part in zip(result, inner)]
         size, level = size * 2, level + 1
+    for turn in (3, 4):
+        off = (((row >> (level + 2)) == (col >> (level + 2))) & ((row >> level) != (col >> level))).astype(bf16)
+        mixes = [dot(inv, blocks(lower * off)).astype(bf16) for lower, inv in zip(lowers, result)]
+        fill(turn)
+        squares = [dot(mix, blocks(mix)) for mix in mixes]
+        halfway = [inv - dot(mix, blocks(inv)) for mix, inv in zip(mixes, result)]
+        result = [part + dot(square, blocks(part)) for part, square in zip(halfway, squares)]
+        level += 2
     return result
 
 

time: 42.2 us -> 42.2 us (level)
  no operation moved by 1% of the time
where the time goes in v10:
time: 42.2 us; the launch traced here: 42.1 us
  starting transfers between devices  19 us (45%)
  Pallas kernels  15.9 us (38%)
  waiting for transfers between devices  6.79 us (16%)
    ppermute x9, starting transfers between devices, around(): lax.ppermute(part, axis, [(i, i + step & 3) for i in range(4)])  13.4 us
    ppermute x9, waiting for transfers between devices, around(): lax.ppermute(part, axis, [(i, i + step & 3) for i in range(4)])  5.69 us
    pallas_call x1, Pallas kernels, shards(): call(local_kernel, 'local', vmem(9), [shape((256, 1024)), shape((256, 128...  5.12 us
    ppermute x1, starting transfers between devices, shards(): arrived = lax.ppermute(send, 'tp', [(0, 1), (1, 0)])  4.14 us
    pallas_call x1, Pallas kernels, shards(): call(own_kernel, 'own', hbm(6), [shape((256, 1024)), shape((256, 128), f3...  3.39 us
    pallas_call x1, Pallas kernels, shards(): call(side_kernel, 'side', vmem(11), [shape((6, 128, 128)), shape((6, 128,...  2.47 us
    pallas_call x1, Pallas kernels, shards(): call(final_kernel, 'final', vmem(10), [shape((256, 1024)), shape((256, 38...  1.51 us
    ppermute x1, starting transfers between devices, shards(): other = lax.ppermute(tokens, 'tp', [(0, 1), (1, 0)])  1.38 us
  transfers between devices with their start and end apart: 11, of which 6 were waited for; matrix products, arithmetic and copies ran while one was open for 0% of the time, Pallas kernels for 17%

profile of v10, /device:TPU:1, one launch (start us, length us, event | category | flops | bytes accessed | tf_op | source)
XLA Modules:
  0.0 42.1 jit_solution(9561534817460474032)
XLA Ops:
  0.0 1.4 %collective-permute-start = (bf16[2,128,1024]{2,1,0:T(8,128)(2,1)}, bf16[2,128,1024]{2,1,0:T(8,128)(2,1)S(1)}, u32[]{:S(2)}, u32[]{:S(2)}) collective-permute-start(bf16[2,128,1024]{2,1,0:T(8,128)(2,1)} %param.18), channel_id=1, source_target_pairs={{0,1},{1,0},{2,3},{3,2},{4,5},{5,4},{6,7},{7,6},{8,9},{9,8},{10,11... | collective-permute-start | bytes 1572872 | tf_op jit(solution)/shard_map/ppermute | solution.py:532
  1.4 3.4 %own.1 = (bf16[256,1024]{1,0:T(8,128)(2,1)S(1)}, f32[256,128]{1,0:T(8,128)S(1)}, f32[256,1536]{1,0:T(8,128)S(1)}, bf16[1024,1536]{1,0:T(8,128)(2,1)S(1)}) custom-call(bf16[256,1024]{1,0:T(8,128)(2,1)} %bitcast.9, f32[1,2048]{1,0:T(1,128)} %bitcast.5, bf16[2048,384]{1,0:T(8,128)(2,1)} %refs_2_.1, bf16[2048,384]{1,0:T(8,128)(2,1)} %refs_3_.1, ...), custom_call_target="tpu_custom_call" | custom-call | flops 1000000000 | tf_op jit(solution)/shard_map/own/pallas_call | solution.py:536
  4.9 0.0 copy-start.2
  4.9 0.0 copy-start.4
  4.9 5.1 %local.1 = (bf16[256,1024]{1,0:T(8,128)(2,1)S(1)}, f32[256,128]{1,0:T(8,128)S(1)}, bf16[256,256]{1,0:T(8,128)(2,1)S(1)}, bf16[256,128]{1,0:T(8,128)(2,1)S(1)}, b...) custom-call(bf16[256,1024]{1,0:T(8,128)(2,1)S(1)} %bitcast.8, ...), custom_call_target="tpu_custom_call" | custom-call | flops 3000000000 | tf_op jit(solution)/shard_map/local/pallas_call | solution.py:550
  10.0 3.1 %collective-permute-start.2 = (bf16[256,128]{1,0:T(8,128)(2,1)S(1)}, bf16[256,128]{1,0:T(8,128)(2,1)S(1)}, u32[]{:S(2)}, u32[]{:S(2)}) collective-permute-start(bf16[256,128]{1,0:T(8,128)(2,1)S(1)} %get-tuple-element.40), channel_id=1, source_target_pairs={{0,16},{8,24},{16,0},{24,8},{1,17},{9,25},{17,1},{25,9},{2,18},{10... | collective-permute-start | bytes 196616 | tf_op jit(solution)/shard_map/ppermute | solution.py:524
  13.1 0.8 %collective-permute-start.3 = (bf16[256,128]{1,0:T(8,128)(2,1)S(1)}, bf16[256,128]{1,0:T(8,128)(2,1)S(1)}, u32[]{:S(2)}, u32[]{:S(2)}) collective-permute-start(bf16[256,128]{1,0:T(8,128)(2,1)S(1)} %get-tuple-element.41), channel_id=1, source_target_pairs={{0,24},{8,0},{16,8},{24,16},{1,25},{9,1},{17,9},{25,17},{2,26},{10... | collective-permute-start | bytes 196616 | tf_op jit(solution)/shard_map/ppermute | solution.py:524
  13.9 0.7 %collective-permute-start.1 = (bf16[320,128]{1,0:T(8,128)(2,1)S(1)}, bf16[320,128]{1,0:T(8,128)(2,1)S(1)}, u32[]{:S(2)}, u32[]{:S(2)}) collective-permute-start(bf16[320,128]{1,0:T(8,128)(2,1)S(1)} %get-tuple-element.39), channel_id=1, source_target_pairs={{0,8},{8,16},{16,24},{24,0},{1,9},{9,17},{17,25},{25,1},{2,10},{10... | collective-permute-start | bytes 245768 | tf_op jit(solution)/shard_map/ppermute | solution.py:524
  14.6 0.0 copy-start.6
  14.6 0.0 copy-start.9
  14.6 2.5 %side.1 = (bf16[6,128,128]{2,1,0:T(8,128)(2,1)S(1)}, f32[6,128,128]{2,1,0:T(8,128)S(1)}, bf16[256,384]{1,0:T(8,128)(2,1)S(1)}, bf16[256,256]{1,0:T(8,128)(2,1)S(1)}) custom-call(bf16[256,1024]{1,0:T(8,128)(2,1)S(1)} %get-tuple-element.34.refs_1_.own_ref, bf16[256,1024]{1,0:T(8,128)(2,1)S(1)} %get-tuple-element.42.other_ref, ...), custom_call_target="tpu_custom_call" | custom-call | flops 1000000000 | tf_op jit(solution)/shard_map/side/pallas_call | solution.py:570
  17.1 0.0 collective-permute-done.3.third_ref
  17.1 1.3 %collective-permute-done.1.first_ref.beside_ref = bf16[320,128]{1,0:T(8,128)(2,1)S(1)} collective-permute-done((bf16[320,128]{1,0:T(8,128)(2,1)S(1)}, bf16[320,128]{1,0:T(8,128)(2,1)S(1)}, u32[]{:S(2)}, u32[]{:S(2)}) %collective-permute-start.1) | collective-permute-done | bytes 81952 | tf_op jit(solution)/shard_map/ppermute | solution.py:524
  18.4 0.6 %row.1 = (f32[3,2,128,128]{3,2,1,0:T(8,128)S(1)}, bf16[320,128]{1,0:T(8,128)(2,1)S(1)}, bf16[256,128]{1,0:T(8,128)(2,1)S(1)}) custom-call(bf16[256,128]{1,0:T(8,128)(2,1)S(1)} %get-tuple-element.38.home_ref, bf16[320,128]{1,0:T(8,128)(2,1)S(1)} %collective-permute-done.1.first_ref.beside_ref, bf16[256,128]{1,0:T(8,128)(2,1)S(1)} %collective-permute-done.2.second_ref, ...), custom_call_target="tpu_custom_call" | custom-call | flops 100000000 | tf_op jit(solution)/shard_map/row/pallas_call | solution.py:579
  19.0 1.7 %collective-permute-start.4 = (bf16[320,128]{1,0:T(8,128)(2,1)S(1)}, bf16[320,128]{1,0:T(8,128)(2,1)S(1)}, u32[]{:S(2)}, u32[]{:S(2)}) collective-permute-start(bf16[320,128]{1,0:T(8,128)(2,1)S(1)} %get-tuple-element.51), channel_id=1, source_target_pairs={{0,32},{32,64},{64,96},{96,0},{1,33},{33,65},{65,97},{97,1},{2,34}... | collective-permute-start | bytes 245768 | tf_op jit(solution)/shard_map/ppermute | solution.py:524
  20.7 2.2 %collective-permute-start.6 = (bf16[256,128]{1,0:T(8,128)(2,1)S(1)}, bf16[256,128]{1,0:T(8,128)(2,1)S(1)}, u32[]{:S(2)}, u32[]{:S(2)}) collective-permute-start(bf16[256,128]{1,0:T(8,128)(2,1)S(1)} %get-tuple-element.52), channel_id=1, source_target_pairs={{0,96},{32,0},{64,32},{96,64},{1,97},{33,1},{65,33},{97,65},{2,98}... | collective-permute-start | bytes 196616 | tf_op jit(solution)/shard_map/ppermute | solution.py:524
  22.9 1.2 %collective-permute-start.5 = (bf16[256,128]{1,0:T(8,128)(2,1)S(1)}, bf16[256,128]{1,0:T(8,128)(2,1)S(1)}, u32[]{:S(2)}, u32[]{:S(2)}) collective-permute-start(bf16[256,128]{1,0:T(8,128)(2,1)S(1)} %get-tuple-element.52), channel_id=1, source_target_pairs={{0,64},{32,96},{64,0},{96,32},{1,65},{33,97},{65,1},{97,33},{2,66}... | collective-permute-start | bytes 196616 | tf_op jit(solution)/shard_map/ppermute | solution.py:524
  24.1 0.1 collective-permute-done.6.third_ref
  24.2 3.7 %collective-permute-done.5.second_ref = bf16[256,128]{1,0:T(8,128)(2,1)S(1)} collective-permute-done((bf16[256,128]{1,0:T(8,128)(2,1)S(1)}, bf16[256,128]{1,0:T(8,128)(2,1)S(1)}, u32[]{:S(2)}, u32[]{:S(2)}) %collective-permute-start.5) | collective-permute-done | bytes 65568 | tf_op jit(solution)/shard_map/ppermute | solution.py:524
  27.9 0.9 %column.1 = (bf16[2,64,128]{2,1,0:T(8,128)(2,1)S(1)}, bf16[2,64,128]{2,1,0:T(8,128)(2,1)S(1)}, bf16[2,64,128]{2,1,0:T(8,128)(2,1)S(1)}, bf16[2,64,128]{2,1,0:T(8,128)(2,1)S(1)}) custom-call(f32[3,2,128,128]{3,2,1,0:T(8,128)S(1)} %get-tuple-element.50.prefix_ref, bf16[320,128]{1,0:T(8,128)(2,1)S(1)} %collective-permute-done.4.first_ref.above_ref, ...), custom_call_target="tpu_custom_call" | custom-call | flops 100000000 | tf_op jit(solution)/shard_map/column/pallas_call | solution.py:589
  28.8 0.3 collective-permute-start.7
  29.1 2.0 %collective-permute-start.8 = (bf16[2,64,128]{2,1,0:T(8,128)(2,1)S(1)}, bf16[2,64,128]{2,1,0:T(8,128)(2,1)S(1)}, u32[]{:S(2)}, u32[]{:S(2)}) collective-permute-start(bf16[2,64,128]{2,1,0:T(8,128)(2,1)S(1)} %get-tuple-element.55), channel_id=1, source_target_pairs={{0,16},{8,24},{16,0},{24,8},{1,17},{9,25},{17,1},{25,9},{2,18},{10... | collective-permute-start | bytes 98312 | tf_op jit(solution)/shard_map/ppermute | solution.py:524
  31.1 1.4 %collective-permute-start.9 = (bf16[2,64,128]{2,1,0:T(8,128)(2,1)S(1)}, bf16[2,64,128]{2,1,0:T(8,128)(2,1)S(1)}, u32[]{:S(2)}, u32[]{:S(2)}) collective-permute-start(bf16[2,64,128]{2,1,0:T(8,128)(2,1)S(1)} %get-tuple-element.56), channel_id=1, source_target_pairs={{0,24},{8,0},{16,8},{24,16},{1,25},{9,1},{17,9},{25,17},{2,26},{10... | collective-permute-start | bytes 98312 | tf_op jit(solution)/shard_map/ppermute | solution.py:524
  32.5 0.6 %pool.1.part_ref = f32[256,2048]{1,0:T(8,128)S(1)} custom-call(bf16[256,256]{1,0:T(8,128)(2,1)S(1)} %get-tuple-element.60.pool_ref, bf16[320,128]{1,0:T(8,128)(2,1)S(1)} %collective-permute-done.1.first_ref.beside_ref, bf16[320,128]{1,0:T(8,128)(2,1)S(1)} %collective-permute-done.4.first_ref.above_ref, ...), custom_call_target="tpu_custom_call" | custom-call | flops 300000000 | tf_op jit(solution)/shard_map/pool/pallas_call | solution.py:599
  33.2 0.2 collective-permute-done.8.two_ref
  33.4 0.5 %collective-permute-done.9.three_ref = bf16[2,64,128]{2,1,0:T(8,128)(2,1)S(1)} collective-permute-done((bf16[2,64,128]{2,1,0:T(8,128)(2,1)S(1)}, bf16[2,64,128]{2,1,0:T(8,128)(2,1)S(1)}, u32[]{:S(2)}, u32[]{:S(2)}) %collective-permute-start.9) | collective-permute-done | bytes 32800 | tf_op jit(solution)/shard_map/ppermute | solution.py:524
  33.8 0.1 copy-done
  33.9 1.5 %final.1 = (bf16[256,1024]{1,0:T(8,128)(2,1)S(1)}, bf16[256,384]{1,0:T(8,128)(2,1)S(1)}) custom-call(bf16[2,64,128]{2,1,0:T(8,128)(2,1)S(1)} %get-tuple-element.53.home_ref, bf16[2,64,128]{2,1,0:T(8,128)(2,1)S(1)} %collective-permute-done.7.one_ref, bf16[2,64,128]{2,1,0:T(8,128)(2,1)S(1)} %collective-permute-done.8.two_ref, ...), custom_call_target="tpu_custom_call" | custom-call | flops 1000000000 | tf_op jit(solution)/shard_map/final/pallas_call | solution.py:602
  35.4 4.1 %collective-permute-start.10 = (bf16[256,1024]{1,0:T(8,128)(2,1)S(1)}, bf16[256,1024]{1,0:T(8,128)(2,1)S(1)}, u32[]{:S(2)}, u32[]{:S(2)}) collective-permute-start(bf16[256,1024]{1,0:T(8,128)(2,1)S(1)} %get-tuple-element.62), channel_id=1, source_target_pairs={{0,1},{1,0},{2,3},{3,2},{4,5},{5,4},{6,7},{7,6},{8,9},{9,8},{10,11... | collective-permute-start | bytes 1572872 | tf_op jit(solution)/shard_map/ppermute | solution.py:611
  39.6 0.4 %keep.1.keep_ref = bf16[256,1024]{1,0:T(8,128)(2,1)S(1)} custom-call(bf16[256,384]{1,0:T(8,128)(2,1)S(1)} %get-tuple-element.61.rec_ref, f32[256,2048]{1,0:T(8,128)S(1)} %pool.1.part_ref, bf16[384,2048]{1,0:T(8,128)(2,1)S(1)} %copy-done), custom_call_target="tpu_custom_call" | custom-call | flops 300000000 | tf_op jit(solution)/shard_map/keep/pallas_call | solution.py:612
  40.0 1.1 %collective-permute-done.10.arrived_ref = bf16[256,1024]{1,0:T(8,128)(2,1)S(1)} collective-permute-done((bf16[256,1024]{1,0:T(8,128)(2,1)S(1)}, bf16[256,1024]{1,0:T(8,128)(2,1)S(1)}, u32[]{:S(2)}, u32[]{:S(2)}) %collective-permute-start.10) | collective-permute-done | bytes 524320 | tf_op jit(solution)/shard_map/ppermute | solution.py:611
  41.1 0.8 %sum.1 = bf16[256,1024]{1,0:T(8,128)(2,1)} custom-call(bf16[256,1024]{1,0:T(8,128)(2,1)S(1)} %keep.1.keep_ref, bf16[256,1024]{1,0:T(8,128)(2,1)S(1)} %collective-permute-done.10.arrived_ref), custom_call_target="tpu_custom_call" | custom-call | tf_op jit(solution)/shard_map/sum/pallas_call | solution.py:613
  (25 shorter events, 0.1 us)
Async XLA Ops:
  0.0 4.8 %collective-permute-start = (bf16[2,128,1024]{2,1,0:T(8,128)(2,1)}, bf16[2,128,1024]{2,1,0:T(8,128)(2,1)S(1)}, u32[]{:S(2)}, u32[]{:S(2)}) collective-permute-start(bf16[2,128,1024]{2,1,0:T(8,128)(2,1)} %param.18), channel_id=1, source_target_pairs={{0,1},{1,0},{2,3},{3,2},{4,5},{5,4},{6,7},{7,6},{8,9},{9,8},{10,11... | collective-permute-start | bytes 1572872 | tf_op jit(solution)/shard_map/ppermute | solution.py:532
  1.4 3.4 %copy-start.7 = (f32[2048]{0:T(1024)S(1)}, f32[2048]{0:T(1024)}, u32[]{:S(2)}) copy-start(f32[2048]{0:T(1024)} %param.19) | copy-start | bytes 24580
  1.4 3.4 %copy-start.10 = (bf16[2048,256]{1,0:T(8,128)(2,1)S(1)}, bf16[2048,256]{1,0:T(8,128)(2,1)}, u32[]{:S(2)}) copy-start(bf16[2048,256]{1,0:T(8,128)(2,1)} %refs_8_.1) | copy-start | bytes 3145732
  1.4 3.4 %copy-start.11 = (f32[768]{0:T(1024)S(1)}, f32[768]{0:T(1024)}, u32[]{:S(2)}) copy-start(f32[768]{0:T(1024)} %refs_4_.3) | copy-start | bytes 9220
  1.4 3.4 %copy-start.12 = (f32[768]{0:T(1024)S(1)}, f32[768]{0:T(1024)}, u32[]{:S(2)}) copy-start(f32[768]{0:T(1024)} %refs_5_.3) | copy-start | bytes 9220
  4.8 9.7 %copy-start.1 = (bf16[2048,384]{1,0:T(8,128)(2,1)S(1)}, bf16[2048,384]{1,0:T(8,128)(2,1)}, u32[]{:S(2)}) copy-start(bf16[2048,384]{1,0:T(8,128)(2,1)} %wr_ref.3) | copy-start | bytes 4718596
  4.9 9.7 %copy-start.2 = (bf16[2048,384]{1,0:T(8,128)(2,1)S(1)}, bf16[2048,384]{1,0:T(8,128)(2,1)}, u32[]{:S(2)}) copy-start(bf16[2048,384]{1,0:T(8,128)(2,1)} %wg_ref.1) | copy-start | bytes 4718596
  4.9 9.7 %copy-start.4 = (bf16[2048,256]{1,0:T(8,128)(2,1)S(1)}, bf16[2048,256]{1,0:T(8,128)(2,1)}, u32[]{:S(2)}) copy-start(bf16[2048,256]{1,0:T(8,128)(2,1)} %wq_ref.1) | copy-start | bytes 3145732
  10.0 7.1 %collective-permute-start.2 = (bf16[256,128]{1,0:T(8,128)(2,1)S(1)}, bf16[256,128]{1,0:T(8,128)(2,1)S(1)}, u32[]{:S(2)}, u32[]{:S(2)}) collective-permute-start(bf16[256,128]{1,0:T(8,128)(2,1)S(1)} %get-tuple-element.40), channel_id=1, source_target_pairs={{0,16},{8,24},{16,0},{24,8},{1,17},{9,25},{17,1},{25,9},{2,18},{10... | collective-permute-start | bytes 196616 | tf_op jit(solution)/shard_map/ppermute | solution.py:524
  13.1 4.0 %collective-permute-start.3 = (bf16[256,128]{1,0:T(8,128)(2,1)S(1)}, bf16[256,128]{1,0:T(8,128)(2,1)S(1)}, u32[]{:S(2)}, u32[]{:S(2)}) collective-permute-start(bf16[256,128]{1,0:T(8,128)(2,1)S(1)} %get-tuple-element.41), channel_id=1, source_target_pairs={{0,24},{8,0},{16,8},{24,16},{1,25},{9,1},{17,9},{25,17},{2,26},{10... | collective-permute-start | bytes 196616 | tf_op jit(solution)/shard_map/ppermute | solution.py:524
  13.9 4.5 %collective-permute-start.1 = (bf16[320,128]{1,0:T(8,128)(2,1)S(1)}, bf16[320,128]{1,0:T(8,128)(2,1)S(1)}, u32[]{:S(2)}, u32[]{:S(2)}) collective-permute-start(bf16[320,128]{1,0:T(8,128)(2,1)S(1)} %get-tuple-element.39), channel_id=1, source_target_pairs={{0,8},{8,16},{16,24},{24,0},{1,9},{9,17},{17,25},{25,1},{2,10},{10... | collective-permute-start | bytes 245768 | tf_op jit(solution)/shard_map/ppermute | solution.py:524
  14.6 13.3 %copy-start.5 = (f32[2,6,64,64]{3,2,1,0:T(8,128)S(1)}, f32[2,6,64,64]{3,2,1,0:T(8,128)}, u32[]{:S(2)}) copy-start(f32[2,6,64,64]{3,2,1,0:T(8,128)} %init_ref.1) | copy-start | bytes 589828
  14.6 17.9 %copy-start.6 = (bf16[4,128,128]{2,1,0:T(8,128)(2,1)S(1)}, bf16[4,128,128]{2,1,0:T(8,128)(2,1)}, u32[]{:S(2)}) copy-start(bf16[4,128,128]{2,1,0:T(8,128)(2,1)} %mix_ref.1) | copy-start | bytes 393220
  14.6 17.9 %copy-start.9 = (f32[512]{0:T(512)S(1)}, f32[512]{0:T(512)}, u32[]{:S(2)}) copy-start(f32[512]{0:T(512)} %param.32) | copy-start | bytes 6148
  17.1 15.4 %copy-start.3 = (bf16[256,2048]{1,0:T(8,128)(2,1)S(1)}, bf16[256,2048]{1,0:T(8,128)(2,1)}, u32[]{:S(2)}) copy-start(bf16[256,2048]{1,0:T(8,128)(2,1)} %wp_ref.1) | copy-start | bytes 3145732
  19.0 8.9 %collective-permute-start.4 = (bf16[320,128]{1,0:T(8,128)(2,1)S(1)}, bf16[320,128]{1,0:T(8,128)(2,1)S(1)}, u32[]{:S(2)}, u32[]{:S(2)}) collective-permute-start(bf16[320,128]{1,0:T(8,128)(2,1)S(1)} %get-tuple-element.51), channel_id=1, source_target_pairs={{0,32},{32,64},{64,96},{96,0},{1,33},{33,65},{65,97},{97,1},{2,34}... | collective-permute-start | bytes 245768 | tf_op jit(solution)/shard_map/ppermute | solution.py:524
  20.7 3.5 %collective-permute-start.6 = (bf16[256,128]{1,0:T(8,128)(2,1)S(1)}, bf16[256,128]{1,0:T(8,128)(2,1)S(1)}, u32[]{:S(2)}, u32[]{:S(2)}) collective-permute-start(bf16[256,128]{1,0:T(8,128)(2,1)S(1)} %get-tuple-element.52), channel_id=1, source_target_pairs={{0,96},{32,0},{64,32},{96,64},{1,97},{33,1},{65,33},{97,65},{2,98}... | collective-permute-start | bytes 196616 | tf_op jit(solution)/shard_map/ppermute | solution.py:524
  22.9 5.0 %collective-permute-start.5 = (bf16[256,128]{1,0:T(8,128)(2,1)S(1)}, bf16[256,128]{1,0:T(8,128)(2,1)S(1)}, u32[]{:S(2)}, u32[]{:S(2)}) collective-permute-start(bf16[256,128]{1,0:T(8,128)(2,1)S(1)} %get-tuple-element.52), channel_id=1, source_target_pairs={{0,64},{32,96},{64,0},{96,32},{1,65},{33,97},{65,1},{97,33},{2,66}... | collective-permute-start | bytes 196616 | tf_op jit(solution)/shard_map/ppermute | solution.py:524
  28.8 4.4 %collective-permute-start.7 = (bf16[2,64,128]{2,1,0:T(8,128)(2,1)S(1)}, bf16[2,64,128]{2,1,0:T(8,128)(2,1)S(1)}, u32[]{:S(2)}, u32[]{:S(2)}) collective-permute-start(bf16[2,64,128]{2,1,0:T(8,128)(2,1)S(1)} %get-tuple-element.54), channel_id=1, source_target_pairs={{0,8},{8,16},{16,24},{24,0},{1,9},{9,17},{17,25},{25,1},{2,10},{10... | collective-permute-start | bytes 98312 | tf_op jit(solution)/shard_map/ppermute | solution.py:524
  29.1 4.3 %collective-permute-start.8 = (bf16[2,64,128]{2,1,0:T(8,128)(2,1)S(1)}, bf16[2,64,128]{2,1,0:T(8,128)(2,1)S(1)}, u32[]{:S(2)}, u32[]{:S(2)}) collective-permute-start(bf16[2,64,128]{2,1,0:T(8,128)(2,1)S(1)} %get-tuple-element.55), channel_id=1, source_target_pairs={{0,16},{8,24},{16,0},{24,8},{1,17},{9,25},{17,1},{25,9},{2,18},{10... | collective-permute-start | bytes 98312 | tf_op jit(solution)/shard_map/ppermute | solution.py:524
  31.1 2.8 %collective-permute-start.9 = (bf16[2,64,128]{2,1,0:T(8,128)(2,1)S(1)}, bf16[2,64,128]{2,1,0:T(8,128)(2,1)S(1)}, u32[]{:S(2)}, u32[]{:S(2)}) collective-permute-start(bf16[2,64,128]{2,1,0:T(8,128)(2,1)S(1)} %get-tuple-element.56), channel_id=1, source_target_pairs={{0,24},{8,0},{16,8},{24,16},{1,25},{9,1},{17,9},{25,17},{2,26},{10... | collective-permute-start | bytes 98312 | tf_op jit(solution)/shard_map/ppermute | solution.py:524
  32.5 1.4 %copy-start = (bf16[384,2048]{1,0:T(8,128)(2,1)S(1)}, bf16[384,2048]{1,0:T(8,128)(2,1)}, u32[]{:S(2)}) copy-start(bf16[384,2048]{1,0:T(8,128)(2,1)} %wr_ref.5) | copy-start | bytes 4718596
  32.5 1.4 %copy-start.8 = (f32[768]{0:T(1024)S(1)}, f32[768]{0:T(1024)}, u32[]{:S(2)}) copy-start(f32[768]{0:T(1024)} %hgain_ref.1) | copy-start | bytes 9220
  35.4 5.7 %collective-permute-start.10 = (bf16[256,1024]{1,0:T(8,128)(2,1)S(1)}, bf16[256,1024]{1,0:T(8,128)(2,1)S(1)}, u32[]{:S(2)}, u32[]{:S(2)}) collective-permute-start(bf16[256,1024]{1,0:T(8,128)(2,1)S(1)} %get-tuple-element.62), channel_id=1, source_target_pairs={{0,1},{1,0},{2,3},{3,2},{4,5},{5,4},{6,7},{7,6},{8,9},{9,8},{10,11... | collective-permute-start | bytes 1572872 | tf_op jit(solution)/shard_map/ppermute | solution.py:611
